TPU v7x, 512 devices: a whole 4x4x16 slice. The times are simulated.
512 devices in a mesh: sp: 16 (over z), fs: 4 (over y), tp: 8 (over x, core).
Axes of the slice: x: 4, y: 4, z: 16, core: 2. Of those that a mesh axis runs over, the one named last changes fastest.
Arguments:
- tokens: bfloat16 [4, 16384, 2048], P('fs', ('sp', 'tp')), may hold values from -6 to 6
- input_norm_gain: float32 [2048], replicated, may hold values from 0.1 to 1.9
- earlier_gate: bfloat16 [2048, 1024], P(('sp', 'fs'), 'tp'), may hold values from -0.125 to 0.125
- later_gate: bfloat16 [2048, 1024], P(('sp', 'fs'), 'tp'), may hold values from -0.125 to 0.125
- convolution_input: bfloat16 [2048, 1024], P(('sp', 'fs'), 'tp'), may hold values from -0.125 to 0.125
- convolution_taps: float32 [3, 1024], P(None, 'tp'), may hold values from -3 to 3
- receptance: bfloat16 [2048, 1024], P(('sp', 'fs'), 'tp'), may hold values from -0.125 to 0.125
- key_matrix: bfloat16 [2048, 1024], P(('sp', 'fs'), 'tp'), may hold values from -0.125 to 0.125
- value_matrix: bfloat16 [2048, 1024], P(('sp', 'fs'), 'tp'), may hold values from -0.125 to 0.125
- decay_matrix: bfloat16 [2048, 1024], P(('sp', 'fs'), 'tp'), may hold values from -0.125 to 0.125
- rate_matrix: bfloat16 [2048, 1024], P(('sp', 'fs'), 'tp'), may hold values from -0.125 to 0.125
- decay_floor: float32 [1024], P('tp'), may hold values from -16 to -3.4
- rate_offset: float32 [1024], P('tp'), may hold values from -7.5 to 1
- decay_spike: float32 [4, 16384, 1024], P('fs', 'sp', 'tp'), may hold values from -1.3 to 0
- initial_state: float32 [4, 16, 64, 64], P('fs', 'tp'), may hold values from -768 to 768
- head_norm_gain: float32 [1024], P('tp'), may hold values from 0.1 to 1.9
- convolution_output: bfloat16 [1024, 2048], P('tp', ('sp', 'fs')), may hold values from -0.125 to 0.125
- state_heads_output: bfloat16 [1024, 2048], P('tp', ('sp', 'fs')), may hold values from -0.125 to 0.125
Outputs:
- mixed: bfloat16 [4, 16384, 2048], P('fs', ('sp', 'tp'))
All inputs are finite; a program needn't handle non-finite values.
Results may differ from a plain program's by a relative error of at most 0.02.
Values may be sent and summed in bfloat16 or wider, within the bound.
No kernel may reach another device: no remote copies, remote signals or barrier semaphores. Data moves between devices by JAX's collectives and lax.ppermute only.
A program may use at most 64 MiB of HBM per device.

v0:
```python
import jax
import jax.numpy as jnp
from jax import lax
from jax.sharding import PartitionSpec as P

HEAD_WIDTH = 64
BLOCK = 64


norm_eps = 1e-06
key_eps = 1e-06


def passed_along(block, axis, distance):
    devices = range(lax.axis_size(axis))
    route = [(i - distance, i) for i in devices if i - distance in devices]
    return lax.ppermute(block, axis, route)


def side_by_side(arrays, axis, dim, along):
    widths = [a.shape[along] for a in arrays]
    both = jnp.concatenate(arrays, axis=along)
    out = lax.all_gather(both, axis, axis=dim, tiled=True)
    return tuple(jnp.split(out, [sum(widths[:k]) for k in range(1, len(widths))], axis=along))


def from_everyone(x, axis):
    devices = lax.axis_size(axis)
    return lax.all_to_all(jnp.broadcast_to(x[None], (devices, *x.shape)), axis, 0, 0, tiled=True)


def collected_together(x, axis):
    leaves = jax.tree.leaves(x)
    order = sorted(range(len(leaves)), key=lambda k: -leaves[k].size)
    width = (1, *leaves[order[0]].shape)[-1]
    lines = [
        jnp.pad(leaves[k].reshape(-1), (0, -leaves[k].size % width)).reshape(-1, width)
        for k in order
    ]
    both, at, found = (from_everyone(jnp.concatenate(lines), axis), 0, {})
    for k, line in zip(order, lines):
        piece = both[:, at : at + len(line)].reshape(len(both), -1)
        found[k] = piece[:, : leaves[k].size].reshape(-1, *leaves[k].shape)
        at += len(line)
    numbers = iter(range(len(leaves)))
    return jax.tree.map(lambda _: found[next(numbers)], x)


def combined_pairwise(pieces, combine):
    while len(jax.tree.leaves(pieces)[0]) > 1:
        pieces = jax.vmap(combine)(
            *(jax.tree.map(lambda part: part[side::2], pieces) for side in (0, 1))
        )
    return jax.tree.map(lambda part: part[0], pieces)


def entering(x, axis, combine, identity):
    devices, position = (lax.axis_size(axis), lax.axis_index(axis))
    passed = jnp.arange(devices) < position

    def kept(part, zero, own):
        part = jnp.where(
            passed.reshape(-1, *(1 for _ in own.shape)),
            part.astype(own.dtype),
            jnp.asarray(zero, own.dtype),
        )
        return part

    pieces = collected_together(
        jax.tree.map(lambda part, kind: part.astype(kind), x, (jnp.bfloat16, jnp.bfloat16)), axis
    )
    return combined_pairwise(jax.tree.map(kept, pieces, identity, x), combine)


def gather_turned(arrays, axis, dims):
    turned = [jnp.moveaxis(a, dim, 0) for a, dim in zip(arrays, dims)]
    both = jnp.concatenate([t.reshape(len(t), -1) for t in turned], axis=1)
    out, at, outs = (lax.all_gather(both, axis, axis=0, tiled=True), 0, [])
    for t, dim in zip(turned, dims):
        piece = out[:, at : at + t[0].size].reshape(-1, *t.shape[1:])
        outs.append(jnp.moveaxis(piece, 0, dim))
        at += t[0].size
    return tuple(outs)


def rms_rows(activations, gain_vector):
    values = activations.astype(jnp.float32)
    inv_scale = lax.rsqrt(jnp.mean(values * values, axis=-1, keepdims=True) + norm_eps)
    return (values * inv_scale * gain_vector).astype(jnp.bfloat16)


def project(activations, weight):
    return jnp.dot(activations, weight, preferred_element_type=jnp.float32).astype(jnp.bfloat16)


def conv_branch(pre_values, post_values, conv_values, convolution_taps):
    product = pre_values.astype(jnp.float32) * conv_values.astype(jnp.float32)
    reach_rows = convolution_taps.shape[0] - 1
    sequence_rows = product.shape[0]
    edge_rows = passed_along(product[sequence_rows - reach_rows :], "sp", 1)
    padded = jnp.concatenate([edge_rows, product], axis=0)
    filtered = convolution_taps[0] * padded[0:sequence_rows]
    for offset in range(1, convolution_taps.shape[0]):
        filtered = filtered + convolution_taps[offset] * padded[offset : offset + sequence_rows]
    return (post_values.astype(jnp.float32) * filtered).astype(jnp.bfloat16)


def pairs(left_side, right_side, allowed):
    return jnp.where(allowed, jnp.einsum("thj,shj->hts", left_side, right_side), 0.0)


def block_pass(carried, inputs):
    queries, key_rows, value_rows, unit_keys, beta_rows, logarithm_decay = inputs
    span_rows = logarithm_decay.shape[0]
    cumulative = jnp.cumsum(logarithm_decay, axis=0)
    previous = cumulative - logarithm_decay
    middle = cumulative[span_rows // 2]
    later_index = lax.broadcasted_iota(jnp.int32, (span_rows, span_rows), 0)
    earlier_index = lax.broadcasted_iota(jnp.int32, (span_rows, span_rows), 1)
    strict = (later_index > earlier_index)[None]
    inclusive = (later_index >= earlier_index)[None]
    ask_keys = unit_keys * jnp.exp(previous - middle)
    ask_reads = queries * jnp.exp(cumulative - middle)
    give_keys = key_rows * jnp.exp(middle - cumulative)
    give_betas = beta_rows * jnp.exp(middle - cumulative)
    key_ask = pairs(ask_keys, give_keys, strict)
    beta_ask = pairs(ask_keys, give_betas, strict)
    key_read = pairs(ask_reads, give_keys, inclusive)
    beta_read = pairs(ask_reads, give_betas, inclusive)
    extended = jnp.concatenate([value_rows, jnp.zeros_like(value_rows)], axis=2)
    from_start = jnp.einsum("thj,hrj->htr", unit_keys * jnp.exp(previous), carried)
    right_side = from_start + jnp.einsum("hts,shr->htr", key_ask, extended)
    system = beta_ask + jnp.eye(span_rows, dtype=jnp.float32)[None]
    removed = jax.scipy.linalg.solve_triangular(system, right_side, lower=True, unit_diagonal=True)
    outputs = (
        jnp.einsum("thj,hrj->thr", queries * jnp.exp(cumulative), carried)
        + jnp.einsum("hts,shr->thr", key_read, extended)
        - jnp.einsum("hts,hsr->thr", beta_read, removed)
    )
    closing = cumulative[span_rows - 1]
    tail_decay = jnp.exp(closing - cumulative)
    carried = (
        carried * jnp.exp(closing)[:, None, :]
        + jnp.einsum("shr,shj->hrj", extended, key_rows * tail_decay)
        - jnp.einsum("hsr,shj->hrj", removed, beta_rows * tail_decay)
    )
    return (carried, outputs)


def compose(earlier, later):
    return (
        jnp.einsum("hij,hjk->hik", earlier[0], later[0]),
        jnp.einsum("hij,hjk->hik", earlier[1], later[0]) + later[1],
    )


def on_device(
    tokens,
    input_norm_gain,
    earlier_gate,
    later_gate,
    convolution_input,
    convolution_taps,
    receptance,
    key_matrix,
    value_matrix,
    decay_matrix,
    rate_matrix,
    decay_floor,
    rate_offset,
    decay_spike,
    initial_state,
    head_norm_gain,
    convolution_output,
    state_heads_output,
):
    normed = rms_rows(tokens[0], input_norm_gain)
    channels = earlier_gate.shape[1]
    gathered = side_by_side(
        (
            earlier_gate,
            later_gate,
            convolution_input,
            receptance,
            key_matrix,
            value_matrix,
            decay_matrix,
            rate_matrix,
        ),
        ("sp", "fs"),
        0,
        1,
    )
    piece = lax.all_gather(normed, "tp", axis=0, tiled=True)
    projected = jnp.concatenate([project(piece, weight) for weight in gathered], axis=1)
    pieces = jnp.split(projected, 8, axis=1)
    conv_mixed = conv_branch(pieces[0], pieces[1], pieces[2], convolution_taps)
    queries_raw, keys_raw, values_raw, decay_pre, rate_pre = pieces[3:]
    sequence_rows = queries_raw.shape[0]
    present_heads = channels // HEAD_WIDTH

    def by_heads(array):
        return array.astype(jnp.float32).reshape(sequence_rows, present_heads, HEAD_WIDTH)

    queries = by_heads(queries_raw)
    key_rows = by_heads(keys_raw)
    value_rows = by_heads(values_raw)
    logarithm_decay = -jnp.exp(
        decay_floor.reshape(present_heads, HEAD_WIDTH) + jnp.tanh(by_heads(decay_pre))
    )
    logarithm_decay = logarithm_decay + decay_spike[0].reshape(
        sequence_rows, present_heads, HEAD_WIDTH
    )
    learn_rate = jax.nn.sigmoid(rate_offset.reshape(present_heads, HEAD_WIDTH) + by_heads(rate_pre))
    unit_keys = key_rows * lax.rsqrt(jnp.sum(key_rows * key_rows, axis=-1, keepdims=True) + key_eps)
    beta_rows = learn_rate * unit_keys
    blocks = sequence_rows // BLOCK

    def in_blocks(array):
        return array.reshape(blocks, BLOCK, present_heads, HEAD_WIDTH)

    identity = jnp.broadcast_to(
        jnp.eye(HEAD_WIDTH, dtype=jnp.float32), (present_heads, HEAD_WIDTH, HEAD_WIDTH)
    )
    initial_rows = jnp.concatenate(
        [jnp.zeros((present_heads, HEAD_WIDTH, HEAD_WIDTH), jnp.float32), identity], axis=1
    )
    ending, outputs = lax.scan(
        block_pass,
        initial_rows,
        tuple(
            (
                in_blocks(array)
                for array in (queries, key_rows, value_rows, unit_keys, beta_rows, logarithm_decay)
            )
        ),
    )
    outputs = outputs.reshape(sequence_rows, present_heads, 2 * HEAD_WIDTH)
    carry_source = ending[:, :HEAD_WIDTH, :]
    carry_map = ending[:, HEAD_WIDTH:, :]
    first_state = initial_state[0]
    prefix_map, prefix_source = entering(
        (carry_map, carry_source), "sp", compose, (identity, jnp.zeros_like(carry_source))
    )
    opening_state = jnp.einsum("hvj,hjk->hvk", first_state, prefix_map) + prefix_source
    reads = outputs[..., :HEAD_WIDTH] + jnp.einsum(
        "thj,hvj->thv", outputs[..., HEAD_WIDTH:], opening_state
    )
    centered = reads - jnp.mean(reads, axis=-1, keepdims=True)
    variance = jnp.mean(centered * centered, axis=-1, keepdims=True)
    state_mixed = (
        centered
        * lax.rsqrt(variance + HEAD_WIDTH * 1e-05)
        * head_norm_gain.reshape(present_heads, HEAD_WIDTH)
    )
    state_mixed = state_mixed.reshape(sequence_rows, channels).astype(jnp.bfloat16)
    conv_whole, state_whole = gather_turned(
        (convolution_output, state_heads_output), ("sp", "fs"), (1, 1)
    )
    mixed = lax.psum_scatter(
        (
            jnp.dot(conv_mixed, conv_whole, preferred_element_type=jnp.float32)
            + jnp.dot(state_mixed, state_whole, preferred_element_type=jnp.float32)
        ).astype(jnp.bfloat16),
        "tp",
        scatter_dimension=0,
        tiled=True,
    )
    return mixed[None]


def solution(mesh):
    placed = (
        P("fs", ("sp", "tp"), None),
        P(),
        P(("sp", "fs"), "tp"),
        P(("sp", "fs"), "tp"),
        P(("sp", "fs"), "tp"),
        P(None, "tp"),
        P(("sp", "fs"), "tp"),
        P(("sp", "fs"), "tp"),
        P(("sp", "fs"), "tp"),
        P(("sp", "fs"), "tp"),
        P(("sp", "fs"), "tp"),
        P("tp"),
        P("tp"),
        P("fs", "sp", "tp"),
        P("fs", "tp", None, None),
        P("tp"),
        P("tp", ("sp", "fs")),
        P("tp", ("sp", "fs")),
    )
    return jax.shard_map(
        on_device,
        mesh=mesh,
        in_specs=placed,
        out_specs=P("fs", ("sp", "tp"), None),
        check_vma=False,
    )
```

profile of v0, /device:TPU:8, one launch (start us, length us, event | category | flops | bytes accessed | tf_op | source)
XLA Modules:
  0.0 573.6 jit_solution(10139626129675810700)
XLA Ops:
  6.5 1.3 fusion.63
  7.8 2.0 fusion.65
  16.2 1.3 pad_maximum_fusion.2
  18.3 2.6 reshape_squeeze.3
  21.9 32.2 %all-gather.4.cloned.1.call-done = bf16[1024,2048]{1,0:T(8,128)(2,1)} async-done(((bf16[128,2048]{1,0:T(8,128)(2,1)}), bf16[1024,2048]{1,0:T(8,128)(2,1)}) %all-gather.4.cloned.1.call-update) | async-done | bytes 4194320 | tf_op jit(solution)/shard_map/all_gather | solution.py:194
  54.1 147.6 %all-gather.6.cloned.1.call-done = bf16[2048,1024]{1,0:T(8,128)(2,1)} async-done(((bf16[32,1024]{1,0:T(8,128)(2,1)}), bf16[2048,1024]{1,0:T(8,128)(2,1)}) %all-gather.6.cloned.1.call-update) | async-done | bytes 4194320 | tf_op jit(solution)/shard_map/all_gather | solution.py:23
  201.7 3.8 bitcast_reduce_fusion
  206.5 1.0 copy.76
  207.5 4.3 fusion.51
  211.9 1.6 reshape.141
  213.5 4.4 fusion.55
  217.9 2.7 tanh.8
  220.5 4.3 fusion.50
  224.9 2.6 reshape.142
  227.5 4.3 fusion.53
  231.8 2.0 reshape.139
  233.8 2.7 negate_add_fusion
  236.5 4.0 divide_multiply_fusion
  240.5 237.3 %while.12 = (s32[]{:T(128)}, f32[2,128,64]{1,2,0:T(8,128)S(1)}, f32[16,64,2,128]{3,1,0,2:T(8,128)S(1)}, f32[16,64,2,64]{3,2,1,0:T(2,128)}, bf16[16,64,2,64]{3,2,...) while((s32[]{:T(128)}, f32[2,128,64]{1,2,0:T(8,128)S(1)}, ...), condition=%wide.region_4.5_spmd, body=%wide.region_2.4_spmd.sunk | while | flops 32329792 | bytes 2025073 | solution.py:228
  240.5 0.9 fusion.188
  241.4 1.2 bitcast_multiply_fusion.9
  244.1 9.8 %custom-call.8 = f32[2,1,64,64]{2,3,1,0:T(8,128)S(1)} custom-call(f32[2,1,64,64]{3,2,1,0:T(8,128)S(1)} %fusion.192), custom_call_target="InvertDiagBlocksLowerTriangular" | custom-call | tf_op jit(solution)/shard_map/while/body/eval_jaxpr/jit(_solve_triangular)/vmap()/triangular_solve | solution.py:134
  255.3 0.9 fusion.188
  256.3 1.2 bitcast_multiply_fusion.9
  259.0 9.8 %custom-call.8 = f32[2,1,64,64]{2,3,1,0:T(8,128)S(1)} custom-call(f32[2,1,64,64]{3,2,1,0:T(8,128)S(1)} %fusion.192), custom_call_target="InvertDiagBlocksLowerTriangular" | custom-call | tf_op jit(solution)/shard_map/while/body/eval_jaxpr/jit(_solve_triangular)/vmap()/triangular_solve | solution.py:134
  270.2 0.9 fusion.188
  271.1 1.2 bitcast_multiply_fusion.9
  273.8 9.8 %custom-call.8 = f32[2,1,64,64]{2,3,1,0:T(8,128)S(1)} custom-call(f32[2,1,64,64]{3,2,1,0:T(8,128)S(1)} %fusion.192), custom_call_target="InvertDiagBlocksLowerTriangular" | custom-call | tf_op jit(solution)/shard_map/while/body/eval_jaxpr/jit(_solve_triangular)/vmap()/triangular_solve | solution.py:134
  285.0 0.9 fusion.188
  285.9 1.2 bitcast_multiply_fusion.9
  288.6 9.9 %custom-call.8 = f32[2,1,64,64]{2,3,1,0:T(8,128)S(1)} custom-call(f32[2,1,64,64]{3,2,1,0:T(8,128)S(1)} %fusion.192), custom_call_target="InvertDiagBlocksLowerTriangular" | custom-call | tf_op jit(solution)/shard_map/while/body/eval_jaxpr/jit(_solve_triangular)/vmap()/triangular_solve | solution.py:134
  299.8 0.9 fusion.188
  300.8 1.2 bitcast_multiply_fusion.9
  303.5 9.9 %custom-call.8 = f32[2,1,64,64]{2,3,1,0:T(8,128)S(1)} custom-call(f32[2,1,64,64]{3,2,1,0:T(8,128)S(1)} %fusion.192), custom_call_target="InvertDiagBlocksLowerTriangular" | custom-call | tf_op jit(solution)/shard_map/while/body/eval_jaxpr/jit(_solve_triangular)/vmap()/triangular_solve | solution.py:134
  314.7 0.9 fusion.188
  315.6 1.2 bitcast_multiply_fusion.9
  318.3 9.8 %custom-call.8 = f32[2,1,64,64]{2,3,1,0:T(8,128)S(1)} custom-call(f32[2,1,64,64]{3,2,1,0:T(8,128)S(1)} %fusion.192), custom_call_target="InvertDiagBlocksLowerTriangular" | custom-call | tf_op jit(solution)/shard_map/while/body/eval_jaxpr/jit(_solve_triangular)/vmap()/triangular_solve | solution.py:134
  330.4 1.2 bitcast_multiply_fusion.9
  333.1 9.8 %custom-call.8 = f32[2,1,64,64]{2,3,1,0:T(8,128)S(1)} custom-call(f32[2,1,64,64]{3,2,1,0:T(8,128)S(1)} %fusion.192), custom_call_target="InvertDiagBlocksLowerTriangular" | custom-call | tf_op jit(solution)/shard_map/while/body/eval_jaxpr/jit(_solve_triangular)/vmap()/triangular_solve | solution.py:134
  345.3 1.2 bitcast_multiply_fusion.9
  347.9 9.8 %custom-call.8 = f32[2,1,64,64]{2,3,1,0:T(8,128)S(1)} custom-call(f32[2,1,64,64]{3,2,1,0:T(8,128)S(1)} %fusion.192), custom_call_target="InvertDiagBlocksLowerTriangular" | custom-call | tf_op jit(solution)/shard_map/while/body/eval_jaxpr/jit(_solve_triangular)/vmap()/triangular_solve | solution.py:134
  360.1 1.2 bitcast_multiply_fusion.9
  362.8 9.8 %custom-call.8 = f32[2,1,64,64]{2,3,1,0:T(8,128)S(1)} custom-call(f32[2,1,64,64]{3,2,1,0:T(8,128)S(1)} %fusion.192), custom_call_target="InvertDiagBlocksLowerTriangular" | custom-call | tf_op jit(solution)/shard_map/while/body/eval_jaxpr/jit(_solve_triangular)/vmap()/triangular_solve | solution.py:134
  374.9 1.2 bitcast_multiply_fusion.9
  377.6 9.8 %custom-call.8 = f32[2,1,64,64]{2,3,1,0:T(8,128)S(1)} custom-call(f32[2,1,64,64]{3,2,1,0:T(8,128)S(1)} %fusion.192), custom_call_target="InvertDiagBlocksLowerTriangular" | custom-call | tf_op jit(solution)/shard_map/while/body/eval_jaxpr/jit(_solve_triangular)/vmap()/triangular_solve | solution.py:134
  389.7 1.2 bitcast_multiply_fusion.9
  392.4 9.8 %custom-call.8 = f32[2,1,64,64]{2,3,1,0:T(8,128)S(1)} custom-call(f32[2,1,64,64]{3,2,1,0:T(8,128)S(1)} %fusion.192), custom_call_target="InvertDiagBlocksLowerTriangular" | custom-call | tf_op jit(solution)/shard_map/while/body/eval_jaxpr/jit(_solve_triangular)/vmap()/triangular_solve | solution.py:134
  404.6 1.2 bitcast_multiply_fusion.9
  407.3 9.8 %custom-call.8 = f32[2,1,64,64]{2,3,1,0:T(8,128)S(1)} custom-call(f32[2,1,64,64]{3,2,1,0:T(8,128)S(1)} %fusion.192), custom_call_target="InvertDiagBlocksLowerTriangular" | custom-call | tf_op jit(solution)/shard_map/while/body/eval_jaxpr/jit(_solve_triangular)/vmap()/triangular_solve | solution.py:134
  419.4 1.2 bitcast_multiply_fusion.9
  422.1 9.8 %custom-call.8 = f32[2,1,64,64]{2,3,1,0:T(8,128)S(1)} custom-call(f32[2,1,64,64]{3,2,1,0:T(8,128)S(1)} %fusion.192), custom_call_target="InvertDiagBlocksLowerTriangular" | custom-call | tf_op jit(solution)/shard_map/while/body/eval_jaxpr/jit(_solve_triangular)/vmap()/triangular_solve | solution.py:134
  434.2 1.2 bitcast_multiply_fusion.9
  436.9 9.8 %custom-call.8 = f32[2,1,64,64]{2,3,1,0:T(8,128)S(1)} custom-call(f32[2,1,64,64]{3,2,1,0:T(8,128)S(1)} %fusion.192), custom_call_target="InvertDiagBlocksLowerTriangular" | custom-call | tf_op jit(solution)/shard_map/while/body/eval_jaxpr/jit(_solve_triangular)/vmap()/triangular_solve | solution.py:134
  449.1 1.2 bitcast_multiply_fusion.9
  451.7 9.8 %custom-call.8 = f32[2,1,64,64]{2,3,1,0:T(8,128)S(1)} custom-call(f32[2,1,64,64]{3,2,1,0:T(8,128)S(1)} %fusion.192), custom_call_target="InvertDiagBlocksLowerTriangular" | custom-call | tf_op jit(solution)/shard_map/while/body/eval_jaxpr/jit(_solve_triangular)/vmap()/triangular_solve | solution.py:134
  463.9 1.2 bitcast_multiply_fusion.9
  466.6 9.8 %custom-call.8 = f32[2,1,64,64]{2,3,1,0:T(8,128)S(1)} custom-call(f32[2,1,64,64]{3,2,1,0:T(8,128)S(1)} %fusion.192), custom_call_target="InvertDiagBlocksLowerTriangular" | custom-call | tf_op jit(solution)/shard_map/while/body/eval_jaxpr/jit(_solve_triangular)/vmap()/triangular_solve | solution.py:134
  479.0 7.5 %all-to-all-start = ((bf16[16,256,64]{1,2,0:T(8,128)(2,1)}), bf16[16,256,64]{1,2,0:T(8,128)(2,1)S(1)}, u32[]{:S(2)}, u32[]{:S(2)}) async-start(bf16[16,256,64]{1,2,0:T(8,128)(2,1)} %broadcast_in_dim.79), calls=%async_computation | async-start | bytes 1048576 | tf_op jit(solution)/shard_map/all_to_all | solution.py:29
  486.8 3.7 fusion.58
  490.5 2.3 fusion.57
  492.9 3.8 collective-permute-start
  498.0 10.0 %fusion.79 = f32[1024,2048]{1,0:T(8,128)} fusion(bf16[2048,256]{1,0:T(8,128)(2,1)} %all-gather.8.cloned.1.call-done, f32[2,128]{1,0:T(2,128)S(1)} %collective-permute-done, f32[1024,128]{1,0:T(8,128)S(1)} %fusion.57, bf16[1024,2048]{1,0:T(8,128)(2,1)} %all-gather.4.cloned.1.call-done, bf16[2048,1024]{1,0:T(8,128)(2,1)} %all-gather.6.cloned.1.call-done, ...), kind=kOutput, calls=%fused_computation.125 | convolution fusion | flops 1075183616 | bytes 14158336 | tf_op jit(solution)/shard_map/dot_general | solution.py:262
  511.1 6.8 %add_convert_fusion = bf16[1024,2048]{1,0:T(8,128)(2,1)} fusion(f32[1024,2048]{1,0:T(8,128)} %fusion.79, bf16[1024,128]{0,1:T(8,128)(2,1)S(1)} %bitcast.179, bf16[2048,256]{1,0:T(8,128)(2,1)} %all-gather.8.cloned.1.call-done), kind=kOutput, calls=%fused_computation.74 | convolution fusion | flops 541065216 | bytes 13369344 | tf_op jit(solution)/shard_map/dot_general | solution.py:263
  517.9 49.1 %reduce-scatter.2.cloned.1.call-done = bf16[128,2048]{1,0:T(8,128)(2,1)} async-done(((bf16[1024,2048]{1,0:T(8,128)(2,1)}), bf16[128,2048]{1,0:T(8,128)(2,1)}) %reduce-scatter.2.cloned.1.call-update) | async-done | bytes 524304 | tf_op jit(solution)/shard_map/reduce_scatter | solution.py:260
  (354 shorter events, 68.0 us)
Async XLA Ops:
  6.5 503.9 %copy-start = (f32[1,2,64,64]{3,2,1,0:T(8,128)S(1)}, f32[1,2,64,64]{3,2,1,0:T(8,128)}, u32[]{:S(2)}) copy-start(f32[1,2,64,64]{3,2,1,0:T(8,128)} %param.34) | copy-start | bytes 98308
  6.5 47.6 %all-gather.4.cloned.1.call-start = ((), (), s32[]{:S(2)}) async-start(), calls=%async_computation.2 | async-start | bytes 4718592 | tf_op jit(solution)/shard_map/all_gather | solution.py:194
  9.9 191.9 %all-gather.6.cloned.1.call-start = ((), (), s32[]{:S(2)}) async-start(), calls=%async_computation.3 | async-start | bytes 4259840 | tf_op jit(solution)/shard_map/all_gather | solution.py:23
  15.5 0.6 copy-start.2
  16.2 480.9 %all-gather.8.cloned.1.call-start = ((), (), s32[]{:S(2)}) async-start(), calls=%async_computation.4 | async-start | bytes 1064960 | tf_op jit(solution)/shard_map/all_gather | solution.py:78
  240.5 246.3 %copy-start.3 = (f32[3,128]{1,0:T(4,128)S(1)}, f32[3,128]{1,0:T(4,128)}, u32[]{:S(2)}) copy-start(f32[3,128]{1,0:T(4,128)} %param.25) | copy-start | bytes 4612
  479.0 29.0 %all-to-all-start = ((bf16[16,256,64]{1,2,0:T(8,128)(2,1)}), bf16[16,256,64]{1,2,0:T(8,128)(2,1)S(1)}, u32[]{:S(2)}, u32[]{:S(2)}) async-start(bf16[16,256,64]{1,2,0:T(8,128)(2,1)} %broadcast_in_dim.79), calls=%async_computation | async-start | bytes 1048576 | tf_op jit(solution)/shard_map/all_to_all | solution.py:29
  486.6 80.5 %reduce-scatter.2.cloned.1.call-start = ((), (), s32[]{:S(2)}) async-start(), calls=%async_computation.5 | async-start | bytes 4718592 | tf_op jit(solution)/shard_map/reduce_scatter | solution.py:260
  486.8 3.7 copy-start.1
  490.5 6.2 %copy-start.4 = (f32[128]{0:T(128)S(1)}, f32[128]{0:T(128)}, u32[]{:S(2)}) copy-start(f32[128]{0:T(128)} %param.35) | copy-start | bytes 1540
  492.9 5.1 collective-permute-start
Sparse Core Ops, SparseCore 0:
  10.0 44.0 all-gather.3
  57.0 144.6 all-gather.5
  204.7 136.9 all-gather.7
  518.1 48.9 reduce-scatter.1
where the time goes:
time: 577 us; the launch traced here: 574 us
  waiting for transfers between devices  230 us (40%)
  other arithmetic  205 us (36%)
  matrix products  75.6 us (13%)
  local copies, waits for them, and re-layouts  36.4 us (6%)
  between operations  13.5 us (2%)
  starting transfers between devices  11.7 us (2%)
    another operation x32, other arithmetic, block_pass(): jax.scipy.linalg.solve_triangular(system, right_side, lower=True, unit_di...  157 us
    all_gather x1, waiting for transfers between devices, side_by_side(): out = lax.all_gather(both, axis, axis=dim, tiled=True)  148 us
    reduce_scatter x1, waiting for transfers between devices, on_device(): lax.psum_scatter((jnp.dot(conv_mixed, conv_whole, preferred_element_type=...  49.1 us
    all_gather x1, waiting for transfers between devices, on_device(): piece = lax.all_gather(normed, 'tp', axis=0, tiled=True)  32.2 us
    dot_general x7, matrix products, project(): jnp.dot(activations, weight, preferred_element_type=jnp.float32)  27.1 us
    mul x16, other arithmetic, block_pass(): ask_reads = queries * jnp.exp(cumulative - middle)  19.7 us
    another operation x16, other arithmetic, block_pass(): cumulative = jnp.cumsum(logarithm_decay, axis=0)  14.6 us
    dynamic_slice x32, local copies, waits for them, and re-layouts, on_device(): lax.scan(block_pass, initial_rows, tuple((in_blocks(array) for array in (...  12.7 us
  transfers between devices with their start and end apart: 6, of which 4 were waited for; matrix products, arithmetic and copies ran while one was open for 53% of the time, Pallas kernels for 0%

commit v1 on v0

v1 whole, which is shorter than its diff:
```python
import functools

import jax
import jax.numpy as jnp
from jax import lax
from jax.experimental import pallas as pl
from jax.experimental.pallas import tpu as pltpu
from jax.sharding import PartitionSpec as P

HEAD_WIDTH = 64
CHUNK = 64
BLOCK = 256
norm_eps = 1e-06
key_eps = 1e-06
f32, bf16 = jnp.float32, jnp.bfloat16


def dot(a, b, ca=1, cb=0):
    return lax.dot_general(
        a.astype(bf16), b.astype(bf16), (((ca,), (cb,)), ((), ())), preferred_element_type=f32
    )


def lanes_of(shape):
    return lax.broadcasted_iota(jnp.int32, shape, 1)


def rows_of(shape):
    return lax.broadcasted_iota(jnp.int32, shape, 0)


def spread(z, first):
    z = z.astype(bf16)
    return jnp.concatenate([z * first, z * (1 - first)], axis=0)


def head_sums(z, low):
    a = jnp.sum(jnp.where(low, z, 0.0), axis=1, keepdims=True)
    b = jnp.sum(jnp.where(low, 0.0, z), axis=1, keepdims=True)
    return jnp.where(low, a, b)


def local_kernel(x_ref, w_ref, spike_ref, vec_ref, conv_ref, o_ref, y_ref, agg_ref, edge_ref, st_ref, tail_ref):
    step = pl.program_id(0)
    width = 2 * HEAD_WIDTH
    pairs = BLOCK // CHUNK

    @pl.when(step == 0)
    def _():
        r, l = rows_of((width, width)), lanes_of((width, width))
        eye = (r - HEAD_WIDTH == l % HEAD_WIDTH) & (r >= HEAD_WIDTH)
        st_ref[...] = jnp.where(eye, 1.0, 0.0).astype(f32)
        tail_ref[...] = jnp.zeros_like(tail_ref)

    x = x_ref[...]

    def section(k):
        two = jnp.dot(x, w_ref[:, 2 * k * width : 2 * (k + 1) * width], preferred_element_type=f32)
        two = two.astype(bf16).astype(f32)
        return two[:, :width], two[:, width:]

    pre, post = section(0)
    cvals, q = section(1)
    keys, vals = section(2)
    dpre, rpre = section(3)

    prod = pre * cvals
    tail = tail_ref[...]
    row = rows_of((BLOCK, width))
    last, before = tail[7:8], tail[6:7]
    one = jnp.where(row == 0, last, pltpu.roll(prod, 1, 0))
    two = jnp.where(row == 0, before, jnp.where(row == 1, last, pltpu.roll(prod, 2, 0)))
    filtered = vec_ref[2:3] * two + vec_ref[3:4] * one + vec_ref[4:5] * prod
    conv_ref[...] = (post * filtered).astype(bf16)
    tail_ref[...] = prod[BLOCK - 8 :]

    @pl.when(step == 0)
    def _():
        edge_ref[0:8] = prod[:8]
        edge_ref[8:16] = post[:8]

    @pl.when(step == pl.num_programs(0) - 1)
    def _():
        edge_ref[16:24] = prod[BLOCK - 8 :]

    low = lanes_of((BLOCK, width)) < HEAD_WIDTH
    logd = spike_ref[...] - jnp.exp(vec_ref[0:1] + jnp.tanh(dpre))
    rate = jax.nn.sigmoid(vec_ref[1:2] + rpre)
    unit = keys * lax.rsqrt(head_sums(keys * keys, low) + key_eps)
    beta = rate * unit
    r, c = rows_of((BLOCK, BLOCK)), lanes_of((BLOCK, BLOCK))
    tri = jnp.where((r >= c) & (r // CHUNK == c // CHUNK), 1.0, 0.0).astype(bf16)
    hi = logd.astype(bf16)
    rest = logd - hi.astype(f32)
    mid = rest.astype(bf16)
    lo = (rest - mid.astype(f32)).astype(bf16)
    sums = jnp.dot(tri, jnp.concatenate([hi, mid, lo], axis=1), preferred_element_type=f32)
    cum_all = sums[:, :width] + sums[:, width : 2 * width] + sums[:, 2 * width :]
    prev_all = cum_all - logd

    shape = (CHUNK, width)
    t, s = rows_of(shape), lanes_of(shape) % HEAD_WIDTH
    strict, inclusive = t > s, t >= s
    low_c = lanes_of(shape) < HEAD_WIDTH
    first = jnp.where(lanes_of((1, width)) < HEAD_WIDTH, 1.0, 0.0).astype(bf16)
    fold = functools.partial(spread, first=first)
    same = (rows_of((width, width)) // HEAD_WIDTH) == (lanes_of((width, width)) // HEAD_WIDTH)
    each = range(pairs)

    def part(a):
        return [a[k * CHUNK : (k + 1) * CHUNK] for k in each]

    q, keys, vals, unit, beta = map(part, (q, keys, vals, unit, beta))
    cum, prev = part(cum_all), part(prev_all)
    center = [cum[k][CHUNK // 2 : CHUNK // 2 + 1] for k in each]
    close = [cum[k][CHUNK - 1 : CHUNK] for k in each]
    e_neg = [jnp.exp(center[k] - cum[k]) for k in each]
    ask_k = [unit[k] * jnp.exp(prev[k] - center[k]) for k in each]
    ask_q = [q[k] * jnp.exp(cum[k] - center[k]) for k in each]
    give_k = [keys[k] * e_neg[k] for k in each]
    give_b = [beta[k] * e_neg[k] for k in each]
    e_center = [jnp.exp(center[k]) for k in each]
    e_tail = [jnp.exp(close[k] - center[k]) for k in each]
    e_close = [jnp.exp(close[k]) for k in each]
    grams = [
        dot(
            jnp.concatenate([ask_k[k], ask_q[k]], axis=0),
            jnp.concatenate([fold(give_k[k]), fold(give_b[k])], axis=0),
            1,
            1,
        )
        for k in each
    ]
    key_ask = [jnp.where(strict, g[:CHUNK, :width], 0.0) for g in grams]
    beta_ask = [jnp.where(strict, g[:CHUNK, width:], 0.0) for g in grams]
    key_read = [jnp.where(inclusive, g[CHUNK:, :width], 0.0) for g in grams]
    beta_read = [jnp.where(inclusive, g[CHUNK:, width:], 0.0) for g in grams]
    both_v = [dot(jnp.concatenate([key_ask[k], key_read[k]], axis=0), fold(vals[k])) for k in each]

    inv = [jnp.where(t == s, 1.0, jnp.where(t // 2 == s // 2, -beta_ask[k], 0.0)) for k in each]
    size = 2
    while size < CHUNK:
        here = (t // (2 * size) == s // (2 * size)) & (t // size != s // size)
        mixed = [dot(inv[k], fold(jnp.where(here, beta_ask[k], 0.0))) for k in each]
        inv = [inv[k] - dot(mixed[k], fold(inv[k])) for k in each]
        size *= 2

    wu = [
        dot(
            inv[k],
            jnp.concatenate([fold(ask_k[k] * e_center[k]), fold(both_v[k][:CHUNK])], axis=1),
        )
        for k in each
    ]
    back = [
        dot(
            beta_read[k],
            jnp.concatenate([fold(wu[k][:, :width]), fold(wu[k][:, width:])], axis=1),
        )
        for k in each
    ]
    q_eff = [ask_q[k] * e_center[k] - back[k][:, :width] for k in each]
    o_loc = [both_v[k][CHUNK:] - back[k][:, width:] for k in each]
    outer = [dot(wu[k], give_b[k] * e_tail[k], 0, 0) for k in each]
    outer_v = [dot(vals[k], give_k[k] * e_tail[k], 0, 0) for k in each]
    step_map = [jnp.where(same, -outer[k][:width], 0.0).astype(bf16) for k in each]
    source_full = [outer_v[k] - outer[k][width:] for k in each]
    source = [jnp.where(low_c, f[:HEAD_WIDTH], f[HEAD_WIDTH:]) for f in source_full]

    state = st_ref[...]
    for k in each:
        got = dot(
            q_eff[k],
            jnp.concatenate([fold(state[:HEAD_WIDTH]), fold(state[HEAD_WIDTH:])], axis=0),
            1,
            1,
        )
        o_ref[k * CHUNK : (k + 1) * CHUNK] = o_loc[k] + got[:, :width]
        y_ref[k * CHUNK : (k + 1) * CHUNK] = got[:, width:].astype(bf16)
        state = state * e_close[k] + dot(state, step_map[k])
        state = jnp.concatenate([state[:HEAD_WIDTH] + source[k], state[HEAD_WIDTH:]], axis=0)
    st_ref[...] = state

    @pl.when(step == pl.num_programs(0) - 1)
    def _():
        agg_ref[...] = state.astype(bf16)


def local_call(x, w, spike, vec):
    rows, depth = x.shape
    width = 2 * HEAD_WIDTH
    whole = lambda *shape: pl.BlockSpec(shape, lambda i: (0,) * len(shape))
    tile = pl.BlockSpec((BLOCK, width), lambda i: (i, 0))
    return pl.pallas_call(
        local_kernel,
        grid=(rows // BLOCK,),
        in_specs=[
            pl.BlockSpec((BLOCK, depth), lambda i: (i, 0)),
            pl.BlockSpec((depth, 8 * width), lambda i: (0, 0)),
            tile,
            whole(8, width),
        ],
        out_specs=[tile, tile, tile, whole(width, width), whole(24, width)],
        out_shape=[
            jax.ShapeDtypeStruct((rows, width), bf16),
            jax.ShapeDtypeStruct((rows, width), f32),
            jax.ShapeDtypeStruct((rows, width), bf16),
            jax.ShapeDtypeStruct((width, width), bf16),
            jax.ShapeDtypeStruct((24, width), f32),
        ],
        scratch_shapes=[pltpu.VMEM((width, width), f32), pltpu.VMEM((8, width), f32)],
        compiler_params=pltpu.CompilerParams(
            dimension_semantics=("arbitrary",), vmem_limit_bytes=50 * 2**20
        ),
        name="local_mix",
    )(x, w, spike, vec)


def finish_kernel(pos_ref, agg_ref, init_ref, o_ref, y_ref, conv_ref, edge_ref, prior_ref, vec_ref, w_ref, out_ref, s_ref):
    step = pl.program_id(0)
    width = 2 * HEAD_WIDTH
    first = jnp.where(lanes_of((1, width)) < HEAD_WIDTH, 1.0, 0.0).astype(bf16)

    @pl.when(step == 0)
    def _():
        def advance(i, state):
            piece = agg_ref[i]
            hi = state.astype(bf16)
            lo = (state - hi.astype(f32)).astype(bf16)
            got = dot(jnp.concatenate([hi, lo], axis=0), spread(piece[HEAD_WIDTH:], first))
            return got[:HEAD_WIDTH] + got[HEAD_WIDTH:] + piece[:HEAD_WIDTH].astype(f32)

        state = lax.fori_loop(0, pos_ref[0], advance, init_ref[...])
        s_ref[...] = spread(state, first)

    low = lanes_of((BLOCK, width)) < HEAD_WIDTH
    reads = o_ref[...] + dot(y_ref[...], s_ref[...], 1, 1)
    centered = reads - head_sums(reads, low) * (1.0 / HEAD_WIDTH)
    variance = head_sums(centered * centered, low) * (1.0 / HEAD_WIDTH)
    mixed = centered * lax.rsqrt(variance + HEAD_WIDTH * 1e-05) * vec_ref[5:6]

    prod, post = edge_ref[0:8], edge_ref[8:16]
    last, before = prior_ref[1:2], prior_ref[0:1]
    row = rows_of((8, width))
    one = jnp.where(row == 0, last, pltpu.roll(prod, 1, 0))
    two = jnp.where(row == 0, before, jnp.where(row == 1, last, pltpu.roll(prod, 2, 0)))
    fixed = post * (vec_ref[2:3] * two + vec_ref[3:4] * one + vec_ref[4:5] * prod)
    conv = conv_ref[...]
    head = jnp.where((step == 0) & (rows_of((16, width)) < 2), jnp.concatenate([fixed, fixed], axis=0), conv[:16].astype(f32))
    conv = jnp.concatenate([head.astype(bf16), conv[16:]], axis=0)
    both = jnp.concatenate([conv, mixed.astype(bf16)], axis=1)
    out_ref[...] = dot(both, w_ref[...], 1, 1).astype(bf16)


def finish_call(pos, agg, init, o, y, conv, edge, prior, vec, w):
    rows, width = o.shape
    whole = lambda a: pl.BlockSpec(a.shape, lambda i, p: (0,) * a.ndim)
    tile = pl.BlockSpec((BLOCK, width), lambda i, p: (i, 0))
    return pl.pallas_call(
        finish_kernel,
        grid_spec=pltpu.PrefetchScalarGridSpec(
            num_scalar_prefetch=1,
            grid=(rows // BLOCK,),
            in_specs=[
                whole(agg), whole(init), tile, tile, tile, whole(edge), whole(prior), whole(vec),
                pl.BlockSpec((w.shape[0], 2 * width), lambda i, p: (0, 4)),
            ],
            out_specs=pl.BlockSpec((BLOCK, w.shape[0]), lambda i, p: (i, 0)),
            scratch_shapes=[pltpu.VMEM((width, width), bf16)],
        ),
        out_shape=jax.ShapeDtypeStruct((rows, w.shape[0]), bf16),
        compiler_params=pltpu.CompilerParams(
            dimension_semantics=("arbitrary",), vmem_limit_bytes=50 * 2**20
        ),
        name="finish_mix",
    )(pos, agg, init, o, y, conv, edge, prior, vec, w)


def pack_kernel(*refs):
    *parts, out_ref = refs
    for k, ref in enumerate(parts):
        piece = ref[...]
        if piece.shape[0] > piece.shape[1]:
            piece = piece.astype(f32).T.astype(bf16)
        out_ref[:, k * 128 : (k + 1) * 128] = piece


def packed(*shards):
    rows, width = shards[0].shape
    return pl.pallas_call(
        pack_kernel,
        out_shape=jax.ShapeDtypeStruct((rows, len(shards) * width), bf16),
        name="pack_shards",
    )(*shards)


def passed_along(block, axis, distance):
    devices = range(lax.axis_size(axis))
    route = [(i - distance, i) for i in devices if i - distance in devices]
    return lax.ppermute(block, axis, route)


def from_everyone(x, axis):
    devices = lax.axis_size(axis)
    return lax.all_to_all(jnp.broadcast_to(x[None], (devices, *x.shape)), axis, 0, 0, tiled=True)


def rms_rows(activations, gain_vector):
    values = activations.astype(f32)
    inv_scale = lax.rsqrt(jnp.mean(values * values, axis=-1, keepdims=True) + norm_eps)
    return (values * inv_scale * gain_vector).astype(bf16)


def on_device(
    tokens,
    input_norm_gain,
    earlier_gate,
    later_gate,
    convolution_input,
    convolution_taps,
    receptance,
    key_matrix,
    value_matrix,
    decay_matrix,
    rate_matrix,
    decay_floor,
    rate_offset,
    decay_spike,
    initial_state,
    head_norm_gain,
    convolution_output,
    state_heads_output,
):
    normed = rms_rows(tokens[0], input_norm_gain)
    channels = earlier_gate.shape[1]
    heads = channels // HEAD_WIDTH
    both = packed(
        earlier_gate,
        later_gate,
        convolution_input,
        receptance,
        key_matrix,
        value_matrix,
        decay_matrix,
        rate_matrix,
        convolution_output,
        state_heads_output,
    )
    weights = lax.all_gather(both, "fs", axis=0, tiled=True)
    weights = lax.all_gather(weights, "sp", axis=0, tiled=True)
    piece = from_everyone(normed, "tp").reshape(-1, normed.shape[1])
    vec = jnp.concatenate(
        [
            decay_floor[None],
            rate_offset[None],
            convolution_taps,
            head_norm_gain[None],
            jnp.zeros((2, channels), f32),
        ],
        axis=0,
    )
    conv, o, y, agg, edge = local_call(piece, weights, decay_spike[0], vec)
    pieces = from_everyone(agg, "sp")
    prior = passed_along(edge[22:24], "sp", 1)
    init = jnp.moveaxis(initial_state[0], 0, 1).reshape(HEAD_WIDTH, heads * HEAD_WIDTH)
    pos = lax.axis_index("sp").astype(jnp.int32)[None]
    partial = finish_call(pos, pieces, init, o, y, conv, edge, prior, vec, weights)
    mixed = lax.psum_scatter(partial, "tp", scatter_dimension=0, tiled=True)
    return mixed[None]


def solution(mesh):
    placed = (
        P("fs", ("sp", "tp"), None),
        P(),
        P(("sp", "fs"), "tp"),
        P(("sp", "fs"), "tp"),
        P(("sp", "fs"), "tp"),
        P(None, "tp"),
        P(("sp", "fs"), "tp"),
        P(("sp", "fs"), "tp"),
        P(("sp", "fs"), "tp"),
        P(("sp", "fs"), "tp"),
        P(("sp", "fs"), "tp"),
        P("tp"),
        P("tp"),
        P("fs", "sp", "tp"),
        P("fs", "tp", None, None),
        P("tp"),
        P("tp", ("sp", "fs")),
        P("tp", ("sp", "fs")),
    )
    return jax.shard_map(
        on_device,
        mesh=mesh,
        in_specs=placed,
        out_specs=P("fs", ("sp", "tp"), None),
        check_vma=False,
    )
```

time: 577 us -> 213 us (0.37)
  other arithmetic: 205 us -> 2.48 us
  waiting for transfers between devices: 230 us -> 131 us
  matrix products: 75.6 us -> 0 us
  local copies, waits for them, and re-layouts: 36.4 us -> 6.55 us
  Pallas kernels: 0 us -> 25.1 us
  blocking collectives: 0 us -> 17.4 us
    another operation x49 -> x0, other arithmetic: 172 us -> none  [the longest x32 157 us: block_pass(): jax.scipy.linalg.solve_triangular(system, right_side, lower=True, unit_di...]
    all_gather x3 -> x1, waiting for transfers between devices: 180 us -> 21.4 us  [on_device(): weights = lax.all_gather(weights, 'sp', axis=0, tiled=True)]
    dot_general x146 -> x0, matrix products: 70.9 us -> none  [the longest x7 27.1 us: project(): jnp.dot(activations, weight, preferred_element_type=jnp.float32)]
    all_to_all x1 -> x2, waiting for transfers between devices: 0.01 us -> 59.8 us  [from_everyone(): lax.all_to_all(jnp.broadcast_to(x[None], (devices, *x.shape)), axis, 0, 0...]
    pallas_call x0 -> x3, Pallas kernels: none -> 25.1 us  [the longest x1 17.7 us: local_call(): pl.pallas_call(local_kernel, grid=(rows // BLOCK,), in_specs=[pl.BlockSpe...]
    mul x17 -> x0, other arithmetic: 23.7 us -> none  [the longest x16 19.7 us: block_pass(): ask_reads = queries * jnp.exp(cumulative - middle)]
    all_gather x0 -> x1, blocking collectives: none -> 17.4 us  [on_device(): weights = lax.all_gather(both, 'fs', axis=0, tiled=True)]
    dynamic_slice x32 -> x0, local copies, waits for them, and re-layouts: 12.7 us -> none  [on_device(): lax.scan(block_pass, initial_rows, tuple((in_blocks(array) for array in (...]
  transfers between devices with their start and end apart: 6 -> 5, of which waited for: 4 -> 5; matrix products, arithmetic and copies ran while one was open for 53% -> 2% of each run, Pallas kernels for 0% -> 0%
where the time goes in v1:
time: 213 us; the launch traced here: 212 us
  waiting for transfers between devices  131 us (62%)
  Pallas kernels  25.1 us (12%)
  blocking collectives  17.4 us (8%)
  starting transfers between devices  15.6 us (7%)
  between operations  13.5 us (6%)
  local copies, waits for them, and re-layouts  6.55 us (3%)
  other arithmetic  2.48 us (1%)
    all_to_all x2, waiting for transfers between devices, from_everyone(): lax.all_to_all(jnp.broadcast_to(x[None], (devices, *x.shape)), axis, 0, 0...  59.8 us
    reduce_scatter x1, waiting for transfers between devices, on_device(): mixed = lax.psum_scatter(partial, 'tp', scatter_dimension=0, tiled=True)  42.9 us
    all_gather x1, waiting for transfers between devices, on_device(): weights = lax.all_gather(weights, 'sp', axis=0, tiled=True)  21.4 us
    pallas_call x1, Pallas kernels, local_call(): pl.pallas_call(local_kernel, grid=(rows // BLOCK,), in_specs=[pl.BlockSpe...  17.7 us
    all_gather x1, blocking collectives, on_device(): weights = lax.all_gather(both, 'fs', axis=0, tiled=True)  17.4 us
    all_to_all x2, starting transfers between devices, from_everyone(): lax.all_to_all(jnp.broadcast_to(x[None], (devices, *x.shape)), axis, 0, 0...  11.7 us
    ppermute x1, waiting for transfers between devices, passed_along(): return lax.ppermute(block, axis, route)  7.25 us
    pallas_call x1, Pallas kernels, finish_call(): pl.pallas_call(finish_kernel, grid_spec=pltpu.PrefetchScalarGridSpec(num_...  5.72 us
  transfers between devices with their start and end apart: 5, of which 5 were waited for; matrix products, arithmetic and copies ran while one was open for 2% of the time, Pallas kernels for 0%

profile of v1, /device:TPU:8, one launch (start us, length us, event | category | flops | bytes accessed | tf_op | source)
XLA Modules:
  0.0 212.0 jit_solution(3521013365216828624)
XLA Ops:
  6.5 0.0 all-gather.2.cloned.1.call-start
  6.5 1.4 copy.19.refs_8_
  7.9 1.4 copy.20.refs_9_
  9.4 1.6 pack_shards.1
  11.0 17.4 %all_gather.6 = bf16[128,1280]{1,0:T(8,128)(2,1)} all-gather(bf16[32,1280]{1,0:T(8,128)(2,1)} %pack_shards.1), channel_id=1, replica_groups=mesh['sp'=16,'fs'=4,'tp'=8] {'fs'}, dimensions={0}, use_global_device_ids=true | all-gather | bytes 409600 | tf_op jit(solution)/shard_map/all_gather | solution.py:349
  28.4 0.0 all-gather.2.cloned.1.call-update
  28.4 1.2 fusion
  29.7 1.2 fusion.3
  30.9 2.6 %broadcast_in_dim.36 = bf16[8,128,2048]{2,1,0:T(8,128)(2,1)} broadcast(bf16[128,2048]{1,0:T(8,128)(2,1)S(1)} %fusion.3), dimensions={1,2} | broadcast | bytes 4718592 | tf_op jit(solution)/shard_map/broadcast_in_dim | solution.py:305
  33.5 0.0 copy-start.2
  33.5 0.0 copy-start.3
  33.5 0.0 copy-start.4
  33.5 0.0 copy-start.5
  33.5 0.0 copy-start
  33.6 4.7 %all-to-all-start = ((bf16[8,128,2048]{2,1,0:T(8,128)(2,1)}), bf16[8,128,2048]{2,1,0:T(8,128)(2,1)}, u32[]{:S(2)}, u32[]{:S(2)}) async-start(bf16[8,128,2048]{2,1,0:T(8,128)(2,1)} %broadcast_in_dim.36), calls=%async_computation | async-start | bytes 8388608 | tf_op jit(solution)/shard_map/all_to_all | solution.py:305
  38.3 0.0 copy-done.2
  38.3 0.0 copy-done.3
  38.3 0.0 copy-done.4
  38.4 0.0 copy-done.5
  38.4 49.6 %all-to-all-done = bf16[8,128,2048]{2,1,0:T(8,128)(2,1)} async-done(((bf16[8,128,2048]{2,1,0:T(8,128)(2,1)}), bf16[8,128,2048]{2,1,0:T(8,128)(2,1)}, u32[]{:S(2)}, u32[]{:S(2)}) %all-to-all-start) | async-done | bytes 4194336 | tf_op jit(solution)/shard_map/all_to_all | solution.py:305
  88.0 21.4 %all-gather.2.cloned.1.call-done.w_ref = bf16[2048,1280]{1,0:T(8,128)(2,1)} async-done(((bf16[128,1280]{1,0:T(8,128)(2,1)}), bf16[2048,1280]{1,0:T(8,128)(2,1)}) %all-gather.2.cloned.1.call-update) | async-done | bytes 5242896 | tf_op jit(solution)/shard_map/all_gather | solution.py:350
  109.3 0.0 copy-done
  109.3 0.0 copy-start.1
  109.3 17.7 %local_mix.1 = (bf16[1024,128]{1,0:T(8,128)(2,1)S(1)}, f32[1024,128]{1,0:T(8,128)S(1)}, bf16[1024,128]{1,0:T(8,128)(2,1)S(1)}, bf16[128,128]{1,0:T(8,128)(2,1)S(1)}, f32[24,128]{1,0:T(8,128)S(1)}) custom-call(bf16[1024,2048]{1,0:T(8,128)(2,1)} %bitcast.2.x_ref, bf16[2048,1280]{1,0:T(8,128)(2,1)} %all-gather.2.cloned.1.call-done.w_ref, ...), custom_call_target="tpu_custom_call" | custom-call | tf_op jit(solution)/shard_map/local_mix/pallas_call | solution.py:194
  127.1 0.9 broadcast_in_dim.41
  128.0 7.0 %all-to-all-start.1 = ((bf16[16,128,128]{2,1,0:T(8,128)(2,1)}), bf16[16,128,128]{2,1,0:T(8,128)(2,1)S(1)}, u32[]{:S(2)}, u32[]{:S(2)}) async-start(bf16[16,128,128]{2,1,0:T(8,128)(2,1)} %broadcast_in_dim.41), calls=%async_computation.1 | async-start | bytes 1048576 | tf_op jit(solution)/shard_map/all_to_all | solution.py:305
  135.0 0.0 reduce-scatter.2.cloned.1.call-start
  135.0 3.8 %collective-permute-start = (f32[2,128]{1,0:T(2,128)S(1)}, f32[2,128]{1,0:T(2,128)S(1)}, u32[]{:S(2)}, u32[]{:S(2)}) collective-permute-start(f32[2,128]{1,0:T(2,128)S(1)} %slice.3), channel_id=1, source_target_pairs={{0,32},{32,64},{64,96},{96,128},{128,160},{160,192},{192,224},{224... | collective-permute-start | bytes 3080 | tf_op jit(solution)/shard_map/ppermute | solution.py:300
  138.9 0.0 copy-done.1
  138.9 0.1 copy.21
  138.9 0.1 reshape.32.init_ref
  139.0 7.3 %collective-permute-done.prior_ref = f32[2,128]{1,0:T(2,128)S(1)} collective-permute-done((f32[2,128]{1,0:T(2,128)S(1)}, f32[2,128]{1,0:T(2,128)S(1)}, u32[]{:S(2)}, u32[]{:S(2)}) %collective-permute-start) | collective-permute-done | bytes 1056 | tf_op jit(solution)/shard_map/ppermute | solution.py:300
  146.3 10.2 %all-to-all-done.1.agg_ref = bf16[16,128,128]{2,1,0:T(8,128)(2,1)S(1)} async-done(((bf16[16,128,128]{2,1,0:T(8,128)(2,1)}), bf16[16,128,128]{2,1,0:T(8,128)(2,1)S(1)}, u32[]{:S(2)}, u32[]{:S(2)}) %all-to-all-start.1) | async-done | bytes 524320 | tf_op jit(solution)/shard_map/all_to_all | solution.py:305
  156.5 5.7 %finish_mix.1 = bf16[1024,2048]{1,0:T(8,128)(2,1)} custom-call(s32[1]{0:T(128)} %bitcast.pos_ref, bf16[16,128,128]{2,1,0:T(8,128)(2,1)S(1)} %all-to-all-done.1.agg_ref, f32[64,128]{1,0:T(8,128)S(1)} %reshape.32.init_ref, f32[1024,128]{1,0:T(8,128)S(1)} %get-tuple-element.11.o_ref, bf16[1024,128]{1,0:T(8,128)(2,1)S(1)} %get-tuple-element.12.y_ref, ...), custom_call_target="tpu_custom_call" | custom-call | tf_op jit(solution)/shard_map/finish_mix/pallas_call | solution.py:259
  162.2 0.0 reduce-scatter.2.cloned.1.call-update
  162.2 42.9 %reduce-scatter.2.cloned.1.call-done = bf16[128,2048]{1,0:T(8,128)(2,1)} async-done(((bf16[1024,2048]{1,0:T(8,128)(2,1)}), bf16[128,2048]{1,0:T(8,128)(2,1)}) %reduce-scatter.2.cloned.1.call-update) | async-done | bytes 524304 | tf_op jit(solution)/shard_map/reduce_scatter | solution.py:368
  (4 shorter events, 0.0 us)
Async XLA Ops:
  6.5 102.8 %all-gather.2.cloned.1.call-start = ((), (), s32[]{:S(2)}) async-start(), calls=%async_computation.3 | async-start | bytes 5570560 | tf_op jit(solution)/shard_map/all_gather | solution.py:350
  33.5 4.8 %copy-start.2 = (f32[3,128]{1,0:T(4,128)S(1)}, f32[3,128]{1,0:T(4,128)}, u32[]{:S(2)}) copy-start(f32[3,128]{1,0:T(4,128)} %param.23) | copy-start | bytes 4612
  33.5 4.8 %copy-start.3 = (f32[128]{0:T(128)S(1)}, f32[128]{0:T(128)}, u32[]{:S(2)}) copy-start(f32[128]{0:T(128)} %param.29) | copy-start | bytes 1540
  33.5 4.8 %copy-start.4 = (f32[128]{0:T(128)S(1)}, f32[128]{0:T(128)}, u32[]{:S(2)}) copy-start(f32[128]{0:T(128)} %param.30) | copy-start | bytes 1540
  33.5 4.8 %copy-start.5 = (f32[128]{0:T(128)S(1)}, f32[128]{0:T(128)}, u32[]{:S(2)}) copy-start(f32[128]{0:T(128)} %param.33) | copy-start | bytes 1540
  33.5 75.8 %copy-start = (f32[1,1024,128]{2,1,0:T(8,128)S(1)}, f32[1,1024,128]{2,1,0:T(8,128)}, u32[]{:S(2)}) copy-start(f32[1,1024,128]{2,1,0:T(8,128)} %param.31) | copy-start | bytes 1572868
  33.6 54.4 %all-to-all-start = ((bf16[8,128,2048]{2,1,0:T(8,128)(2,1)}), bf16[8,128,2048]{2,1,0:T(8,128)(2,1)}, u32[]{:S(2)}, u32[]{:S(2)}) async-start(bf16[8,128,2048]{2,1,0:T(8,128)(2,1)} %broadcast_in_dim.36), calls=%async_computation | async-start | bytes 8388608 | tf_op jit(solution)/shard_map/all_to_all | solution.py:305
  109.3 29.5 %copy-start.1 = (f32[1,2,64,64]{3,2,1,0:T(8,128)S(1)}, f32[1,2,64,64]{3,2,1,0:T(8,128)}, u32[]{:S(2)}) copy-start(f32[1,2,64,64]{3,2,1,0:T(8,128)} %param.32) | copy-start | bytes 98308
  128.0 28.5 %all-to-all-start.1 = ((bf16[16,128,128]{2,1,0:T(8,128)(2,1)}), bf16[16,128,128]{2,1,0:T(8,128)(2,1)S(1)}, u32[]{:S(2)}, u32[]{:S(2)}) async-start(bf16[16,128,128]{2,1,0:T(8,128)(2,1)} %broadcast_in_dim.41), calls=%async_computation.1 | async-start | bytes 1048576 | tf_op jit(solution)/shard_map/all_to_all | solution.py:305
  135.0 70.2 %reduce-scatter.2.cloned.1.call-start = ((), (), s32[]{:S(2)}) async-start(), calls=%async_computation.4 | async-start | bytes 4718592 | tf_op jit(solution)/shard_map/reduce_scatter | solution.py:368
  135.0 11.3 %collective-permute-start = (f32[2,128]{1,0:T(2,128)S(1)}, f32[2,128]{1,0:T(2,128)S(1)}, u32[]{:S(2)}, u32[]{:S(2)}) collective-permute-start(f32[2,128]{1,0:T(2,128)S(1)} %slice.3), channel_id=1, source_target_pairs={{0,32},{32,64},{64,96},{96,128},{128,160},{160,192},{192,224},{224... | collective-permute-start | bytes 3080 | tf_op jit(solution)/shard_map/ppermute | solution.py:300
Sparse Core Ops, SparseCore 0:
  28.5 80.7 all-gather.1
  162.4 42.7 reduce-scatter.1

commit v2 on v1

--- a/solution.py
+++ b/solution.py
@@ -6,6 +6,7 @@
 from jax.experimental import pallas as pl
 from jax.experimental.pallas import tpu as pltpu
 from jax.sharding import PartitionSpec as P
+
 
 HEAD_WIDTH = 64
 CHUNK = 64
@@ -216,7 +217,7 @@
     )(x, w, spike, vec)
 
 
-def finish_kernel(pos_ref, agg_ref, init_ref, o_ref, y_ref, conv_ref, edge_ref, prior_ref, vec_ref, w_ref, out_ref, s_ref):
+def finish_kernel(pos_ref, agg_ref, init_ref, o_ref, y_ref, conv_ref, edge_ref, prior_ref, vec_ref, out_ref, s_ref):
     step = pl.program_id(0)
     width = 2 * HEAD_WIDTH
     first = jnp.where(lanes_of((1, width)) < HEAD_WIDTH, 1.0, 0.0).astype(bf16)
@@ -248,11 +249,11 @@
     conv = conv_ref[...]
     head = jnp.where((step == 0) & (rows_of((16, width)) < 2), jnp.concatenate([fixed, fixed], axis=0), conv[:16].astype(f32))
     conv = jnp.concatenate([head.astype(bf16), conv[16:]], axis=0)
-    both = jnp.concatenate([conv, mixed.astype(bf16)], axis=1)
-    out_ref[...] = dot(both, w_ref[...], 1, 1).astype(bf16)
-
-
-def finish_call(pos, agg, init, o, y, conv, edge, prior, vec, w):
+    out_ref[:, :width] = conv
+    out_ref[:, width:] = mixed.astype(bf16)
+
+
+def finish_call(pos, agg, init, o, y, conv, edge, prior, vec):
     rows, width = o.shape
     whole = lambda a: pl.BlockSpec(a.shape, lambda i, p: (0,) * a.ndim)
     tile = pl.BlockSpec((BLOCK, width), lambda i, p: (i, 0))
@@ -261,28 +262,53 @@
         grid_spec=pltpu.PrefetchScalarGridSpec(
             num_scalar_prefetch=1,
             grid=(rows // BLOCK,),
-            in_specs=[
-                whole(agg), whole(init), tile, tile, tile, whole(edge), whole(prior), whole(vec),
-                pl.BlockSpec((w.shape[0], 2 * width), lambda i, p: (0, 4)),
-            ],
-            out_specs=pl.BlockSpec((BLOCK, w.shape[0]), lambda i, p: (i, 0)),
+            in_specs=[whole(agg), whole(init), tile, tile, tile, whole(edge), whole(prior), whole(vec)],
+            out_specs=pl.BlockSpec((BLOCK, 2 * width), lambda i, p: (i, 0)),
             scratch_shapes=[pltpu.VMEM((width, width), bf16)],
         ),
-        out_shape=jax.ShapeDtypeStruct((rows, w.shape[0]), bf16),
+        out_shape=jax.ShapeDtypeStruct((rows, 2 * width), bf16),
         compiler_params=pltpu.CompilerParams(
             dimension_semantics=("arbitrary",), vmem_limit_bytes=50 * 2**20
         ),
         name="finish_mix",
-    )(pos, agg, init, o, y, conv, edge, prior, vec, w)
+    )(pos, agg, init, o, y, conv, edge, prior, vec)
+
+
+def outward_kernel(pick_ref, m_ref, *refs):
+    *weights, out_ref = refs
+    rows = out_ref.shape[0]
+    at = pl.multiple_of(pick_ref[0], rows)
+    total = None
+    for k, w_ref in enumerate(weights):
+        got = dot(m_ref[pick_ref[1 + k], pl.ds(at, rows), :], w_ref[...], 1, 1)
+        total = got if total is None else total + got
+    out_ref[...] = total.astype(out_ref.dtype)
+
+
+def outward_call(pick, gathered, weights, dtype):
+    _, rows, depth = gathered.shape
+    columns = weights[0].shape[0]
+    step = 512
+    return pl.pallas_call(
+        outward_kernel,
+        grid_spec=pltpu.PrefetchScalarGridSpec(
+            num_scalar_prefetch=1,
+            grid=(columns // step,),
+            in_specs=[pl.BlockSpec(gathered.shape, lambda i, p: (0, 0, 0))]
+            + [pl.BlockSpec((step, depth), lambda i, p: (i, 0)) for _ in weights],
+            out_specs=pl.BlockSpec((rows // 2, step), lambda i, p: (0, i)),
+        ),
+        out_shape=jax.ShapeDtypeStruct((rows // 2, columns), dtype),
+        compiler_params=pltpu.CompilerParams(dimension_semantics=("arbitrary",)),
+        name="outward",
+    )(pick, gathered, *weights)
 
 
 def pack_kernel(*refs):
     *parts, out_ref = refs
     for k, ref in enumerate(parts):
-        piece = ref[...]
-        if piece.shape[0] > piece.shape[1]:
-            piece = piece.astype(f32).T.astype(bf16)
-        out_ref[:, k * 128 : (k + 1) * 128] = piece
+        width = ref.shape[1]
+        out_ref[:, k * width : (k + 1) * width] = ref[...]
 
 
 def packed(*shards):
@@ -300,6 +326,11 @@
     return lax.ppermute(block, axis, route)
 
 
+def turned(x, distance):
+    devices = lax.axis_size("tp")
+    return lax.ppermute(x, "tp", [(i, (i + distance) % devices) for i in range(devices)])
+
+
 def from_everyone(x, axis):
     devices = lax.axis_size(axis)
     return lax.all_to_all(jnp.broadcast_to(x[None], (devices, *x.shape)), axis, 0, 0, tiled=True)
@@ -311,7 +342,7 @@
     return (values * inv_scale * gain_vector).astype(bf16)
 
 
-def on_device(
+def mixing(
     tokens,
     input_norm_gain,
     earlier_gate,
@@ -343,12 +374,16 @@
         value_matrix,
         decay_matrix,
         rate_matrix,
-        convolution_output,
-        state_heads_output,
-    )
+    )
+    outer = from_everyone(from_everyone(packed(convolution_output.T, state_heads_output.T), "sp"), "fs")
+    outer = jnp.swapaxes(outer, 0, 1).reshape(-1, 2 * channels)
     weights = lax.all_gather(both, "fs", axis=0, tiled=True)
     weights = lax.all_gather(weights, "sp", axis=0, tiled=True)
     piece = from_everyone(normed, "tp").reshape(-1, normed.shape[1])
+    piece, outer = lax.optimization_barrier((piece, outer))
+    half = outer.shape[0] // 2
+    before, after = turned(outer, 2), turned(outer, -2)
+    across = jnp.concatenate([turned(before[:half], 2), turned(after[half:], -2)], axis=0)
     vec = jnp.concatenate(
         [
             decay_floor[None],
@@ -364,9 +399,22 @@
     prior = passed_along(edge[22:24], "sp", 1)
     init = jnp.moveaxis(initial_state[0], 0, 1).reshape(HEAD_WIDTH, heads * HEAD_WIDTH)
     pos = lax.axis_index("sp").astype(jnp.int32)[None]
-    partial = finish_call(pos, pieces, init, o, y, conv, edge, prior, vec, weights)
-    mixed = lax.psum_scatter(partial, "tp", scatter_dimension=0, tiled=True)
-    return mixed[None]
+    mixed = finish_call(pos, pieces, init, o, y, conv, edge, prior, vec)
+    devices = lax.axis_size("tp")
+    chips = devices // 2
+    groups = [list(range(core, devices, 2)) for core in range(2)]
+    gathered = lax.all_to_all(
+        mixed.reshape(chips, -1, 2 * channels), "tp", 0, 0, tiled=True, axis_index_groups=groups
+    )
+    me = lax.axis_index("tp").astype(jnp.int32)
+    chip, core = lax.shift_right_logical(me, 1), me & 1
+    near = [(chip + k) & (chips - 1) for k in (0, chips - 1, 1, 2)]
+    own = gathered.shape[1] // 2
+    weights = (outer, before, after, across)
+    given = outward_call(jnp.stack([(1 - core) * own, *near]), gathered, weights, bf16)
+    taken = lax.ppermute(given, "tp", [(i, i ^ 1) for i in range(devices)])
+    kept = outward_call(jnp.stack([core * own, *near]), gathered, weights, f32)
+    return (kept + taken.astype(f32)).astype(bf16)[None]
 
 
 def solution(mesh):
@@ -391,7 +439,7 @@
         P("tp", ("sp", "fs")),
     )
     return jax.shard_map(
-        on_device,
+        mixing,
         mesh=mesh,
         in_specs=placed,
         out_specs=P("fs", ("sp", "tp"), None),

time: 213 us -> 236 us (1.11)
  the two profiles are of different devices: /device:TPU:8 before, /device:TPU:1 now
where the time goes in v2:
time: 236 us; the launch traced here: 235 us
  waiting for transfers between devices  84.7 us (36%)
  starting transfers between devices  50.9 us (22%)
  blocking collectives  40.1 us (17%)
  Pallas kernels  34.8 us (15%)
  between operations  13.7 us (6%)
  local copies, waits for them, and re-layouts  8.77 us (4%)
  other arithmetic  2.51 us (1%)
    all_to_all x3, waiting for transfers between devices, from_everyone(): lax.all_to_all(jnp.broadcast_to(x[None], (devices, *x.shape)), axis, 0, 0...  58 us
    all_to_all x1, blocking collectives, from_everyone(): lax.all_to_all(jnp.broadcast_to(x[None], (devices, *x.shape)), axis, 0, 0...  27.4 us
    all_to_all x3, starting transfers between devices, from_everyone(): lax.all_to_all(jnp.broadcast_to(x[None], (devices, *x.shape)), axis, 0, 0...  24.7 us
    ppermute x4, waiting for transfers between devices, turned(): lax.ppermute(x, 'tp', [(i, (i + distance) % devices) for i in range(devic...  20.1 us
    pallas_call x1, Pallas kernels, local_call(): pl.pallas_call(local_kernel, grid=(rows // BLOCK,), in_specs=[pl.BlockSpe...  17.8 us
    ppermute x4, starting transfers between devices, turned(): lax.ppermute(x, 'tp', [(i, (i + distance) % devices) for i in range(devic...  13 us
    all_gather x1, blocking collectives, mixing(): weights = lax.all_gather(both, 'fs', axis=0, tiled=True)  12.7 us
    pallas_call x2, Pallas kernels, outward_call(): pl.pallas_call(outward_kernel, grid_spec=pltpu.PrefetchScalarGridSpec(num...  11.7 us
  transfers between devices with their start and end apart: 11, of which 5 were waited for; matrix products, arithmetic and copies ran while one was open for 3% of the time, Pallas kernels for 4%

profile of v2, /device:TPU:1, one launch (start us, length us, event | category | flops | bytes accessed | tf_op | source)
XLA Modules:
  0.0 235.5 jit_solution(12536428769203791799)
XLA Ops:
  6.5 0.0 copy-start.6
  6.5 0.0 copy-start.8
  6.5 0.0 all-gather.2.cloned.1.call-start
  6.5 1.5 pack_shards.3
  8.0 12.7 %all_gather.6 = bf16[128,1024]{1,0:T(8,128)(2,1)} all-gather(bf16[32,1024]{1,0:T(8,128)(2,1)} %pack_shards.3), channel_id=1, replica_groups=mesh['sp'=16,'fs'=4,'tp'=8] {'fs'}, dimensions={0}, use_global_device_ids=true | all-gather | bytes 327680 | tf_op jit(solution)/shard_map/all_gather | solution.py:380
  20.7 0.0 all-gather.2.cloned.1.call-update
  20.7 1.3 pack_shards.2
  22.0 0.7 broadcast_in_dim.49
  22.8 27.4 %all_to_all.25 = bf16[16,32,256]{2,1,0:T(8,128)(2,1)S(1)} all-to-all(bf16[16,32,256]{2,1,0:T(8,128)(2,1)S(1)} %broadcast_in_dim.49), channel_id=1, replica_groups=mesh['sp'=16,'fs'=4,'tp'=8] {'sp'}, dimensions={0} | all-to-all | bytes 524288 | tf_op jit(solution)/shard_map/all_to_all | solution.py:336
  50.2 1.1 broadcast_in_dim.50
  51.4 3.5 %all-to-all-start.2 = ((bf16[4,16,32,256]{3,2,1,0:T(8,128)(2,1)}), bf16[4,16,32,256]{3,2,1,0:T(8,128)(2,1)S(1)}, u32[]{:S(2)}, u32[]{:S(2)}) async-start(bf16[4,16,32,256]{3,2,1,0:T(8,128)(2,1)} %broadcast_in_dim.50), calls=%async_computation.2 | async-start | bytes 2097152 | tf_op jit(solution)/shard_map/all_to_all | solution.py:336
  54.9 0.0 copy-done.6
  54.9 0.2 fusion
  55.1 0.0 copy-done.8
  55.1 0.2 fusion.4
  55.3 9.4 %all-to-all-done.2 = bf16[4,16,32,256]{3,2,1,0:T(8,128)(2,1)S(1)} async-done(((bf16[4,16,32,256]{3,2,1,0:T(8,128)(2,1)}), bf16[4,16,32,256]{3,2,1,0:T(8,128)(2,1)S(1)}, u32[]{:S(2)}, u32[]{:S(2)}) %all-to-all-start.2) | async-done | bytes 1048608 | tf_op jit(solution)/shard_map/all_to_all | solution.py:336
  64.7 2.5 %broadcast_in_dim.48 = bf16[8,128,2048]{2,1,0:T(8,128)(2,1)} broadcast(bf16[128,2048]{1,0:T(8,128)(2,1)S(1)} %fusion.4), dimensions={1,2} | broadcast | bytes 4718592 | tf_op jit(solution)/shard_map/broadcast_in_dim | solution.py:336
  67.2 0.0 copy-start.9
  67.2 0.0 copy-start.10
  67.2 0.0 copy-start
  67.2 15.7 %all-to-all-start = ((bf16[8,128,2048]{2,1,0:T(8,128)(2,1)}), bf16[8,128,2048]{2,1,0:T(8,128)(2,1)}, u32[]{:S(2)}, u32[]{:S(2)}) async-start(bf16[8,128,2048]{2,1,0:T(8,128)(2,1)} %broadcast_in_dim.48), calls=%async_computation | async-start | bytes 8388608 | tf_op jit(solution)/shard_map/all_to_all | solution.py:336
  82.9 0.0 copy-done.9
  82.9 0.0 copy-done.10
  82.9 0.0 copy-done.11
  82.9 0.0 copy-done.12
  83.0 0.1 copy.20
  83.1 0.0 copy-start.1
  83.1 48.7 %all-to-all-done = bf16[8,128,2048]{2,1,0:T(8,128)(2,1)} async-done(((bf16[8,128,2048]{2,1,0:T(8,128)(2,1)}), bf16[8,128,2048]{2,1,0:T(8,128)(2,1)}, u32[]{:S(2)}, u32[]{:S(2)}) %all-to-all-start) | async-done | bytes 4194336 | tf_op jit(solution)/shard_map/all_to_all | solution.py:336
  131.7 0.0 copy-done
  131.7 17.8 %local_mix.1 = (bf16[1024,128]{1,0:T(8,128)(2,1)S(1)}, f32[1024,128]{1,0:T(8,128)S(1)}, bf16[1024,128]{1,0:T(8,128)(2,1)S(1)}, bf16[128,128]{1,0:T(8,128)(2,1)S(1)}, f32[24,128]{1,0:T(8,128)S(1)}) custom-call(bf16[1024,2048]{1,0:T(8,128)(2,1)} %bitcast.7.x_ref, bf16[2048,1024]{1,0:T(8,128)(2,1)} %all-gather.2.cloned.1.call-done.w_ref, ...), custom_call_target="tpu_custom_call" | custom-call | tf_op jit(solution)/shard_map/local_mix/pallas_call | solution.py:195
  149.5 0.9 broadcast_in_dim.55
  150.4 5.4 %all-to-all-start.3 = ((bf16[16,128,128]{2,1,0:T(8,128)(2,1)}), bf16[16,128,128]{2,1,0:T(8,128)(2,1)S(1)}, u32[]{:S(2)}, u32[]{:S(2)}) async-start(bf16[16,128,128]{2,1,0:T(8,128)(2,1)} %broadcast_in_dim.55), calls=%async_computation.3 | async-start | bytes 1048576 | tf_op jit(solution)/shard_map/all_to_all | solution.py:336
  155.8 2.2 collective-permute-start.1
  158.1 0.0 copy-done.1
  158.1 4.3 %collective-permute-start.2 = (bf16[2048,256]{1,0:T(8,128)(2,1)S(1)}, bf16[2048,256]{1,0:T(8,128)(2,1)S(1)}, u32[]{:S(2)}, u32[]{:S(2)}) collective-permute-start(bf16[2048,256]{1,0:T(8,128)(2,1)S(1)} %bitcast.26), channel_id=1, source_target_pairs={{0,6},{1,7},{2,0},{3,1},{4,2},{5,3},{6,4},{7,5},{8,14},{9,15},{10,... | collective-permute-start | bytes 3145736 | tf_op jit(solution)/shard_map/ppermute | solution.py:331
  162.4 20.1 %collective-permute-done.1.refs_1_ = bf16[2048,256]{1,0:T(8,128)(2,1)S(1)} collective-permute-done((bf16[2048,256]{1,0:T(8,128)(2,1)S(1)}, bf16[2048,256]{1,0:T(8,128)(2,1)S(1)}, u32[]{:S(2)}, u32[]{:S(2)}) %collective-permute-start.1) | collective-permute-done | bytes 1048608 | tf_op jit(solution)/shard_map/ppermute | solution.py:331
  182.4 0.9 slice.12
  183.3 1.9 collective-permute-start.3
  185.2 0.0 collective-permute-done.2.refs_2_
  185.2 0.0 copy-start.3
  185.3 4.6 %collective-permute-start.4 = (bf16[1024,256]{1,0:T(8,128)(2,1)S(1)}, bf16[1024,256]{1,0:T(8,128)(2,1)S(1)}, u32[]{:S(2)}, u32[]{:S(2)}) collective-permute-start(bf16[1024,256]{1,0:T(8,128)(2,1)S(1)} %slice.13), channel_id=1, source_target_pairs={{0,6},{1,7},{2,0},{3,1},{4,2},{5,3},{6,4},{7,5},{8,14},{9,15},{10,... | collective-permute-start | bytes 1572872 | tf_op jit(solution)/shard_map/ppermute | solution.py:331
  189.9 0.0 copy-done.2
  189.9 0.0 copy-done.3
  189.9 3.0 %collective-permute-start = (f32[2,128]{1,0:T(2,128)S(1)}, f32[2,128]{1,0:T(2,128)S(1)}, u32[]{:S(2)}, u32[]{:S(2)}) collective-permute-start(f32[2,128]{1,0:T(2,128)S(1)} %slice.9), channel_id=1, source_target_pairs={{0,32},{32,64},{64,96},{96,128},{128,160},{160,192},{192,224},{224... | collective-permute-start | bytes 3080 | tf_op jit(solution)/shard_map/ppermute | solution.py:326
  192.9 0.0 copy-done.7
  192.9 0.1 copy.21
  193.0 0.1 reshape.41.init_ref
  193.1 0.5 collective-permute-done.prior_ref
  193.6 0.0 all-to-all-done.3.agg_ref
  193.6 2.5 %finish_mix.1 = bf16[1024,256]{1,0:T(8,128)(2,1)} custom-call(s32[1]{0:T(128)} %bitcast.5.pos_ref, bf16[16,128,128]{2,1,0:T(8,128)(2,1)S(1)} %all-to-all-done.3.agg_ref, f32[64,128]{1,0:T(8,128)S(1)} %reshape.41.init_ref, f32[1024,128]{1,0:T(8,128)S(1)} %get-tuple-element.14.o_ref, bf16[1024,128]{1,0:T(8,128)(2,1)S(1)} %get-tuple-element.15.y_ref, ...), custom_call_target="tpu_custom_call" | custom-call | tf_op jit(solution)/shard_map/finish_mix/pallas_call | solution.py:260
  196.1 3.5 %all-to-all-start.4 = ((bf16[4,256,256]{2,1,0:T(8,128)(2,1)}), bf16[4,256,256]{2,1,0:T(8,128)(2,1)S(1)}, u32[]{:S(2)}, u32[]{:S(2)}) async-start(bf16[4,256,256]{2,1,0:T(8,128)(2,1)} %bitcast.18), calls=%async_computation.4 | async-start | bytes 1048576 | tf_op jit(solution)/shard_map/all_to_all | solution.py:406
  199.6 0.7 stack.35.pick_ref
  200.3 0.0 collective-permute-done.3
  200.3 0.0 collective-permute-done.4
  200.4 0.0 copy-start.4
  200.4 6.1 %all-to-all-done.4.m_ref = bf16[4,256,256]{2,1,0:T(8,128)(2,1)S(1)} async-done(((bf16[4,256,256]{2,1,0:T(8,128)(2,1)}), bf16[4,256,256]{2,1,0:T(8,128)(2,1)S(1)}, u32[]{:S(2)}, u32[]{:S(2)}) %all-to-all-start.4) | async-done | bytes 524320 | tf_op jit(solution)/shard_map/all_to_all | solution.py:406
  206.5 0.0 copy-done.4
  206.5 0.8 copy-done.5
  207.3 5.8 %outward.3 = bf16[128,2048]{1,0:T(8,128)(2,1)} custom-call(s32[5]{0:T(128)} %stack.35.pick_ref, bf16[4,256,256]{2,1,0:T(8,128)(2,1)} %copy-done.5, bf16[2048,256]{1,0:T(8,128)(2,1)} %bitcast.27, bf16[2048,256]{1,0:T(8,128)(2,1)} %copy-done.2, bf16[2048,256]{1,0:T(8,128)(2,1)} %copy-done.3, bf16[2048,256]{1,0:T(8,128)(2,1)} %copy-done.4), custom_call_target="tpu_custom_call" | custom-call | tf_op jit(solution)/shard_map/outward/pallas_call | solution.py:292
  213.1 6.8 %collective-permute-start.5 = (bf16[128,2048]{1,0:T(8,128)(2,1)}, bf16[128,2048]{1,0:T(8,128)(2,1)S(1)}, u32[]{:S(2)}, u32[]{:S(2)}) collective-permute-start(bf16[128,2048]{1,0:T(8,128)(2,1)} %outward.3), channel_id=1, source_target_pairs={{0,1},{1,0},{2,3},{3,2},{4,5},{5,4},{6,7},{7,6},{8,9},{9,8},{10,11... | collective-permute-start | bytes 1572872 | tf_op jit(solution)/shard_map/ppermute | solution.py:415
  220.0 0.7 stack.33.pick_ref
  220.6 5.9 %outward.2 = f32[128,2048]{1,0:T(8,128)} custom-call(s32[5]{0:T(128)} %stack.33.pick_ref, bf16[4,256,256]{2,1,0:T(8,128)(2,1)} %copy-done.5, bf16[2048,256]{1,0:T(8,128)(2,1)} %bitcast.28, bf16[2048,256]{1,0:T(8,128)(2,1)} %copy-done.2, bf16[2048,256]{1,0:T(8,128)(2,1)} %copy-done.3, bf16[2048,256]{1,0:T(8,128)(2,1)} %copy-done.4), custom_call_target="tpu_custom_call" | custom-call | tf_op jit(solution)/shard_map/outward/pallas_call | solution.py:292
  226.5 0.0 collective-permute-done.5
  226.5 2.1 fusion.3
  (13 shorter events, 0.2 us)
Async XLA Ops:
  6.5 48.4 %copy-start.6 = (bf16[1,128,2048]{2,1,0:T(8,128)(2,1)S(1)}, bf16[1,128,2048]{2,1,0:T(8,128)(2,1)}, u32[]{:S(2)}) copy-start(bf16[1,128,2048]{2,1,0:T(8,128)(2,1)} %param.18) | copy-start | bytes 1572868
  6.5 48.6 %copy-start.8 = (f32[2048]{0:T(1024)S(1)}, f32[2048]{0:T(1024)}, u32[]{:S(2)}) copy-start(f32[2048]{0:T(1024)} %param.19) | copy-start | bytes 24580
  6.5 125.2 %all-gather.2.cloned.1.call-start = ((), (), s32[]{:S(2)}) async-start(), calls=%async_computation.5 | async-start | bytes 4456448 | tf_op jit(solution)/shard_map/all_gather | solution.py:381
  51.4 13.3 %all-to-all-start.2 = ((bf16[4,16,32,256]{3,2,1,0:T(8,128)(2,1)}), bf16[4,16,32,256]{3,2,1,0:T(8,128)(2,1)S(1)}, u32[]{:S(2)}, u32[]{:S(2)}) async-start(bf16[4,16,32,256]{3,2,1,0:T(8,128)(2,1)} %broadcast_in_dim.50), calls=%async_computation.2 | async-start | bytes 2097152 | tf_op jit(solution)/shard_map/all_to_all | solution.py:336
  67.2 15.7 %copy-start.9 = (f32[3,128]{1,0:T(4,128)S(1)}, f32[3,128]{1,0:T(4,128)}, u32[]{:S(2)}) copy-start(f32[3,128]{1,0:T(4,128)} %param.23) | copy-start | bytes 4612
  67.2 15.7 %copy-start.10 = (f32[128]{0:T(128)S(1)}, f32[128]{0:T(128)}, u32[]{:S(2)}) copy-start(f32[128]{0:T(128)} %param.29) | copy-start | bytes 1540
  67.2 15.7 %copy-start.11 = (f32[128]{0:T(128)S(1)}, f32[128]{0:T(128)}, u32[]{:S(2)}) copy-start(f32[128]{0:T(128)} %param.30) | copy-start | bytes 1540
  67.2 15.7 %copy-start.12 = (f32[128]{0:T(128)S(1)}, f32[128]{0:T(128)}, u32[]{:S(2)}) copy-start(f32[128]{0:T(128)} %param.33) | copy-start | bytes 1540
  67.2 64.5 %copy-start = (f32[1,1024,128]{2,1,0:T(8,128)S(1)}, f32[1,1024,128]{2,1,0:T(8,128)}, u32[]{:S(2)}) copy-start(f32[1,1024,128]{2,1,0:T(8,128)} %param.31) | copy-start | bytes 1572868
  67.2 64.5 %all-to-all-start = ((bf16[8,128,2048]{2,1,0:T(8,128)(2,1)}), bf16[8,128,2048]{2,1,0:T(8,128)(2,1)}, u32[]{:S(2)}, u32[]{:S(2)}) async-start(bf16[8,128,2048]{2,1,0:T(8,128)(2,1)} %broadcast_in_dim.48), calls=%async_computation | async-start | bytes 8388608 | tf_op jit(solution)/shard_map/all_to_all | solution.py:336
  83.1 75.0 %copy-start.1 = (bf16[16,4,32,256]{3,2,1,0:T(8,128)(2,1)}, bf16[16,4,32,256]{3,2,1,0:T(8,128)(2,1)S(1)}, u32[]{:S(2)}) copy-start(bf16[16,4,32,256]{3,2,1,0:T(8,128)(2,1)S(1)} %copy.20) | copy-start | bytes 3145732
  131.7 61.2 %copy-start.7 = (f32[1,2,64,64]{3,2,1,0:T(8,128)S(1)}, f32[1,2,64,64]{3,2,1,0:T(8,128)}, u32[]{:S(2)}) copy-start(f32[1,2,64,64]{3,2,1,0:T(8,128)} %param.32) | copy-start | bytes 98308
  150.4 43.2 %all-to-all-start.3 = ((bf16[16,128,128]{2,1,0:T(8,128)(2,1)}), bf16[16,128,128]{2,1,0:T(8,128)(2,1)S(1)}, u32[]{:S(2)}, u32[]{:S(2)}) async-start(bf16[16,128,128]{2,1,0:T(8,128)(2,1)} %broadcast_in_dim.55), calls=%async_computation.3 | async-start | bytes 1048576 | tf_op jit(solution)/shard_map/all_to_all | solution.py:336
  155.8 26.6 %collective-permute-start.1 = (bf16[2048,256]{1,0:T(8,128)(2,1)S(1)}, bf16[2048,256]{1,0:T(8,128)(2,1)S(1)}, u32[]{:S(2)}, u32[]{:S(2)}) collective-permute-start(bf16[2048,256]{1,0:T(8,128)(2,1)S(1)} %bitcast.25), channel_id=1, source_target_pairs={{0,2},{1,3},{2,4},{3,5},{4,6},{5,7},{6,0},{7,1},{8,10},{9,11},{10,... | collective-permute-start | bytes 3145736 | tf_op jit(solution)/shard_map/ppermute | solution.py:331
  158.1 27.2 %collective-permute-start.2 = (bf16[2048,256]{1,0:T(8,128)(2,1)S(1)}, bf16[2048,256]{1,0:T(8,128)(2,1)S(1)}, u32[]{:S(2)}, u32[]{:S(2)}) collective-permute-start(bf16[2048,256]{1,0:T(8,128)(2,1)S(1)} %bitcast.26), channel_id=1, source_target_pairs={{0,6},{1,7},{2,0},{3,1},{4,2},{5,3},{6,4},{7,5},{8,14},{9,15},{10,... | collective-permute-start | bytes 3145736 | tf_op jit(solution)/shard_map/ppermute | solution.py:331
  182.4 7.5 %copy-start.2 = (bf16[2048,256]{1,0:T(8,128)(2,1)}, bf16[2048,256]{1,0:T(8,128)(2,1)S(1)}, u32[]{:S(2)}) copy-start(bf16[2048,256]{1,0:T(8,128)(2,1)S(1)} %collective-permute-done.1.refs_1_) | copy-start | bytes 3145732
  183.3 17.0 %collective-permute-start.3 = (bf16[1024,256]{1,0:T(8,128)(2,1)}, bf16[1024,256]{1,0:T(8,128)(2,1)S(1)}, u32[]{:S(2)}, u32[]{:S(2)}) collective-permute-start(bf16[1024,256]{1,0:T(8,128)(2,1)} %slice.12), channel_id=1, source_target_pairs={{0,2},{1,3},{2,4},{3,5},{4,6},{5,7},{6,0},{7,1},{8,10},{9,11},{10,... | collective-permute-start | bytes 1572872 | tf_op jit(solution)/shard_map/ppermute | solution.py:331
  185.2 4.7 %copy-start.3 = (bf16[2048,256]{1,0:T(8,128)(2,1)}, bf16[2048,256]{1,0:T(8,128)(2,1)S(1)}, u32[]{:S(2)}) copy-start(bf16[2048,256]{1,0:T(8,128)(2,1)S(1)} %collective-permute-done.2.refs_2_) | copy-start | bytes 3145732
  185.3 15.1 %collective-permute-start.4 = (bf16[1024,256]{1,0:T(8,128)(2,1)S(1)}, bf16[1024,256]{1,0:T(8,128)(2,1)S(1)}, u32[]{:S(2)}, u32[]{:S(2)}) collective-permute-start(bf16[1024,256]{1,0:T(8,128)(2,1)S(1)} %slice.13), channel_id=1, source_target_pairs={{0,6},{1,7},{2,0},{3,1},{4,2},{5,3},{6,4},{7,5},{8,14},{9,15},{10,... | collective-permute-start | bytes 1572872 | tf_op jit(solution)/shard_map/ppermute | solution.py:331
  189.9 3.7 %collective-permute-start = (f32[2,128]{1,0:T(2,128)S(1)}, f32[2,128]{1,0:T(2,128)S(1)}, u32[]{:S(2)}, u32[]{:S(2)}) collective-permute-start(f32[2,128]{1,0:T(2,128)S(1)} %slice.9), channel_id=1, source_target_pairs={{0,32},{32,64},{64,96},{96,128},{128,160},{160,192},{192,224},{224... | collective-permute-start | bytes 3080 | tf_op jit(solution)/shard_map/ppermute | solution.py:326
  196.1 10.4 %all-to-all-start.4 = ((bf16[4,256,256]{2,1,0:T(8,128)(2,1)}), bf16[4,256,256]{2,1,0:T(8,128)(2,1)S(1)}, u32[]{:S(2)}, u32[]{:S(2)}) async-start(bf16[4,256,256]{2,1,0:T(8,128)(2,1)} %bitcast.18), calls=%async_computation.4 | async-start | bytes 1048576 | tf_op jit(solution)/shard_map/all_to_all | solution.py:406
  200.4 6.1 %copy-start.4 = (bf16[2048,256]{1,0:T(8,128)(2,1)}, bf16[2048,256]{1,0:T(8,128)(2,1)S(1)}, u32[]{:S(2)}) copy-start(bf16[2048,256]{1,0:T(8,128)(2,1)S(1)} %constant_dynamic-update-slice_fusion.refs_3_) | copy-start | bytes 3145732
  206.5 0.8 copy-start.5
  213.1 13.4 %collective-permute-start.5 = (bf16[128,2048]{1,0:T(8,128)(2,1)}, bf16[128,2048]{1,0:T(8,128)(2,1)S(1)}, u32[]{:S(2)}, u32[]{:S(2)}) collective-permute-start(bf16[128,2048]{1,0:T(8,128)(2,1)} %outward.3), channel_id=1, source_target_pairs={{0,1},{1,0},{2,3},{3,2},{4,5},{5,4},{6,7},{7,6},{8,9},{9,8},{10,11... | collective-permute-start | bytes 1572872 | tf_op jit(solution)/shard_map/ppermute | solution.py:415
Sparse Core Ops, SparseCore 0:
  20.8 80.8 all-gather.1

commit v3 on v2

--- a/solution.py
+++ b/solution.py
@@ -41,7 +41,7 @@
     return jnp.where(low, a, b)
 
 
-def local_kernel(x_ref, w_ref, spike_ref, vec_ref, conv_ref, o_ref, y_ref, agg_ref, edge_ref, st_ref, tail_ref):
+def local_kernel(x_ref, w_ref, spike_ref, vec_ref, o_ref, y_ref, agg_ref, st_ref):
     step = pl.program_id(0)
     width = 2 * HEAD_WIDTH
     pairs = BLOCK // CHUNK
@@ -51,38 +51,17 @@
         r, l = rows_of((width, width)), lanes_of((width, width))
         eye = (r - HEAD_WIDTH == l % HEAD_WIDTH) & (r >= HEAD_WIDTH)
         st_ref[...] = jnp.where(eye, 1.0, 0.0).astype(f32)
-        tail_ref[...] = jnp.zeros_like(tail_ref)
 
     x = x_ref[...]
 
-    def section(k):
-        two = jnp.dot(x, w_ref[:, 2 * k * width : 2 * (k + 1) * width], preferred_element_type=f32)
-        two = two.astype(bf16).astype(f32)
-        return two[:, :width], two[:, width:]
-
-    pre, post = section(0)
-    cvals, q = section(1)
-    keys, vals = section(2)
-    dpre, rpre = section(3)
-
-    prod = pre * cvals
-    tail = tail_ref[...]
-    row = rows_of((BLOCK, width))
-    last, before = tail[7:8], tail[6:7]
-    one = jnp.where(row == 0, last, pltpu.roll(prod, 1, 0))
-    two = jnp.where(row == 0, before, jnp.where(row == 1, last, pltpu.roll(prod, 2, 0)))
-    filtered = vec_ref[2:3] * two + vec_ref[3:4] * one + vec_ref[4:5] * prod
-    conv_ref[...] = (post * filtered).astype(bf16)
-    tail_ref[...] = prod[BLOCK - 8 :]
-
-    @pl.when(step == 0)
-    def _():
-        edge_ref[0:8] = prod[:8]
-        edge_ref[8:16] = post[:8]
-
-    @pl.when(step == pl.num_programs(0) - 1)
-    def _():
-        edge_ref[16:24] = prod[BLOCK - 8 :]
+    def section(first, last):
+        out = jnp.dot(x, w_ref[:, first * width : last * width], preferred_element_type=f32)
+        out = out.astype(bf16).astype(f32)
+        return [out[:, k * width : (k + 1) * width] for k in range(last - first)]
+
+    keys, vals = section(0, 2)
+    dpre, rpre = section(2, 4)
+    (q,) = section(4, 5)
 
     low = lanes_of((BLOCK, width)) < HEAD_WIDTH
     logd = spike_ref[...] - jnp.exp(vec_ref[0:1] + jnp.tanh(dpre))
@@ -195,21 +174,14 @@
     return pl.pallas_call(
         local_kernel,
         grid=(rows // BLOCK,),
-        in_specs=[
-            pl.BlockSpec((BLOCK, depth), lambda i: (i, 0)),
-            pl.BlockSpec((depth, 8 * width), lambda i: (0, 0)),
-            tile,
-            whole(8, width),
-        ],
-        out_specs=[tile, tile, tile, whole(width, width), whole(24, width)],
+        in_specs=[pl.BlockSpec((BLOCK, depth), lambda i: (i, 0)), whole(*w.shape), tile, whole(8, width)],
+        out_specs=[tile, tile, whole(width, width)],
         out_shape=[
-            jax.ShapeDtypeStruct((rows, width), bf16),
             jax.ShapeDtypeStruct((rows, width), f32),
             jax.ShapeDtypeStruct((rows, width), bf16),
             jax.ShapeDtypeStruct((width, width), bf16),
-            jax.ShapeDtypeStruct((24, width), f32),
         ],
-        scratch_shapes=[pltpu.VMEM((width, width), f32), pltpu.VMEM((8, width), f32)],
+        scratch_shapes=[pltpu.VMEM((width, width), f32)],
         compiler_params=pltpu.CompilerParams(
             dimension_semantics=("arbitrary",), vmem_limit_bytes=50 * 2**20
         ),
@@ -217,7 +189,48 @@
     )(x, w, spike, vec)
 
 
-def finish_kernel(pos_ref, agg_ref, init_ref, o_ref, y_ref, conv_ref, edge_ref, prior_ref, vec_ref, out_ref, s_ref):
+def conv_kernel(x_ref, w_ref, halo_ref, vec_ref, out_ref, tail_ref):
+    width = vec_ref.shape[1]
+
+    def project(x):
+        out = jnp.dot(x, w_ref[...], preferred_element_type=f32).astype(bf16).astype(f32)
+        return out[:, :width] * out[:, width : 2 * width], out[:, 2 * width :]
+
+    @pl.when(pl.program_id(0) == 0)
+    def _():
+        tail_ref[...] = project(halo_ref[...])[0]
+
+    prod, post = project(x_ref[...])
+    rows = prod.shape[0]
+    tail = tail_ref[...]
+    row = rows_of((rows, width))
+    last, before = tail[-1:], tail[-2:-1]
+    one = jnp.where(row == 0, last, pltpu.roll(prod, 1, 0))
+    two = jnp.where(row == 0, before, jnp.where(row == 1, last, pltpu.roll(prod, 2, 0)))
+    filtered = vec_ref[2:3] * two + vec_ref[3:4] * one + vec_ref[4:5] * prod
+    out_ref[...] = (post * filtered).astype(bf16)
+    tail_ref[...] = prod[rows - tail_ref.shape[0] :]
+
+
+def conv_call(x, w, halo, vec):
+    rows, depth = x.shape
+    width = vec.shape[1]
+    whole = lambda a: pl.BlockSpec(a.shape, lambda i: (0,) * a.ndim)
+    return pl.pallas_call(
+        conv_kernel,
+        grid=(rows // BLOCK,),
+        in_specs=[pl.BlockSpec((BLOCK, depth), lambda i: (i, 0)), whole(w), whole(halo), whole(vec)],
+        out_specs=pl.BlockSpec((BLOCK, width), lambda i: (i, 0)),
+        out_shape=jax.ShapeDtypeStruct((rows, width), bf16),
+        scratch_shapes=[pltpu.VMEM((halo.shape[0], width), f32)],
+        compiler_params=pltpu.CompilerParams(
+            dimension_semantics=("arbitrary",), vmem_limit_bytes=40 * 2**20
+        ),
+        name="conv_mix",
+    )(x, w, halo, vec)
+
+
+def finish_kernel(pos_ref, agg_ref, init_ref, o_ref, y_ref, conv_ref, vec_ref, out_ref, s_ref):
     step = pl.program_id(0)
     width = 2 * HEAD_WIDTH
     first = jnp.where(lanes_of((1, width)) < HEAD_WIDTH, 1.0, 0.0).astype(bf16)
@@ -239,21 +252,11 @@
     centered = reads - head_sums(reads, low) * (1.0 / HEAD_WIDTH)
     variance = head_sums(centered * centered, low) * (1.0 / HEAD_WIDTH)
     mixed = centered * lax.rsqrt(variance + HEAD_WIDTH * 1e-05) * vec_ref[5:6]
-
-    prod, post = edge_ref[0:8], edge_ref[8:16]
-    last, before = prior_ref[1:2], prior_ref[0:1]
-    row = rows_of((8, width))
-    one = jnp.where(row == 0, last, pltpu.roll(prod, 1, 0))
-    two = jnp.where(row == 0, before, jnp.where(row == 1, last, pltpu.roll(prod, 2, 0)))
-    fixed = post * (vec_ref[2:3] * two + vec_ref[3:4] * one + vec_ref[4:5] * prod)
-    conv = conv_ref[...]
-    head = jnp.where((step == 0) & (rows_of((16, width)) < 2), jnp.concatenate([fixed, fixed], axis=0), conv[:16].astype(f32))
-    conv = jnp.concatenate([head.astype(bf16), conv[16:]], axis=0)
-    out_ref[:, :width] = conv
+    out_ref[:, :width] = conv_ref[...]
     out_ref[:, width:] = mixed.astype(bf16)
 
 
-def finish_call(pos, agg, init, o, y, conv, edge, prior, vec):
+def finish_call(pos, agg, init, o, y, conv, vec):
     rows, width = o.shape
     whole = lambda a: pl.BlockSpec(a.shape, lambda i, p: (0,) * a.ndim)
     tile = pl.BlockSpec((BLOCK, width), lambda i, p: (i, 0))
@@ -262,7 +265,7 @@
         grid_spec=pltpu.PrefetchScalarGridSpec(
             num_scalar_prefetch=1,
             grid=(rows // BLOCK,),
-            in_specs=[whole(agg), whole(init), tile, tile, tile, whole(edge), whole(prior), whole(vec)],
+            in_specs=[whole(agg), whole(init), tile, tile, tile, whole(vec)],
             out_specs=pl.BlockSpec((BLOCK, 2 * width), lambda i, p: (i, 0)),
             scratch_shapes=[pltpu.VMEM((width, width), bf16)],
         ),
@@ -271,7 +274,7 @@
             dimension_semantics=("arbitrary",), vmem_limit_bytes=50 * 2**20
         ),
         name="finish_mix",
-    )(pos, agg, init, o, y, conv, edge, prior, vec)
+    )(pos, agg, init, o, y, conv, vec)
 
 
 def outward_kernel(pick_ref, m_ref, *refs):
@@ -280,14 +283,14 @@
     at = pl.multiple_of(pick_ref[0], rows)
     total = None
     for k, w_ref in enumerate(weights):
-        got = dot(m_ref[pick_ref[1 + k], pl.ds(at, rows), :], w_ref[...], 1, 1)
+        got = dot(m_ref[pick_ref[1 + k], pl.ds(at, rows), :], w_ref[...])
         total = got if total is None else total + got
     out_ref[...] = total.astype(out_ref.dtype)
 
 
 def outward_call(pick, gathered, weights, dtype):
     _, rows, depth = gathered.shape
-    columns = weights[0].shape[0]
+    columns = weights[0].shape[1]
     step = 512
     return pl.pallas_call(
         outward_kernel,
@@ -295,7 +298,7 @@
             num_scalar_prefetch=1,
             grid=(columns // step,),
             in_specs=[pl.BlockSpec(gathered.shape, lambda i, p: (0, 0, 0))]
-            + [pl.BlockSpec((step, depth), lambda i, p: (i, 0)) for _ in weights],
+            + [pl.BlockSpec((depth, step), lambda i, p: (0, i)) for _ in weights],
             out_specs=pl.BlockSpec((rows // 2, step), lambda i, p: (0, i)),
         ),
         out_shape=jax.ShapeDtypeStruct((rows // 2, columns), dtype),
@@ -326,9 +329,9 @@
     return lax.ppermute(block, axis, route)
 
 
-def turned(x, distance):
-    devices = lax.axis_size("tp")
-    return lax.ppermute(x, "tp", [(i, (i + distance) % devices) for i in range(devices)])
+def turned(x, axis, distance):
+    devices = lax.axis_size(axis)
+    return lax.ppermute(x, axis, [(i, (i + distance) % devices) for i in range(devices)])
 
 
 def from_everyone(x, axis):
@@ -362,28 +365,8 @@
     convolution_output,
     state_heads_output,
 ):
-    normed = rms_rows(tokens[0], input_norm_gain)
     channels = earlier_gate.shape[1]
     heads = channels // HEAD_WIDTH
-    both = packed(
-        earlier_gate,
-        later_gate,
-        convolution_input,
-        receptance,
-        key_matrix,
-        value_matrix,
-        decay_matrix,
-        rate_matrix,
-    )
-    outer = from_everyone(from_everyone(packed(convolution_output.T, state_heads_output.T), "sp"), "fs")
-    outer = jnp.swapaxes(outer, 0, 1).reshape(-1, 2 * channels)
-    weights = lax.all_gather(both, "fs", axis=0, tiled=True)
-    weights = lax.all_gather(weights, "sp", axis=0, tiled=True)
-    piece = from_everyone(normed, "tp").reshape(-1, normed.shape[1])
-    piece, outer = lax.optimization_barrier((piece, outer))
-    half = outer.shape[0] // 2
-    before, after = turned(outer, 2), turned(outer, -2)
-    across = jnp.concatenate([turned(before[:half], 2), turned(after[half:], -2)], axis=0)
     vec = jnp.concatenate(
         [
             decay_floor[None],
@@ -394,12 +377,32 @@
         ],
         axis=0,
     )
-    conv, o, y, agg, edge = local_call(piece, weights, decay_spike[0], vec)
-    pieces = from_everyone(agg, "sp")
-    prior = passed_along(edge[22:24], "sp", 1)
     init = jnp.moveaxis(initial_state[0], 0, 1).reshape(HEAD_WIDTH, heads * HEAD_WIDTH)
     pos = lax.axis_index("sp").astype(jnp.int32)[None]
-    mixed = finish_call(pos, pieces, init, o, y, conv, edge, prior, vec)
+
+    def rows_whole(shards):
+        return lax.all_gather(shards, "fs", axis=1, tiled=True).reshape(-1, shards.shape[2])
+
+    early = from_everyone(packed(key_matrix, value_matrix, decay_matrix, rate_matrix, receptance), "sp")
+    normed = rms_rows(tokens[0], input_norm_gain)
+    piece = lax.all_gather(normed, "tp", axis=0, tiled=True)
+    early = rows_whole(early)
+    halo = passed_along(piece[-16:], "sp", 1)
+    outer = packed(convolution_output.T, state_heads_output.T)
+    late = packed(earlier_gate, convolution_input, later_gate)
+    outer = from_everyone(outer, "sp")
+    late = from_everyone(late, "sp")
+    others = [turned(outer, "fs", -k) for k in (1, 2, 3)]
+    outer = jnp.roll(jnp.stack([outer, *others], axis=1), lax.axis_index("fs"), axis=1)
+    outer = outer.reshape(-1, 2 * channels).T
+    before, after = turned(outer, "tp", 2), turned(outer, "tp", -2)
+    far = turned(before[:channels], "tp", 2), turned(after[channels:], "tp", -2)
+    across = jnp.concatenate(far, axis=0)
+    o, y, agg = local_call(piece, early, decay_spike[0], vec)
+    pieces = from_everyone(agg, "sp")
+    late = rows_whole(late)
+    conv = conv_call(piece, late, halo, vec)
+    mixed = finish_call(pos, pieces, init, o, y, conv, vec)
     devices = lax.axis_size("tp")
     chips = devices // 2
     groups = [list(range(core, devices, 2)) for core in range(2)]

time: 236 us -> 262 us (1.11)
  the two profiles are of different devices: /device:TPU:1 before, /device:TPU:129 now
where the time goes in v3:
time: 262 us; the launch traced here: 261 us
  waiting for transfers between devices  71.7 us (27%)
  starting transfers between devices  66.7 us (25%)
  blocking collectives  45.1 us (17%)
  Pallas kernels  35.8 us (14%)
  local copies, waits for them, and re-layouts  24.8 us (9%)
  between operations  13.5 us (5%)
  other arithmetic  3.31 us (1%)
    all_to_all x1, blocking collectives, from_everyone(): lax.all_to_all(jnp.broadcast_to(x[None], (devices, *x.shape)), axis, 0, 0...  45.1 us
    all_to_all x3, starting transfers between devices, from_everyone(): lax.all_to_all(jnp.broadcast_to(x[None], (devices, *x.shape)), axis, 0, 0...  31.6 us
    ppermute x7, waiting for transfers between devices, turned(): lax.ppermute(x, axis, [(i, (i + distance) % devices) for i in range(devic...  30.3 us
    ppermute x7, starting transfers between devices, turned(): lax.ppermute(x, axis, [(i, (i + distance) % devices) for i in range(devic...  22.3 us
    all_gather x1, waiting for transfers between devices, mixing(): piece = lax.all_gather(normed, 'tp', axis=0, tiled=True)  20.9 us
    pallas_call x1, Pallas kernels, local_call(): pl.pallas_call(local_kernel, grid=(rows // BLOCK,), in_specs=[pl.BlockSpe...  14.5 us
    unnamed x42, local copies, waits for them, and re-layouts  12.1 us
    all_to_all x3, waiting for transfers between devices, from_everyone(): lax.all_to_all(jnp.broadcast_to(x[None], (devices, *x.shape)), axis, 0, 0...  12.1 us
  transfers between devices with their start and end apart: 16, of which 7 were waited for; matrix products, arithmetic and copies ran while one was open for 7% of the time, Pallas kernels for 11%

profile of v3, /device:TPU:129, one launch (start us, length us, event | category | flops | bytes accessed | tf_op | source)
XLA Modules:
  0.0 260.9 jit_solution(6970602298582849929)
XLA Ops:
  6.5 1.4 pack_shards.3
  8.0 0.8 broadcast_in_dim.21
  8.8 45.1 %all_to_all.25 = bf16[16,32,640]{2,1,0:T(8,128)(2,1)} all-to-all(bf16[16,32,640]{2,1,0:T(8,128)(2,1)S(1)} %broadcast_in_dim.21), channel_id=1, replica_groups=mesh['sp'=16,'fs'=4,'tp'=8] {'sp'}, dimensions={0} | all-to-all | bytes 1310720 | tf_op jit(solution)/shard_map/all_to_all | solution.py:339
  54.0 0.0 all-gather.6.cloned.1.call-update
  54.0 0.0 all-gather.4.cloned.1.call-start
  54.1 0.2 fusion
  54.3 1.0 fusion.2
  55.3 0.0 all-gather.4.cloned.1.call-update
  55.3 1.3 pack_shards.5
  56.6 1.4 broadcast_in_dim.52
  58.1 8.8 %all-to-all-start.4 = ((bf16[16,32,256]{2,1,0:T(8,128)(2,1)}), bf16[16,32,256]{2,1,0:T(8,128)(2,1)S(1)}, u32[]{:S(2)}, u32[]{:S(2)}) async-start(bf16[16,32,256]{2,1,0:T(8,128)(2,1)} %broadcast_in_dim.52), calls=%async_computation.4 | async-start | bytes 524288 | tf_op jit(solution)/shard_map/all_to_all | solution.py:339
  66.9 1.3 pack_shards.4
  68.2 12.1 %all-to-all-done.4 = bf16[16,32,256]{2,1,0:T(8,128)(2,1)S(1)} async-done(((bf16[16,32,256]{2,1,0:T(8,128)(2,1)}), bf16[16,32,256]{2,1,0:T(8,128)(2,1)S(1)}, u32[]{:S(2)}, u32[]{:S(2)}) %all-to-all-start.4) | async-done | bytes 262176 | tf_op jit(solution)/shard_map/all_to_all | solution.py:339
  80.3 1.5 broadcast_in_dim.51
  81.8 10.9 %all-to-all-start.2 = ((bf16[16,32,384]{2,1,0:T(8,128)(2,1)}), bf16[16,32,384]{2,1,0:T(8,128)(2,1)S(1)}, u32[]{:S(2)}, u32[]{:S(2)}) async-start(bf16[16,32,384]{2,1,0:T(8,128)(2,1)} %broadcast_in_dim.51), calls=%async_computation.2 | async-start | bytes 786432 | tf_op jit(solution)/shard_map/all_to_all | solution.py:339
  92.7 0.0 all-gather.8.cloned.1.call-start
  92.8 4.6 %collective-permute-start.1 = (bf16[16,32,256]{2,1,0:T(8,128)(2,1)S(1)}, bf16[16,32,256]{2,1,0:T(8,128)(2,1)S(1)}, u32[]{:S(2)}, u32[]{:S(2)}) collective-permute-start(bf16[16,32,256]{2,1,0:T(8,128)(2,1)S(1)} %all-to-all-done.4), channel_id=1, source_target_pairs={{0,24},{8,0},{16,8},{24,16},{1,25},{9,1},{17,9},{25,17},{2,26},{10... | collective-permute-start | bytes 786440 | tf_op jit(solution)/shard_map/ppermute | solution.py:334
  97.5 2.1 collective-permute-start.2
  99.7 0.7 bitcast_dynamic-update-slice_fusion.6
  100.4 2.6 collective-permute-start.3
  103.0 0.7 bitcast_dynamic-update-slice_fusion.4
  103.7 3.6 %collective-permute-done.2 = bf16[16,32,256]{2,1,0:T(8,128)(2,1)S(1)} collective-permute-done((bf16[16,32,256]{2,1,0:T(8,128)(2,1)S(1)}, bf16[16,32,256]{2,1,0:T(8,128)(2,1)S(1)}, u32[]{:S(2)}, u32[]{:S(2)}) %collective-permute-start.2) | collective-permute-done | bytes 262176 | tf_op jit(solution)/shard_map/ppermute | solution.py:334
  107.3 0.7 bitcast_dynamic-update-slice_fusion.2
  108.0 6.2 %collective-permute-done.3 = bf16[16,32,256]{2,1,0:T(8,128)(2,1)S(1)} collective-permute-done((bf16[16,32,256]{2,1,0:T(8,128)(2,1)S(1)}, bf16[16,32,256]{2,1,0:T(8,128)(2,1)S(1)}, u32[]{:S(2)}, u32[]{:S(2)}) %collective-permute-start.3) | collective-permute-done | bytes 262176 | tf_op jit(solution)/shard_map/ppermute | solution.py:334
  114.3 0.8 bitcast_dynamic-update-slice_fusion
  115.0 0.8 bitcast_dynamic-update-slice_fusion.7
  115.8 0.7 copy-done.10
  116.6 0.7 bitcast_dynamic-update-slice_fusion.5
  117.3 20.9 %all-gather.4.cloned.1.call-done.x_ref = bf16[1024,2048]{1,0:T(8,128)(2,1)} async-done(((bf16[128,2048]{1,0:T(8,128)(2,1)}), bf16[1024,2048]{1,0:T(8,128)(2,1)}) %all-gather.4.cloned.1.call-update) | async-done | bytes 4194320 | tf_op jit(solution)/shard_map/all_gather | solution.py:388
  138.2 1.7 copy-done.1
  139.9 14.5 %local_mix.1 = (f32[1024,128]{1,0:T(8,128)S(1)}, bf16[1024,128]{1,0:T(8,128)(2,1)S(1)}, bf16[128,128]{1,0:T(8,128)(2,1)S(1)}) custom-call(bf16[1024,2048]{1,0:T(8,128)(2,1)} %all-gather.4.cloned.1.call-done.x_ref, bf16[2048,640]{1,0:T(8,128)(2,1)S(1)} %bitcast.39, f32[1024,128]{1,0:T(8,128)S(1)} %bitcast.41, f32[8,128]{1,0:T(8,128)S(1)} %concatenate.11.vec_ref), custom_call_target="tpu_custom_call" | custom-call | tf_op jit(solution)/shard_map/local_mix/pallas_call | solution.py:174
  154.5 0.9 broadcast_in_dim.50
  155.4 11.8 %all-to-all-start.1 = ((bf16[16,128,128]{2,1,0:T(8,128)(2,1)}), bf16[16,128,128]{2,1,0:T(8,128)(2,1)S(1)}, u32[]{:S(2)}, u32[]{:S(2)}) async-start(bf16[16,128,128]{2,1,0:T(8,128)(2,1)} %broadcast_in_dim.50), calls=%async_computation.1 | async-start | bytes 1048576 | tf_op jit(solution)/shard_map/all_to_all | solution.py:339
  167.2 0.7 bitcast_dynamic-update-slice_fusion.3
  167.9 0.7 bitcast_dynamic-update-slice_fusion.1
  168.7 1.3 constant_dynamic-slice_fusion
  170.0 0.1 copy.28
  170.1 0.6 copy.29
  170.7 2.1 collective-permute-start.4
  172.8 4.4 %collective-permute-start.5 = (bf16[256,2048]{1,0:T(8,128)(2,1)S(1)}, bf16[256,2048]{1,0:T(8,128)(2,1)S(1)}, u32[]{:S(2)}, u32[]{:S(2)}) collective-permute-start(bf16[256,2048]{1,0:T(8,128)(2,1)S(1)} %bitcast.43), channel_id=1, source_target_pairs={{0,6},{1,7},{2,0},{3,1},{4,2},{5,3},{6,4},{7,5},{8,14},{9,15},{10,... | collective-permute-start | bytes 3145736 | tf_op jit(solution)/shard_map/ppermute | solution.py:334
  177.2 20.5 %collective-permute-done.4.refs_1_ = bf16[256,2048]{1,0:T(8,128)(2,1)S(1)} collective-permute-done((bf16[256,2048]{1,0:T(8,128)(2,1)S(1)}, bf16[256,2048]{1,0:T(8,128)(2,1)S(1)}, u32[]{:S(2)}, u32[]{:S(2)}) %collective-permute-start.4) | collective-permute-done | bytes 1048608 | tf_op jit(solution)/shard_map/ppermute | solution.py:334
  197.7 0.9 slice.13
  198.7 1.9 collective-permute-start.6
  200.6 0.9 slice.14
  201.5 4.6 %collective-permute-start.7 = (bf16[128,2048]{1,0:T(8,128)(2,1)}, bf16[128,2048]{1,0:T(8,128)(2,1)}, u32[]{:S(2)}, u32[]{:S(2)}) collective-permute-start(bf16[128,2048]{1,0:T(8,128)(2,1)} %slice.14), channel_id=1, source_target_pairs={{0,6},{1,7},{2,0},{3,1},{4,2},{5,3},{6,4},{7,5},{8,14},{9,15},{10,... | collective-permute-start | bytes 1572872 | tf_op jit(solution)/shard_map/ppermute | solution.py:334
  206.1 0.8 slice.12
  207.0 3.1 %collective-permute-start = (bf16[16,2048]{1,0:T(8,128)(2,1)S(1)}, bf16[16,2048]{1,0:T(8,128)(2,1)S(1)}, u32[]{:S(2)}, u32[]{:S(2)}) collective-permute-start(bf16[16,2048]{1,0:T(8,128)(2,1)S(1)} %slice.12), channel_id=1, source_target_pairs={{0,32},{32,64},{64,96},{96,128},{128,160},{160,192},{192,224},{224... | collective-permute-start | bytes 196616 | tf_op jit(solution)/shard_map/ppermute | solution.py:329
  210.1 0.1 copy.27
  210.1 0.1 reshape.31.init_ref
  210.2 0.6 stack.52.pick_ref
  210.8 2.6 collective-permute-done.halo_ref
  213.5 2.2 copy-done
  215.6 1.4 copy-done.2
  217.1 3.2 %conv_mix.1.conv_ref = bf16[1024,128]{1,0:T(8,128)(2,1)S(1)} custom-call(bf16[1024,2048]{1,0:T(8,128)(2,1)S(1)} %copy-done, bf16[2048,384]{1,0:T(8,128)(2,1)S(1)} %bitcast.40, bf16[16,2048]{1,0:T(8,128)(2,1)S(1)} %collective-permute-done.halo_ref, f32[8,128]{1,0:T(8,128)S(1)} %concatenate.11.vec_ref), custom_call_target="tpu_custom_call" | custom-call | tf_op jit(solution)/shard_map/conv_mix/pallas_call | solution.py:219
  220.3 3.1 %finish_mix.1 = bf16[1024,256]{1,0:T(8,128)(2,1)} custom-call(s32[1]{0:T(128)} %bitcast.5.pos_ref, bf16[16,128,128]{2,1,0:T(8,128)(2,1)S(1)} %all-to-all-done.1.agg_ref, f32[64,128]{1,0:T(8,128)S(1)} %reshape.31.init_ref, f32[1024,128]{1,0:T(8,128)S(1)} %get-tuple-element.9.o_ref, bf16[1024,128]{1,0:T(8,128)(2,1)S(1)} %get-tuple-element.10.y_ref, ...), custom_call_target="tpu_custom_call" | custom-call | tf_op jit(solution)/shard_map/finish_mix/pallas_call | solution.py:263
  223.4 3.5 %all-to-all-start.3 = ((bf16[4,256,256]{2,1,0:T(8,128)(2,1)}), bf16[4,256,256]{2,1,0:T(8,128)(2,1)S(1)}, u32[]{:S(2)}, u32[]{:S(2)}) async-start(bf16[4,256,256]{2,1,0:T(8,128)(2,1)} %bitcast.16), calls=%async_computation.3 | async-start | bytes 1048576 | tf_op jit(solution)/shard_map/all_to_all | solution.py:409
  227.0 1.1 constant_dynamic-update-slice_fusion.refs_3_
  228.0 5.7 %all-to-all-done.3.m_ref = bf16[4,256,256]{2,1,0:T(8,128)(2,1)S(1)} async-done(((bf16[4,256,256]{2,1,0:T(8,128)(2,1)}), bf16[4,256,256]{2,1,0:T(8,128)(2,1)S(1)}, u32[]{:S(2)}, u32[]{:S(2)}) %all-to-all-start.3) | async-done | bytes 524320 | tf_op jit(solution)/shard_map/all_to_all | solution.py:409
  233.8 0.8 copy-done.8
  234.6 5.4 %outward.3 = bf16[128,2048]{1,0:T(8,128)(2,1)} custom-call(s32[5]{0:T(128)} %stack.52.pick_ref, bf16[4,256,256]{2,1,0:T(8,128)(2,1)} %copy-done.8, bf16[256,2048]{1,0:T(8,128)(2,1)} %bitcast.44, bf16[256,2048]{1,0:T(8,128)(2,1)} %copy-done.5, bf16[256,2048]{1,0:T(8,128)(2,1)} %copy-done.6, bf16[256,2048]{1,0:T(8,128)(2,1)} %copy-done.7), custom_call_target="tpu_custom_call" | custom-call | tf_op jit(solution)/shard_map/outward/pallas_call | solution.py:295
  240.0 6.1 %collective-permute-start.8 = (bf16[128,2048]{1,0:T(8,128)(2,1)}, bf16[128,2048]{1,0:T(8,128)(2,1)S(1)}, u32[]{:S(2)}, u32[]{:S(2)}) collective-permute-start(bf16[128,2048]{1,0:T(8,128)(2,1)} %outward.3), channel_id=1, source_target_pairs={{0,1},{1,0},{2,3},{3,2},{4,5},{5,4},{6,7},{7,6},{8,9},{9,8},{10,11... | collective-permute-start | bytes 1572872 | tf_op jit(solution)/shard_map/ppermute | solution.py:418
  246.1 0.7 stack.46.pick_ref
  246.8 5.5 %outward.2 = f32[128,2048]{1,0:T(8,128)} custom-call(s32[5]{0:T(128)} %stack.46.pick_ref, bf16[4,256,256]{2,1,0:T(8,128)(2,1)} %copy-done.8, bf16[256,2048]{1,0:T(8,128)(2,1)} %bitcast.45, bf16[256,2048]{1,0:T(8,128)(2,1)} %copy-done.5, bf16[256,2048]{1,0:T(8,128)(2,1)} %copy-done.6, bf16[256,2048]{1,0:T(8,128)(2,1)} %copy-done.7), custom_call_target="tpu_custom_call" | custom-call | tf_op jit(solution)/shard_map/outward/pallas_call | solution.py:295
  252.3 2.1 fusion.3
  (44 shorter events, 0.2 us)
Async XLA Ops:
  6.5 47.5 %copy-start.9 = (bf16[1,128,2048]{2,1,0:T(8,128)(2,1)S(1)}, bf16[1,128,2048]{2,1,0:T(8,128)(2,1)}, u32[]{:S(2)}) copy-start(bf16[1,128,2048]{2,1,0:T(8,128)(2,1)} %param.18) | copy-start | bytes 1572868
  6.5 47.8 %copy-start.12 = (f32[2048]{0:T(1024)S(1)}, f32[2048]{0:T(1024)}, u32[]{:S(2)}) copy-start(f32[2048]{0:T(1024)} %param.19) | copy-start | bytes 24580
  6.5 110.8 %all-gather.6.cloned.1.call-start = ((), (), s32[]{:S(2)}) async-start(), calls=%async_computation.6 | async-start | bytes 3276800 | tf_op jit(solution)/shard_map/all_gather | solution.py:384
  54.0 43.5 %copy-start.13 = (f32[3,128]{1,0:T(4,128)S(1)}, f32[3,128]{1,0:T(4,128)}, u32[]{:S(2)}) copy-start(f32[3,128]{1,0:T(4,128)} %param.23) | copy-start | bytes 4612
  54.0 43.5 %copy-start.14 = (f32[128]{0:T(128)S(1)}, f32[128]{0:T(128)}, u32[]{:S(2)}) copy-start(f32[128]{0:T(128)} %param.29) | copy-start | bytes 1540
  54.0 43.5 %copy-start.15 = (f32[128]{0:T(128)S(1)}, f32[128]{0:T(128)}, u32[]{:S(2)}) copy-start(f32[128]{0:T(128)} %param.30) | copy-start | bytes 1540
  54.0 43.5 %copy-start.16 = (f32[128]{0:T(128)S(1)}, f32[128]{0:T(128)}, u32[]{:S(2)}) copy-start(f32[128]{0:T(128)} %param.33) | copy-start | bytes 1540
  54.0 84.2 %all-gather.4.cloned.1.call-start = ((), (), s32[]{:S(2)}) async-start(), calls=%async_computation.5 | async-start | bytes 4718592 | tf_op jit(solution)/shard_map/all_gather | solution.py:388
  58.1 22.2 %all-to-all-start.4 = ((bf16[16,32,256]{2,1,0:T(8,128)(2,1)}), bf16[16,32,256]{2,1,0:T(8,128)(2,1)S(1)}, u32[]{:S(2)}, u32[]{:S(2)}) async-start(bf16[16,32,256]{2,1,0:T(8,128)(2,1)} %broadcast_in_dim.52), calls=%async_computation.4 | async-start | bytes 524288 | tf_op jit(solution)/shard_map/all_to_all | solution.py:339
  81.8 56.4 %copy-start.3 = (f32[1,1024,128]{2,1,0:T(8,128)S(1)}, f32[1,1024,128]{2,1,0:T(8,128)}, u32[]{:S(2)}) copy-start(f32[1,1024,128]{2,1,0:T(8,128)} %param.31) | copy-start | bytes 1572868
  81.8 34.0 %all-to-all-start.2 = ((bf16[16,32,384]{2,1,0:T(8,128)(2,1)}), bf16[16,32,384]{2,1,0:T(8,128)(2,1)S(1)}, u32[]{:S(2)}, u32[]{:S(2)}) async-start(bf16[16,32,384]{2,1,0:T(8,128)(2,1)} %broadcast_in_dim.51), calls=%async_computation.2 | async-start | bytes 786432 | tf_op jit(solution)/shard_map/all_to_all | solution.py:339
  92.7 118.1 %all-gather.8.cloned.1.call-start = ((), (), s32[]{:S(2)}) async-start(), calls=%async_computation.7 | async-start | bytes 1966080 | tf_op jit(solution)/shard_map/all_gather | solution.py:384
  92.8 10.2 %collective-permute-start.1 = (bf16[16,32,256]{2,1,0:T(8,128)(2,1)S(1)}, bf16[16,32,256]{2,1,0:T(8,128)(2,1)S(1)}, u32[]{:S(2)}, u32[]{:S(2)}) collective-permute-start(bf16[16,32,256]{2,1,0:T(8,128)(2,1)S(1)} %all-to-all-done.4), channel_id=1, source_target_pairs={{0,24},{8,0},{16,8},{24,16},{1,25},{9,1},{17,9},{25,17},{2,26},{10... | collective-permute-start | bytes 786440 | tf_op jit(solution)/shard_map/ppermute | solution.py:334
  97.5 9.8 %collective-permute-start.2 = (bf16[16,32,256]{2,1,0:T(8,128)(2,1)S(1)}, bf16[16,32,256]{2,1,0:T(8,128)(2,1)S(1)}, u32[]{:S(2)}, u32[]{:S(2)}) collective-permute-start(bf16[16,32,256]{2,1,0:T(8,128)(2,1)S(1)} %all-to-all-done.4), channel_id=1, source_target_pairs={{0,16},{8,24},{16,0},{24,8},{1,17},{9,25},{17,1},{25,9},{2,18},{10... | collective-permute-start | bytes 786440 | tf_op jit(solution)/shard_map/ppermute | solution.py:334
  100.4 13.9 %collective-permute-start.3 = (bf16[16,32,256]{2,1,0:T(8,128)(2,1)S(1)}, bf16[16,32,256]{2,1,0:T(8,128)(2,1)S(1)}, u32[]{:S(2)}, u32[]{:S(2)}) collective-permute-start(bf16[16,32,256]{2,1,0:T(8,128)(2,1)S(1)} %all-to-all-done.4), channel_id=1, source_target_pairs={{0,8},{8,16},{16,24},{24,0},{1,9},{9,17},{17,25},{25,1},{2,10},{10... | collective-permute-start | bytes 786440 | tf_op jit(solution)/shard_map/ppermute | solution.py:334
  115.8 0.8 copy-start.10
  138.2 1.7 copy-start.1
  155.4 64.9 %all-to-all-start.1 = ((bf16[16,128,128]{2,1,0:T(8,128)(2,1)}), bf16[16,128,128]{2,1,0:T(8,128)(2,1)S(1)}, u32[]{:S(2)}, u32[]{:S(2)}) async-start(bf16[16,128,128]{2,1,0:T(8,128)(2,1)} %broadcast_in_dim.50), calls=%async_computation.1 | async-start | bytes 1048576 | tf_op jit(solution)/shard_map/all_to_all | solution.py:339
  170.1 40.0 %copy-start.11 = (f32[1,2,64,64]{3,2,1,0:T(8,128)S(1)}, f32[1,2,64,64]{3,2,1,0:T(8,128)}, u32[]{:S(2)}) copy-start(f32[1,2,64,64]{3,2,1,0:T(8,128)} %param.32) | copy-start | bytes 98308
  170.7 49.5 %copy-start.4 = (bf16[2048,256]{0,1:T(8,128)(2,1)}, bf16[2048,256]{0,1:T(8,128)(2,1)S(1)}, u32[]{:S(2)}) copy-start(bf16[2048,256]{0,1:T(8,128)(2,1)S(1)} %copy.29) | copy-start | bytes 3145732
  170.7 27.0 %collective-permute-start.4 = (bf16[256,2048]{1,0:T(8,128)(2,1)S(1)}, bf16[256,2048]{1,0:T(8,128)(2,1)S(1)}, u32[]{:S(2)}, u32[]{:S(2)}) collective-permute-start(bf16[256,2048]{1,0:T(8,128)(2,1)S(1)} %bitcast.42), channel_id=1, source_target_pairs={{0,2},{1,3},{2,4},{3,5},{4,6},{5,7},{6,0},{7,1},{8,10},{9,11},{10,... | collective-permute-start | bytes 3145736 | tf_op jit(solution)/shard_map/ppermute | solution.py:334
  172.8 27.7 %collective-permute-start.5 = (bf16[256,2048]{1,0:T(8,128)(2,1)S(1)}, bf16[256,2048]{1,0:T(8,128)(2,1)S(1)}, u32[]{:S(2)}, u32[]{:S(2)}) collective-permute-start(bf16[256,2048]{1,0:T(8,128)(2,1)S(1)} %bitcast.43), channel_id=1, source_target_pairs={{0,6},{1,7},{2,0},{3,1},{4,2},{5,3},{6,4},{7,5},{8,14},{9,15},{10,... | collective-permute-start | bytes 3145736 | tf_op jit(solution)/shard_map/ppermute | solution.py:334
  197.7 8.4 %copy-start.5 = (bf16[256,2048]{1,0:T(8,128)(2,1)}, bf16[256,2048]{1,0:T(8,128)(2,1)S(1)}, u32[]{:S(2)}) copy-start(bf16[256,2048]{1,0:T(8,128)(2,1)S(1)} %collective-permute-done.4.refs_1_) | copy-start | bytes 3145732
  198.7 28.2 %collective-permute-start.6 = (bf16[128,2048]{1,0:T(8,128)(2,1)}, bf16[128,2048]{1,0:T(8,128)(2,1)S(1)}, u32[]{:S(2)}, u32[]{:S(2)}) collective-permute-start(bf16[128,2048]{1,0:T(8,128)(2,1)} %slice.13), channel_id=1, source_target_pairs={{0,2},{1,3},{2,4},{3,5},{4,6},{5,7},{6,0},{7,1},{8,10},{9,11},{10,... | collective-permute-start | bytes 1572872 | tf_op jit(solution)/shard_map/ppermute | solution.py:334
  200.6 6.4 %copy-start.6 = (bf16[256,2048]{1,0:T(8,128)(2,1)}, bf16[256,2048]{1,0:T(8,128)(2,1)S(1)}, u32[]{:S(2)}) copy-start(bf16[256,2048]{1,0:T(8,128)(2,1)S(1)} %collective-permute-done.5.refs_2_) | copy-start | bytes 3145732
  201.5 25.4 %collective-permute-start.7 = (bf16[128,2048]{1,0:T(8,128)(2,1)}, bf16[128,2048]{1,0:T(8,128)(2,1)}, u32[]{:S(2)}, u32[]{:S(2)}) collective-permute-start(bf16[128,2048]{1,0:T(8,128)(2,1)} %slice.14), channel_id=1, source_target_pairs={{0,6},{1,7},{2,0},{3,1},{4,2},{5,3},{6,4},{7,5},{8,14},{9,15},{10,... | collective-permute-start | bytes 1572872 | tf_op jit(solution)/shard_map/ppermute | solution.py:334
  207.0 6.5 %collective-permute-start = (bf16[16,2048]{1,0:T(8,128)(2,1)S(1)}, bf16[16,2048]{1,0:T(8,128)(2,1)S(1)}, u32[]{:S(2)}, u32[]{:S(2)}) collective-permute-start(bf16[16,2048]{1,0:T(8,128)(2,1)S(1)} %slice.12), channel_id=1, source_target_pairs={{0,32},{32,64},{64,96},{96,128},{128,160},{160,192},{192,224},{224... | collective-permute-start | bytes 196616 | tf_op jit(solution)/shard_map/ppermute | solution.py:329
  213.5 2.2 copy-start
  215.6 1.4 copy-start.2
  223.4 10.4 %all-to-all-start.3 = ((bf16[4,256,256]{2,1,0:T(8,128)(2,1)}), bf16[4,256,256]{2,1,0:T(8,128)(2,1)S(1)}, u32[]{:S(2)}, u32[]{:S(2)}) async-start(bf16[4,256,256]{2,1,0:T(8,128)(2,1)} %bitcast.16), calls=%async_computation.3 | async-start | bytes 1048576 | tf_op jit(solution)/shard_map/all_to_all | solution.py:409
  228.0 5.8 %copy-start.7 = (bf16[256,2048]{1,0:T(8,128)(2,1)}, bf16[256,2048]{1,0:T(8,128)(2,1)S(1)}, u32[]{:S(2)}) copy-start(bf16[256,2048]{1,0:T(8,128)(2,1)S(1)} %constant_dynamic-update-slice_fusion.refs_3_) | copy-start | bytes 3145732
  233.8 0.8 copy-start.8
  240.0 12.3 %collective-permute-start.8 = (bf16[128,2048]{1,0:T(8,128)(2,1)}, bf16[128,2048]{1,0:T(8,128)(2,1)S(1)}, u32[]{:S(2)}, u32[]{:S(2)}) collective-permute-start(bf16[128,2048]{1,0:T(8,128)(2,1)} %outward.3), channel_id=1, source_target_pairs={{0,1},{1,0},{2,3},{3,2},{4,5},{5,4},{6,7},{7,6},{8,9},{9,8},{10,11... | collective-permute-start | bytes 1572872 | tf_op jit(solution)/shard_map/ppermute | solution.py:418
Sparse Core Ops, SparseCore 0:
  54.1 41.4 all-gather.5
  97.7 40.4 all-gather.3
  140.3 33.6 all-gather.7

commit v4 on v2

--- a/solution.py
+++ b/solution.py
@@ -41,7 +41,7 @@
     return jnp.where(low, a, b)
 
 
-def local_kernel(x_ref, w_ref, spike_ref, vec_ref, conv_ref, o_ref, y_ref, agg_ref, edge_ref, st_ref, tail_ref):
+def local_kernel(place_ref, same_ref, other_ref, w_ref, spike_ref, vec_ref, conv_ref, o_ref, y_ref, agg_ref, edge_ref, st_ref, tail_ref):
     step = pl.program_id(0)
     width = 2 * HEAD_WIDTH
     pairs = BLOCK // CHUNK
@@ -53,7 +53,9 @@
         st_ref[...] = jnp.where(eye, 1.0, 0.0).astype(f32)
         tail_ref[...] = jnp.zeros_like(tail_ref)
 
-    x = x_ref[...]
+    mine, theirs = same_ref[0], other_ref[0]
+    low_core = place_ref[1] == 0
+    x = jnp.concatenate([jnp.where(low_core, mine, theirs), jnp.where(low_core, theirs, mine)], axis=0)
 
     def section(k):
         two = jnp.dot(x, w_ref[:, 2 * k * width : 2 * (k + 1) * width], preferred_element_type=f32)
@@ -187,21 +189,21 @@
         agg_ref[...] = state.astype(bf16)
 
 
-def local_call(x, w, spike, vec):
-    rows, depth = x.shape
-    width = 2 * HEAD_WIDTH
-    whole = lambda *shape: pl.BlockSpec(shape, lambda i: (0,) * len(shape))
-    tile = pl.BlockSpec((BLOCK, width), lambda i: (i, 0))
+def local_call(place, same, other, w, spike, vec):
+    chips, part, depth = same.shape
+    rows, width = spike.shape
+    whole = lambda *shape: pl.BlockSpec(shape, lambda i, p: (0,) * len(shape))
+    tile = pl.BlockSpec((BLOCK, width), lambda i, p: (i, 0))
+    tokens = pl.BlockSpec((1, part, depth), lambda i, p: ((i - p[0]) & (chips - 1), 0, 0))
     return pl.pallas_call(
         local_kernel,
-        grid=(rows // BLOCK,),
-        in_specs=[
-            pl.BlockSpec((BLOCK, depth), lambda i: (i, 0)),
-            pl.BlockSpec((depth, 8 * width), lambda i: (0, 0)),
-            tile,
-            whole(8, width),
-        ],
-        out_specs=[tile, tile, tile, whole(width, width), whole(24, width)],
+        grid_spec=pltpu.PrefetchScalarGridSpec(
+            num_scalar_prefetch=1,
+            grid=(rows // BLOCK,),
+            in_specs=[tokens, tokens, whole(depth, 8 * width), tile, whole(8, width)],
+            out_specs=[tile, tile, tile, whole(width, width), whole(24, width)],
+            scratch_shapes=[pltpu.VMEM((width, width), f32), pltpu.VMEM((8, width), f32)],
+        ),
         out_shape=[
             jax.ShapeDtypeStruct((rows, width), bf16),
             jax.ShapeDtypeStruct((rows, width), f32),
@@ -209,12 +211,11 @@
             jax.ShapeDtypeStruct((width, width), bf16),
             jax.ShapeDtypeStruct((24, width), f32),
         ],
-        scratch_shapes=[pltpu.VMEM((width, width), f32), pltpu.VMEM((8, width), f32)],
         compiler_params=pltpu.CompilerParams(
             dimension_semantics=("arbitrary",), vmem_limit_bytes=50 * 2**20
         ),
         name="local_mix",
-    )(x, w, spike, vec)
+    )(place, same, other, w, spike, vec)
 
 
 def finish_kernel(pos_ref, agg_ref, init_ref, o_ref, y_ref, conv_ref, edge_ref, prior_ref, vec_ref, out_ref, s_ref):
@@ -275,30 +276,33 @@
 
 
 def outward_kernel(pick_ref, m_ref, *refs):
-    *weights, out_ref = refs
-    rows = out_ref.shape[0]
-    at = pl.multiple_of(pick_ref[0], rows)
+    *weights, keep_ref, give_ref = refs
     total = None
     for k, w_ref in enumerate(weights):
-        got = dot(m_ref[pick_ref[1 + k], pl.ds(at, rows), :], w_ref[...], 1, 1)
+        got = dot(m_ref[pick_ref[1 + k]], w_ref[...])
         total = got if total is None else total + got
-    out_ref[...] = total.astype(out_ref.dtype)
-
-
-def outward_call(pick, gathered, weights, dtype):
+    total = total.astype(bf16)
+    rows = keep_ref.shape[0]
+    first = pick_ref[0] == 0
+    keep_ref[...] = jnp.where(first, total[:rows], total[rows:])
+    give_ref[...] = jnp.where(first, total[rows:], total[:rows])
+
+
+def outward_call(pick, gathered, weights):
     _, rows, depth = gathered.shape
-    columns = weights[0].shape[0]
+    columns = weights[0].shape[1]
     step = 512
+    tile = pl.BlockSpec((rows // 2, step), lambda i, p: (0, i))
     return pl.pallas_call(
         outward_kernel,
         grid_spec=pltpu.PrefetchScalarGridSpec(
             num_scalar_prefetch=1,
             grid=(columns // step,),
             in_specs=[pl.BlockSpec(gathered.shape, lambda i, p: (0, 0, 0))]
-            + [pl.BlockSpec((step, depth), lambda i, p: (i, 0)) for _ in weights],
-            out_specs=pl.BlockSpec((rows // 2, step), lambda i, p: (0, i)),
+            + [pl.BlockSpec((depth, step), lambda i, p: (0, i)) for _ in weights],
+            out_specs=[tile, tile],
         ),
-        out_shape=jax.ShapeDtypeStruct((rows // 2, columns), dtype),
+        out_shape=[jax.ShapeDtypeStruct((rows // 2, columns), bf16)] * 2,
         compiler_params=pltpu.CompilerParams(dimension_semantics=("arbitrary",)),
         name="outward",
     )(pick, gathered, *weights)
@@ -362,9 +366,16 @@
     convolution_output,
     state_heads_output,
 ):
-    normed = rms_rows(tokens[0], input_norm_gain)
     channels = earlier_gate.shape[1]
     heads = channels // HEAD_WIDTH
+    devices = lax.axis_size("tp")
+    chips = devices // 2
+    me = lax.axis_index("tp").astype(jnp.int32)
+    chip, core = lax.shift_right_logical(me, 1), me & 1
+
+    def core_swap(x):
+        return lax.ppermute(x, "tp", [(i, i ^ 1) for i in range(devices)])
+
     both = packed(
         earlier_gate,
         later_gate,
@@ -375,15 +386,22 @@
         decay_matrix,
         rate_matrix,
     )
-    outer = from_everyone(from_everyone(packed(convolution_output.T, state_heads_output.T), "sp"), "fs")
-    outer = jnp.swapaxes(outer, 0, 1).reshape(-1, 2 * channels)
     weights = lax.all_gather(both, "fs", axis=0, tiled=True)
     weights = lax.all_gather(weights, "sp", axis=0, tiled=True)
-    piece = from_everyone(normed, "tp").reshape(-1, normed.shape[1])
-    piece, outer = lax.optimization_barrier((piece, outer))
-    half = outer.shape[0] // 2
+    outer = from_everyone(packed(convolution_output.T, state_heads_output.T), "sp")
+    outer = from_everyone(outer, "fs")
+    outer = jnp.swapaxes(outer, 0, 1).reshape(-1, 2 * channels).T
+
+    normed = rms_rows(tokens[0], input_norm_gain)
+    behind, ahead = turned(normed, 2), turned(normed, -2)
+    cut = normed.shape[0] // 2
+    far = turned(behind[:cut], 2), turned(ahead[cut:], -2)
+    same = jnp.stack([normed, ahead, jnp.concatenate(far, axis=0), behind])
+    other = core_swap(same)
+
     before, after = turned(outer, 2), turned(outer, -2)
-    across = jnp.concatenate([turned(before[:half], 2), turned(after[half:], -2)], axis=0)
+    far = turned(before[:channels], 2), turned(after[channels:], -2)
+    across = jnp.concatenate(far, axis=0)
     vec = jnp.concatenate(
         [
             decay_floor[None],
@@ -394,27 +412,22 @@
         ],
         axis=0,
     )
-    conv, o, y, agg, edge = local_call(piece, weights, decay_spike[0], vec)
+    conv, o, y, agg, edge = local_call(
+        jnp.stack([chip, core]), same, other, weights, decay_spike[0], vec
+    )
     pieces = from_everyone(agg, "sp")
     prior = passed_along(edge[22:24], "sp", 1)
     init = jnp.moveaxis(initial_state[0], 0, 1).reshape(HEAD_WIDTH, heads * HEAD_WIDTH)
     pos = lax.axis_index("sp").astype(jnp.int32)[None]
     mixed = finish_call(pos, pieces, init, o, y, conv, edge, prior, vec)
-    devices = lax.axis_size("tp")
-    chips = devices // 2
-    groups = [list(range(core, devices, 2)) for core in range(2)]
+    groups = [list(range(side, devices, 2)) for side in range(2)]
     gathered = lax.all_to_all(
         mixed.reshape(chips, -1, 2 * channels), "tp", 0, 0, tiled=True, axis_index_groups=groups
     )
-    me = lax.axis_index("tp").astype(jnp.int32)
-    chip, core = lax.shift_right_logical(me, 1), me & 1
     near = [(chip + k) & (chips - 1) for k in (0, chips - 1, 1, 2)]
-    own = gathered.shape[1] // 2
-    weights = (outer, before, after, across)
-    given = outward_call(jnp.stack([(1 - core) * own, *near]), gathered, weights, bf16)
-    taken = lax.ppermute(given, "tp", [(i, i ^ 1) for i in range(devices)])
-    kept = outward_call(jnp.stack([core * own, *near]), gathered, weights, f32)
-    return (kept + taken.astype(f32)).astype(bf16)[None]
+    kept, given = outward_call(jnp.stack([core, *near]), gathered, (outer, before, after, across))
+    taken = core_swap(given)
+    return (kept.astype(f32) + taken.astype(f32)).astype(bf16)[None]
 
 
 def solution(mesh):

time: 236 us -> 217 us (0.919)
  the two profiles are of different devices: /device:TPU:1 before, /device:TPU:137 now
where the time goes in v4:
time: 217 us; the launch traced here: 216 us
  starting transfers between devices  75.2 us (35%)
  blocking collectives  41.8 us (19%)
  waiting for transfers between devices  38.4 us (18%)
  Pallas kernels  29.8 us (14%)
  between operations  13.7 us (6%)
  local copies, waits for them, and re-layouts  10.1 us (5%)
  other arithmetic  7.28 us (3%)
    all_to_all x1, blocking collectives, from_everyone(): lax.all_to_all(jnp.broadcast_to(x[None], (devices, *x.shape)), axis, 0, 0...  31.3 us
    ppermute x8, starting transfers between devices, turned(): lax.ppermute(x, 'tp', [(i, (i + distance) % devices) for i in range(devic...  27.2 us
    ppermute x2, starting transfers between devices, core_swap(): return lax.ppermute(x, 'tp', [(i, i ^ 1) for i in range(devices)])  26.3 us
    ppermute x8, waiting for transfers between devices, turned(): lax.ppermute(x, 'tp', [(i, (i + distance) % devices) for i in range(devic...  22.8 us
    pallas_call x1, Pallas kernels, local_call(): pl.pallas_call(local_kernel, grid_spec=pltpu.PrefetchScalarGridSpec(num_s...  18.2 us
    all_to_all x2, starting transfers between devices, from_everyone(): lax.all_to_all(jnp.broadcast_to(x[None], (devices, *x.shape)), axis, 0, 0...  14.7 us
    all_gather x1, blocking collectives, mixing(): weights = lax.all_gather(both, 'fs', axis=0, tiled=True)  10.5 us
    all_gather x1, waiting for transfers between devices, mixing(): weights = lax.all_gather(weights, 'sp', axis=0, tiled=True)  6.07 us
  transfers between devices with their start and end apart: 15, of which 8 were waited for; matrix products, arithmetic and copies ran while one was open for 6% of the time, Pallas kernels for 10%

profile of v4, /device:TPU:137, one launch (start us, length us, event | category | flops | bytes accessed | tf_op | source)
XLA Modules:
  0.0 216.2 jit_solution(18067236093864180158)
XLA Ops:
  6.5 0.0 all-gather.2.cloned.1.call-start
  6.5 1.5 pack_shards.2
  8.0 10.5 %all_gather.6 = bf16[128,1024]{1,0:T(8,128)(2,1)} all-gather(bf16[32,1024]{1,0:T(8,128)(2,1)} %pack_shards.2), channel_id=1, replica_groups=mesh['sp'=16,'fs'=4,'tp'=8] {'fs'}, dimensions={0}, use_global_device_ids=true | all-gather | bytes 327680 | tf_op jit(solution)/shard_map/all_gather | solution.py:389
  18.6 0.0 all-gather.2.cloned.1.call-update
  18.6 1.2 fusion.2
  19.8 1.2 fusion.4
  21.1 4.4 %collective-permute-start = (bf16[128,2048]{1,0:T(8,128)(2,1)S(1)}, bf16[128,2048]{1,0:T(8,128)(2,1)S(1)}, u32[]{:S(2)}, u32[]{:S(2)}) collective-permute-start(bf16[128,2048]{1,0:T(8,128)(2,1)S(1)} %fusion.4), channel_id=1, source_target_pairs={{0,6},{1,7},{2,0},{3,1},{4,2},{5,3},{6,4},{7,5},{8,14},{9,15},{10,... | collective-permute-start | bytes 1572872 | tf_op jit(solution)/shard_map/ppermute | solution.py:335
  25.5 1.9 collective-permute-start.1
  27.4 5.8 %collective-permute-done = bf16[128,2048]{1,0:T(8,128)(2,1)S(1)} collective-permute-done((bf16[128,2048]{1,0:T(8,128)(2,1)S(1)}, bf16[128,2048]{1,0:T(8,128)(2,1)S(1)}, u32[]{:S(2)}, u32[]{:S(2)}) %collective-permute-start) | collective-permute-done | bytes 524320 | tf_op jit(solution)/shard_map/ppermute | solution.py:335
  33.2 5.3 %collective-permute-start.3 = (bf16[64,2048]{1,0:T(8,128)(2,1)S(1)}, bf16[64,2048]{1,0:T(8,128)(2,1)S(1)}, u32[]{:S(2)}, u32[]{:S(2)}) collective-permute-start(bf16[64,2048]{1,0:T(8,128)(2,1)S(1)} %slice.21), channel_id=1, source_target_pairs={{0,6},{1,7},{2,0},{3,1},{4,2},{5,3},{6,4},{7,5},{8,14},{9,15},{10,... | collective-permute-start | bytes 786440 | tf_op jit(solution)/shard_map/ppermute | solution.py:335
  38.5 0.0 collective-permute-done.1
  38.6 1.9 collective-permute-start.2
  40.5 0.0 copy-done.3
  40.5 0.0 copy-done.9
  40.5 0.2 fusion.6
  40.7 1.1 collective-permute-done.3
  41.8 5.1 %collective-permute-done.2 = bf16[64,2048]{1,0:T(8,128)(2,1)S(1)} collective-permute-done((bf16[64,2048]{1,0:T(8,128)(2,1)S(1)}, bf16[64,2048]{1,0:T(8,128)(2,1)S(1)}, u32[]{:S(2)}, u32[]{:S(2)}) %collective-permute-start.2) | collective-permute-done | bytes 262176 | tf_op jit(solution)/shard_map/ppermute | solution.py:335
  46.9 0.3 pad_maximum_fusion.same_ref
  47.2 7.8 %collective-permute-start.4 = (bf16[4,128,2048]{2,1,0:T(8,128)(2,1)S(1)}, bf16[4,128,2048]{2,1,0:T(8,128)(2,1)}, u32[]{:S(2)}, u32[]{:S(2)}) collective-permute-start(bf16[4,128,2048]{2,1,0:T(8,128)(2,1)S(1)} %pad_maximum_fusion.same_ref), channel_id=1, source_target_pairs={{0,1},{1,0},{2,3},{3,2},{4,5},{5,4},{6,7},{7,6},{8,9},{9,8},{10,11... | collective-permute-start | bytes 6291464 | tf_op jit(solution)/shard_map/ppermute | solution.py:377
  55.0 1.3 pack_shards.3
  56.3 0.0 copy-start
  56.3 0.8 broadcast_in_dim.44
  57.1 31.3 %all_to_all.20 = bf16[16,32,256]{2,1,0:T(8,128)(2,1)S(1)} all-to-all(bf16[16,32,256]{2,1,0:T(8,128)(2,1)S(1)} %broadcast_in_dim.44), channel_id=1, replica_groups=mesh['sp'=16,'fs'=4,'tp'=8] {'sp'}, dimensions={0} | all-to-all | bytes 524288 | tf_op jit(solution)/shard_map/all_to_all | solution.py:340
  88.4 1.2 broadcast_in_dim.45
  89.6 5.6 %all-to-all-start.3 = ((bf16[4,16,32,256]{3,2,1,0:T(8,128)(2,1)}), bf16[4,16,32,256]{3,2,1,0:T(8,128)(2,1)}, u32[]{:S(2)}, u32[]{:S(2)}) async-start(bf16[4,16,32,256]{3,2,1,0:T(8,128)(2,1)} %broadcast_in_dim.45), calls=%async_computation.3 | async-start | bytes 2097152 | tf_op jit(solution)/shard_map/all_to_all | solution.py:340
  95.2 0.0 copy-done.11
  95.2 0.0 copy-done.12
  95.2 0.0 copy-done.13
  95.2 0.1 pad_add_fusion.place_ref
  95.3 0.0 collective-permute-done.4.other_ref
  95.3 6.1 %all-gather.2.cloned.1.call-done.w_ref = bf16[2048,1024]{1,0:T(8,128)(2,1)} async-done(((bf16[128,1024]{1,0:T(8,128)(2,1)}), bf16[2048,1024]{1,0:T(8,128)(2,1)}) %all-gather.2.cloned.1.call-update) | async-done | bytes 4194320 | tf_op jit(solution)/shard_map/all_gather | solution.py:390
  101.4 18.2 %local_mix.1 = (bf16[1024,128]{1,0:T(8,128)(2,1)S(1)}, f32[1024,128]{1,0:T(8,128)S(1)}, bf16[1024,128]{1,0:T(8,128)(2,1)S(1)}, bf16[128,128]{1,0:T(8,128)(2,1)S(1)}, f32[24,128]{1,0:T(8,128)S(1)}) custom-call(s32[2]{0:T(128)S(1)} %pad_add_fusion.place_ref, bf16[4,128,2048]{2,1,0:T(8,128)(2,1)S(1)} %pad_maximum_fusion.same_ref, ...), custom_call_target="tpu_custom_call" | custom-call | tf_op jit(solution)/shard_map/local_mix/pallas_call | solution.py:198
  119.5 0.7 copy-done.1
  120.2 0.0 all-to-all-done.3
  120.2 0.9 broadcast_in_dim.43
  121.1 9.1 %all-to-all-start = ((bf16[16,128,128]{2,1,0:T(8,128)(2,1)}), bf16[16,128,128]{2,1,0:T(8,128)(2,1)S(1)}, u32[]{:S(2)}, u32[]{:S(2)}) async-start(bf16[16,128,128]{2,1,0:T(8,128)(2,1)} %broadcast_in_dim.43), calls=%async_computation | async-start | bytes 1048576 | tf_op jit(solution)/shard_map/all_to_all | solution.py:340
  130.3 2.3 %copy.24 = bf16[4,16,32,256]{3,2,0,1:T(8,128)(2,1)} copy(bf16[4,16,32,256]{3,2,1,0:T(8,128)(2,1)} %all-to-all-done.3) | data formatting | bytes 2097152 | tf_op jit(solution)/shard_map/all_to_all | solution.py:340
  132.6 1.5 copy.25
  134.1 4.6 %collective-permute-start.7 = (bf16[256,2048]{1,0:T(8,128)(2,1)S(1)}, bf16[256,2048]{1,0:T(8,128)(2,1)S(1)}, u32[]{:S(2)}, u32[]{:S(2)}) collective-permute-start(bf16[256,2048]{1,0:T(8,128)(2,1)S(1)} %bitcast.40), channel_id=1, source_target_pairs={{0,6},{1,7},{2,0},{3,1},{4,2},{5,3},{6,4},{7,5},{8,14},{9,15},{10,... | collective-permute-start | bytes 3145736 | tf_op jit(solution)/shard_map/ppermute | solution.py:335
  138.7 1.9 collective-permute-start.6
  140.6 10.8 %collective-permute-done.7.refs_2_ = bf16[256,2048]{1,0:T(8,128)(2,1)S(1)} collective-permute-done((bf16[256,2048]{1,0:T(8,128)(2,1)S(1)}, bf16[256,2048]{1,0:T(8,128)(2,1)S(1)}, u32[]{:S(2)}, u32[]{:S(2)}) %collective-permute-start.7) | collective-permute-done | bytes 1048608 | tf_op jit(solution)/shard_map/ppermute | solution.py:335
  151.5 5.3 %collective-permute-start.9 = (bf16[128,2048]{1,0:T(8,128)(2,1)S(1)}, bf16[128,2048]{1,0:T(8,128)(2,1)}, u32[]{:S(2)}, u32[]{:S(2)}) collective-permute-start(bf16[128,2048]{1,0:T(8,128)(2,1)S(1)} %slice.23), channel_id=1, source_target_pairs={{0,6},{1,7},{2,0},{3,1},{4,2},{5,3},{6,4},{7,5},{8,14},{9,15},{10,... | collective-permute-start | bytes 1572872 | tf_op jit(solution)/shard_map/ppermute | solution.py:335
  156.7 0.0 collective-permute-done.6.refs_1_
  156.8 0.9 slice.22
  157.6 1.9 collective-permute-start.8
  159.6 3.1 %collective-permute-start.5 = (f32[2,128]{1,0:T(2,128)S(1)}, f32[2,128]{1,0:T(2,128)S(1)}, u32[]{:S(2)}, u32[]{:S(2)}) collective-permute-start(f32[2,128]{1,0:T(2,128)S(1)} %slice.17), channel_id=1, source_target_pairs={{0,32},{32,64},{64,96},{96,128},{128,160},{160,192},{192,224},{224... | collective-permute-start | bytes 3080 | tf_op jit(solution)/shard_map/ppermute | solution.py:330
  162.7 0.0 copy-done.8
  162.7 0.1 copy.23
  162.8 0.1 reshape.36.init_ref
  162.9 2.5 %collective-permute-done.5.prior_ref = f32[2,128]{1,0:T(2,128)S(1)} collective-permute-done((f32[2,128]{1,0:T(2,128)S(1)}, f32[2,128]{1,0:T(2,128)S(1)}, u32[]{:S(2)}, u32[]{:S(2)}) %collective-permute-start.5) | collective-permute-done | bytes 1056 | tf_op jit(solution)/shard_map/ppermute | solution.py:330
  165.4 0.0 all-to-all-done.agg_ref
  165.4 0.0 copy-done.2
  165.4 3.1 %finish_mix.1 = bf16[1024,256]{1,0:T(8,128)(2,1)} custom-call(s32[1]{0:T(128)} %bitcast.5.pos_ref, bf16[16,128,128]{2,1,0:T(8,128)(2,1)S(1)} %all-to-all-done.agg_ref, f32[64,128]{1,0:T(8,128)S(1)} %reshape.36.init_ref, f32[1024,128]{1,0:T(8,128)S(1)} %get-tuple-element.13.o_ref, bf16[1024,128]{1,0:T(8,128)(2,1)S(1)} %copy-done.2, ...), custom_call_target="tpu_custom_call" | custom-call | tf_op jit(solution)/shard_map/finish_mix/pallas_call | solution.py:261
  168.5 3.9 %all-to-all-start.1 = ((bf16[4,256,256]{2,1,0:T(8,128)(2,1)}), bf16[4,256,256]{2,1,0:T(8,128)(2,1)S(1)}, u32[]{:S(2)}, u32[]{:S(2)}) async-start(bf16[4,256,256]{2,1,0:T(8,128)(2,1)} %bitcast.17), calls=%async_computation.1 | async-start | bytes 1048576 | tf_op jit(solution)/shard_map/all_to_all | solution.py:424
  172.4 0.7 stack.43.pick_ref
  173.1 0.0 collective-permute-done.9
  173.1 0.0 collective-permute-done.8
  173.1 2.3 %pad_maximum_fusion.1.refs_3_ = bf16[256,2048]{1,0:T(8,128)(2,1)} fusion(bf16[128,2048]{1,0:T(8,128)(2,1)} %collective-permute-done.9, bf16[128,2048]{1,0:T(8,128)(2,1)} %collective-permute-done.8), kind=kLoop, calls=%fused_computation.10 | loop fusion | flops 2097152 | bytes 2097152 | tf_op jit(solution)/shard_map/concatenate | solution.py:404
  175.4 5.3 %all-to-all-done.1.m_ref = bf16[4,256,256]{2,1,0:T(8,128)(2,1)S(1)} async-done(((bf16[4,256,256]{2,1,0:T(8,128)(2,1)}), bf16[4,256,256]{2,1,0:T(8,128)(2,1)S(1)}, u32[]{:S(2)}, u32[]{:S(2)}) %all-to-all-start.1) | async-done | bytes 524320 | tf_op jit(solution)/shard_map/all_to_all | solution.py:424
  180.7 0.8 copy-done.7
  181.5 5.7 %outward.1 = (bf16[128,2048]{1,0:T(8,128)(2,1)}, bf16[128,2048]{1,0:T(8,128)(2,1)}) custom-call(s32[5]{0:T(128)} %stack.43.pick_ref, bf16[4,256,256]{2,1,0:T(8,128)(2,1)} %copy-done.7, bf16[256,2048]{1,0:T(8,128)(2,1)} %bitcast.42, bf16[256,2048]{1,0:T(8,128)(2,1)} %copy-done.6, bf16[256,2048]{1,0:T(8,128)(2,1)} %copy-done.5, ...), custom_call_target="tpu_custom_call" | custom-call | tf_op jit(solution)/shard_map/outward/pallas_call | solution.py:296
  187.2 18.5 %collective-permute-start.10 = (bf16[128,2048]{1,0:T(8,128)(2,1)}, bf16[128,2048]{1,0:T(8,128)(2,1)S(1)}, u32[]{:S(2)}, u32[]{:S(2)}) collective-permute-start(bf16[128,2048]{1,0:T(8,128)(2,1)} %get-tuple-element.18), channel_id=1, source_target_pairs={{0,1},{1,0},{2,3},{3,2},{4,5},{5,4},{6,7},{7,6},{8,9},{9,8},{10,11... | collective-permute-start | bytes 1572872 | tf_op jit(solution)/shard_map/ppermute | solution.py:377
  205.7 1.7 collective-permute-done.10
  207.4 2.0 fusion.7
  (26 shorter events, 0.2 us)
Async XLA Ops:
  6.5 33.9 %copy-start.3 = (bf16[1,128,2048]{2,1,0:T(8,128)(2,1)S(1)}, bf16[1,128,2048]{2,1,0:T(8,128)(2,1)}, u32[]{:S(2)}) copy-start(bf16[1,128,2048]{2,1,0:T(8,128)(2,1)} %param.18) | copy-start | bytes 1572868
  6.5 34.0 %copy-start.9 = (f32[2048]{0:T(1024)S(1)}, f32[2048]{0:T(1024)}, u32[]{:S(2)}) copy-start(f32[2048]{0:T(1024)} %param.19) | copy-start | bytes 24580
  6.5 94.8 %all-gather.2.cloned.1.call-start = ((), (), s32[]{:S(2)}) async-start(), calls=%async_computation.4 | async-start | bytes 4456448 | tf_op jit(solution)/shard_map/all_gather | solution.py:390
  21.1 12.1 %collective-permute-start = (bf16[128,2048]{1,0:T(8,128)(2,1)S(1)}, bf16[128,2048]{1,0:T(8,128)(2,1)S(1)}, u32[]{:S(2)}, u32[]{:S(2)}) collective-permute-start(bf16[128,2048]{1,0:T(8,128)(2,1)S(1)} %fusion.4), channel_id=1, source_target_pairs={{0,6},{1,7},{2,0},{3,1},{4,2},{5,3},{6,4},{7,5},{8,14},{9,15},{10,... | collective-permute-start | bytes 1572872 | tf_op jit(solution)/shard_map/ppermute | solution.py:335
  25.5 13.0 %collective-permute-start.1 = (bf16[128,2048]{1,0:T(8,128)(2,1)S(1)}, bf16[128,2048]{1,0:T(8,128)(2,1)S(1)}, u32[]{:S(2)}, u32[]{:S(2)}) collective-permute-start(bf16[128,2048]{1,0:T(8,128)(2,1)S(1)} %fusion.4), channel_id=1, source_target_pairs={{0,2},{1,3},{2,4},{3,5},{4,6},{5,7},{6,0},{7,1},{8,10},{9,11},{10,... | collective-permute-start | bytes 1572872 | tf_op jit(solution)/shard_map/ppermute | solution.py:335
  33.2 8.6 %collective-permute-start.3 = (bf16[64,2048]{1,0:T(8,128)(2,1)S(1)}, bf16[64,2048]{1,0:T(8,128)(2,1)S(1)}, u32[]{:S(2)}, u32[]{:S(2)}) collective-permute-start(bf16[64,2048]{1,0:T(8,128)(2,1)S(1)} %slice.21), channel_id=1, source_target_pairs={{0,6},{1,7},{2,0},{3,1},{4,2},{5,3},{6,4},{7,5},{8,14},{9,15},{10,... | collective-permute-start | bytes 786440 | tf_op jit(solution)/shard_map/ppermute | solution.py:335
  38.6 8.3 %collective-permute-start.2 = (bf16[64,2048]{1,0:T(8,128)(2,1)S(1)}, bf16[64,2048]{1,0:T(8,128)(2,1)S(1)}, u32[]{:S(2)}, u32[]{:S(2)}) collective-permute-start(bf16[64,2048]{1,0:T(8,128)(2,1)S(1)} %slice.20), channel_id=1, source_target_pairs={{0,2},{1,3},{2,4},{3,5},{4,6},{5,7},{6,0},{7,1},{8,10},{9,11},{10,... | collective-permute-start | bytes 786440 | tf_op jit(solution)/shard_map/ppermute | solution.py:335
  47.2 48.1 %collective-permute-start.4 = (bf16[4,128,2048]{2,1,0:T(8,128)(2,1)S(1)}, bf16[4,128,2048]{2,1,0:T(8,128)(2,1)}, u32[]{:S(2)}, u32[]{:S(2)}) collective-permute-start(bf16[4,128,2048]{2,1,0:T(8,128)(2,1)S(1)} %pad_maximum_fusion.same_ref), channel_id=1, source_target_pairs={{0,1},{1,0},{2,3},{3,2},{4,5},{5,4},{6,7},{7,6},{8,9},{9,8},{10,11... | collective-permute-start | bytes 6291464 | tf_op jit(solution)/shard_map/ppermute | solution.py:377
  56.3 38.9 %copy-start.10 = (f32[3,128]{1,0:T(4,128)S(1)}, f32[3,128]{1,0:T(4,128)}, u32[]{:S(2)}) copy-start(f32[3,128]{1,0:T(4,128)} %param.23) | copy-start | bytes 4612
  56.3 38.9 %copy-start.11 = (f32[128]{0:T(128)S(1)}, f32[128]{0:T(128)}, u32[]{:S(2)}) copy-start(f32[128]{0:T(128)} %param.29) | copy-start | bytes 1540
  56.3 38.9 %copy-start.12 = (f32[128]{0:T(128)S(1)}, f32[128]{0:T(128)}, u32[]{:S(2)}) copy-start(f32[128]{0:T(128)} %param.30) | copy-start | bytes 1540
  56.3 38.9 %copy-start.13 = (f32[128]{0:T(128)S(1)}, f32[128]{0:T(128)}, u32[]{:S(2)}) copy-start(f32[128]{0:T(128)} %param.33) | copy-start | bytes 1540
  56.3 45.1 %copy-start = (f32[1,1024,128]{2,1,0:T(8,128)S(1)}, f32[1,1024,128]{2,1,0:T(8,128)}, u32[]{:S(2)}) copy-start(f32[1,1024,128]{2,1,0:T(8,128)} %param.31) | copy-start | bytes 1572868
  89.6 30.6 %all-to-all-start.3 = ((bf16[4,16,32,256]{3,2,1,0:T(8,128)(2,1)}), bf16[4,16,32,256]{3,2,1,0:T(8,128)(2,1)}, u32[]{:S(2)}, u32[]{:S(2)}) async-start(bf16[4,16,32,256]{3,2,1,0:T(8,128)(2,1)} %broadcast_in_dim.45), calls=%async_computation.3 | async-start | bytes 2097152 | tf_op jit(solution)/shard_map/all_to_all | solution.py:340
  119.5 0.7 copy-start.1
  121.1 44.3 %all-to-all-start = ((bf16[16,128,128]{2,1,0:T(8,128)(2,1)}), bf16[16,128,128]{2,1,0:T(8,128)(2,1)S(1)}, u32[]{:S(2)}, u32[]{:S(2)}) async-start(bf16[16,128,128]{2,1,0:T(8,128)(2,1)} %broadcast_in_dim.43), calls=%async_computation | async-start | bytes 1048576 | tf_op jit(solution)/shard_map/all_to_all | solution.py:340
  132.5 30.1 %copy-start.8 = (f32[1,2,64,64]{3,2,1,0:T(8,128)S(1)}, f32[1,2,64,64]{3,2,1,0:T(8,128)}, u32[]{:S(2)}) copy-start(f32[1,2,64,64]{3,2,1,0:T(8,128)} %param.32) | copy-start | bytes 98308
  132.6 32.9 %copy-start.2 = (bf16[1024,128]{1,0:T(8,128)(2,1)S(1)}, bf16[1024,128]{1,0:T(8,128)(2,1)}, u32[]{:S(2)}) copy-start(bf16[1024,128]{1,0:T(8,128)(2,1)} %copy-done.1) | copy-start | bytes 786436
  134.1 34.4 %copy-start.4 = (bf16[2048,256]{0,1:T(8,128)(2,1)}, bf16[2048,256]{0,1:T(8,128)(2,1)S(1)}, u32[]{:S(2)}) copy-start(bf16[2048,256]{0,1:T(8,128)(2,1)S(1)} %copy.25) | copy-start | bytes 3145732
  134.1 17.3 %collective-permute-start.7 = (bf16[256,2048]{1,0:T(8,128)(2,1)S(1)}, bf16[256,2048]{1,0:T(8,128)(2,1)S(1)}, u32[]{:S(2)}, u32[]{:S(2)}) collective-permute-start(bf16[256,2048]{1,0:T(8,128)(2,1)S(1)} %bitcast.40), channel_id=1, source_target_pairs={{0,6},{1,7},{2,0},{3,1},{4,2},{5,3},{6,4},{7,5},{8,14},{9,15},{10,... | collective-permute-start | bytes 3145736 | tf_op jit(solution)/shard_map/ppermute | solution.py:335
  138.7 18.1 %collective-permute-start.6 = (bf16[256,2048]{1,0:T(8,128)(2,1)S(1)}, bf16[256,2048]{1,0:T(8,128)(2,1)S(1)}, u32[]{:S(2)}, u32[]{:S(2)}) collective-permute-start(bf16[256,2048]{1,0:T(8,128)(2,1)S(1)} %bitcast.41), channel_id=1, source_target_pairs={{0,2},{1,3},{2,4},{3,5},{4,6},{5,7},{6,0},{7,1},{8,10},{9,11},{10,... | collective-permute-start | bytes 3145736 | tf_op jit(solution)/shard_map/ppermute | solution.py:335
  151.4 8.1 %copy-start.5 = (bf16[256,2048]{1,0:T(8,128)(2,1)}, bf16[256,2048]{1,0:T(8,128)(2,1)S(1)}, u32[]{:S(2)}) copy-start(bf16[256,2048]{1,0:T(8,128)(2,1)S(1)} %collective-permute-done.7.refs_2_) | copy-start | bytes 3145732
  151.5 21.6 %collective-permute-start.9 = (bf16[128,2048]{1,0:T(8,128)(2,1)S(1)}, bf16[128,2048]{1,0:T(8,128)(2,1)}, u32[]{:S(2)}, u32[]{:S(2)}) collective-permute-start(bf16[128,2048]{1,0:T(8,128)(2,1)S(1)} %slice.23), channel_id=1, source_target_pairs={{0,6},{1,7},{2,0},{3,1},{4,2},{5,3},{6,4},{7,5},{8,14},{9,15},{10,... | collective-permute-start | bytes 1572872 | tf_op jit(solution)/shard_map/ppermute | solution.py:335
  156.7 2.8 %copy-start.6 = (bf16[256,2048]{1,0:T(8,128)(2,1)}, bf16[256,2048]{1,0:T(8,128)(2,1)S(1)}, u32[]{:S(2)}) copy-start(bf16[256,2048]{1,0:T(8,128)(2,1)S(1)} %collective-permute-done.6.refs_1_) | copy-start | bytes 3145732
  157.6 15.5 %collective-permute-start.8 = (bf16[128,2048]{1,0:T(8,128)(2,1)}, bf16[128,2048]{1,0:T(8,128)(2,1)}, u32[]{:S(2)}, u32[]{:S(2)}) collective-permute-start(bf16[128,2048]{1,0:T(8,128)(2,1)} %slice.22), channel_id=1, source_target_pairs={{0,2},{1,3},{2,4},{3,5},{4,6},{5,7},{6,0},{7,1},{8,10},{9,11},{10,... | collective-permute-start | bytes 1572872 | tf_op jit(solution)/shard_map/ppermute | solution.py:335
  159.6 5.8 %collective-permute-start.5 = (f32[2,128]{1,0:T(2,128)S(1)}, f32[2,128]{1,0:T(2,128)S(1)}, u32[]{:S(2)}, u32[]{:S(2)}) collective-permute-start(f32[2,128]{1,0:T(2,128)S(1)} %slice.17), channel_id=1, source_target_pairs={{0,32},{32,64},{64,96},{96,128},{128,160},{160,192},{192,224},{224... | collective-permute-start | bytes 3080 | tf_op jit(solution)/shard_map/ppermute | solution.py:330
  168.5 12.2 %all-to-all-start.1 = ((bf16[4,256,256]{2,1,0:T(8,128)(2,1)}), bf16[4,256,256]{2,1,0:T(8,128)(2,1)S(1)}, u32[]{:S(2)}, u32[]{:S(2)}) async-start(bf16[4,256,256]{2,1,0:T(8,128)(2,1)} %bitcast.17), calls=%async_computation.1 | async-start | bytes 1048576 | tf_op jit(solution)/shard_map/all_to_all | solution.py:424
  180.7 0.8 copy-start.7
  187.2 20.3 %collective-permute-start.10 = (bf16[128,2048]{1,0:T(8,128)(2,1)}, bf16[128,2048]{1,0:T(8,128)(2,1)S(1)}, u32[]{:S(2)}, u32[]{:S(2)}) collective-permute-start(bf16[128,2048]{1,0:T(8,128)(2,1)} %get-tuple-element.18), channel_id=1, source_target_pairs={{0,1},{1,0},{2,3},{3,2},{4,5},{5,4},{6,7},{7,6},{8,9},{9,8},{10,11... | collective-permute-start | bytes 1572872 | tf_op jit(solution)/shard_map/ppermute | solution.py:377
Sparse Core Ops, SparseCore 0:
  18.7 82.5 all-gather.1

commit v5 on v4

v5 whole, which is shorter than its diff:
```python
import functools

import jax
import jax.numpy as jnp
from jax import lax
from jax.experimental import pallas as pl
from jax.experimental.pallas import tpu as pltpu
from jax.sharding import PartitionSpec as P


HEAD_WIDTH = 64
CHUNK = 64
BLOCK = 256
norm_eps = 1e-06
key_eps = 1e-06
f32, bf16 = jnp.float32, jnp.bfloat16


def dot(a, b, ca=1, cb=0):
    return lax.dot_general(
        a.astype(bf16), b.astype(bf16), (((ca,), (cb,)), ((), ())), preferred_element_type=f32
    )


def lanes_of(shape):
    return lax.broadcasted_iota(jnp.int32, shape, 1)


def rows_of(shape):
    return lax.broadcasted_iota(jnp.int32, shape, 0)


def spread(z, first):
    z = z.astype(bf16)
    return jnp.concatenate([z * first, z * (1 - first)], axis=0)


def head_sums(z, low):
    a = jnp.sum(jnp.where(low, z, 0.0), axis=1, keepdims=True)
    b = jnp.sum(jnp.where(low, 0.0, z), axis=1, keepdims=True)
    return jnp.where(low, a, b)


def own_block(place_ref, same_ref, other_ref):
    mine, theirs = same_ref[0], other_ref[0]
    low_core = place_ref[1] == 0
    return jnp.concatenate([jnp.where(low_core, mine, theirs), jnp.where(low_core, theirs, mine)], axis=0)


def chunk_masks():
    shape = (CHUNK, 2 * HEAD_WIDTH)
    return rows_of(shape), lanes_of(shape) % HEAD_WIDTH, lanes_of(shape) < HEAD_WIDTH


def first_lanes():
    return jnp.where(lanes_of((1, 2 * HEAD_WIDTH)) < HEAD_WIDTH, 1.0, 0.0).astype(bf16)


def cut(a):
    return [a[k * CHUNK : (k + 1) * CHUNK] for k in range(a.shape[0] // CHUNK)]


def maps_kernel(
    place_ref,
    same_ref,
    other_ref,
    w_ref,
    spike_ref,
    vec_ref,
    gk_ref,
    gb_ref,
    wu_ref,
    v_ref,
    pos_ref,
    full_ref,
    states_ref,
    agg_ref,
    st_ref,
):
    step = pl.program_id(0)
    width = 2 * HEAD_WIDTH
    each = range(BLOCK // CHUNK)

    @pl.when(step == 0)
    def _():
        r, l = rows_of((width, width)), lanes_of((width, width))
        eye = (r - HEAD_WIDTH == l % HEAD_WIDTH) & (r >= HEAD_WIDTH)
        st_ref[...] = jnp.where(eye, 1.0, 0.0).astype(f32)

    x = own_block(place_ref, same_ref, other_ref)

    def section(k):
        two = jnp.dot(x, w_ref[:, 2 * k * width : 2 * (k + 1) * width], preferred_element_type=f32)
        two = two.astype(bf16)
        return two[:, :width], two[:, width:]

    dpre, rpre = (a.astype(f32) for a in section(1))
    keys, vals = section(0)
    v_ref[...] = vals
    keys = keys.astype(f32)

    low = lanes_of((BLOCK, width)) < HEAD_WIDTH
    logd = spike_ref[...] - jnp.exp(vec_ref[0:1] + jnp.tanh(dpre))
    rate = jax.nn.sigmoid(vec_ref[1:2] + rpre)
    unit = keys * lax.rsqrt(head_sums(keys * keys, low) + key_eps)
    beta = rate * unit
    r, c = rows_of((BLOCK, BLOCK)), lanes_of((BLOCK, BLOCK))
    tri = jnp.where((r >= c) & (r // CHUNK == c // CHUNK), 1.0, 0.0).astype(bf16)
    hi = logd.astype(bf16)
    rest = logd - hi.astype(f32)
    mid = rest.astype(bf16)
    lo = (rest - mid.astype(f32)).astype(bf16)
    sums = jnp.dot(tri, jnp.concatenate([hi, mid, lo], axis=1), preferred_element_type=f32)
    cum_all = sums[:, :width] + sums[:, width : 2 * width] + sums[:, 2 * width :]
    prev_all = cum_all - logd

    t, s, low_c = chunk_masks()
    strict = t > s
    fold = functools.partial(spread, first=first_lanes())
    same = (rows_of((width, width)) // HEAD_WIDTH) == (lanes_of((width, width)) // HEAD_WIDTH)

    keys, vals, unit, beta, cum, prev = map(cut, (keys, vals, unit, beta, cum_all, prev_all))
    center = [cum[k][CHUNK // 2 : CHUNK // 2 + 1] for k in each]
    close = [cum[k][CHUNK - 1 : CHUNK] for k in each]
    e_neg = [jnp.exp(center[k] - cum[k]) for k in each]
    ask_k = [unit[k] * jnp.exp(prev[k] - center[k]) for k in each]
    give_k = [keys[k] * e_neg[k] for k in each]
    give_b = [beta[k] * e_neg[k] for k in each]
    e_center = [jnp.exp(center[k]) for k in each]
    e_tail = [jnp.exp(close[k] - center[k]) for k in each]
    e_close = [jnp.exp(close[k]) for k in each]
    grams = [dot(ask_k[k], jnp.concatenate([fold(give_k[k]), fold(give_b[k])], axis=0), 1, 1) for k in each]
    key_ask = [jnp.where(strict, g[:, :width], 0.0) for g in grams]
    beta_ask = [jnp.where(strict, g[:, width:], 0.0) for g in grams]
    asked = [dot(key_ask[k], fold(vals[k])) for k in each]

    inv = [jnp.where(t == s, 1.0, jnp.where(t // 2 == s // 2, -beta_ask[k], 0.0)) for k in each]
    size = 2
    while size < CHUNK:
        here = (t // (2 * size) == s // (2 * size)) & (t // size != s // size)
        mixed = [dot(inv[k], fold(jnp.where(here, beta_ask[k], 0.0))) for k in each]
        inv = [inv[k] - dot(mixed[k], fold(inv[k])) for k in each]
        size *= 2

    wu = [
        dot(inv[k], jnp.concatenate([fold(ask_k[k] * e_center[k]), fold(asked[k])], axis=1))
        for k in each
    ]
    outer = [dot(wu[k], give_b[k] * e_tail[k], 0, 0) for k in each]
    outer_v = [dot(vals[k], give_k[k] * e_tail[k], 0, 0) for k in each]
    step_map = [jnp.where(same, -outer[k][:width], 0.0).astype(bf16) for k in each]
    source_full = [outer_v[k] - outer[k][width:] for k in each]
    source = [jnp.where(low_c, f[:HEAD_WIDTH], f[HEAD_WIDTH:]) for f in source_full]

    state = st_ref[...]
    for k in each:
        rounded = state.astype(bf16)
        states_ref[k] = rounded
        state = state * e_close[k] + dot(rounded, step_map[k])
        state = jnp.concatenate([state[:HEAD_WIDTH] + source[k], state[HEAD_WIDTH:]], axis=0)
    st_ref[...] = state

    for k in each:
        at = slice(k * CHUNK, (k + 1) * CHUNK)
        gk_ref[at] = give_k[k].astype(bf16)
        gb_ref[at] = give_b[k].astype(bf16)
        wu_ref[at] = wu[k].astype(bf16)
        pos_ref[at] = jnp.exp(cum[k] - center[k])
        full_ref[at] = jnp.exp(cum[k])

    @pl.when(step == pl.num_programs(0) - 1)
    def _():
        for k in range(agg_ref.shape[0]):
            agg_ref[k] = state.astype(bf16)


def token_specs(same):
    chips, part, depth = same.shape
    tokens = pl.BlockSpec((1, part, depth), lambda i, p: ((i - p[0]) & (chips - 1), 0, 0))
    return [tokens, tokens]


def maps_call(place, same, other, w, spike, vec, copies):
    rows, width = spike.shape
    depth = w.shape[0]
    tile = pl.BlockSpec((BLOCK, width), lambda i, p: (i, 0))
    wide = pl.BlockSpec((BLOCK, 2 * width), lambda i, p: (i, 0))
    pairs = BLOCK // CHUNK
    like = lambda n, t: jax.ShapeDtypeStruct((rows, n), t)
    return pl.pallas_call(
        maps_kernel,
        grid_spec=pltpu.PrefetchScalarGridSpec(
            num_scalar_prefetch=1,
            grid=(rows // BLOCK,),
            in_specs=token_specs(same)
            + [
                pl.BlockSpec((depth, 4 * width), lambda i, p: (0, 0)),
                tile,
                pl.BlockSpec(vec.shape, lambda i, p: (0, 0)),
            ],
            out_specs=[
                tile,
                tile,
                wide,
                tile,
                tile,
                tile,
                pl.BlockSpec((pairs, width, width), lambda i, p: (i, 0, 0)),
                pl.BlockSpec((copies, width, width), lambda i, p: (0, 0, 0)),
            ],
            scratch_shapes=[pltpu.VMEM((width, width), f32)],
        ),
        out_shape=[
            like(width, bf16),
            like(width, bf16),
            like(2 * width, bf16),
            like(width, bf16),
            like(width, f32),
            like(width, f32),
            jax.ShapeDtypeStruct((rows // CHUNK, width, width), bf16),
            jax.ShapeDtypeStruct((copies, width, width), bf16),
        ],
        compiler_params=pltpu.CompilerParams(
            dimension_semantics=("arbitrary",), vmem_limit_bytes=50 * 2**20
        ),
        name="state_maps",
    )(place, same, other, w, spike, vec)


def conv_kernel(place_ref, same_ref, other_ref, w_ref, halo_ref, vec_ref, q_ref, out_ref, tail_ref):
    width = vec_ref.shape[1]

    def project(x, first, last):
        out = jnp.dot(x, w_ref[:, first * width : last * width], preferred_element_type=f32)
        return out.astype(bf16)

    @pl.when(pl.program_id(0) == 0)
    def _():
        two = project(halo_ref[...], 1, 3).astype(f32)
        tail_ref[...] = two[:, :width] * two[:, width:]

    x = own_block(place_ref, same_ref, other_ref)
    two = project(x, 0, 2)
    q_ref[...] = two[:, :width]
    rest = project(x, 2, 4).astype(f32)
    prod, post = two[:, width:].astype(f32) * rest[:, :width], rest[:, width:]
    rows = prod.shape[0]
    tail = tail_ref[...]
    row = rows_of((rows, width))
    last, before = tail[-1:], tail[-2:-1]
    one = jnp.where(row == 0, last, pltpu.roll(prod, 1, 0))
    two = jnp.where(row == 0, before, jnp.where(row == 1, last, pltpu.roll(prod, 2, 0)))
    filtered = vec_ref[2:3] * two + vec_ref[3:4] * one + vec_ref[4:5] * prod
    out_ref[...] = (post * filtered).astype(bf16)
    tail_ref[...] = prod[rows - tail_ref.shape[0] :]


def conv_call(place, same, other, w, halo, vec):
    rows, width = same.shape[0] * same.shape[1] * 2, vec.shape[1]
    depth = w.shape[0]
    tile = pl.BlockSpec((BLOCK, width), lambda i, p: (i, 0))
    whole = lambda a: pl.BlockSpec(a.shape, lambda i, p: (0,) * a.ndim)
    return pl.pallas_call(
        conv_kernel,
        grid_spec=pltpu.PrefetchScalarGridSpec(
            num_scalar_prefetch=1,
            grid=(rows // BLOCK,),
            in_specs=token_specs(same)
            + [pl.BlockSpec((depth, 4 * width), lambda i, p: (0, 1)), whole(halo), whole(vec)],
            out_specs=[tile, tile],
            scratch_shapes=[pltpu.VMEM((halo.shape[0], width), f32)],
        ),
        out_shape=[jax.ShapeDtypeStruct((rows, width), bf16)] * 2,
        compiler_params=pltpu.CompilerParams(
            dimension_semantics=("arbitrary",), vmem_limit_bytes=40 * 2**20
        ),
        name="conv_mix",
    )(place, same, other, w, halo, vec)


def reads_kernel(q_ref, gk_ref, gb_ref, wu_ref, v_ref, pos_ref, full_ref, states_ref, o_ref, y_ref):
    width = 2 * HEAD_WIDTH
    each = range(BLOCK // CHUNK)
    t, s, _ = chunk_masks()
    inclusive = t >= s
    fold = functools.partial(spread, first=first_lanes())
    q_all = q_ref[...].astype(f32)
    ask, full = cut(q_all * pos_ref[...]), cut(q_all * full_ref[...])
    gk, gb, wu, v = map(cut, (gk_ref[...], gb_ref[...], wu_ref[...], v_ref[...]))
    grams = [dot(ask[k], jnp.concatenate([fold(gk[k]), fold(gb[k])], axis=0), 1, 1) for k in each]
    key_read = [jnp.where(inclusive, g[:, :width], 0.0) for g in grams]
    beta_read = [jnp.where(inclusive, g[:, width:], 0.0) for g in grams]
    forward = [dot(key_read[k], fold(v[k])) for k in each]
    back = [
        dot(beta_read[k], jnp.concatenate([fold(wu[k][:, :width]), fold(wu[k][:, width:])], axis=1))
        for k in each
    ]
    for k in each:
        start = states_ref[k]
        got = dot(
            full[k] - back[k][:, :width],
            jnp.concatenate([fold(start[:HEAD_WIDTH]), fold(start[HEAD_WIDTH:])], axis=0),
            1,
            1,
        )
        at = slice(k * CHUNK, (k + 1) * CHUNK)
        o_ref[at] = forward[k] - back[k][:, width:] + got[:, :width]
        y_ref[at] = got[:, width:].astype(bf16)


def reads_call(q, gk, gb, wu, v, pos, full, states):
    rows, width = q.shape
    tile = pl.BlockSpec((BLOCK, width), lambda i: (i, 0))
    wide = pl.BlockSpec((BLOCK, 2 * width), lambda i: (i, 0))
    starts = pl.BlockSpec((BLOCK // CHUNK, width, width), lambda i: (i, 0, 0))
    return pl.pallas_call(
        reads_kernel,
        grid=(rows // BLOCK,),
        in_specs=[tile, tile, tile, wide, tile, tile, tile, starts],
        out_specs=[tile, tile],
        out_shape=[jax.ShapeDtypeStruct((rows, width), f32), jax.ShapeDtypeStruct((rows, width), bf16)],
        compiler_params=pltpu.CompilerParams(
            dimension_semantics=("arbitrary",), vmem_limit_bytes=40 * 2**20
        ),
        name="local_reads",
    )(q, gk, gb, wu, v, pos, full, states)


def moved(state, piece, first):
    hi = state.astype(bf16)
    lo = (state - hi.astype(f32)).astype(bf16)
    got = dot(jnp.concatenate([hi, lo], axis=0), spread(piece[HEAD_WIDTH:], first))
    return got[: state.shape[0]] + got[state.shape[0] :]


def group_kernel(pieces_ref, out_ref):
    first = first_lanes()
    total = pieces_ref[0].astype(f32)
    for k in range(1, pieces_ref.shape[0]):
        piece = pieces_ref[k]
        total = moved(total, piece, first)
        total = jnp.concatenate(
            [total[:HEAD_WIDTH] + piece[:HEAD_WIDTH].astype(f32), total[HEAD_WIDTH:]], axis=0
        )
    for k in range(out_ref.shape[0]):
        out_ref[k] = total.astype(bf16)


def finish_kernel(at_ref, near_ref, far_ref, init_ref, o_ref, y_ref, conv_ref, vec_ref, out_ref, s_ref):
    width = 2 * HEAD_WIDTH
    first = first_lanes()

    @pl.when(pl.program_id(0) == 0)
    def _():
        def through(ref):
            def advance(i, state):
                piece = ref[i]
                return moved(state, piece, first) + piece[:HEAD_WIDTH].astype(f32)

            return advance

        state = lax.fori_loop(0, at_ref[0], through(far_ref), init_ref[...])
        state = lax.fori_loop(0, at_ref[1], through(near_ref), state)
        s_ref[...] = spread(state, first)

    low = lanes_of((BLOCK, width)) < HEAD_WIDTH
    reads = o_ref[...] + dot(y_ref[...], s_ref[...], 1, 1)
    centered = reads - head_sums(reads, low) * (1.0 / HEAD_WIDTH)
    variance = head_sums(centered * centered, low) * (1.0 / HEAD_WIDTH)
    mixed = centered * lax.rsqrt(variance + HEAD_WIDTH * 1e-05) * vec_ref[5:6]
    out_ref[:, :width] = conv_ref[...]
    out_ref[:, width:] = mixed.astype(bf16)


def finish_call(at, near, far, init, o, y, conv, vec):
    rows, width = o.shape
    whole = lambda a: pl.BlockSpec(a.shape, lambda i, p: (0,) * a.ndim)
    tile = pl.BlockSpec((BLOCK, width), lambda i, p: (i, 0))
    return pl.pallas_call(
        finish_kernel,
        grid_spec=pltpu.PrefetchScalarGridSpec(
            num_scalar_prefetch=1,
            grid=(rows // BLOCK,),
            in_specs=[whole(near), whole(far), whole(init), tile, tile, tile, whole(vec)],
            out_specs=pl.BlockSpec((BLOCK, 2 * width), lambda i, p: (i, 0)),
            scratch_shapes=[pltpu.VMEM((width, width), bf16)],
        ),
        out_shape=jax.ShapeDtypeStruct((rows, 2 * width), bf16),
        compiler_params=pltpu.CompilerParams(
            dimension_semantics=("arbitrary",), vmem_limit_bytes=50 * 2**20
        ),
        name="finish_mix",
    )(at, near, far, init, o, y, conv, vec)


def outward_kernel(pick_ref, m_ref, *refs):
    *weights, keep_ref, give_ref = refs
    total = None
    for k, w_ref in enumerate(weights):
        got = dot(m_ref[pick_ref[1 + k]], w_ref[...])
        total = got if total is None else total + got
    total = total.astype(bf16)
    rows = keep_ref.shape[0]
    first = pick_ref[0] == 0
    keep_ref[...] = jnp.where(first, total[:rows], total[rows:])
    give_ref[...] = jnp.where(first, total[rows:], total[:rows])


def outward_call(pick, gathered, weights):
    _, rows, depth = gathered.shape
    columns = weights[0].shape[1]
    step = 512
    tile = pl.BlockSpec((rows // 2, step), lambda i, p: (0, i))
    return pl.pallas_call(
        outward_kernel,
        grid_spec=pltpu.PrefetchScalarGridSpec(
            num_scalar_prefetch=1,
            grid=(columns // step,),
            in_specs=[pl.BlockSpec(gathered.shape, lambda i, p: (0, 0, 0))]
            + [pl.BlockSpec((depth, step), lambda i, p: (0, i)) for _ in weights],
            out_specs=[tile, tile],
        ),
        out_shape=[jax.ShapeDtypeStruct((rows // 2, columns), bf16)] * 2,
        compiler_params=pltpu.CompilerParams(dimension_semantics=("arbitrary",)),
        name="outward",
    )(pick, gathered, *weights)


def pack_kernel(*refs):
    *parts, out_ref = refs
    for k, ref in enumerate(parts):
        width = ref.shape[1]
        for n in range(out_ref.shape[0]):
            out_ref[n, :, k * width : (k + 1) * width] = ref[...]


def packed(copies, *shards):
    rows, width = shards[0].shape
    return pl.pallas_call(
        pack_kernel,
        out_shape=jax.ShapeDtypeStruct((copies, rows, len(shards) * width), bf16),
        name="pack_shards",
    )(*shards)


def passed_along(block, axis, distance):
    devices = range(lax.axis_size(axis))
    route = [(i - distance, i) for i in devices if i - distance in devices]
    return lax.ppermute(block, axis, route)


def turned(x, distance):
    devices = lax.axis_size("tp")
    return lax.ppermute(x, "tp", [(i, (i + distance) % devices) for i in range(devices)])


def from_everyone(copies, axis, groups=None):
    return lax.all_to_all(copies, axis, 0, 0, tiled=True, axis_index_groups=groups)


def rms_rows(activations, gain_vector):
    values = activations.astype(f32)
    inv_scale = lax.rsqrt(jnp.mean(values * values, axis=-1, keepdims=True) + norm_eps)
    return (values * inv_scale * gain_vector).astype(bf16)


def mixing(
    tokens,
    input_norm_gain,
    earlier_gate,
    later_gate,
    convolution_input,
    convolution_taps,
    receptance,
    key_matrix,
    value_matrix,
    decay_matrix,
    rate_matrix,
    decay_floor,
    rate_offset,
    decay_spike,
    initial_state,
    head_norm_gain,
    convolution_output,
    state_heads_output,
):
    channels = earlier_gate.shape[1]
    heads = channels // HEAD_WIDTH
    devices = lax.axis_size("tp")
    chips = devices // 2
    me = lax.axis_index("tp").astype(jnp.int32)
    chip, core = lax.shift_right_logical(me, 1), me & 1

    def core_swap(x):
        return lax.ppermute(x, "tp", [(i, i ^ 1) for i in range(devices)])

    blocks, seqs = lax.axis_size("sp"), lax.axis_size("fs")
    weights = from_everyone(
        packed(
            seqs,
            key_matrix,
            value_matrix,
            decay_matrix,
            rate_matrix,
            receptance,
            earlier_gate,
            convolution_input,
            later_gate,
        ),
        "fs",
    )
    weights = weights.reshape(-1, 8 * channels)
    weights = lax.all_gather(weights, "sp", axis=0, tiled=True)
    outer = from_everyone(packed(blocks, convolution_output.T, state_heads_output.T), "sp")
    outer = from_everyone(jnp.broadcast_to(outer[None], (seqs, *outer.shape)), "fs")
    outer = jnp.swapaxes(outer, 0, 1).reshape(-1, 2 * channels).T

    normed = rms_rows(tokens[0], input_norm_gain)
    behind, ahead = turned(normed, 2), turned(normed, -2)
    cut = normed.shape[0] // 2
    far = turned(behind[:cut], 2), turned(ahead[cut:], -2)
    same = jnp.stack([normed, ahead, jnp.concatenate(far, axis=0), behind])
    other = core_swap(same)

    before, after = turned(outer, 2), turned(outer, -2)
    far = turned(before[:channels], 2), turned(after[channels:], -2)
    across = jnp.concatenate(far, axis=0)
    vec = jnp.concatenate(
        [
            decay_floor[None],
            rate_offset[None],
            convolution_taps,
            head_norm_gain[None],
            jnp.zeros((2, channels), f32),
        ],
        axis=0,
    )
    place = jnp.stack([chip, core])
    last_rows = jnp.where(core == 0, other[:, -16:], same[:, -16:])
    last_rows = lax.dynamic_index_in_dim(last_rows, (chips - 1 - chip) & (chips - 1), 0, keepdims=False)
    halo = passed_along(last_rows, "sp", 1)
    few = 4
    near_blocks = [list(range(k, k + few)) for k in range(0, blocks, few)]
    far_blocks = [list(range(k, blocks, few)) for k in range(few)]
    *kept, agg = maps_call(place, same, other, weights, decay_spike[0], vec, few)
    near_maps = from_everyone(agg, "sp", near_blocks)
    q, conv = conv_call(place, same, other, weights, halo, vec)
    total = pl.pallas_call(
        group_kernel,
        out_shape=jax.ShapeDtypeStruct((blocks // few, *agg.shape[1:]), bf16),
        name="group_map",
    )(near_maps)
    far_maps = from_everyone(total, "sp", far_blocks)
    o, y = reads_call(q, *kept)
    init = jnp.moveaxis(initial_state[0], 0, 1).reshape(HEAD_WIDTH, heads * HEAD_WIDTH)
    block = lax.axis_index("sp").astype(jnp.int32)
    at = jnp.stack([lax.shift_right_logical(block, 2), block & (few - 1)])
    mixed = finish_call(at, near_maps, far_maps, init, o, y, conv, vec)
    groups = [list(range(side, devices, 2)) for side in range(2)]
    gathered = lax.all_to_all(
        mixed.reshape(chips, -1, 2 * channels), "tp", 0, 0, tiled=True, axis_index_groups=groups
    )
    near = [(chip + k) & (chips - 1) for k in (0, chips - 1, 1, 2)]
    kept, given = outward_call(jnp.stack([core, *near]), gathered, (outer, before, after, across))
    taken = core_swap(given)
    return (kept.astype(f32) + taken.astype(f32)).astype(bf16)[None]


def solution(mesh):
    placed = (
        P("fs", ("sp", "tp"), None),
        P(),
        P(("sp", "fs"), "tp"),
        P(("sp", "fs"), "tp"),
        P(("sp", "fs"), "tp"),
        P(None, "tp"),
        P(("sp", "fs"), "tp"),
        P(("sp", "fs"), "tp"),
        P(("sp", "fs"), "tp"),
        P(("sp", "fs"), "tp"),
        P(("sp", "fs"), "tp"),
        P("tp"),
        P("tp"),
        P("fs", "sp", "tp"),
        P("fs", "tp", None, None),
        P("tp"),
        P("tp", ("sp", "fs")),
        P("tp", ("sp", "fs")),
    )
    return jax.shard_map(
        mixing,
        mesh=mesh,
        in_specs=placed,
        out_specs=P("fs", ("sp", "tp"), None),
        check_vma=False,
    )
```

time: 217 us -> 211 us (0.972)
  the two profiles are of different devices: /device:TPU:137 before, /device:TPU:129 now
where the time goes in v5:
time: 211 us; the launch traced here: 210 us
  starting transfers between devices  77.7 us (37%)
  Pallas kernels  36.5 us (17%)
  blocking collectives  33.2 us (16%)
  waiting for transfers between devices  23.1 us (11%)
  local copies, waits for them, and re-layouts  16.9 us (8%)
  between operations  13.8 us (7%)
  other arithmetic  8.45 us (4%)
    all_to_all x3, blocking collectives, from_everyone(): lax.all_to_all(copies, axis, 0, 0, tiled=True, axis_index_groups=groups)  33.2 us
    ppermute x8, starting transfers between devices, turned(): lax.ppermute(x, 'tp', [(i, (i + distance) % devices) for i in range(devic...  28.8 us
    all_to_all x2, starting transfers between devices, from_everyone(): lax.all_to_all(copies, axis, 0, 0, tiled=True, axis_index_groups=groups)  21.6 us
    ppermute x2, starting transfers between devices, core_swap(): return lax.ppermute(x, 'tp', [(i, i ^ 1) for i in range(devices)])  20.9 us
    pallas_call x1, Pallas kernels, maps_call(): pl.pallas_call(maps_kernel, grid_spec=pltpu.PrefetchScalarGridSpec(num_sc...  15.1 us
    all_gather x1, waiting for transfers between devices, mixing(): weights = lax.all_gather(weights, 'sp', axis=0, tiled=True)  10.7 us
    unnamed x48, local copies, waits for them, and re-layouts  6.82 us
    pallas_call x1, Pallas kernels, outward_call(): pl.pallas_call(outward_kernel, grid_spec=pltpu.PrefetchScalarGridSpec(num...  5.72 us
  transfers between devices with their start and end apart: 15, of which 6 were waited for; matrix products, arithmetic and copies ran while one was open for 8% of the time, Pallas kernels for 14%

profile of v5, /device:TPU:129, one launch (start us, length us, event | category | flops | bytes accessed | tf_op | source)
XLA Modules:
  0.0 209.7 jit_solution(18180983038063363389)
XLA Ops:
  6.5 1.6 pack_shards.2
  8.1 10.0 %all_to_all.30 = bf16[4,32,1024]{2,1,0:T(8,128)(2,1)} all-to-all(bf16[4,32,1024]{2,1,0:T(8,128)(2,1)} %pack_shards.2), channel_id=1, replica_groups=mesh['sp'=16,'fs'=4,'tp'=8] {'fs'}, dimensions={0} | all-to-all | bytes 524288 | tf_op jit(solution)/shard_map/all_to_all | solution.py:458
  18.1 0.0 all-gather.2.cloned.1.call-update
  18.1 1.2 fusion.2
  19.4 1.2 fusion.4
  20.6 3.1 %collective-permute-start.1 = (bf16[128,2048]{1,0:T(8,128)(2,1)S(1)}, bf16[128,2048]{1,0:T(8,128)(2,1)S(1)}, u32[]{:S(2)}, u32[]{:S(2)}) collective-permute-start(bf16[128,2048]{1,0:T(8,128)(2,1)S(1)} %fusion.4), channel_id=1, source_target_pairs={{0,2},{1,3},{2,4},{3,5},{4,6},{5,7},{6,0},{7,1},{8,10},{9,11},{10,... | collective-permute-start | bytes 1572872 | tf_op jit(solution)/shard_map/ppermute | solution.py:454
  23.7 3.4 %collective-permute-start = (bf16[128,2048]{1,0:T(8,128)(2,1)S(1)}, bf16[128,2048]{1,0:T(8,128)(2,1)S(1)}, u32[]{:S(2)}, u32[]{:S(2)}) collective-permute-start(bf16[128,2048]{1,0:T(8,128)(2,1)S(1)} %fusion.4), channel_id=1, source_target_pairs={{0,6},{1,7},{2,0},{3,1},{4,2},{5,3},{6,4},{7,5},{8,14},{9,15},{10,... | collective-permute-start | bytes 1572872 | tf_op jit(solution)/shard_map/ppermute | solution.py:454
  27.1 1.5 pack_shards.3
  28.6 13.3 %all-to-all-start.4 = ((bf16[16,32,256]{2,1,0:T(8,128)(2,1)}), bf16[16,32,256]{2,1,0:T(8,128)(2,1)}, u32[]{:S(2)}, u32[]{:S(2)}) async-start(bf16[16,32,256]{2,1,0:T(8,128)(2,1)} %pack_shards.3), calls=%async_computation.4 | async-start | bytes 524288 | tf_op jit(solution)/shard_map/all_to_all | solution.py:458
  41.9 0.0 collective-permute-done.1
  41.9 1.9 collective-permute-start.2
  43.8 0.0 collective-permute-done
  43.8 0.0 copy-start.17
  43.9 4.6 %collective-permute-start.3 = (bf16[64,2048]{1,0:T(8,128)(2,1)S(1)}, bf16[64,2048]{1,0:T(8,128)(2,1)S(1)}, u32[]{:S(2)}, u32[]{:S(2)}) collective-permute-start(bf16[64,2048]{1,0:T(8,128)(2,1)S(1)} %slice.25), channel_id=1, source_target_pairs={{0,6},{1,7},{2,0},{3,1},{4,2},{5,3},{6,4},{7,5},{8,14},{9,15},{10,... | collective-permute-start | bytes 786440 | tf_op jit(solution)/shard_map/ppermute | solution.py:454
  48.5 0.2 fusion.6
  48.7 2.0 collective-permute-done.2
  50.6 1.1 collective-permute-done.3
  51.8 1.3 pad_maximum_fusion.same_ref
  53.1 6.2 %collective-permute-start.4 = (bf16[4,128,2048]{2,1,0:T(8,128)(2,1)S(1)}, bf16[4,128,2048]{2,1,0:T(8,128)(2,1)}, u32[]{:S(2)}, u32[]{:S(2)}) collective-permute-start(bf16[4,128,2048]{2,1,0:T(8,128)(2,1)S(1)} %pad_maximum_fusion.same_ref), channel_id=1, source_target_pairs={{0,1},{1,0},{2,3},{3,2},{4,5},{5,4},{6,7},{7,6},{8,9},{9,8},{10,11... | collective-permute-start | bytes 6291464 | tf_op jit(solution)/shard_map/ppermute | solution.py:495
  59.4 0.0 all-to-all-done.4
  59.4 1.1 broadcast_in_dim.27
  60.5 14.3 %all_to_all.31 = bf16[4,16,32,256]{3,2,1,0:T(8,128)(2,1)S(1)} all-to-all(bf16[4,16,32,256]{3,2,1,0:T(8,128)(2,1)S(1)} %broadcast_in_dim.27), channel_id=1, replica_groups=mesh['sp'=16,'fs'=4,'tp'=8] {'fs'}, dimensions={0} | all-to-all | bytes 2097152 | tf_op jit(solution)/shard_map/all_to_all | solution.py:458
  74.8 0.0 copy-start.4
  74.8 1.1 copy.24
  75.9 2.3 %copy.25 = bf16[2048,256]{0,1:T(8,128)(2,1)} copy(bf16[2048,256]{1,0:T(8,128)(2,1)} %bitcast.47) | data formatting | bytes 2097152 | tf_op jit(solution)/shard_map/reshape | solution.py:516
  78.2 3.3 %collective-permute-start.6 = (bf16[256,2048]{1,0:T(8,128)(2,1)}, bf16[256,2048]{1,0:T(8,128)(2,1)}, u32[]{:S(2)}, u32[]{:S(2)}) collective-permute-start(bf16[256,2048]{1,0:T(8,128)(2,1)} %bitcast.44), channel_id=1, source_target_pairs={{0,2},{1,3},{2,4},{3,5},{4,6},{5,7},{6,0},{7,1},{8,10},{9,11},{10,... | collective-permute-start | bytes 3145736 | tf_op jit(solution)/shard_map/ppermute | solution.py:454
  81.5 6.0 %collective-permute-start.7 = (bf16[256,2048]{1,0:T(8,128)(2,1)}, bf16[256,2048]{1,0:T(8,128)(2,1)}, u32[]{:S(2)}, u32[]{:S(2)}) collective-permute-start(bf16[256,2048]{1,0:T(8,128)(2,1)} %bitcast.45), channel_id=1, source_target_pairs={{0,6},{1,7},{2,0},{3,1},{4,2},{5,3},{6,4},{7,5},{8,14},{9,15},{10,... | collective-permute-start | bytes 3145736 | tf_op jit(solution)/shard_map/ppermute | solution.py:454
  87.6 0.1 pad_add_fusion.1.place_ref
  87.7 10.7 %all-gather.2.cloned.1.call-done.w_ref = bf16[2048,1024]{1,0:T(8,128)(2,1)} async-done(((bf16[128,1024]{1,0:T(8,128)(2,1)}), bf16[2048,1024]{1,0:T(8,128)(2,1)}) %all-gather.2.cloned.1.call-update) | async-done | bytes 4194320 | tf_op jit(solution)/shard_map/all_gather | solution.py:513
  98.4 15.1 %state_maps.1 = (bf16[1024,128]{1,0:T(8,128)(2,1)S(1)}, bf16[1024,128]{1,0:T(8,128)(2,1)S(1)}, bf16[1024,256]{1,0:T(8,128)(2,1)S(1)}, bf16[1024,128]{1,0:T(8,128...) custom-call(s32[2]{0:T(128)S(1)} %pad_add_fusion.1.place_ref, ...), custom_call_target="tpu_custom_call" | custom-call | tf_op jit(solution)/shard_map/state_maps/pallas_call | solution.py:190
  113.6 0.0 copy-start.5
  113.6 0.8 copy-done.5
  114.4 0.8 copy-done.7
  115.2 0.8 copy-done.9
  116.0 0.7 copy-done.11
  116.7 0.7 copy-done.13
  117.4 8.9 %all_to_all.32.pieces_ref.near_ref = bf16[4,128,128]{2,1,0:T(8,128)(2,1)} all-to-all(bf16[4,128,128]{2,1,0:T(8,128)(2,1)S(1)} %get-tuple-element.19), channel_id=1, replica_groups={{0,32,64,96},{128,160,192,224},{256,288,320,352},{384,416,448,480},{1,3..., dimensions={0} | all-to-all | bytes 262144 | tf_op jit(solution)/shard_map/all_to_all | solution.py:458
  126.2 2.0 group_map.1
  128.2 8.3 %all-to-all-start.2 = ((bf16[4,128,128]{2,1,0:T(8,128)(2,1)}), bf16[4,128,128]{2,1,0:T(8,128)(2,1)S(1)}, u32[]{:S(2)}, u32[]{:S(2)}) async-start(bf16[4,128,128]{2,1,0:T(8,128)(2,1)} %group_map.1), calls=%async_computation.2 | async-start | bytes 262144 | tf_op jit(solution)/shard_map/all_to_all | solution.py:458
  136.5 0.0 collective-permute-done.6.refs_1_
  136.6 1.9 slice.28
  138.5 2.7 %collective-permute-start.8 = (bf16[128,2048]{1,0:T(8,128)(2,1)}, bf16[128,2048]{1,0:T(8,128)(2,1)}, u32[]{:S(2)}, u32[]{:S(2)}) collective-permute-start(bf16[128,2048]{1,0:T(8,128)(2,1)} %slice.28), channel_id=1, source_target_pairs={{0,2},{1,3},{2,4},{3,5},{4,6},{5,7},{6,0},{7,1},{8,10},{9,11},{10,... | collective-permute-start | bytes 1572872 | tf_op jit(solution)/shard_map/ppermute | solution.py:454
  141.1 1.9 slice.29
  143.0 3.8 %collective-permute-start.9 = (bf16[128,2048]{1,0:T(8,128)(2,1)}, bf16[128,2048]{1,0:T(8,128)(2,1)}, u32[]{:S(2)}, u32[]{:S(2)}) collective-permute-start(bf16[128,2048]{1,0:T(8,128)(2,1)} %slice.29), channel_id=1, source_target_pairs={{0,6},{1,7},{2,0},{3,1},{4,2},{5,3},{6,4},{7,5},{8,14},{9,15},{10,... | collective-permute-start | bytes 1572872 | tf_op jit(solution)/shard_map/ppermute | solution.py:454
  146.9 0.1 copy.23
  146.9 0.1 reshape.38.init_ref
  147.1 1.0 slice.26
  148.1 2.9 %collective-permute-start.5 = (bf16[16,2048]{1,0:T(8,128)(2,1)S(1)}, bf16[16,2048]{1,0:T(8,128)(2,1)S(1)}, u32[]{:S(2)}, u32[]{:S(2)}) collective-permute-start(bf16[16,2048]{1,0:T(8,128)(2,1)S(1)} %fusion.8), channel_id=1, source_target_pairs={{0,32},{32,64},{64,96},{96,128},{128,160},{160,192},{192,224},{224... | collective-permute-start | bytes 196616 | tf_op jit(solution)/shard_map/ppermute | solution.py:449
  151.0 0.1 pad_add_fusion.at_ref
  151.1 3.6 %collective-permute-done.5.halo_ref = bf16[16,2048]{1,0:T(8,128)(2,1)S(1)} collective-permute-done((bf16[16,2048]{1,0:T(8,128)(2,1)S(1)}, bf16[16,2048]{1,0:T(8,128)(2,1)S(1)}, u32[]{:S(2)}, u32[]{:S(2)}) %collective-permute-start.5) | collective-permute-done | bytes 65568 | tf_op jit(solution)/shard_map/ppermute | solution.py:449
  154.6 2.2 %copy-done.2 = bf16[2048,1024]{1,0:T(8,128)(2,1)S(1)} copy-done((bf16[2048,1024]{1,0:T(8,128)(2,1)S(1)}, bf16[2048,1024]{1,0:T(8,128)(2,1)}, u32[]{:S(2)}) %copy-start.2) | copy-done | bytes 4194328
  156.9 5.3 %conv_mix.1 = (bf16[1024,128]{1,0:T(8,128)(2,1)S(1)}, bf16[1024,128]{1,0:T(8,128)(2,1)S(1)}) custom-call(s32[2]{0:T(128)S(1)} %pad_add_fusion.1.place_ref, bf16[4,128,2048]{2,1,0:T(8,128)(2,1)S(1)} %copy-done.1, bf16[4,128,2048]{2,1,0:T(8,128)(2,1)} %collective-permute-done.4.other_ref, bf16[2048,1024]{1,0:T(8,128)(2,1)S(1)} %copy-done.2, ...), custom_call_target="tpu_custom_call" | custom-call | tf_op jit(solution)/shard_map/conv_mix/pallas_call | solution.py:263
  162.2 2.1 %local_reads.1 = (f32[1024,128]{1,0:T(8,128)S(1)}, bf16[1024,128]{1,0:T(8,128)(2,1)S(1)}) custom-call(bf16[1024,128]{1,0:T(8,128)(2,1)S(1)} %get-tuple-element.20.q_ref, bf16[1024,128]{1,0:T(8,128)(2,1)S(1)} %get-tuple-element.21.gk_ref, bf16[1024,128]{1,0:T(8,128)(2,1)S(1)} %copy-done.12, bf16[1024,256]{1,0:T(8,128)(2,1)S(1)} %get-tuple-element.23.wu_ref, ...), custom_call_target="tpu_custom_call" | custom-call | tf_op jit(solution)/shard_map/local_reads/pallas_call | solution.py:316
  164.3 0.0 all-to-all-done.2.far_ref
  164.4 3.2 %finish_mix.1 = bf16[1024,256]{1,0:T(8,128)(2,1)} custom-call(s32[2]{0:T(128)S(1)} %pad_add_fusion.at_ref, bf16[4,128,128]{2,1,0:T(8,128)(2,1)S(1)} %copy-done.3, bf16[4,128,128]{2,1,0:T(8,128)(2,1)S(1)} %all-to-all-done.2.far_ref, f32[64,128]{1,0:T(8,128)S(1)} %reshape.38.init_ref, f32[1024,128]{1,0:T(8,128)S(1)} %get-tuple-element.28.o_ref, ...), custom_call_target="tpu_custom_call" | custom-call | tf_op jit(solution)/shard_map/finish_mix/pallas_call | solution.py:379
  167.6 3.5 %all-to-all-start.3 = ((bf16[4,256,256]{2,1,0:T(8,128)(2,1)}), bf16[4,256,256]{2,1,0:T(8,128)(2,1)S(1)}, u32[]{:S(2)}, u32[]{:S(2)}) async-start(bf16[4,256,256]{2,1,0:T(8,128)(2,1)} %bitcast.20), calls=%async_computation.3 | async-start | bytes 1048576 | tf_op jit(solution)/shard_map/all_to_all | solution.py:560
  171.1 0.6 stack.52.pick_ref
  171.7 2.3 %pad_maximum_fusion.1.refs_3_ = bf16[256,2048]{1,0:T(8,128)(2,1)} fusion(bf16[128,2048]{1,0:T(8,128)(2,1)} %collective-permute-done.9, bf16[128,2048]{1,0:T(8,128)(2,1)} %collective-permute-done.8), kind=kLoop, calls=%fused_computation.10 | loop fusion | flops 2097152 | bytes 2097152 | tf_op jit(solution)/shard_map/concatenate | solution.py:527
  174.0 4.0 %all-to-all-done.3.m_ref = bf16[4,256,256]{2,1,0:T(8,128)(2,1)S(1)} async-done(((bf16[4,256,256]{2,1,0:T(8,128)(2,1)}), bf16[4,256,256]{2,1,0:T(8,128)(2,1)S(1)}, u32[]{:S(2)}, u32[]{:S(2)}) %all-to-all-start.3) | async-done | bytes 524320 | tf_op jit(solution)/shard_map/all_to_all | solution.py:560
  178.0 0.8 copy-done.16
  178.8 5.7 %outward.1 = (bf16[128,2048]{1,0:T(8,128)(2,1)}, bf16[128,2048]{1,0:T(8,128)(2,1)}) custom-call(s32[5]{0:T(128)} %stack.52.pick_ref, bf16[4,256,256]{2,1,0:T(8,128)(2,1)} %copy-done.16, bf16[256,2048]{1,0:T(8,128)(2,1)} %bitcast.46, bf16[256,2048]{1,0:T(8,128)(2,1)} %collective-permute-done.6.refs_1_, bf16[256,2048]{1,0:T(8,128)(2,1)} %collective-permute-done.7.refs_2_, ...), custom_call_target="tpu_custom_call" | custom-call | tf_op jit(solution)/shard_map/outward/pallas_call | solution.py:414
  184.5 14.7 %collective-permute-start.10 = (bf16[128,2048]{1,0:T(8,128)(2,1)}, bf16[128,2048]{1,0:T(8,128)(2,1)S(1)}, u32[]{:S(2)}, u32[]{:S(2)}) collective-permute-start(bf16[128,2048]{1,0:T(8,128)(2,1)} %get-tuple-element.32), channel_id=1, source_target_pairs={{0,1},{1,0},{2,3},{3,2},{4,5},{5,4},{6,7},{7,6},{8,9},{9,8},{10,11... | collective-permute-start | bytes 1572872 | tf_op jit(solution)/shard_map/ppermute | solution.py:495
  199.2 1.7 collective-permute-done.10
  200.9 2.0 fusion.7
  (51 shorter events, 0.2 us)
Async XLA Ops:
  6.5 91.9 %all-gather.2.cloned.1.call-start = ((), (), s32[]{:S(2)}) async-start(), calls=%async_computation.6 | async-start | bytes 4456448 | tf_op jit(solution)/shard_map/all_gather | solution.py:513
  8.1 40.3 %copy-start.15 = (bf16[1,128,2048]{2,1,0:T(8,128)(2,1)S(1)}, bf16[1,128,2048]{2,1,0:T(8,128)(2,1)}, u32[]{:S(2)}) copy-start(bf16[1,128,2048]{2,1,0:T(8,128)(2,1)} %param.18) | copy-start | bytes 1572868
  8.1 40.4 %copy-start.19 = (f32[2048]{0:T(1024)S(1)}, f32[2048]{0:T(1024)}, u32[]{:S(2)}) copy-start(f32[2048]{0:T(1024)} %param.19) | copy-start | bytes 24580
  20.6 21.3 %collective-permute-start.1 = (bf16[128,2048]{1,0:T(8,128)(2,1)S(1)}, bf16[128,2048]{1,0:T(8,128)(2,1)S(1)}, u32[]{:S(2)}, u32[]{:S(2)}) collective-permute-start(bf16[128,2048]{1,0:T(8,128)(2,1)S(1)} %fusion.4), channel_id=1, source_target_pairs={{0,2},{1,3},{2,4},{3,5},{4,6},{5,7},{6,0},{7,1},{8,10},{9,11},{10,... | collective-permute-start | bytes 1572872 | tf_op jit(solution)/shard_map/ppermute | solution.py:454
  23.7 20.1 %collective-permute-start = (bf16[128,2048]{1,0:T(8,128)(2,1)S(1)}, bf16[128,2048]{1,0:T(8,128)(2,1)S(1)}, u32[]{:S(2)}, u32[]{:S(2)}) collective-permute-start(bf16[128,2048]{1,0:T(8,128)(2,1)S(1)} %fusion.4), channel_id=1, source_target_pairs={{0,6},{1,7},{2,0},{3,1},{4,2},{5,3},{6,4},{7,5},{8,14},{9,15},{10,... | collective-permute-start | bytes 1572872 | tf_op jit(solution)/shard_map/ppermute | solution.py:454
  28.6 30.8 %all-to-all-start.4 = ((bf16[16,32,256]{2,1,0:T(8,128)(2,1)}), bf16[16,32,256]{2,1,0:T(8,128)(2,1)}, u32[]{:S(2)}, u32[]{:S(2)}) async-start(bf16[16,32,256]{2,1,0:T(8,128)(2,1)} %pack_shards.3), calls=%async_computation.4 | async-start | bytes 524288 | tf_op jit(solution)/shard_map/all_to_all | solution.py:458
  41.9 8.7 %collective-permute-start.2 = (bf16[64,2048]{1,0:T(8,128)(2,1)S(1)}, bf16[64,2048]{1,0:T(8,128)(2,1)S(1)}, u32[]{:S(2)}, u32[]{:S(2)}) collective-permute-start(bf16[64,2048]{1,0:T(8,128)(2,1)S(1)} %slice.24), channel_id=1, source_target_pairs={{0,2},{1,3},{2,4},{3,5},{4,6},{5,7},{6,0},{7,1},{8,10},{9,11},{10,... | collective-permute-start | bytes 786440 | tf_op jit(solution)/shard_map/ppermute | solution.py:454
  43.8 8.0 %copy-start.17 = (bf16[128,2048]{1,0:T(8,128)(2,1)}, bf16[128,2048]{1,0:T(8,128)(2,1)S(1)}, u32[]{:S(2)}) copy-start(bf16[128,2048]{1,0:T(8,128)(2,1)S(1)} %collective-permute-done) | copy-start | bytes 1572868
  43.9 7.9 %collective-permute-start.3 = (bf16[64,2048]{1,0:T(8,128)(2,1)S(1)}, bf16[64,2048]{1,0:T(8,128)(2,1)S(1)}, u32[]{:S(2)}, u32[]{:S(2)}) collective-permute-start(bf16[64,2048]{1,0:T(8,128)(2,1)S(1)} %slice.25), channel_id=1, source_target_pairs={{0,6},{1,7},{2,0},{3,1},{4,2},{5,3},{6,4},{7,5},{8,14},{9,15},{10,... | collective-permute-start | bytes 786440 | tf_op jit(solution)/shard_map/ppermute | solution.py:454
  53.1 22.8 %copy-start = (bf16[4,128,2048]{2,1,0:T(8,128)(2,1)}, bf16[4,128,2048]{2,1,0:T(8,128)(2,1)S(1)}, u32[]{:S(2)}) copy-start(bf16[4,128,2048]{2,1,0:T(8,128)(2,1)S(1)} %pad_maximum_fusion.same_ref) | copy-start | bytes 6291460
  53.1 34.6 %collective-permute-start.4 = (bf16[4,128,2048]{2,1,0:T(8,128)(2,1)S(1)}, bf16[4,128,2048]{2,1,0:T(8,128)(2,1)}, u32[]{:S(2)}, u32[]{:S(2)}) collective-permute-start(bf16[4,128,2048]{2,1,0:T(8,128)(2,1)S(1)} %pad_maximum_fusion.same_ref), channel_id=1, source_target_pairs={{0,1},{1,0},{2,3},{3,2},{4,5},{5,4},{6,7},{7,6},{8,9},{9,8},{10,11... | collective-permute-start | bytes 6291464 | tf_op jit(solution)/shard_map/ppermute | solution.py:495
  74.8 12.8 %copy-start.20 = (f32[3,128]{1,0:T(4,128)S(1)}, f32[3,128]{1,0:T(4,128)}, u32[]{:S(2)}) copy-start(f32[3,128]{1,0:T(4,128)} %param.23) | copy-start | bytes 4612
  74.8 12.8 %copy-start.21 = (f32[128]{0:T(128)S(1)}, f32[128]{0:T(128)}, u32[]{:S(2)}) copy-start(f32[128]{0:T(128)} %param.29) | copy-start | bytes 1540
  74.8 12.8 %copy-start.22 = (f32[128]{0:T(128)S(1)}, f32[128]{0:T(128)}, u32[]{:S(2)}) copy-start(f32[128]{0:T(128)} %param.30) | copy-start | bytes 1540
  74.8 12.8 %copy-start.23 = (f32[128]{0:T(128)S(1)}, f32[128]{0:T(128)}, u32[]{:S(2)}) copy-start(f32[128]{0:T(128)} %param.33) | copy-start | bytes 1540
  74.8 23.6 %copy-start.4 = (f32[1,1024,128]{2,1,0:T(8,128)S(1)}, f32[1,1024,128]{2,1,0:T(8,128)}, u32[]{:S(2)}) copy-start(f32[1,1024,128]{2,1,0:T(8,128)} %param.31) | copy-start | bytes 1572868
  78.2 58.4 %collective-permute-start.6 = (bf16[256,2048]{1,0:T(8,128)(2,1)}, bf16[256,2048]{1,0:T(8,128)(2,1)}, u32[]{:S(2)}, u32[]{:S(2)}) collective-permute-start(bf16[256,2048]{1,0:T(8,128)(2,1)} %bitcast.44), channel_id=1, source_target_pairs={{0,2},{1,3},{2,4},{3,5},{4,6},{5,7},{6,0},{7,1},{8,10},{9,11},{10,... | collective-permute-start | bytes 3145736 | tf_op jit(solution)/shard_map/ppermute | solution.py:454
  81.5 59.6 %collective-permute-start.7 = (bf16[256,2048]{1,0:T(8,128)(2,1)}, bf16[256,2048]{1,0:T(8,128)(2,1)}, u32[]{:S(2)}, u32[]{:S(2)}) collective-permute-start(bf16[256,2048]{1,0:T(8,128)(2,1)} %bitcast.45), channel_id=1, source_target_pairs={{0,6},{1,7},{2,0},{3,1},{4,2},{5,3},{6,4},{7,5},{8,14},{9,15},{10,... | collective-permute-start | bytes 3145736 | tf_op jit(solution)/shard_map/ppermute | solution.py:454
  113.6 0.8 copy-start.5
  114.4 0.8 copy-start.7
  115.2 0.8 copy-start.9
  116.0 0.7 copy-start.11
  116.7 0.7 copy-start.13
  117.4 29.5 %copy-start.18 = (f32[1,2,64,64]{3,2,1,0:T(8,128)S(1)}, f32[1,2,64,64]{3,2,1,0:T(8,128)}, u32[]{:S(2)}) copy-start(f32[1,2,64,64]{3,2,1,0:T(8,128)} %param.32) | copy-start | bytes 98308
  117.4 29.7 %copy-start.1 = (bf16[4,128,2048]{2,1,0:T(8,128)(2,1)S(1)}, bf16[4,128,2048]{2,1,0:T(8,128)(2,1)}, u32[]{:S(2)}) copy-start(bf16[4,128,2048]{2,1,0:T(8,128)(2,1)} %copy-done) | copy-start | bytes 6291460
  128.2 36.1 %all-to-all-start.2 = ((bf16[4,128,128]{2,1,0:T(8,128)(2,1)}), bf16[4,128,128]{2,1,0:T(8,128)(2,1)S(1)}, u32[]{:S(2)}, u32[]{:S(2)}) async-start(bf16[4,128,128]{2,1,0:T(8,128)(2,1)} %group_map.1), calls=%async_computation.2 | async-start | bytes 262144 | tf_op jit(solution)/shard_map/all_to_all | solution.py:458
  138.5 33.2 %collective-permute-start.8 = (bf16[128,2048]{1,0:T(8,128)(2,1)}, bf16[128,2048]{1,0:T(8,128)(2,1)}, u32[]{:S(2)}, u32[]{:S(2)}) collective-permute-start(bf16[128,2048]{1,0:T(8,128)(2,1)} %slice.28), channel_id=1, source_target_pairs={{0,2},{1,3},{2,4},{3,5},{4,6},{5,7},{6,0},{7,1},{8,10},{9,11},{10,... | collective-permute-start | bytes 1572872 | tf_op jit(solution)/shard_map/ppermute | solution.py:454
  143.0 28.7 %collective-permute-start.9 = (bf16[128,2048]{1,0:T(8,128)(2,1)}, bf16[128,2048]{1,0:T(8,128)(2,1)}, u32[]{:S(2)}, u32[]{:S(2)}) collective-permute-start(bf16[128,2048]{1,0:T(8,128)(2,1)} %slice.29), channel_id=1, source_target_pairs={{0,6},{1,7},{2,0},{3,1},{4,2},{5,3},{6,4},{7,5},{8,14},{9,15},{10,... | collective-permute-start | bytes 1572872 | tf_op jit(solution)/shard_map/ppermute | solution.py:454
  148.1 6.6 %collective-permute-start.5 = (bf16[16,2048]{1,0:T(8,128)(2,1)S(1)}, bf16[16,2048]{1,0:T(8,128)(2,1)S(1)}, u32[]{:S(2)}, u32[]{:S(2)}) collective-permute-start(bf16[16,2048]{1,0:T(8,128)(2,1)S(1)} %fusion.8), channel_id=1, source_target_pairs={{0,32},{32,64},{64,96},{96,128},{128,160},{160,192},{192,224},{224... | collective-permute-start | bytes 196616 | tf_op jit(solution)/shard_map/ppermute | solution.py:449
  154.6 2.2 %copy-start.2 = (bf16[2048,1024]{1,0:T(8,128)(2,1)S(1)}, bf16[2048,1024]{1,0:T(8,128)(2,1)}, u32[]{:S(2)}) copy-start(bf16[2048,1024]{1,0:T(8,128)(2,1)} %all-gather.2.cloned.1.call-done.w_ref) | copy-start | bytes 12582916
  156.8 5.3 %copy-start.6 = (f32[1024,128]{1,0:T(8,128)S(1)}, f32[1024,128]{1,0:T(8,128)}, u32[]{:S(2)}) copy-start(f32[1024,128]{1,0:T(8,128)} %copy-done.5) | copy-start | bytes 1572868
  156.8 5.3 %copy-start.8 = (f32[1024,128]{1,0:T(8,128)S(1)}, f32[1024,128]{1,0:T(8,128)}, u32[]{:S(2)}) copy-start(f32[1024,128]{1,0:T(8,128)} %copy-done.7) | copy-start | bytes 1572868
  156.8 5.3 %copy-start.10 = (bf16[16,128,128]{2,1,0:T(8,128)(2,1)S(1)}, bf16[16,128,128]{2,1,0:T(8,128)(2,1)}, u32[]{:S(2)}) copy-start(bf16[16,128,128]{2,1,0:T(8,128)(2,1)} %copy-done.9) | copy-start | bytes 1572868
  156.8 5.3 %copy-start.12 = (bf16[1024,128]{1,0:T(8,128)(2,1)S(1)}, bf16[1024,128]{1,0:T(8,128)(2,1)}, u32[]{:S(2)}) copy-start(bf16[1024,128]{1,0:T(8,128)(2,1)} %copy-done.11) | copy-start | bytes 786436
  156.8 5.3 %copy-start.14 = (bf16[1024,128]{1,0:T(8,128)(2,1)S(1)}, bf16[1024,128]{1,0:T(8,128)(2,1)}, u32[]{:S(2)}) copy-start(bf16[1024,128]{1,0:T(8,128)(2,1)} %copy-done.13) | copy-start | bytes 786436
  162.1 2.2 %copy-start.3 = (bf16[4,128,128]{2,1,0:T(8,128)(2,1)S(1)}, bf16[4,128,128]{2,1,0:T(8,128)(2,1)}, u32[]{:S(2)}) copy-start(bf16[4,128,128]{2,1,0:T(8,128)(2,1)} %all_to_all.32.pieces_ref.near_ref) | copy-start | bytes 393220
  167.6 10.4 %all-to-all-start.3 = ((bf16[4,256,256]{2,1,0:T(8,128)(2,1)}), bf16[4,256,256]{2,1,0:T(8,128)(2,1)S(1)}, u32[]{:S(2)}, u32[]{:S(2)}) async-start(bf16[4,256,256]{2,1,0:T(8,128)(2,1)} %bitcast.20), calls=%async_computation.3 | async-start | bytes 1048576 | tf_op jit(solution)/shard_map/all_to_all | solution.py:560
  178.0 0.8 copy-start.16
  184.5 16.4 %collective-permute-start.10 = (bf16[128,2048]{1,0:T(8,128)(2,1)}, bf16[128,2048]{1,0:T(8,128)(2,1)S(1)}, u32[]{:S(2)}, u32[]{:S(2)}) collective-permute-start(bf16[128,2048]{1,0:T(8,128)(2,1)} %get-tuple-element.32), channel_id=1, source_target_pairs={{0,1},{1,0},{2,3},{3,2},{4,5},{5,4},{6,7},{7,6},{8,9},{9,8},{10,11... | collective-permute-start | bytes 1572872 | tf_op jit(solution)/shard_map/ppermute | solution.py:495
Sparse Core Ops, SparseCore 0:
  18.2 80.1 all-gather.1

commit v6 on v5

--- a/solution.py
+++ b/solution.py
@@ -11,9 +11,18 @@
 HEAD_WIDTH = 64
 CHUNK = 64
 BLOCK = 256
+MAPS_BLOCK = 512
 norm_eps = 1e-06
 key_eps = 1e-06
 f32, bf16 = jnp.float32, jnp.bfloat16
+
+
+def array(shape, dtype):
+    return pltpu.HBM(tuple(shape), dtype)
+
+
+def in_hbm(*arrays):
+    return [pltpu.with_memory_space_constraint(a, pltpu.HBM) for a in arrays]
 
 
 def dot(a, b, ca=1, cb=0):
@@ -41,10 +50,13 @@
     return jnp.where(low, a, b)
 
 
-def own_block(place_ref, same_ref, other_ref):
-    mine, theirs = same_ref[0], other_ref[0]
+def own_block(place_ref, *token_refs):
     low_core = place_ref[1] == 0
-    return jnp.concatenate([jnp.where(low_core, mine, theirs), jnp.where(low_core, theirs, mine)], axis=0)
+    rows = []
+    for k in range(0, len(token_refs), 2):
+        mine, theirs = token_refs[k][0], token_refs[k + 1][0]
+        rows += [jnp.where(low_core, mine, theirs), jnp.where(low_core, theirs, mine)]
+    return jnp.concatenate(rows, axis=0)
 
 
 def chunk_masks():
@@ -60,26 +72,12 @@
     return [a[k * CHUNK : (k + 1) * CHUNK] for k in range(a.shape[0] // CHUNK)]
 
 
-def maps_kernel(
-    place_ref,
-    same_ref,
-    other_ref,
-    w_ref,
-    spike_ref,
-    vec_ref,
-    gk_ref,
-    gb_ref,
-    wu_ref,
-    v_ref,
-    pos_ref,
-    full_ref,
-    states_ref,
-    agg_ref,
-    st_ref,
-):
+def maps_kernel(place_ref, *refs):
+    *token_refs, w_ref, spike_ref, vec_ref = refs[:-9]
+    gk_ref, gb_ref, wu_ref, v_ref, pos_ref, full_ref, states_ref, agg_ref, st_ref = refs[-9:]
     step = pl.program_id(0)
     width = 2 * HEAD_WIDTH
-    each = range(BLOCK // CHUNK)
+    each = range(MAPS_BLOCK // CHUNK)
 
     @pl.when(step == 0)
     def _():
@@ -87,7 +85,7 @@
         eye = (r - HEAD_WIDTH == l % HEAD_WIDTH) & (r >= HEAD_WIDTH)
         st_ref[...] = jnp.where(eye, 1.0, 0.0).astype(f32)
 
-    x = own_block(place_ref, same_ref, other_ref)
+    x = own_block(place_ref, *token_refs)
 
     def section(k):
         two = jnp.dot(x, w_ref[:, 2 * k * width : 2 * (k + 1) * width], preferred_element_type=f32)
@@ -99,7 +97,7 @@
     v_ref[...] = vals
     keys = keys.astype(f32)
 
-    low = lanes_of((BLOCK, width)) < HEAD_WIDTH
+    low = lanes_of((MAPS_BLOCK, width)) < HEAD_WIDTH
     logd = spike_ref[...] - jnp.exp(vec_ref[0:1] + jnp.tanh(dpre))
     rate = jax.nn.sigmoid(vec_ref[1:2] + rpre)
     unit = keys * lax.rsqrt(head_sums(keys * keys, low) + key_eps)
@@ -110,7 +108,14 @@
     rest = logd - hi.astype(f32)
     mid = rest.astype(bf16)
     lo = (rest - mid.astype(f32)).astype(bf16)
-    sums = jnp.dot(tri, jnp.concatenate([hi, mid, lo], axis=1), preferred_element_type=f32)
+    terms = jnp.concatenate([hi, mid, lo], axis=1)
+    sums = jnp.concatenate(
+        [
+            jnp.dot(tri, terms[k : k + BLOCK], preferred_element_type=f32)
+            for k in range(0, MAPS_BLOCK, BLOCK)
+        ],
+        axis=0,
+    )
     cum_all = sums[:, :width] + sums[:, width : 2 * width] + sums[:, 2 * width :]
     prev_all = cum_all - logd
 
@@ -174,25 +179,28 @@
             agg_ref[k] = state.astype(bf16)
 
 
-def token_specs(same):
+def token_specs(same, pairs=1):
     chips, part, depth = same.shape
-    tokens = pl.BlockSpec((1, part, depth), lambda i, p: ((i - p[0]) & (chips - 1), 0, 0))
-    return [tokens, tokens]
+    specs = []
+    for k in range(pairs):
+        place = lambda i, p, k=k: ((pairs * i + k - p[0]) & (chips - 1), 0, 0)
+        specs += [pl.BlockSpec((1, part, depth), place)] * 2
+    return specs
 
 
 def maps_call(place, same, other, w, spike, vec, copies):
     rows, width = spike.shape
     depth = w.shape[0]
-    tile = pl.BlockSpec((BLOCK, width), lambda i, p: (i, 0))
-    wide = pl.BlockSpec((BLOCK, 2 * width), lambda i, p: (i, 0))
-    pairs = BLOCK // CHUNK
-    like = lambda n, t: jax.ShapeDtypeStruct((rows, n), t)
+    tile = pl.BlockSpec((MAPS_BLOCK, width), lambda i, p: (i, 0))
+    wide = pl.BlockSpec((MAPS_BLOCK, 2 * width), lambda i, p: (i, 0))
+    pairs = MAPS_BLOCK // CHUNK
+    like = lambda n, t: array((rows, n), t)
     return pl.pallas_call(
         maps_kernel,
         grid_spec=pltpu.PrefetchScalarGridSpec(
             num_scalar_prefetch=1,
-            grid=(rows // BLOCK,),
-            in_specs=token_specs(same)
+            grid=(rows // MAPS_BLOCK,),
+            in_specs=token_specs(same, MAPS_BLOCK // BLOCK)
             + [
                 pl.BlockSpec((depth, 4 * width), lambda i, p: (0, 0)),
                 tile,
@@ -217,14 +225,14 @@
             like(width, bf16),
             like(width, f32),
             like(width, f32),
-            jax.ShapeDtypeStruct((rows // CHUNK, width, width), bf16),
-            jax.ShapeDtypeStruct((copies, width, width), bf16),
+            array((rows // CHUNK, width, width), bf16),
+            array((copies, width, width), bf16),
         ],
         compiler_params=pltpu.CompilerParams(
-            dimension_semantics=("arbitrary",), vmem_limit_bytes=50 * 2**20
+            dimension_semantics=("arbitrary",), vmem_limit_bytes=28 * 2**20
         ),
         name="state_maps",
-    )(place, same, other, w, spike, vec)
+    )(place, *(in_hbm(same, other) * (MAPS_BLOCK // BLOCK)), *in_hbm(w), spike, vec)
 
 
 def conv_kernel(place_ref, same_ref, other_ref, w_ref, halo_ref, vec_ref, q_ref, out_ref, tail_ref):
@@ -270,12 +278,12 @@
             out_specs=[tile, tile],
             scratch_shapes=[pltpu.VMEM((halo.shape[0], width), f32)],
         ),
-        out_shape=[jax.ShapeDtypeStruct((rows, width), bf16)] * 2,
+        out_shape=[array((rows, width), bf16)] * 2,
         compiler_params=pltpu.CompilerParams(
-            dimension_semantics=("arbitrary",), vmem_limit_bytes=40 * 2**20
+            dimension_semantics=("arbitrary",), vmem_limit_bytes=20 * 2**20
         ),
         name="conv_mix",
-    )(place, same, other, w, halo, vec)
+    )(place, *in_hbm(same, other, w), halo, vec)
 
 
 def reads_kernel(q_ref, gk_ref, gb_ref, wu_ref, v_ref, pos_ref, full_ref, states_ref, o_ref, y_ref):
@@ -318,12 +326,12 @@
         grid=(rows // BLOCK,),
         in_specs=[tile, tile, tile, wide, tile, tile, tile, starts],
         out_specs=[tile, tile],
-        out_shape=[jax.ShapeDtypeStruct((rows, width), f32), jax.ShapeDtypeStruct((rows, width), bf16)],
+        out_shape=[array((rows, width), f32), array((rows, width), bf16)],
         compiler_params=pltpu.CompilerParams(
-            dimension_semantics=("arbitrary",), vmem_limit_bytes=40 * 2**20
+            dimension_semantics=("arbitrary",), vmem_limit_bytes=20 * 2**20
         ),
         name="local_reads",
-    )(q, gk, gb, wu, v, pos, full, states)
+    )(*in_hbm(q, gk, gb, wu, v, pos, full, states))
 
 
 def moved(state, piece, first):
@@ -385,43 +393,38 @@
             out_specs=pl.BlockSpec((BLOCK, 2 * width), lambda i, p: (i, 0)),
             scratch_shapes=[pltpu.VMEM((width, width), bf16)],
         ),
-        out_shape=jax.ShapeDtypeStruct((rows, 2 * width), bf16),
+        out_shape=array((rows, 2 * width), bf16),
         compiler_params=pltpu.CompilerParams(
-            dimension_semantics=("arbitrary",), vmem_limit_bytes=50 * 2**20
+            dimension_semantics=("arbitrary",), vmem_limit_bytes=12 * 2**20
         ),
         name="finish_mix",
-    )(at, near, far, init, o, y, conv, vec)
+    )(at, near, far, init, *in_hbm(o, y, conv), vec)
 
 
 def outward_kernel(pick_ref, m_ref, *refs):
     *weights, keep_ref, give_ref = refs
-    total = None
-    for k, w_ref in enumerate(weights):
-        got = dot(m_ref[pick_ref[1 + k]], w_ref[...])
-        total = got if total is None else total + got
-    total = total.astype(bf16)
-    rows = keep_ref.shape[0]
+    rows, columns = keep_ref.shape
     first = pick_ref[0] == 0
-    keep_ref[...] = jnp.where(first, total[:rows], total[rows:])
-    give_ref[...] = jnp.where(first, total[rows:], total[:rows])
+    step = 512
+    for at in range(0, columns, step):
+        total = None
+        for k, w_ref in enumerate(weights):
+            got = dot(m_ref[pick_ref[1 + k]], w_ref[:, at : at + step])
+            total = got if total is None else total + got
+        total = total.astype(bf16)
+        keep_ref[:, at : at + step] = jnp.where(first, total[:rows], total[rows:])
+        give_ref[:, at : at + step] = jnp.where(first, total[rows:], total[:rows])
 
 
 def outward_call(pick, gathered, weights):
-    _, rows, depth = gathered.shape
-    columns = weights[0].shape[1]
-    step = 512
-    tile = pl.BlockSpec((rows // 2, step), lambda i, p: (0, i))
+    rows, columns = gathered.shape[1] // 2, weights[0].shape[1]
+    here = pl.BlockSpec(memory_space=pltpu.VMEM)
     return pl.pallas_call(
         outward_kernel,
-        grid_spec=pltpu.PrefetchScalarGridSpec(
-            num_scalar_prefetch=1,
-            grid=(columns // step,),
-            in_specs=[pl.BlockSpec(gathered.shape, lambda i, p: (0, 0, 0))]
-            + [pl.BlockSpec((depth, step), lambda i, p: (0, i)) for _ in weights],
-            out_specs=[tile, tile],
-        ),
-        out_shape=[jax.ShapeDtypeStruct((rows // 2, columns), bf16)] * 2,
-        compiler_params=pltpu.CompilerParams(dimension_semantics=("arbitrary",)),
+        in_specs=[pl.BlockSpec(memory_space=pltpu.SMEM)] + [here] * (1 + len(weights)),
+        out_specs=[here, here],
+        out_shape=[jax.ShapeDtypeStruct((rows, columns), bf16)] * 2,
+        compiler_params=pltpu.CompilerParams(vmem_limit_bytes=24 * 2**20),
         name="outward",
     )(pick, gathered, *weights)
 
@@ -516,15 +519,10 @@
     outer = jnp.swapaxes(outer, 0, 1).reshape(-1, 2 * channels).T
 
     normed = rms_rows(tokens[0], input_norm_gain)
-    behind, ahead = turned(normed, 2), turned(normed, -2)
-    cut = normed.shape[0] // 2
-    far = turned(behind[:cut], 2), turned(ahead[cut:], -2)
-    same = jnp.stack([normed, ahead, jnp.concatenate(far, axis=0), behind])
+    others = [turned(normed, -2), turned(normed, 4), turned(normed, 2)]
+    same = jnp.stack([normed, *others])
     other = core_swap(same)
-
-    before, after = turned(outer, 2), turned(outer, -2)
-    far = turned(before[:channels], 2), turned(after[channels:], -2)
-    across = jnp.concatenate(far, axis=0)
+    after, across, before = [turned(outer, k) for k in (-2, 4, 2)]
     vec = jnp.concatenate(
         [
             decay_floor[None],
@@ -547,7 +545,7 @@
     q, conv = conv_call(place, same, other, weights, halo, vec)
     total = pl.pallas_call(
         group_kernel,
-        out_shape=jax.ShapeDtypeStruct((blocks // few, *agg.shape[1:]), bf16),
+        out_shape=array((blocks // few, *agg.shape[1:]), bf16),
         name="group_map",
     )(near_maps)
     far_maps = from_everyone(total, "sp", far_blocks)
@@ -560,8 +558,8 @@
     gathered = lax.all_to_all(
         mixed.reshape(chips, -1, 2 * channels), "tp", 0, 0, tiled=True, axis_index_groups=groups
     )
-    near = [(chip + k) & (chips - 1) for k in (0, chips - 1, 1, 2)]
-    kept, given = outward_call(jnp.stack([core, *near]), gathered, (outer, before, after, across))
+    near = [(chip + k) & (chips - 1) for k in (0, 1, 2, chips - 1)]
+    kept, given = outward_call(jnp.stack([core, *near]), gathered, (outer, after, across, before))
     taken = core_swap(given)
     return (kept.astype(f32) + taken.astype(f32)).astype(bf16)[None]
 

time: 211 us -> 201 us (0.953)
  the two profiles are of different devices: /device:TPU:129 before, /device:TPU:41 now
where the time goes in v6:
time: 201 us; the launch traced here: 200 us
  starting transfers between devices  56.5 us (28%)
  blocking collectives  42.5 us (21%)
  waiting for transfers between devices  39.9 us (20%)
  Pallas kernels  37.3 us (19%)
  between operations  13.7 us (7%)
  other arithmetic  5.39 us (3%)
  local copies, waits for them, and re-layouts  4.77 us (2%)
    all_to_all x2, blocking collectives, from_everyone(): lax.all_to_all(copies, axis, 0, 0, tiled=True, axis_index_groups=groups)  42.5 us
    ppermute x6, waiting for transfers between devices, turned(): lax.ppermute(x, 'tp', [(i, (i + distance) % devices) for i in range(devic...  24.2 us
    ppermute x6, starting transfers between devices, turned(): lax.ppermute(x, 'tp', [(i, (i + distance) % devices) for i in range(devic...  20.6 us
    all_to_all x3, starting transfers between devices, from_everyone(): lax.all_to_all(copies, axis, 0, 0, tiled=True, axis_index_groups=groups)  15.4 us
    ppermute x2, starting transfers between devices, core_swap(): return lax.ppermute(x, 'tp', [(i, i ^ 1) for i in range(devices)])  13.9 us
    pallas_call x1, Pallas kernels, maps_call(): pl.pallas_call(maps_kernel, grid_spec=pltpu.PrefetchScalarGridSpec(num_sc...  12.9 us
    all_gather x1, waiting for transfers between devices, mixing(): weights = lax.all_gather(weights, 'sp', axis=0, tiled=True)  7.35 us
    pallas_call x1, Pallas kernels, conv_call(): pl.pallas_call(conv_kernel, grid_spec=pltpu.PrefetchScalarGridSpec(num_sc...  6.93 us
  transfers between devices with their start and end apart: 14, of which 7 were waited for; matrix products, arithmetic and copies ran while one was open for 4% of the time, Pallas kernels for 16%

profile of v6, /device:TPU:41, one launch (start us, length us, event | category | flops | bytes accessed | tf_op | source)
XLA Modules:
  0.0 200.0 jit_solution(4943568101244252049)
XLA Ops:
  6.5 0.0 all-gather.2.cloned.1.call-start
  6.5 1.6 pack_shards.2
  8.2 8.9 %all_to_all.30 = bf16[4,32,1024]{2,1,0:T(8,128)(2,1)} all-to-all(bf16[4,32,1024]{2,1,0:T(8,128)(2,1)} %pack_shards.2), channel_id=1, replica_groups=mesh['sp'=16,'fs'=4,'tp'=8] {'fs'}, dimensions={0} | all-to-all | bytes 524288 | tf_op jit(solution)/shard_map/all_to_all | solution.py:461
  17.1 0.0 all-gather.2.cloned.1.call-update
  17.1 1.2 fusion.2
  18.3 1.2 fusion.4
  19.6 4.7 %collective-permute-start.1 = (bf16[128,2048]{1,0:T(8,128)(2,1)S(1)}, bf16[128,2048]{1,0:T(8,128)(2,1)S(1)}, u32[]{:S(2)}, u32[]{:S(2)}) collective-permute-start(bf16[128,2048]{1,0:T(8,128)(2,1)S(1)} %fusion.4), channel_id=1, source_target_pairs={{0,4},{1,5},{2,6},{3,7},{4,0},{5,1},{6,2},{7,3},{8,12},{9,13},{10,... | collective-permute-start | bytes 1572872 | tf_op jit(solution)/shard_map/ppermute | solution.py:457
  24.2 2.2 %collective-permute-start.2 = (bf16[128,2048]{1,0:T(8,128)(2,1)S(1)}, bf16[128,2048]{1,0:T(8,128)(2,1)S(1)}, u32[]{:S(2)}, u32[]{:S(2)}) collective-permute-start(bf16[128,2048]{1,0:T(8,128)(2,1)S(1)} %fusion.4), channel_id=1, source_target_pairs={{0,2},{1,3},{2,4},{3,5},{4,6},{5,7},{6,0},{7,1},{8,10},{9,11},{10,... | collective-permute-start | bytes 1572872 | tf_op jit(solution)/shard_map/ppermute | solution.py:457
  26.5 4.3 %collective-permute-start = (bf16[128,2048]{1,0:T(8,128)(2,1)S(1)}, bf16[128,2048]{1,0:T(8,128)(2,1)S(1)}, u32[]{:S(2)}, u32[]{:S(2)}) collective-permute-start(bf16[128,2048]{1,0:T(8,128)(2,1)S(1)} %fusion.4), channel_id=1, source_target_pairs={{0,6},{1,7},{2,0},{3,1},{4,2},{5,3},{6,4},{7,5},{8,14},{9,15},{10,... | collective-permute-start | bytes 1572872 | tf_op jit(solution)/shard_map/ppermute | solution.py:457
  30.7 0.0 copy-done.3
  30.7 0.0 copy-done.5
  30.8 0.2 fusion.6
  30.9 3.5 %collective-permute-done.1 = bf16[128,2048]{1,0:T(8,128)(2,1)S(1)} collective-permute-done((bf16[128,2048]{1,0:T(8,128)(2,1)S(1)}, bf16[128,2048]{1,0:T(8,128)(2,1)S(1)}, u32[]{:S(2)}, u32[]{:S(2)}) %collective-permute-start.1) | collective-permute-done | bytes 524320 | tf_op jit(solution)/shard_map/ppermute | solution.py:457
  34.5 13.6 %collective-permute-done.2 = bf16[128,2048]{1,0:T(8,128)(2,1)S(1)} collective-permute-done((bf16[128,2048]{1,0:T(8,128)(2,1)S(1)}, bf16[128,2048]{1,0:T(8,128)(2,1)S(1)}, u32[]{:S(2)}, u32[]{:S(2)}) %collective-permute-start.2) | collective-permute-done | bytes 524320 | tf_op jit(solution)/shard_map/ppermute | solution.py:457
  48.0 0.0 collective-permute-done
  48.0 1.6 pad_maximum_fusion.refs_0_.refs_2_.same_ref
  49.7 2.5 %collective-permute-start.3 = (bf16[4,128,2048]{2,1,0:T(8,128)(2,1)}, bf16[4,128,2048]{2,1,0:T(8,128)(2,1)}, u32[]{:S(2)}, u32[]{:S(2)}) collective-permute-start(bf16[4,128,2048]{2,1,0:T(8,128)(2,1)} %pad_maximum_fusion.refs_0_.refs_2_.same_ref), channel_id=1, source_target_pairs={{0,1},{1,0},{2,3},{3,2},{4,5},{5,4},{6,7},{7,6},{8,9},{9,8},{10,11... | collective-permute-start | bytes 6291464 | tf_op jit(solution)/shard_map/ppermute | solution.py:498
  52.2 0.0 copy-start.6
  52.2 0.0 copy-start.7
  52.2 0.0 copy-start.8
  52.2 0.0 copy-start.9
  52.3 0.0 copy-start.2
  52.3 1.5 pack_shards.3
  53.8 33.6 %all_to_all.31 = bf16[16,32,256]{2,1,0:T(8,128)(2,1)S(1)} all-to-all(bf16[16,32,256]{2,1,0:T(8,128)(2,1)} %pack_shards.3), channel_id=1, replica_groups=mesh['sp'=16,'fs'=4,'tp'=8] {'sp'}, dimensions={0} | all-to-all | bytes 524288 | tf_op jit(solution)/shard_map/all_to_all | solution.py:461
  87.3 1.2 broadcast_in_dim.27
  88.5 4.9 %all-to-all-start.5 = ((bf16[4,16,32,256]{3,2,1,0:T(8,128)(2,1)}), bf16[4,16,32,256]{3,2,1,0:T(8,128)(2,1)S(1)}, u32[]{:S(2)}, u32[]{:S(2)}) async-start(bf16[4,16,32,256]{3,2,1,0:T(8,128)(2,1)} %broadcast_in_dim.27), calls=%async_computation.5 | async-start | bytes 2097152 | tf_op jit(solution)/shard_map/all_to_all | solution.py:461
  93.4 0.0 copy-done.6
  93.5 0.1 pad_add_fusion.1.place_ref
  93.6 0.0 collective-permute-done.3.refs_1_.refs_3_.other_ref
  93.6 7.4 %all-gather.2.cloned.1.call-done.refs_4_.w_ref = bf16[2048,1024]{1,0:T(8,128)(2,1)} async-done(((bf16[128,1024]{1,0:T(8,128)(2,1)}), bf16[2048,1024]{1,0:T(8,128)(2,1)}) %all-gather.2.cloned.1.call-update) | async-done | bytes 4194320 | tf_op jit(solution)/shard_map/all_gather | solution.py:516
  100.9 12.9 %state_maps.1 = (bf16[1024,128]{1,0:T(8,128)(2,1)}, bf16[1024,128]{1,0:T(8,128)(2,1)}, bf16[1024,256]{1,0:T(8,128)(2,1)}, bf16[1024,128]{1,0:T(8,128)(2,1)}, f32...) custom-call(s32[2]{0:T(128)S(1)} %pad_add_fusion.1.place_ref, ...), custom_call_target="tpu_custom_call" | custom-call | tf_op jit(solution)/shard_map/state_maps/pallas_call | solution.py:198
  113.8 0.0 all-to-all-done.5
  113.8 3.9 %all-to-all-start.1 = ((bf16[4,128,128]{2,1,0:T(8,128)(2,1)}), bf16[4,128,128]{2,1,0:T(8,128)(2,1)S(1)}, u32[]{:S(2)}, u32[]{:S(2)}) async-start(bf16[4,128,128]{2,1,0:T(8,128)(2,1)} %get-tuple-element.19), calls=%async_computation.1 | async-start | bytes 262144 | tf_op jit(solution)/shard_map/all_to_all | solution.py:461
  117.7 0.1 copy.24
  117.8 0.6 copy.25
  118.4 4.5 %collective-permute-start.5 = (bf16[256,2048]{1,0:T(8,128)(2,1)S(1)}, bf16[256,2048]{1,0:T(8,128)(2,1)S(1)}, u32[]{:S(2)}, u32[]{:S(2)}) collective-permute-start(bf16[256,2048]{1,0:T(8,128)(2,1)S(1)} %bitcast.42), channel_id=1, source_target_pairs={{0,6},{1,7},{2,0},{3,1},{4,2},{5,3},{6,4},{7,5},{8,14},{9,15},{10,... | collective-permute-start | bytes 3145736 | tf_op jit(solution)/shard_map/ppermute | solution.py:457
  123.0 2.2 %collective-permute-start.6 = (bf16[256,2048]{1,0:T(8,128)(2,1)S(1)}, bf16[256,2048]{1,0:T(8,128)(2,1)}, u32[]{:S(2)}, u32[]{:S(2)}) collective-permute-start(bf16[256,2048]{1,0:T(8,128)(2,1)S(1)} %bitcast.43), channel_id=1, source_target_pairs={{0,4},{1,5},{2,6},{3,7},{4,0},{5,1},{6,2},{7,3},{8,12},{9,13},{10,... | collective-permute-start | bytes 3145736 | tf_op jit(solution)/shard_map/ppermute | solution.py:457
  125.2 2.8 %collective-permute-start.7 = (bf16[256,2048]{1,0:T(8,128)(2,1)S(1)}, bf16[256,2048]{1,0:T(8,128)(2,1)}, u32[]{:S(2)}, u32[]{:S(2)}) collective-permute-start(bf16[256,2048]{1,0:T(8,128)(2,1)S(1)} %bitcast.44), channel_id=1, source_target_pairs={{0,2},{1,3},{2,4},{3,5},{4,6},{5,7},{6,0},{7,1},{8,10},{9,11},{10,... | collective-permute-start | bytes 3145736 | tf_op jit(solution)/shard_map/ppermute | solution.py:457
  128.0 0.0 all-to-all-done.1.pieces_ref.near_ref
  128.0 0.0 copy-start
  128.0 0.6 copy-done
  128.6 2.0 group_map.1
  130.6 6.6 %all-to-all-start.2 = ((bf16[4,128,128]{2,1,0:T(8,128)(2,1)}), bf16[4,128,128]{2,1,0:T(8,128)(2,1)S(1)}, u32[]{:S(2)}, u32[]{:S(2)}) async-start(bf16[4,128,128]{2,1,0:T(8,128)(2,1)} %group_map.1), calls=%async_computation.2 | async-start | bytes 262144 | tf_op jit(solution)/shard_map/all_to_all | solution.py:461
  137.2 0.1 copy.23
  137.3 0.1 reshape.38.init_ref
  137.4 1.0 slice.9
  138.4 1.0 slice.8
  139.4 3.1 %collective-permute-start.4 = (bf16[16,2048]{1,0:T(8,128)(2,1)S(1)}, bf16[16,2048]{1,0:T(8,128)(2,1)S(1)}, u32[]{:S(2)}, u32[]{:S(2)}) collective-permute-start(bf16[16,2048]{1,0:T(8,128)(2,1)S(1)} %fusion.8), channel_id=1, source_target_pairs={{0,32},{32,64},{64,96},{96,128},{128,160},{160,192},{192,224},{224... | collective-permute-start | bytes 196616 | tf_op jit(solution)/shard_map/ppermute | solution.py:452
  142.5 0.1 pad_add_fusion.at_ref
  142.5 4.0 %collective-permute-done.4.halo_ref = bf16[16,2048]{1,0:T(8,128)(2,1)S(1)} collective-permute-done((bf16[16,2048]{1,0:T(8,128)(2,1)S(1)}, bf16[16,2048]{1,0:T(8,128)(2,1)S(1)}, u32[]{:S(2)}, u32[]{:S(2)}) %collective-permute-start.4) | collective-permute-done | bytes 65568 | tf_op jit(solution)/shard_map/ppermute | solution.py:452
  146.5 6.9 %conv_mix.1 = (bf16[1024,128]{1,0:T(8,128)(2,1)}, bf16[1024,128]{1,0:T(8,128)(2,1)}) custom-call(s32[2]{0:T(128)S(1)} %pad_add_fusion.1.place_ref, bf16[4,128,2048]{2,1,0:T(8,128)(2,1)} %pad_maximum_fusion.refs_0_.refs_2_.same_ref, bf16[4,128,2048]{2,1,0:T(8,128)(2,1)} %collective-permute-done.3.refs_1_.refs_3_.other_ref, ...), custom_call_target="tpu_custom_call" | custom-call | tf_op jit(solution)/shard_map/conv_mix/pallas_call | solution.py:271
  153.5 4.8 %local_reads.1 = (f32[1024,128]{1,0:T(8,128)}, bf16[1024,128]{1,0:T(8,128)(2,1)}) custom-call(bf16[1024,128]{1,0:T(8,128)(2,1)} %get-tuple-element.20.q_ref, bf16[1024,128]{1,0:T(8,128)(2,1)} %get-tuple-element.21.gk_ref, bf16[1024,128]{1,0:T(8,128)(2,1)} %get-tuple-element.22.gb_ref, bf16[1024,256]{1,0:T(8,128)(2,1)} %get-tuple-element.23.wu_ref, ...), custom_call_target="tpu_custom_call" | custom-call | tf_op jit(solution)/shard_map/local_reads/pallas_call | solution.py:324
  158.3 0.0 all-to-all-done.2.far_ref
  158.3 4.7 %finish_mix.1 = bf16[1024,256]{1,0:T(8,128)(2,1)} custom-call(s32[2]{0:T(128)S(1)} %pad_add_fusion.at_ref, bf16[4,128,128]{2,1,0:T(8,128)(2,1)S(1)} %copy-done.1, bf16[4,128,128]{2,1,0:T(8,128)(2,1)S(1)} %all-to-all-done.2.far_ref, f32[64,128]{1,0:T(8,128)S(1)} %reshape.38.init_ref, f32[1024,128]{1,0:T(8,128)} %get-tuple-element.28.o_ref, ...), custom_call_target="tpu_custom_call" | custom-call | tf_op jit(solution)/shard_map/finish_mix/pallas_call | solution.py:387
  163.0 3.5 %all-to-all-start.3 = ((bf16[4,256,256]{2,1,0:T(8,128)(2,1)}), bf16[4,256,256]{2,1,0:T(8,128)(2,1)S(1)}, u32[]{:S(2)}, u32[]{:S(2)}) async-start(bf16[4,256,256]{2,1,0:T(8,128)(2,1)} %bitcast.48), calls=%async_computation.3 | async-start | bytes 1048576 | tf_op jit(solution)/shard_map/all_to_all | solution.py:558
  166.5 0.1 stack.52.pick_ref
  166.6 0.0 collective-permute-done.5.refs_1_
  166.6 0.0 collective-permute-done.6.refs_2_
  166.6 7.1 %collective-permute-done.7.refs_3_ = bf16[256,2048]{1,0:T(8,128)(2,1)} collective-permute-done((bf16[256,2048]{1,0:T(8,128)(2,1)S(1)}, bf16[256,2048]{1,0:T(8,128)(2,1)}, u32[]{:S(2)}, u32[]{:S(2)}) %collective-permute-start.7) | collective-permute-done | bytes 1048608 | tf_op jit(solution)/shard_map/ppermute | solution.py:457
  173.7 2.9 %all-to-all-done.3.m_ref = bf16[4,256,256]{2,1,0:T(8,128)(2,1)S(1)} async-done(((bf16[4,256,256]{2,1,0:T(8,128)(2,1)}), bf16[4,256,256]{2,1,0:T(8,128)(2,1)S(1)}, u32[]{:S(2)}, u32[]{:S(2)}) %all-to-all-start.3) | async-done | bytes 524320 | tf_op jit(solution)/shard_map/all_to_all | solution.py:558
  176.6 2.8 %outward.1 = (bf16[128,2048]{1,0:T(8,128)(2,1)S(1)}, bf16[128,2048]{1,0:T(8,128)(2,1)S(1)}) custom-call(s32[5]{0:T(128)S(1)} %stack.52.pick_ref, bf16[4,256,256]{2,1,0:T(8,128)(2,1)S(1)} %all-to-all-done.3.m_ref, bf16[256,2048]{1,0:T(8,128)(2,1)S(1)} %bitcast.45, bf16[256,2048]{1,0:T(8,128)(2,1)S(1)} %collective-permute-done.5.refs_1_, ...), custom_call_target="tpu_custom_call" | custom-call | tf_op jit(solution)/shard_map/outward/pallas_call | solution.py:422
  179.4 11.3 %collective-permute-start.8 = (bf16[128,2048]{1,0:T(8,128)(2,1)S(1)}, bf16[128,2048]{1,0:T(8,128)(2,1)S(1)}, u32[]{:S(2)}, u32[]{:S(2)}) collective-permute-start(bf16[128,2048]{1,0:T(8,128)(2,1)S(1)} %get-tuple-element.32), channel_id=1, source_target_pairs={{0,1},{1,0},{2,3},{3,2},{4,5},{5,4},{6,7},{7,6},{8,9},{9,8},{10,11... | collective-permute-start | bytes 1572872 | tf_op jit(solution)/shard_map/ppermute | solution.py:498
  190.7 1.5 collective-permute-done.8
  192.2 0.9 fusion.7
  (14 shorter events, 0.1 us)
Async XLA Ops:
  6.5 24.2 %copy-start.3 = (bf16[1,128,2048]{2,1,0:T(8,128)(2,1)S(1)}, bf16[1,128,2048]{2,1,0:T(8,128)(2,1)}, u32[]{:S(2)}) copy-start(bf16[1,128,2048]{2,1,0:T(8,128)(2,1)} %param.18) | copy-start | bytes 1572868
  6.5 24.2 %copy-start.5 = (f32[2048]{0:T(1024)S(1)}, f32[2048]{0:T(1024)}, u32[]{:S(2)}) copy-start(f32[2048]{0:T(1024)} %param.19) | copy-start | bytes 24580
  6.5 94.4 %all-gather.2.cloned.1.call-start = ((), (), s32[]{:S(2)}) async-start(), calls=%async_computation.6 | async-start | bytes 4456448 | tf_op jit(solution)/shard_map/all_gather | solution.py:516
  19.6 14.9 %collective-permute-start.1 = (bf16[128,2048]{1,0:T(8,128)(2,1)S(1)}, bf16[128,2048]{1,0:T(8,128)(2,1)S(1)}, u32[]{:S(2)}, u32[]{:S(2)}) collective-permute-start(bf16[128,2048]{1,0:T(8,128)(2,1)S(1)} %fusion.4), channel_id=1, source_target_pairs={{0,4},{1,5},{2,6},{3,7},{4,0},{5,1},{6,2},{7,3},{8,12},{9,13},{10,... | collective-permute-start | bytes 1572872 | tf_op jit(solution)/shard_map/ppermute | solution.py:457
  24.2 23.8 %collective-permute-start.2 = (bf16[128,2048]{1,0:T(8,128)(2,1)S(1)}, bf16[128,2048]{1,0:T(8,128)(2,1)S(1)}, u32[]{:S(2)}, u32[]{:S(2)}) collective-permute-start(bf16[128,2048]{1,0:T(8,128)(2,1)S(1)} %fusion.4), channel_id=1, source_target_pairs={{0,2},{1,3},{2,4},{3,5},{4,6},{5,7},{6,0},{7,1},{8,10},{9,11},{10,... | collective-permute-start | bytes 1572872 | tf_op jit(solution)/shard_map/ppermute | solution.py:457
  26.5 21.6 %collective-permute-start = (bf16[128,2048]{1,0:T(8,128)(2,1)S(1)}, bf16[128,2048]{1,0:T(8,128)(2,1)S(1)}, u32[]{:S(2)}, u32[]{:S(2)}) collective-permute-start(bf16[128,2048]{1,0:T(8,128)(2,1)S(1)} %fusion.4), channel_id=1, source_target_pairs={{0,6},{1,7},{2,0},{3,1},{4,2},{5,3},{6,4},{7,5},{8,14},{9,15},{10,... | collective-permute-start | bytes 1572872 | tf_op jit(solution)/shard_map/ppermute | solution.py:457
  49.7 43.9 %collective-permute-start.3 = (bf16[4,128,2048]{2,1,0:T(8,128)(2,1)}, bf16[4,128,2048]{2,1,0:T(8,128)(2,1)}, u32[]{:S(2)}, u32[]{:S(2)}) collective-permute-start(bf16[4,128,2048]{2,1,0:T(8,128)(2,1)} %pad_maximum_fusion.refs_0_.refs_2_.same_ref), channel_id=1, source_target_pairs={{0,1},{1,0},{2,3},{3,2},{4,5},{5,4},{6,7},{7,6},{8,9},{9,8},{10,11... | collective-permute-start | bytes 6291464 | tf_op jit(solution)/shard_map/ppermute | solution.py:498
  52.2 41.2 %copy-start.6 = (f32[3,128]{1,0:T(4,128)S(1)}, f32[3,128]{1,0:T(4,128)}, u32[]{:S(2)}) copy-start(f32[3,128]{1,0:T(4,128)} %param.23) | copy-start | bytes 4612
  52.2 41.2 %copy-start.7 = (f32[128]{0:T(128)S(1)}, f32[128]{0:T(128)}, u32[]{:S(2)}) copy-start(f32[128]{0:T(128)} %param.29) | copy-start | bytes 1540
  52.2 41.2 %copy-start.8 = (f32[128]{0:T(128)S(1)}, f32[128]{0:T(128)}, u32[]{:S(2)}) copy-start(f32[128]{0:T(128)} %param.30) | copy-start | bytes 1540
  52.2 41.2 %copy-start.9 = (f32[128]{0:T(128)S(1)}, f32[128]{0:T(128)}, u32[]{:S(2)}) copy-start(f32[128]{0:T(128)} %param.33) | copy-start | bytes 1540
  52.3 48.7 %copy-start.2 = (f32[1,1024,128]{2,1,0:T(8,128)S(1)}, f32[1,1024,128]{2,1,0:T(8,128)}, u32[]{:S(2)}) copy-start(f32[1,1024,128]{2,1,0:T(8,128)} %param.31) | copy-start | bytes 1572868
  88.5 25.3 %all-to-all-start.5 = ((bf16[4,16,32,256]{3,2,1,0:T(8,128)(2,1)}), bf16[4,16,32,256]{3,2,1,0:T(8,128)(2,1)S(1)}, u32[]{:S(2)}, u32[]{:S(2)}) async-start(bf16[4,16,32,256]{3,2,1,0:T(8,128)(2,1)} %broadcast_in_dim.27), calls=%async_computation.5 | async-start | bytes 2097152 | tf_op jit(solution)/shard_map/all_to_all | solution.py:461
  113.8 14.1 %all-to-all-start.1 = ((bf16[4,128,128]{2,1,0:T(8,128)(2,1)}), bf16[4,128,128]{2,1,0:T(8,128)(2,1)S(1)}, u32[]{:S(2)}, u32[]{:S(2)}) async-start(bf16[4,128,128]{2,1,0:T(8,128)(2,1)} %get-tuple-element.19), calls=%async_computation.1 | async-start | bytes 262144 | tf_op jit(solution)/shard_map/all_to_all | solution.py:461
  117.7 19.5 %copy-start.4 = (f32[1,2,64,64]{3,2,1,0:T(8,128)S(1)}, f32[1,2,64,64]{3,2,1,0:T(8,128)}, u32[]{:S(2)}) copy-start(f32[1,2,64,64]{3,2,1,0:T(8,128)} %param.32) | copy-start | bytes 98308
  118.4 48.2 %collective-permute-start.5 = (bf16[256,2048]{1,0:T(8,128)(2,1)S(1)}, bf16[256,2048]{1,0:T(8,128)(2,1)S(1)}, u32[]{:S(2)}, u32[]{:S(2)}) collective-permute-start(bf16[256,2048]{1,0:T(8,128)(2,1)S(1)} %bitcast.42), channel_id=1, source_target_pairs={{0,6},{1,7},{2,0},{3,1},{4,2},{5,3},{6,4},{7,5},{8,14},{9,15},{10,... | collective-permute-start | bytes 3145736 | tf_op jit(solution)/shard_map/ppermute | solution.py:457
  123.0 43.6 %collective-permute-start.6 = (bf16[256,2048]{1,0:T(8,128)(2,1)S(1)}, bf16[256,2048]{1,0:T(8,128)(2,1)}, u32[]{:S(2)}, u32[]{:S(2)}) collective-permute-start(bf16[256,2048]{1,0:T(8,128)(2,1)S(1)} %bitcast.43), channel_id=1, source_target_pairs={{0,4},{1,5},{2,6},{3,7},{4,0},{5,1},{6,2},{7,3},{8,12},{9,13},{10,... | collective-permute-start | bytes 3145736 | tf_op jit(solution)/shard_map/ppermute | solution.py:457
  125.2 48.5 %collective-permute-start.7 = (bf16[256,2048]{1,0:T(8,128)(2,1)S(1)}, bf16[256,2048]{1,0:T(8,128)(2,1)}, u32[]{:S(2)}, u32[]{:S(2)}) collective-permute-start(bf16[256,2048]{1,0:T(8,128)(2,1)S(1)} %bitcast.44), channel_id=1, source_target_pairs={{0,2},{1,3},{2,4},{3,5},{4,6},{5,7},{6,0},{7,1},{8,10},{9,11},{10,... | collective-permute-start | bytes 3145736 | tf_op jit(solution)/shard_map/ppermute | solution.py:457
  128.0 0.6 copy-start
  130.6 27.7 %all-to-all-start.2 = ((bf16[4,128,128]{2,1,0:T(8,128)(2,1)}), bf16[4,128,128]{2,1,0:T(8,128)(2,1)S(1)}, u32[]{:S(2)}, u32[]{:S(2)}) async-start(bf16[4,128,128]{2,1,0:T(8,128)(2,1)} %group_map.1), calls=%async_computation.2 | async-start | bytes 262144 | tf_op jit(solution)/shard_map/all_to_all | solution.py:461
  139.4 7.2 %collective-permute-start.4 = (bf16[16,2048]{1,0:T(8,128)(2,1)S(1)}, bf16[16,2048]{1,0:T(8,128)(2,1)S(1)}, u32[]{:S(2)}, u32[]{:S(2)}) collective-permute-start(bf16[16,2048]{1,0:T(8,128)(2,1)S(1)} %fusion.8), channel_id=1, source_target_pairs={{0,32},{32,64},{64,96},{96,128},{128,160},{160,192},{192,224},{224... | collective-permute-start | bytes 196616 | tf_op jit(solution)/shard_map/ppermute | solution.py:452
  153.5 4.8 %copy-start.1 = (bf16[4,128,128]{2,1,0:T(8,128)(2,1)S(1)}, bf16[4,128,128]{2,1,0:T(8,128)(2,1)}, u32[]{:S(2)}) copy-start(bf16[4,128,128]{2,1,0:T(8,128)(2,1)} %copy-done) | copy-start | bytes 393220
  163.0 13.5 %all-to-all-start.3 = ((bf16[4,256,256]{2,1,0:T(8,128)(2,1)}), bf16[4,256,256]{2,1,0:T(8,128)(2,1)S(1)}, u32[]{:S(2)}, u32[]{:S(2)}) async-start(bf16[4,256,256]{2,1,0:T(8,128)(2,1)} %bitcast.48), calls=%async_computation.3 | async-start | bytes 1048576 | tf_op jit(solution)/shard_map/all_to_all | solution.py:558
  179.4 12.9 %collective-permute-start.8 = (bf16[128,2048]{1,0:T(8,128)(2,1)S(1)}, bf16[128,2048]{1,0:T(8,128)(2,1)S(1)}, u32[]{:S(2)}, u32[]{:S(2)}) collective-permute-start(bf16[128,2048]{1,0:T(8,128)(2,1)S(1)} %get-tuple-element.32), channel_id=1, source_target_pairs={{0,1},{1,0},{2,3},{3,2},{4,5},{5,4},{6,7},{7,6},{8,9},{9,8},{10,11... | collective-permute-start | bytes 1572872 | tf_op jit(solution)/shard_map/ppermute | solution.py:498
Sparse Core Ops, SparseCore 0:
  17.2 83.6 all-gather.1

commit v7 on v6

--- a/solution.py
+++ b/solution.py
@@ -288,7 +288,7 @@
 
 def reads_kernel(q_ref, gk_ref, gb_ref, wu_ref, v_ref, pos_ref, full_ref, states_ref, o_ref, y_ref):
     width = 2 * HEAD_WIDTH
-    each = range(BLOCK // CHUNK)
+    each = range(MAPS_BLOCK // CHUNK)
     t, s, _ = chunk_masks()
     inclusive = t >= s
     fold = functools.partial(spread, first=first_lanes())
@@ -318,12 +318,12 @@
 
 def reads_call(q, gk, gb, wu, v, pos, full, states):
     rows, width = q.shape
-    tile = pl.BlockSpec((BLOCK, width), lambda i: (i, 0))
-    wide = pl.BlockSpec((BLOCK, 2 * width), lambda i: (i, 0))
-    starts = pl.BlockSpec((BLOCK // CHUNK, width, width), lambda i: (i, 0, 0))
+    tile = pl.BlockSpec((MAPS_BLOCK, width), lambda i: (i, 0))
+    wide = pl.BlockSpec((MAPS_BLOCK, 2 * width), lambda i: (i, 0))
+    starts = pl.BlockSpec((MAPS_BLOCK // CHUNK, width, width), lambda i: (i, 0, 0))
     return pl.pallas_call(
         reads_kernel,
-        grid=(rows // BLOCK,),
+        grid=(rows // MAPS_BLOCK,),
         in_specs=[tile, tile, tile, wide, tile, tile, tile, starts],
         out_specs=[tile, tile],
         out_shape=[array((rows, width), f32), array((rows, width), bf16)],
@@ -341,37 +341,56 @@
     return got[: state.shape[0]] + got[state.shape[0] :]
 
 
-def group_kernel(pieces_ref, out_ref):
+def group_kernel(at_ref, pieces_ref, out_ref, before_ref):
     first = first_lanes()
-    total = pieces_ref[0].astype(f32)
-    for k in range(1, pieces_ref.shape[0]):
+
+    def join(total, k):
         piece = pieces_ref[k]
         total = moved(total, piece, first)
-        total = jnp.concatenate(
-            [total[:HEAD_WIDTH] + piece[:HEAD_WIDTH].astype(f32), total[HEAD_WIDTH:]], axis=0
-        )
+        source = total[:HEAD_WIDTH] + piece[:HEAD_WIDTH].astype(f32)
+        return jnp.concatenate([source, total[HEAD_WIDTH:]], axis=0)
+
+    total = pieces_ref[0].astype(f32)
+    r, l = rows_of(total.shape), lanes_of(total.shape) % HEAD_WIDTH
+    before = jnp.where(r - HEAD_WIDTH == l, 1.0, 0.0)
+    for k in range(1, pieces_ref.shape[0]):
+        before = jnp.where(at_ref[1] == k, total, before)
+        total = join(total, k)
+    before_ref[...] = before
     for k in range(out_ref.shape[0]):
         out_ref[k] = total.astype(bf16)
 
 
-def finish_kernel(at_ref, near_ref, far_ref, init_ref, o_ref, y_ref, conv_ref, vec_ref, out_ref, s_ref):
+def group_call(at, pieces, copies):
+    here = pl.BlockSpec(memory_space=pltpu.VMEM)
+    return pl.pallas_call(
+        group_kernel,
+        in_specs=[pl.BlockSpec(memory_space=pltpu.SMEM), here],
+        out_specs=[here, here],
+        out_shape=[
+            jax.ShapeDtypeStruct((copies, *pieces.shape[1:]), bf16),
+            jax.ShapeDtypeStruct(pieces.shape[1:], f32),
+        ],
+        name="group_map",
+    )(at, pieces)
+
+
+def finish_kernel(at_ref, before_ref, far_ref, init_ref, o_ref, y_ref, conv_ref, vec_ref, out_ref, s_ref):
     width = 2 * HEAD_WIDTH
     first = first_lanes()
 
     @pl.when(pl.program_id(0) == 0)
     def _():
-        def through(ref):
-            def advance(i, state):
-                piece = ref[i]
-                return moved(state, piece, first) + piece[:HEAD_WIDTH].astype(f32)
-
-            return advance
-
-        state = lax.fori_loop(0, at_ref[0], through(far_ref), init_ref[...])
-        state = lax.fori_loop(0, at_ref[1], through(near_ref), state)
+        def advance(i, state):
+            piece = far_ref[i]
+            return moved(state, piece, first) + piece[:HEAD_WIDTH].astype(f32)
+
+        state = lax.fori_loop(0, at_ref[0], advance, init_ref[...])
+        before = before_ref[...]
+        state = moved(state, before, first) + before[:HEAD_WIDTH]
         s_ref[...] = spread(state, first)
 
-    low = lanes_of((BLOCK, width)) < HEAD_WIDTH
+    low = lanes_of((MAPS_BLOCK, width)) < HEAD_WIDTH
     reads = o_ref[...] + dot(y_ref[...], s_ref[...], 1, 1)
     centered = reads - head_sums(reads, low) * (1.0 / HEAD_WIDTH)
     variance = head_sums(centered * centered, low) * (1.0 / HEAD_WIDTH)
@@ -380,17 +399,17 @@
     out_ref[:, width:] = mixed.astype(bf16)
 
 
-def finish_call(at, near, far, init, o, y, conv, vec):
+def finish_call(at, before, far, init, o, y, conv, vec):
     rows, width = o.shape
     whole = lambda a: pl.BlockSpec(a.shape, lambda i, p: (0,) * a.ndim)
-    tile = pl.BlockSpec((BLOCK, width), lambda i, p: (i, 0))
+    tile = pl.BlockSpec((MAPS_BLOCK, width), lambda i, p: (i, 0))
     return pl.pallas_call(
         finish_kernel,
         grid_spec=pltpu.PrefetchScalarGridSpec(
             num_scalar_prefetch=1,
-            grid=(rows // BLOCK,),
-            in_specs=[whole(near), whole(far), whole(init), tile, tile, tile, whole(vec)],
-            out_specs=pl.BlockSpec((BLOCK, 2 * width), lambda i, p: (i, 0)),
+            grid=(rows // MAPS_BLOCK,),
+            in_specs=[whole(before), whole(far), whole(init), tile, tile, tile, whole(vec)],
+            out_specs=pl.BlockSpec((MAPS_BLOCK, 2 * width), lambda i, p: (i, 0)),
             scratch_shapes=[pltpu.VMEM((width, width), bf16)],
         ),
         out_shape=array((rows, 2 * width), bf16),
@@ -398,7 +417,7 @@
             dimension_semantics=("arbitrary",), vmem_limit_bytes=12 * 2**20
         ),
         name="finish_mix",
-    )(at, near, far, init, *in_hbm(o, y, conv), vec)
+    )(at, before, far, init, *in_hbm(o, y, conv), vec)
 
 
 def outward_kernel(pick_ref, m_ref, *refs):
@@ -542,18 +561,14 @@
     far_blocks = [list(range(k, blocks, few)) for k in range(few)]
     *kept, agg = maps_call(place, same, other, weights, decay_spike[0], vec, few)
     near_maps = from_everyone(agg, "sp", near_blocks)
+    block = lax.axis_index("sp").astype(jnp.int32)
+    at = jnp.stack([lax.shift_right_logical(block, 2), block & (few - 1)])
+    total, earlier = group_call(at, near_maps, blocks // few)
+    far_maps = from_everyone(total, "sp", far_blocks)
     q, conv = conv_call(place, same, other, weights, halo, vec)
-    total = pl.pallas_call(
-        group_kernel,
-        out_shape=array((blocks // few, *agg.shape[1:]), bf16),
-        name="group_map",
-    )(near_maps)
-    far_maps = from_everyone(total, "sp", far_blocks)
     o, y = reads_call(q, *kept)
     init = jnp.moveaxis(initial_state[0], 0, 1).reshape(HEAD_WIDTH, heads * HEAD_WIDTH)
-    block = lax.axis_index("sp").astype(jnp.int32)
-    at = jnp.stack([lax.shift_right_logical(block, 2), block & (few - 1)])
-    mixed = finish_call(at, near_maps, far_maps, init, o, y, conv, vec)
+    mixed = finish_call(at, earlier, far_maps, init, o, y, conv, vec)
     groups = [list(range(side, devices, 2)) for side in range(2)]
     gathered = lax.all_to_all(
         mixed.reshape(chips, -1, 2 * channels), "tp", 0, 0, tiled=True, axis_index_groups=groups

time: 201 us -> 199 us (0.990)
  the two profiles are of different devices: /device:TPU:41 before, /device:TPU:1 now
where the time goes in v7:
time: 199 us; the launch traced here: 198 us
  starting transfers between devices  54.1 us (27%)
  blocking collectives  44.7 us (22%)
  waiting for transfers between devices  40.2 us (20%)
  Pallas kernels  34.9 us (18%)
  between operations  13.7 us (7%)
  other arithmetic  5.94 us (3%)
  local copies, waits for them, and re-layouts  4.8 us (2%)
    all_to_all x2, blocking collectives, from_everyone(): lax.all_to_all(copies, axis, 0, 0, tiled=True, axis_index_groups=groups)  44.7 us
    ppermute x6, waiting for transfers between devices, turned(): lax.ppermute(x, 'tp', [(i, (i + distance) % devices) for i in range(devic...  26.7 us
    ppermute x6, starting transfers between devices, turned(): lax.ppermute(x, 'tp', [(i, (i + distance) % devices) for i in range(devic...  20.6 us
    all_to_all x3, starting transfers between devices, from_everyone(): lax.all_to_all(copies, axis, 0, 0, tiled=True, axis_index_groups=groups)  13.7 us
    ppermute x2, starting transfers between devices, core_swap(): return lax.ppermute(x, 'tp', [(i, i ^ 1) for i in range(devices)])  13 us
    pallas_call x1, Pallas kernels, maps_call(): pl.pallas_call(maps_kernel, grid_spec=pltpu.PrefetchScalarGridSpec(num_sc...  12.9 us
    all_gather x1, waiting for transfers between devices, mixing(): weights = lax.all_gather(weights, 'sp', axis=0, tiled=True)  8.03 us
    pallas_call x1, Pallas kernels, conv_call(): pl.pallas_call(conv_kernel, grid_spec=pltpu.PrefetchScalarGridSpec(num_sc...  6.94 us
  transfers between devices with their start and end apart: 14, of which 8 were waited for; matrix products, arithmetic and copies ran while one was open for 5% of the time, Pallas kernels for 15%

profile of v7, /device:TPU:1, one launch (start us, length us, event | category | flops | bytes accessed | tf_op | source)
XLA Modules:
  0.0 198.3 jit_solution(620423629813853934)
XLA Ops:
  6.5 1.6 pack_shards.2
  8.2 10.6 %all_to_all.30 = bf16[4,32,1024]{2,1,0:T(8,128)(2,1)} all-to-all(bf16[4,32,1024]{2,1,0:T(8,128)(2,1)} %pack_shards.2), channel_id=1, replica_groups=mesh['sp'=16,'fs'=4,'tp'=8] {'fs'}, dimensions={0} | all-to-all | bytes 524288 | tf_op jit(solution)/shard_map/all_to_all | solution.py:480
  18.8 0.0 all-gather.2.cloned.1.call-update
  18.8 1.2 fusion.2
  20.1 1.2 fusion.4
  21.3 4.7 %collective-permute-start.1 = (bf16[128,2048]{1,0:T(8,128)(2,1)S(1)}, bf16[128,2048]{1,0:T(8,128)(2,1)S(1)}, u32[]{:S(2)}, u32[]{:S(2)}) collective-permute-start(bf16[128,2048]{1,0:T(8,128)(2,1)S(1)} %fusion.4), channel_id=1, source_target_pairs={{0,4},{1,5},{2,6},{3,7},{4,0},{5,1},{6,2},{7,3},{8,12},{9,13},{10,... | collective-permute-start | bytes 1572872 | tf_op jit(solution)/shard_map/ppermute | solution.py:476
  26.0 2.2 %collective-permute-start.2 = (bf16[128,2048]{1,0:T(8,128)(2,1)S(1)}, bf16[128,2048]{1,0:T(8,128)(2,1)S(1)}, u32[]{:S(2)}, u32[]{:S(2)}) collective-permute-start(bf16[128,2048]{1,0:T(8,128)(2,1)S(1)} %fusion.4), channel_id=1, source_target_pairs={{0,2},{1,3},{2,4},{3,5},{4,6},{5,7},{6,0},{7,1},{8,10},{9,11},{10,... | collective-permute-start | bytes 1572872 | tf_op jit(solution)/shard_map/ppermute | solution.py:476
  28.2 4.3 %collective-permute-start = (bf16[128,2048]{1,0:T(8,128)(2,1)S(1)}, bf16[128,2048]{1,0:T(8,128)(2,1)S(1)}, u32[]{:S(2)}, u32[]{:S(2)}) collective-permute-start(bf16[128,2048]{1,0:T(8,128)(2,1)S(1)} %fusion.4), channel_id=1, source_target_pairs={{0,6},{1,7},{2,0},{3,1},{4,2},{5,3},{6,4},{7,5},{8,14},{9,15},{10,... | collective-permute-start | bytes 1572872 | tf_op jit(solution)/shard_map/ppermute | solution.py:476
  32.5 0.0 copy-done.3
  32.5 0.0 copy-done.6
  32.5 0.2 fusion.6
  32.7 0.7 collective-permute-done.1
  33.4 13.8 %collective-permute-done.2 = bf16[128,2048]{1,0:T(8,128)(2,1)S(1)} collective-permute-done((bf16[128,2048]{1,0:T(8,128)(2,1)S(1)}, bf16[128,2048]{1,0:T(8,128)(2,1)S(1)}, u32[]{:S(2)}, u32[]{:S(2)}) %collective-permute-start.2) | collective-permute-done | bytes 524320 | tf_op jit(solution)/shard_map/ppermute | solution.py:476
  47.2 0.4 collective-permute-done
  47.6 1.6 pad_maximum_fusion.refs_0_.refs_2_.same_ref
  49.2 4.7 %collective-permute-start.3 = (bf16[4,128,2048]{2,1,0:T(8,128)(2,1)}, bf16[4,128,2048]{2,1,0:T(8,128)(2,1)}, u32[]{:S(2)}, u32[]{:S(2)}) collective-permute-start(bf16[4,128,2048]{2,1,0:T(8,128)(2,1)} %pad_maximum_fusion.refs_0_.refs_2_.same_ref), channel_id=1, source_target_pairs={{0,1},{1,0},{2,3},{3,2},{4,5},{5,4},{6,7},{7,6},{8,9},{9,8},{10,11... | collective-permute-start | bytes 6291464 | tf_op jit(solution)/shard_map/ppermute | solution.py:517
  54.0 0.0 copy-start.7
  54.0 0.0 copy-start.8
  54.0 0.0 copy-start.9
  54.0 0.0 copy-start.10
  54.0 0.0 copy-start
  54.0 1.5 pack_shards.3
  55.5 34.1 %all_to_all.31 = bf16[16,32,256]{2,1,0:T(8,128)(2,1)S(1)} all-to-all(bf16[16,32,256]{2,1,0:T(8,128)(2,1)} %pack_shards.3), channel_id=1, replica_groups=mesh['sp'=16,'fs'=4,'tp'=8] {'sp'}, dimensions={0} | all-to-all | bytes 524288 | tf_op jit(solution)/shard_map/all_to_all | solution.py:480
  89.6 1.2 broadcast_in_dim.27
  90.8 3.5 %all-to-all-start.5 = ((bf16[4,16,32,256]{3,2,1,0:T(8,128)(2,1)}), bf16[4,16,32,256]{3,2,1,0:T(8,128)(2,1)S(1)}, u32[]{:S(2)}, u32[]{:S(2)}) async-start(bf16[4,16,32,256]{3,2,1,0:T(8,128)(2,1)} %broadcast_in_dim.27), calls=%async_computation.5 | async-start | bytes 2097152 | tf_op jit(solution)/shard_map/all_to_all | solution.py:480
  94.4 0.1 pad_add_fusion.1.place_ref
  94.5 0.0 collective-permute-done.3.refs_1_.refs_3_.other_ref
  94.5 8.0 %all-gather.2.cloned.1.call-done.refs_4_.w_ref = bf16[2048,1024]{1,0:T(8,128)(2,1)} async-done(((bf16[128,1024]{1,0:T(8,128)(2,1)}), bf16[2048,1024]{1,0:T(8,128)(2,1)}) %all-gather.2.cloned.1.call-update) | async-done | bytes 4194320 | tf_op jit(solution)/shard_map/all_gather | solution.py:535
  102.5 12.9 %state_maps.1 = (bf16[1024,128]{1,0:T(8,128)(2,1)}, bf16[1024,128]{1,0:T(8,128)(2,1)}, bf16[1024,256]{1,0:T(8,128)(2,1)}, bf16[1024,128]{1,0:T(8,128)(2,1)}, f32...) custom-call(s32[2]{0:T(128)S(1)} %pad_add_fusion.1.place_ref, ...), custom_call_target="tpu_custom_call" | custom-call | tf_op jit(solution)/shard_map/state_maps/pallas_call | solution.py:198
  115.4 0.0 all-to-all-done.5
  115.4 3.9 %all-to-all-start.1 = ((bf16[4,128,128]{2,1,0:T(8,128)(2,1)}), bf16[4,128,128]{2,1,0:T(8,128)(2,1)S(1)}, u32[]{:S(2)}, u32[]{:S(2)}) async-start(bf16[4,128,128]{2,1,0:T(8,128)(2,1)} %get-tuple-element.21), calls=%async_computation.1 | async-start | bytes 262144 | tf_op jit(solution)/shard_map/all_to_all | solution.py:480
  119.3 0.1 copy.24
  119.4 0.0 copy-start.5
  119.4 0.6 copy.25
  120.0 4.3 %collective-permute-start.5 = (bf16[256,2048]{1,0:T(8,128)(2,1)S(1)}, bf16[256,2048]{1,0:T(8,128)(2,1)S(1)}, u32[]{:S(2)}, u32[]{:S(2)}) collective-permute-start(bf16[256,2048]{1,0:T(8,128)(2,1)S(1)} %bitcast.42), channel_id=1, source_target_pairs={{0,6},{1,7},{2,0},{3,1},{4,2},{5,3},{6,4},{7,5},{8,14},{9,15},{10,... | collective-permute-start | bytes 3145736 | tf_op jit(solution)/shard_map/ppermute | solution.py:476
  124.4 2.5 %collective-permute-start.6 = (bf16[256,2048]{1,0:T(8,128)(2,1)S(1)}, bf16[256,2048]{1,0:T(8,128)(2,1)}, u32[]{:S(2)}, u32[]{:S(2)}) collective-permute-start(bf16[256,2048]{1,0:T(8,128)(2,1)S(1)} %bitcast.43), channel_id=1, source_target_pairs={{0,4},{1,5},{2,6},{3,7},{4,0},{5,1},{6,2},{7,3},{8,12},{9,13},{10,... | collective-permute-start | bytes 3145736 | tf_op jit(solution)/shard_map/ppermute | solution.py:476
  126.9 2.5 %collective-permute-start.7 = (bf16[256,2048]{1,0:T(8,128)(2,1)S(1)}, bf16[256,2048]{1,0:T(8,128)(2,1)}, u32[]{:S(2)}, u32[]{:S(2)}) collective-permute-start(bf16[256,2048]{1,0:T(8,128)(2,1)S(1)} %bitcast.44), channel_id=1, source_target_pairs={{0,2},{1,3},{2,4},{3,5},{4,6},{5,7},{6,0},{7,1},{8,10},{9,11},{10,... | collective-permute-start | bytes 3145736 | tf_op jit(solution)/shard_map/ppermute | solution.py:476
  129.4 0.6 pad_add_fusion.at_ref
  130.0 0.0 all-to-all-done.1.pieces_ref
  130.1 0.7 copy-done.4
  130.7 2.0 %group_map.1 = (bf16[4,128,128]{2,1,0:T(8,128)(2,1)}, f32[128,128]{1,0:T(8,128)}) custom-call(s32[2]{0:T(128)} %pad_add_fusion.at_ref, bf16[4,128,128]{2,1,0:T(8,128)(2,1)} %copy-done.4), custom_call_target="tpu_custom_call" | custom-call | tf_op jit(solution)/shard_map/group_map/pallas_call | solution.py:366
  132.7 6.3 %all-to-all-start.2 = ((bf16[4,128,128]{2,1,0:T(8,128)(2,1)}), bf16[4,128,128]{2,1,0:T(8,128)(2,1)S(1)}, u32[]{:S(2)}, u32[]{:S(2)}) async-start(bf16[4,128,128]{2,1,0:T(8,128)(2,1)} %get-tuple-element.23), calls=%async_computation.2 | async-start | bytes 262144 | tf_op jit(solution)/shard_map/all_to_all | solution.py:480
  139.0 1.0 slice.9
  140.0 1.0 slice.8
  141.0 3.3 %collective-permute-start.4 = (bf16[16,2048]{1,0:T(8,128)(2,1)S(1)}, bf16[16,2048]{1,0:T(8,128)(2,1)S(1)}, u32[]{:S(2)}, u32[]{:S(2)}) collective-permute-start(bf16[16,2048]{1,0:T(8,128)(2,1)S(1)} %fusion.8), channel_id=1, source_target_pairs={{0,32},{32,64},{64,96},{96,128},{128,160},{160,192},{192,224},{224... | collective-permute-start | bytes 196616 | tf_op jit(solution)/shard_map/ppermute | solution.py:471
  144.4 0.1 copy.23
  144.4 0.1 reshape.38.init_ref
  144.5 2.8 %collective-permute-done.4.halo_ref = bf16[16,2048]{1,0:T(8,128)(2,1)S(1)} collective-permute-done((bf16[16,2048]{1,0:T(8,128)(2,1)S(1)}, bf16[16,2048]{1,0:T(8,128)(2,1)S(1)}, u32[]{:S(2)}, u32[]{:S(2)}) %collective-permute-start.4) | collective-permute-done | bytes 65568 | tf_op jit(solution)/shard_map/ppermute | solution.py:471
  147.3 6.9 %conv_mix.1 = (bf16[1024,128]{1,0:T(8,128)(2,1)}, bf16[1024,128]{1,0:T(8,128)(2,1)}) custom-call(s32[2]{0:T(128)S(1)} %pad_add_fusion.1.place_ref, bf16[4,128,2048]{2,1,0:T(8,128)(2,1)} %pad_maximum_fusion.refs_0_.refs_2_.same_ref, bf16[4,128,2048]{2,1,0:T(8,128)(2,1)} %collective-permute-done.3.refs_1_.refs_3_.other_ref, ...), custom_call_target="tpu_custom_call" | custom-call | tf_op jit(solution)/shard_map/conv_mix/pallas_call | solution.py:271
  154.2 3.6 %local_reads.1 = (f32[1024,128]{1,0:T(8,128)}, bf16[1024,128]{1,0:T(8,128)(2,1)}) custom-call(bf16[1024,128]{1,0:T(8,128)(2,1)} %get-tuple-element.24.q_ref, bf16[1024,128]{1,0:T(8,128)(2,1)} %get-tuple-element.25.gk_ref, bf16[1024,128]{1,0:T(8,128)(2,1)} %get-tuple-element.26.gb_ref, bf16[1024,256]{1,0:T(8,128)(2,1)} %get-tuple-element.27.wu_ref, ...), custom_call_target="tpu_custom_call" | custom-call | tf_op jit(solution)/shard_map/local_reads/pallas_call | solution.py:324
  157.9 0.0 all-to-all-done.2.far_ref
  157.9 0.0 copy-done.1
  157.9 0.0 copy-done.2
  157.9 3.5 %finish_mix.1 = bf16[1024,256]{1,0:T(8,128)(2,1)} custom-call(s32[2]{0:T(128)S(1)} %copy-done.2, f32[128,128]{1,0:T(8,128)S(1)} %copy-done.1, bf16[4,128,128]{2,1,0:T(8,128)(2,1)S(1)} %all-to-all-done.2.far_ref, f32[64,128]{1,0:T(8,128)S(1)} %reshape.38.init_ref, f32[1024,128]{1,0:T(8,128)} %get-tuple-element.32.o_ref, ...), custom_call_target="tpu_custom_call" | custom-call | tf_op jit(solution)/shard_map/finish_mix/pallas_call | solution.py:406
  161.4 3.5 %all-to-all-start.3 = ((bf16[4,256,256]{2,1,0:T(8,128)(2,1)}), bf16[4,256,256]{2,1,0:T(8,128)(2,1)S(1)}, u32[]{:S(2)}, u32[]{:S(2)}) async-start(bf16[4,256,256]{2,1,0:T(8,128)(2,1)} %bitcast.48), calls=%async_computation.3 | async-start | bytes 1048576 | tf_op jit(solution)/shard_map/all_to_all | solution.py:573
  164.9 0.1 stack.52.pick_ref
  165.0 0.0 collective-permute-done.5.refs_1_
  165.0 0.0 collective-permute-done.6.refs_2_
  165.0 11.8 %collective-permute-done.7.refs_3_ = bf16[256,2048]{1,0:T(8,128)(2,1)} collective-permute-done((bf16[256,2048]{1,0:T(8,128)(2,1)S(1)}, bf16[256,2048]{1,0:T(8,128)(2,1)}, u32[]{:S(2)}, u32[]{:S(2)}) %collective-permute-start.7) | collective-permute-done | bytes 1048608 | tf_op jit(solution)/shard_map/ppermute | solution.py:476
  176.8 1.1 all-to-all-done.3.m_ref
  177.9 2.8 %outward.1 = (bf16[128,2048]{1,0:T(8,128)(2,1)S(1)}, bf16[128,2048]{1,0:T(8,128)(2,1)S(1)}) custom-call(s32[5]{0:T(128)S(1)} %stack.52.pick_ref, bf16[4,256,256]{2,1,0:T(8,128)(2,1)S(1)} %all-to-all-done.3.m_ref, bf16[256,2048]{1,0:T(8,128)(2,1)S(1)} %bitcast.45, bf16[256,2048]{1,0:T(8,128)(2,1)S(1)} %collective-permute-done.5.refs_1_, ...), custom_call_target="tpu_custom_call" | custom-call | tf_op jit(solution)/shard_map/outward/pallas_call | solution.py:441
  180.7 8.2 %collective-permute-start.8 = (bf16[128,2048]{1,0:T(8,128)(2,1)S(1)}, bf16[128,2048]{1,0:T(8,128)(2,1)S(1)}, u32[]{:S(2)}, u32[]{:S(2)}) collective-permute-start(bf16[128,2048]{1,0:T(8,128)(2,1)S(1)} %get-tuple-element.36), channel_id=1, source_target_pairs={{0,1},{1,0},{2,3},{3,2},{4,5},{5,4},{6,7},{7,6},{8,9},{9,8},{10,11... | collective-permute-start | bytes 1572872 | tf_op jit(solution)/shard_map/ppermute | solution.py:517
  189.0 1.5 collective-permute-done.8
  190.5 0.9 fusion.7
  (16 shorter events, 0.1 us)
Async XLA Ops:
  6.5 26.0 %copy-start.3 = (bf16[1,128,2048]{2,1,0:T(8,128)(2,1)S(1)}, bf16[1,128,2048]{2,1,0:T(8,128)(2,1)}, u32[]{:S(2)}) copy-start(bf16[1,128,2048]{2,1,0:T(8,128)(2,1)} %param.18) | copy-start | bytes 1572868
  6.5 26.0 %copy-start.6 = (f32[2048]{0:T(1024)S(1)}, f32[2048]{0:T(1024)}, u32[]{:S(2)}) copy-start(f32[2048]{0:T(1024)} %param.19) | copy-start | bytes 24580
  6.5 96.0 %all-gather.2.cloned.1.call-start = ((), (), s32[]{:S(2)}) async-start(), calls=%async_computation.6 | async-start | bytes 4456448 | tf_op jit(solution)/shard_map/all_gather | solution.py:535
  21.3 12.1 %collective-permute-start.1 = (bf16[128,2048]{1,0:T(8,128)(2,1)S(1)}, bf16[128,2048]{1,0:T(8,128)(2,1)S(1)}, u32[]{:S(2)}, u32[]{:S(2)}) collective-permute-start(bf16[128,2048]{1,0:T(8,128)(2,1)S(1)} %fusion.4), channel_id=1, source_target_pairs={{0,4},{1,5},{2,6},{3,7},{4,0},{5,1},{6,2},{7,3},{8,12},{9,13},{10,... | collective-permute-start | bytes 1572872 | tf_op jit(solution)/shard_map/ppermute | solution.py:476
  26.0 21.2 %collective-permute-start.2 = (bf16[128,2048]{1,0:T(8,128)(2,1)S(1)}, bf16[128,2048]{1,0:T(8,128)(2,1)S(1)}, u32[]{:S(2)}, u32[]{:S(2)}) collective-permute-start(bf16[128,2048]{1,0:T(8,128)(2,1)S(1)} %fusion.4), channel_id=1, source_target_pairs={{0,2},{1,3},{2,4},{3,5},{4,6},{5,7},{6,0},{7,1},{8,10},{9,11},{10,... | collective-permute-start | bytes 1572872 | tf_op jit(solution)/shard_map/ppermute | solution.py:476
  28.2 19.4 %collective-permute-start = (bf16[128,2048]{1,0:T(8,128)(2,1)S(1)}, bf16[128,2048]{1,0:T(8,128)(2,1)S(1)}, u32[]{:S(2)}, u32[]{:S(2)}) collective-permute-start(bf16[128,2048]{1,0:T(8,128)(2,1)S(1)} %fusion.4), channel_id=1, source_target_pairs={{0,6},{1,7},{2,0},{3,1},{4,2},{5,3},{6,4},{7,5},{8,14},{9,15},{10,... | collective-permute-start | bytes 1572872 | tf_op jit(solution)/shard_map/ppermute | solution.py:476
  49.2 45.2 %collective-permute-start.3 = (bf16[4,128,2048]{2,1,0:T(8,128)(2,1)}, bf16[4,128,2048]{2,1,0:T(8,128)(2,1)}, u32[]{:S(2)}, u32[]{:S(2)}) collective-permute-start(bf16[4,128,2048]{2,1,0:T(8,128)(2,1)} %pad_maximum_fusion.refs_0_.refs_2_.same_ref), channel_id=1, source_target_pairs={{0,1},{1,0},{2,3},{3,2},{4,5},{5,4},{6,7},{7,6},{8,9},{9,8},{10,11... | collective-permute-start | bytes 6291464 | tf_op jit(solution)/shard_map/ppermute | solution.py:517
  54.0 40.4 %copy-start.7 = (f32[3,128]{1,0:T(4,128)S(1)}, f32[3,128]{1,0:T(4,128)}, u32[]{:S(2)}) copy-start(f32[3,128]{1,0:T(4,128)} %param.23) | copy-start | bytes 4612
  54.0 40.4 %copy-start.8 = (f32[128]{0:T(128)S(1)}, f32[128]{0:T(128)}, u32[]{:S(2)}) copy-start(f32[128]{0:T(128)} %param.29) | copy-start | bytes 1540
  54.0 40.4 %copy-start.9 = (f32[128]{0:T(128)S(1)}, f32[128]{0:T(128)}, u32[]{:S(2)}) copy-start(f32[128]{0:T(128)} %param.30) | copy-start | bytes 1540
  54.0 40.4 %copy-start.10 = (f32[128]{0:T(128)S(1)}, f32[128]{0:T(128)}, u32[]{:S(2)}) copy-start(f32[128]{0:T(128)} %param.33) | copy-start | bytes 1540
  54.0 48.5 %copy-start = (f32[1,1024,128]{2,1,0:T(8,128)S(1)}, f32[1,1024,128]{2,1,0:T(8,128)}, u32[]{:S(2)}) copy-start(f32[1,1024,128]{2,1,0:T(8,128)} %param.31) | copy-start | bytes 1572868
  90.8 24.6 %all-to-all-start.5 = ((bf16[4,16,32,256]{3,2,1,0:T(8,128)(2,1)}), bf16[4,16,32,256]{3,2,1,0:T(8,128)(2,1)S(1)}, u32[]{:S(2)}, u32[]{:S(2)}) async-start(bf16[4,16,32,256]{3,2,1,0:T(8,128)(2,1)} %broadcast_in_dim.27), calls=%async_computation.5 | async-start | bytes 2097152 | tf_op jit(solution)/shard_map/all_to_all | solution.py:480
  115.4 14.6 %all-to-all-start.1 = ((bf16[4,128,128]{2,1,0:T(8,128)(2,1)}), bf16[4,128,128]{2,1,0:T(8,128)(2,1)S(1)}, u32[]{:S(2)}, u32[]{:S(2)}) async-start(bf16[4,128,128]{2,1,0:T(8,128)(2,1)} %get-tuple-element.21), calls=%async_computation.1 | async-start | bytes 262144 | tf_op jit(solution)/shard_map/all_to_all | solution.py:480
  119.4 25.0 %copy-start.5 = (f32[1,2,64,64]{3,2,1,0:T(8,128)S(1)}, f32[1,2,64,64]{3,2,1,0:T(8,128)}, u32[]{:S(2)}) copy-start(f32[1,2,64,64]{3,2,1,0:T(8,128)} %param.32) | copy-start | bytes 98308
  120.0 45.0 %collective-permute-start.5 = (bf16[256,2048]{1,0:T(8,128)(2,1)S(1)}, bf16[256,2048]{1,0:T(8,128)(2,1)S(1)}, u32[]{:S(2)}, u32[]{:S(2)}) collective-permute-start(bf16[256,2048]{1,0:T(8,128)(2,1)S(1)} %bitcast.42), channel_id=1, source_target_pairs={{0,6},{1,7},{2,0},{3,1},{4,2},{5,3},{6,4},{7,5},{8,14},{9,15},{10,... | collective-permute-start | bytes 3145736 | tf_op jit(solution)/shard_map/ppermute | solution.py:476
  124.4 40.6 %collective-permute-start.6 = (bf16[256,2048]{1,0:T(8,128)(2,1)S(1)}, bf16[256,2048]{1,0:T(8,128)(2,1)}, u32[]{:S(2)}, u32[]{:S(2)}) collective-permute-start(bf16[256,2048]{1,0:T(8,128)(2,1)S(1)} %bitcast.43), channel_id=1, source_target_pairs={{0,4},{1,5},{2,6},{3,7},{4,0},{5,1},{6,2},{7,3},{8,12},{9,13},{10,... | collective-permute-start | bytes 3145736 | tf_op jit(solution)/shard_map/ppermute | solution.py:476
  126.9 49.9 %collective-permute-start.7 = (bf16[256,2048]{1,0:T(8,128)(2,1)S(1)}, bf16[256,2048]{1,0:T(8,128)(2,1)}, u32[]{:S(2)}, u32[]{:S(2)}) collective-permute-start(bf16[256,2048]{1,0:T(8,128)(2,1)S(1)} %bitcast.44), channel_id=1, source_target_pairs={{0,2},{1,3},{2,4},{3,5},{4,6},{5,7},{6,0},{7,1},{8,10},{9,11},{10,... | collective-permute-start | bytes 3145736 | tf_op jit(solution)/shard_map/ppermute | solution.py:476
  130.1 0.7 copy-start.4
  132.7 25.2 %all-to-all-start.2 = ((bf16[4,128,128]{2,1,0:T(8,128)(2,1)}), bf16[4,128,128]{2,1,0:T(8,128)(2,1)S(1)}, u32[]{:S(2)}, u32[]{:S(2)}) async-start(bf16[4,128,128]{2,1,0:T(8,128)(2,1)} %get-tuple-element.23), calls=%async_computation.2 | async-start | bytes 262144 | tf_op jit(solution)/shard_map/all_to_all | solution.py:480
  141.0 6.3 %collective-permute-start.4 = (bf16[16,2048]{1,0:T(8,128)(2,1)S(1)}, bf16[16,2048]{1,0:T(8,128)(2,1)S(1)}, u32[]{:S(2)}, u32[]{:S(2)}) collective-permute-start(bf16[16,2048]{1,0:T(8,128)(2,1)S(1)} %fusion.8), channel_id=1, source_target_pairs={{0,32},{32,64},{64,96},{96,128},{128,160},{160,192},{192,224},{224... | collective-permute-start | bytes 196616 | tf_op jit(solution)/shard_map/ppermute | solution.py:471
  154.2 3.7 %copy-start.1 = (f32[128,128]{1,0:T(8,128)S(1)}, f32[128,128]{1,0:T(8,128)}, u32[]{:S(2)}) copy-start(f32[128,128]{1,0:T(8,128)} %get-tuple-element.22.before_ref) | copy-start | bytes 196612
  154.2 3.7 %copy-start.2 = (s32[2]{0:T(128)S(1)}, s32[2]{0:T(128)}, u32[]{:S(2)}) copy-start(s32[2]{0:T(128)} %pad_add_fusion.at_ref) | copy-start | bytes 28
  161.4 16.5 %all-to-all-start.3 = ((bf16[4,256,256]{2,1,0:T(8,128)(2,1)}), bf16[4,256,256]{2,1,0:T(8,128)(2,1)S(1)}, u32[]{:S(2)}, u32[]{:S(2)}) async-start(bf16[4,256,256]{2,1,0:T(8,128)(2,1)} %bitcast.48), calls=%async_computation.3 | async-start | bytes 1048576 | tf_op jit(solution)/shard_map/all_to_all | solution.py:573
  180.7 9.8 %collective-permute-start.8 = (bf16[128,2048]{1,0:T(8,128)(2,1)S(1)}, bf16[128,2048]{1,0:T(8,128)(2,1)S(1)}, u32[]{:S(2)}, u32[]{:S(2)}) collective-permute-start(bf16[128,2048]{1,0:T(8,128)(2,1)S(1)} %get-tuple-element.36), channel_id=1, source_target_pairs={{0,1},{1,0},{2,3},{3,2},{4,5},{5,4},{6,7},{7,6},{8,9},{9,8},{10,11... | collective-permute-start | bytes 1572872 | tf_op jit(solution)/shard_map/ppermute | solution.py:517
Sparse Core Ops, SparseCore 0:
  18.9 83.5 all-gather.1

commit v8 on v7

--- a/solution.py
+++ b/solution.py
@@ -11,7 +11,9 @@
 HEAD_WIDTH = 64
 CHUNK = 64
 BLOCK = 256
-MAPS_BLOCK = 512
+MAPS_BLOCK = 1024
+READS_BLOCK = 512
+CONV_BLOCK = 1024
 norm_eps = 1e-06
 key_eps = 1e-06
 f32, bf16 = jnp.float32, jnp.bfloat16
@@ -50,11 +52,13 @@
     return jnp.where(low, a, b)
 
 
-def own_block(place_ref, *token_refs):
+def own_block(place_ref, same_ref, other_ref, first, pairs=1):
+    chips = same_ref.shape[0]
     low_core = place_ref[1] == 0
     rows = []
-    for k in range(0, len(token_refs), 2):
-        mine, theirs = token_refs[k][0], token_refs[k + 1][0]
+    for k in range(pairs):
+        at = (first + k - place_ref[0]) & (chips - 1)
+        mine, theirs = same_ref[at], other_ref[at]
         rows += [jnp.where(low_core, mine, theirs), jnp.where(low_core, theirs, mine)]
     return jnp.concatenate(rows, axis=0)
 
@@ -72,9 +76,23 @@
     return [a[k * CHUNK : (k + 1) * CHUNK] for k in range(a.shape[0] // CHUNK)]
 
 
-def maps_kernel(place_ref, *refs):
-    *token_refs, w_ref, spike_ref, vec_ref = refs[:-9]
-    gk_ref, gb_ref, wu_ref, v_ref, pos_ref, full_ref, states_ref, agg_ref, st_ref = refs[-9:]
+def maps_kernel(
+    place_ref,
+    same_ref,
+    other_ref,
+    w_ref,
+    spike_ref,
+    vec_ref,
+    gk_ref,
+    gb_ref,
+    wu_ref,
+    v_ref,
+    pos_ref,
+    full_ref,
+    states_ref,
+    agg_ref,
+    st_ref,
+):
     step = pl.program_id(0)
     width = 2 * HEAD_WIDTH
     each = range(MAPS_BLOCK // CHUNK)
@@ -85,7 +103,8 @@
         eye = (r - HEAD_WIDTH == l % HEAD_WIDTH) & (r >= HEAD_WIDTH)
         st_ref[...] = jnp.where(eye, 1.0, 0.0).astype(f32)
 
-    x = own_block(place_ref, *token_refs)
+    pairs = MAPS_BLOCK // BLOCK
+    x = own_block(place_ref, same_ref, other_ref, step * pairs, pairs)
 
     def section(k):
         two = jnp.dot(x, w_ref[:, 2 * k * width : 2 * (k + 1) * width], preferred_element_type=f32)
@@ -179,13 +198,8 @@
             agg_ref[k] = state.astype(bf16)
 
 
-def token_specs(same, pairs=1):
-    chips, part, depth = same.shape
-    specs = []
-    for k in range(pairs):
-        place = lambda i, p, k=k: ((pairs * i + k - p[0]) & (chips - 1), 0, 0)
-        specs += [pl.BlockSpec((1, part, depth), place)] * 2
-    return specs
+def token_specs():
+    return [pl.BlockSpec(memory_space=pltpu.VMEM)] * 2
 
 
 def maps_call(place, same, other, w, spike, vec, copies):
@@ -200,7 +214,7 @@
         grid_spec=pltpu.PrefetchScalarGridSpec(
             num_scalar_prefetch=1,
             grid=(rows // MAPS_BLOCK,),
-            in_specs=token_specs(same, MAPS_BLOCK // BLOCK)
+            in_specs=token_specs()
             + [
                 pl.BlockSpec((depth, 4 * width), lambda i, p: (0, 0)),
                 tile,
@@ -232,7 +246,7 @@
             dimension_semantics=("arbitrary",), vmem_limit_bytes=28 * 2**20
         ),
         name="state_maps",
-    )(place, *(in_hbm(same, other) * (MAPS_BLOCK // BLOCK)), *in_hbm(w), spike, vec)
+    )(place, same, other, *in_hbm(w), spike, vec)
 
 
 def conv_kernel(place_ref, same_ref, other_ref, w_ref, halo_ref, vec_ref, q_ref, out_ref, tail_ref):
@@ -247,7 +261,8 @@
         two = project(halo_ref[...], 1, 3).astype(f32)
         tail_ref[...] = two[:, :width] * two[:, width:]
 
-    x = own_block(place_ref, same_ref, other_ref)
+    pairs = CONV_BLOCK // BLOCK
+    x = own_block(place_ref, same_ref, other_ref, pl.program_id(0) * pairs, pairs)
     two = project(x, 0, 2)
     q_ref[...] = two[:, :width]
     rest = project(x, 2, 4).astype(f32)
@@ -266,14 +281,14 @@
 def conv_call(place, same, other, w, halo, vec):
     rows, width = same.shape[0] * same.shape[1] * 2, vec.shape[1]
     depth = w.shape[0]
-    tile = pl.BlockSpec((BLOCK, width), lambda i, p: (i, 0))
+    tile = pl.BlockSpec((CONV_BLOCK, width), lambda i, p: (i, 0))
     whole = lambda a: pl.BlockSpec(a.shape, lambda i, p: (0,) * a.ndim)
     return pl.pallas_call(
         conv_kernel,
         grid_spec=pltpu.PrefetchScalarGridSpec(
             num_scalar_prefetch=1,
-            grid=(rows // BLOCK,),
-            in_specs=token_specs(same)
+            grid=(rows // CONV_BLOCK,),
+            in_specs=token_specs()
             + [pl.BlockSpec((depth, 4 * width), lambda i, p: (0, 1)), whole(halo), whole(vec)],
             out_specs=[tile, tile],
             scratch_shapes=[pltpu.VMEM((halo.shape[0], width), f32)],
@@ -283,12 +298,12 @@
             dimension_semantics=("arbitrary",), vmem_limit_bytes=20 * 2**20
         ),
         name="conv_mix",
-    )(place, *in_hbm(same, other, w), halo, vec)
+    )(place, same, other, *in_hbm(w), halo, vec)
 
 
 def reads_kernel(q_ref, gk_ref, gb_ref, wu_ref, v_ref, pos_ref, full_ref, states_ref, o_ref, y_ref):
     width = 2 * HEAD_WIDTH
-    each = range(MAPS_BLOCK // CHUNK)
+    each = range(READS_BLOCK // CHUNK)
     t, s, _ = chunk_masks()
     inclusive = t >= s
     fold = functools.partial(spread, first=first_lanes())
@@ -318,12 +333,12 @@
 
 def reads_call(q, gk, gb, wu, v, pos, full, states):
     rows, width = q.shape
-    tile = pl.BlockSpec((MAPS_BLOCK, width), lambda i: (i, 0))
-    wide = pl.BlockSpec((MAPS_BLOCK, 2 * width), lambda i: (i, 0))
-    starts = pl.BlockSpec((MAPS_BLOCK // CHUNK, width, width), lambda i: (i, 0, 0))
+    tile = pl.BlockSpec((READS_BLOCK, width), lambda i: (i, 0))
+    wide = pl.BlockSpec((READS_BLOCK, 2 * width), lambda i: (i, 0))
+    starts = pl.BlockSpec((READS_BLOCK // CHUNK, width, width), lambda i: (i, 0, 0))
     return pl.pallas_call(
         reads_kernel,
-        grid=(rows // MAPS_BLOCK,),
+        grid=(rows // READS_BLOCK,),
         in_specs=[tile, tile, tile, wide, tile, tile, tile, starts],
         out_specs=[tile, tile],
         out_shape=[array((rows, width), f32), array((rows, width), bf16)],
@@ -390,7 +405,7 @@
         state = moved(state, before, first) + before[:HEAD_WIDTH]
         s_ref[...] = spread(state, first)
 
-    low = lanes_of((MAPS_BLOCK, width)) < HEAD_WIDTH
+    low = lanes_of((READS_BLOCK, width)) < HEAD_WIDTH
     reads = o_ref[...] + dot(y_ref[...], s_ref[...], 1, 1)
     centered = reads - head_sums(reads, low) * (1.0 / HEAD_WIDTH)
     variance = head_sums(centered * centered, low) * (1.0 / HEAD_WIDTH)
@@ -402,14 +417,14 @@
 def finish_call(at, before, far, init, o, y, conv, vec):
     rows, width = o.shape
     whole = lambda a: pl.BlockSpec(a.shape, lambda i, p: (0,) * a.ndim)
-    tile = pl.BlockSpec((MAPS_BLOCK, width), lambda i, p: (i, 0))
+    tile = pl.BlockSpec((READS_BLOCK, width), lambda i, p: (i, 0))
     return pl.pallas_call(
         finish_kernel,
         grid_spec=pltpu.PrefetchScalarGridSpec(
             num_scalar_prefetch=1,
-            grid=(rows // MAPS_BLOCK,),
+            grid=(rows // READS_BLOCK,),
             in_specs=[whole(before), whole(far), whole(init), tile, tile, tile, whole(vec)],
-            out_specs=pl.BlockSpec((MAPS_BLOCK, 2 * width), lambda i, p: (i, 0)),
+            out_specs=pl.BlockSpec((READS_BLOCK, 2 * width), lambda i, p: (i, 0)),
             scratch_shapes=[pltpu.VMEM((width, width), bf16)],
         ),
         out_shape=array((rows, 2 * width), bf16),
@@ -421,18 +436,17 @@
 
 
 def outward_kernel(pick_ref, m_ref, *refs):
-    *weights, keep_ref, give_ref = refs
-    rows, columns = keep_ref.shape
-    first = pick_ref[0] == 0
+    *weights, out_ref = refs
+    rows, columns = out_ref.shape
+    at = pl.multiple_of(pick_ref[0], rows)
+    parts = [m_ref[pick_ref[1 + k], pl.ds(at, rows), :] for k in range(len(weights))]
     step = 512
-    for at in range(0, columns, step):
+    for first in range(0, columns, step):
         total = None
-        for k, w_ref in enumerate(weights):
-            got = dot(m_ref[pick_ref[1 + k]], w_ref[:, at : at + step])
+        for part, w_ref in zip(parts, weights):
+            got = dot(part, w_ref[:, first : first + step])
             total = got if total is None else total + got
-        total = total.astype(bf16)
-        keep_ref[:, at : at + step] = jnp.where(first, total[:rows], total[rows:])
-        give_ref[:, at : at + step] = jnp.where(first, total[rows:], total[:rows])
+        out_ref[:, first : first + step] = total.astype(bf16)
 
 
 def outward_call(pick, gathered, weights):
@@ -441,8 +455,8 @@
     return pl.pallas_call(
         outward_kernel,
         in_specs=[pl.BlockSpec(memory_space=pltpu.SMEM)] + [here] * (1 + len(weights)),
-        out_specs=[here, here],
-        out_shape=[jax.ShapeDtypeStruct((rows, columns), bf16)] * 2,
+        out_specs=here,
+        out_shape=jax.ShapeDtypeStruct((rows, columns), bf16),
         compiler_params=pltpu.CompilerParams(vmem_limit_bytes=24 * 2**20),
         name="outward",
     )(pick, gathered, *weights)
@@ -574,8 +588,10 @@
         mixed.reshape(chips, -1, 2 * channels), "tp", 0, 0, tiled=True, axis_index_groups=groups
     )
     near = [(chip + k) & (chips - 1) for k in (0, 1, 2, chips - 1)]
-    kept, given = outward_call(jnp.stack([core, *near]), gathered, (outer, after, across, before))
+    own, ways = normed.shape[0], (outer, after, across, before)
+    given = outward_call(jnp.stack([(1 - core) * own, *near]), gathered, ways)
     taken = core_swap(given)
+    kept = outward_call(jnp.stack([core * own, *near]), gathered, ways)
     return (kept.astype(f32) + taken.astype(f32)).astype(bf16)[None]
 
 

time: 199 us -> 199 us (level)
  starting transfers between devices: 54.1 us -> 48 us
  waiting for transfers between devices: 40.2 us -> 44.9 us
  local copies, waits for them, and re-layouts: 4.8 us -> 7.95 us
    ppermute x6, waiting for transfers between devices: 26.7 us -> 38.1 us  [turned(): lax.ppermute(x, 'tp', [(i, (i + distance) % devices) for i in range(devic...]
    ppermute x2, starting transfers between devices: 13 us -> 7.76 us  [core_swap(): return lax.ppermute(x, 'tp', [(i, i ^ 1) for i in range(devices)])]
    all_gather x1, waiting for transfers between devices: 8.03 us -> 4.56 us  [mixing(): weights = lax.all_gather(weights, 'sp', axis=0, tiled=True)]
    ppermute x1, waiting for transfers between devices: 2.77 us -> 0.31 us  [passed_along(): return lax.ppermute(block, axis, route)]
    pallas_call x1 -> x2, Pallas kernels: 2.8 us -> 5.18 us  [outward_call(): pl.pallas_call(outward_kernel, in_specs=[pl.BlockSpec(memory_space=pltpu....]
    all_to_all x1, local copies, waits for them, and re-layouts: 0.08 us -> 2.39 us  [from_everyone(): lax.all_to_all(copies, axis, 0, 0, tiled=True, axis_index_groups=groups)]
    pallas_call x1, Pallas kernels: 12.9 us -> 10.8 us  [maps_call(): pl.pallas_call(maps_kernel, grid_spec=pltpu.PrefetchScalarGridSpec(num_sc...]
  transfers between devices with their start and end apart: 14 -> 14, of which waited for: 8 -> 7; matrix products, arithmetic and copies ran while one was open for 5% -> 6% of each run, Pallas kernels for 15% -> 15%
where the time goes in v8:
time: 199 us; the launch traced here: 197 us
  starting transfers between devices  48 us (24%)
  waiting for transfers between devices  44.9 us (23%)
  blocking collectives  44.1 us (22%)
  Pallas kernels  34.3 us (17%)
  between operations  13.7 us (7%)
  local copies, waits for them, and re-layouts  7.95 us (4%)
  other arithmetic  4.52 us (2%)
    all_to_all x2, blocking collectives, from_everyone(): lax.all_to_all(copies, axis, 0, 0, tiled=True, axis_index_groups=groups)  44.1 us
    ppermute x6, waiting for transfers between devices, turned(): lax.ppermute(x, 'tp', [(i, (i + distance) % devices) for i in range(devic...  38.1 us
    ppermute x6, starting transfers between devices, turned(): lax.ppermute(x, 'tp', [(i, (i + distance) % devices) for i in range(devic...  18.8 us
    all_to_all x3, starting transfers between devices, from_everyone(): lax.all_to_all(copies, axis, 0, 0, tiled=True, axis_index_groups=groups)  14.6 us
    pallas_call x1, Pallas kernels, maps_call(): pl.pallas_call(maps_kernel, grid_spec=pltpu.PrefetchScalarGridSpec(num_sc...  10.8 us
    ppermute x2, starting transfers between devices, core_swap(): return lax.ppermute(x, 'tp', [(i, i ^ 1) for i in range(devices)])  7.76 us
    pallas_call x1, Pallas kernels, conv_call(): pl.pallas_call(conv_kernel, grid_spec=pltpu.PrefetchScalarGridSpec(num_sc...  5.97 us
    pallas_call x2, Pallas kernels, outward_call(): pl.pallas_call(outward_kernel, in_specs=[pl.BlockSpec(memory_space=pltpu....  5.18 us
  transfers between devices with their start and end apart: 14, of which 7 were waited for; matrix products, arithmetic and copies ran while one was open for 6% of the time, Pallas kernels for 15%

profile of v8, /device:TPU:1, one launch (start us, length us, event | category | flops | bytes accessed | tf_op | source)
XLA Modules:
  0.0 197.4 jit_solution(175709927153272994)
XLA Ops:
  6.5 1.6 pack_shards.2
  8.2 10.6 %all_to_all.30 = bf16[4,32,1024]{2,1,0:T(8,128)(2,1)} all-to-all(bf16[4,32,1024]{2,1,0:T(8,128)(2,1)} %pack_shards.2), channel_id=1, replica_groups=mesh['sp'=16,'fs'=4,'tp'=8] {'fs'}, dimensions={0} | all-to-all | bytes 524288 | tf_op jit(solution)/shard_map/all_to_all | solution.py:494
  18.8 0.0 all-gather.2.cloned.1.call-update
  18.8 1.2 fusion.2
  20.1 1.2 fusion.4
  21.3 4.4 %collective-permute-start = (bf16[128,2048]{1,0:T(8,128)(2,1)S(1)}, bf16[128,2048]{1,0:T(8,128)(2,1)S(1)}, u32[]{:S(2)}, u32[]{:S(2)}) collective-permute-start(bf16[128,2048]{1,0:T(8,128)(2,1)S(1)} %fusion.4), channel_id=1, source_target_pairs={{0,6},{1,7},{2,0},{3,1},{4,2},{5,3},{6,4},{7,5},{8,14},{9,15},{10,... | collective-permute-start | bytes 1572872 | tf_op jit(solution)/shard_map/ppermute | solution.py:490
  25.7 2.4 %collective-permute-start.1 = (bf16[128,2048]{1,0:T(8,128)(2,1)S(1)}, bf16[128,2048]{1,0:T(8,128)(2,1)S(1)}, u32[]{:S(2)}, u32[]{:S(2)}) collective-permute-start(bf16[128,2048]{1,0:T(8,128)(2,1)S(1)} %fusion.4), channel_id=1, source_target_pairs={{0,4},{1,5},{2,6},{3,7},{4,0},{5,1},{6,2},{7,3},{8,12},{9,13},{10,... | collective-permute-start | bytes 1572872 | tf_op jit(solution)/shard_map/ppermute | solution.py:490
  28.2 2.5 %collective-permute-start.2 = (bf16[128,2048]{1,0:T(8,128)(2,1)S(1)}, bf16[128,2048]{1,0:T(8,128)(2,1)S(1)}, u32[]{:S(2)}, u32[]{:S(2)}) collective-permute-start(bf16[128,2048]{1,0:T(8,128)(2,1)S(1)} %fusion.4), channel_id=1, source_target_pairs={{0,2},{1,3},{2,4},{3,5},{4,6},{5,7},{6,0},{7,1},{8,10},{9,11},{10,... | collective-permute-start | bytes 1572872 | tf_op jit(solution)/shard_map/ppermute | solution.py:490
  30.7 0.2 fusion.6
  30.9 5.9 %collective-permute-done = bf16[128,2048]{1,0:T(8,128)(2,1)S(1)} collective-permute-done((bf16[128,2048]{1,0:T(8,128)(2,1)S(1)}, bf16[128,2048]{1,0:T(8,128)(2,1)S(1)}, u32[]{:S(2)}, u32[]{:S(2)}) %collective-permute-start) | collective-permute-done | bytes 524320 | tf_op jit(solution)/shard_map/ppermute | solution.py:490
  36.8 1.4 collective-permute-done.1
  38.2 15.3 %collective-permute-done.2 = bf16[128,2048]{1,0:T(8,128)(2,1)S(1)} collective-permute-done((bf16[128,2048]{1,0:T(8,128)(2,1)S(1)}, bf16[128,2048]{1,0:T(8,128)(2,1)S(1)}, u32[]{:S(2)}, u32[]{:S(2)}) %collective-permute-start.2) | collective-permute-done | bytes 524320 | tf_op jit(solution)/shard_map/ppermute | solution.py:490
  53.5 0.3 pad_maximum_fusion.same_ref
  53.8 3.1 %collective-permute-start.3 = (bf16[4,128,2048]{2,1,0:T(8,128)(2,1)S(1)}, bf16[4,128,2048]{2,1,0:T(8,128)(2,1)}, u32[]{:S(2)}, u32[]{:S(2)}) collective-permute-start(bf16[4,128,2048]{2,1,0:T(8,128)(2,1)S(1)} %pad_maximum_fusion.same_ref), channel_id=1, source_target_pairs={{0,1},{1,0},{2,3},{3,2},{4,5},{5,4},{6,7},{7,6},{8,9},{9,8},{10,11... | collective-permute-start | bytes 6291464 | tf_op jit(solution)/shard_map/ppermute | solution.py:531
  56.9 0.0 copy-start.6
  56.9 0.0 copy-start.7
  56.9 0.0 copy-start.8
  56.9 0.0 copy-start.9
  56.9 0.0 copy-start
  56.9 1.5 pack_shards.3
  58.4 33.4 %all_to_all.31 = bf16[16,32,256]{2,1,0:T(8,128)(2,1)S(1)} all-to-all(bf16[16,32,256]{2,1,0:T(8,128)(2,1)} %pack_shards.3), channel_id=1, replica_groups=mesh['sp'=16,'fs'=4,'tp'=8] {'sp'}, dimensions={0} | all-to-all | bytes 524288 | tf_op jit(solution)/shard_map/all_to_all | solution.py:494
  91.9 1.2 broadcast_in_dim.27
  93.1 4.3 %all-to-all-start.5 = ((bf16[4,16,32,256]{3,2,1,0:T(8,128)(2,1)}), bf16[4,16,32,256]{3,2,1,0:T(8,128)(2,1)}, u32[]{:S(2)}, u32[]{:S(2)}) async-start(bf16[4,16,32,256]{3,2,1,0:T(8,128)(2,1)} %broadcast_in_dim.27), calls=%async_computation.5 | async-start | bytes 2097152 | tf_op jit(solution)/shard_map/all_to_all | solution.py:494
  97.4 0.0 copy-done.6
  97.4 0.0 copy-done.7
  97.4 0.0 copy-done.8
  97.4 0.0 copy-done.9
  97.4 0.1 pad_add_fusion.1.place_ref
  97.5 0.0 collective-permute-done.3.other_ref
  97.5 4.6 %all-gather.2.cloned.1.call-done.w_ref = bf16[2048,1024]{1,0:T(8,128)(2,1)} async-done(((bf16[128,1024]{1,0:T(8,128)(2,1)}), bf16[2048,1024]{1,0:T(8,128)(2,1)}) %all-gather.2.cloned.1.call-update) | async-done | bytes 4194320 | tf_op jit(solution)/shard_map/all_gather | solution.py:549
  102.1 10.8 %state_maps.1 = (bf16[1024,128]{1,0:T(8,128)(2,1)}, bf16[1024,128]{1,0:T(8,128)(2,1)}, bf16[1024,256]{1,0:T(8,128)(2,1)}, bf16[1024,128]{1,0:T(8,128)(2,1)}, f32...) custom-call(s32[2]{0:T(128)S(1)} %pad_add_fusion.1.place_ref, ...), custom_call_target="tpu_custom_call" | custom-call | tf_op jit(solution)/shard_map/state_maps/pallas_call | solution.py:212
  112.9 0.0 all-to-all-done.5
  112.9 4.1 %all-to-all-start.1 = ((bf16[4,128,128]{2,1,0:T(8,128)(2,1)}), bf16[4,128,128]{2,1,0:T(8,128)(2,1)S(1)}, u32[]{:S(2)}, u32[]{:S(2)}) async-start(bf16[4,128,128]{2,1,0:T(8,128)(2,1)} %get-tuple-element.19), calls=%async_computation.1 | async-start | bytes 262144 | tf_op jit(solution)/shard_map/all_to_all | solution.py:494
  117.0 2.4 %copy.24 = bf16[4,16,32,256]{3,2,0,1:T(8,128)(2,1)} copy(bf16[4,16,32,256]{3,2,1,0:T(8,128)(2,1)} %all-to-all-done.5) | data formatting | bytes 2097152 | tf_op jit(solution)/shard_map/all_to_all | solution.py:494
  119.4 1.5 copy.25
  120.9 4.5 %collective-permute-start.5 = (bf16[256,2048]{1,0:T(8,128)(2,1)S(1)}, bf16[256,2048]{1,0:T(8,128)(2,1)}, u32[]{:S(2)}, u32[]{:S(2)}) collective-permute-start(bf16[256,2048]{1,0:T(8,128)(2,1)S(1)} %bitcast.44), channel_id=1, source_target_pairs={{0,6},{1,7},{2,0},{3,1},{4,2},{5,3},{6,4},{7,5},{8,14},{9,15},{10,... | collective-permute-start | bytes 3145736 | tf_op jit(solution)/shard_map/ppermute | solution.py:490
  125.3 2.5 %collective-permute-start.6 = (bf16[256,2048]{1,0:T(8,128)(2,1)S(1)}, bf16[256,2048]{1,0:T(8,128)(2,1)}, u32[]{:S(2)}, u32[]{:S(2)}) collective-permute-start(bf16[256,2048]{1,0:T(8,128)(2,1)S(1)} %bitcast.45), channel_id=1, source_target_pairs={{0,4},{1,5},{2,6},{3,7},{4,0},{5,1},{6,2},{7,3},{8,12},{9,13},{10,... | collective-permute-start | bytes 3145736 | tf_op jit(solution)/shard_map/ppermute | solution.py:490
  127.9 2.5 %collective-permute-start.7 = (bf16[256,2048]{1,0:T(8,128)(2,1)S(1)}, bf16[256,2048]{1,0:T(8,128)(2,1)}, u32[]{:S(2)}, u32[]{:S(2)}) collective-permute-start(bf16[256,2048]{1,0:T(8,128)(2,1)S(1)} %bitcast.46), channel_id=1, source_target_pairs={{0,2},{1,3},{2,4},{3,5},{4,6},{5,7},{6,0},{7,1},{8,10},{9,11},{10,... | collective-permute-start | bytes 3145736 | tf_op jit(solution)/shard_map/ppermute | solution.py:490
  130.4 0.6 pad_add_fusion.at_ref
  130.9 0.0 all-to-all-done.1.pieces_ref
  131.0 0.6 copy-done.4
  131.6 2.0 %group_map.1 = (bf16[4,128,128]{2,1,0:T(8,128)(2,1)}, f32[128,128]{1,0:T(8,128)}) custom-call(s32[2]{0:T(128)} %pad_add_fusion.at_ref, bf16[4,128,128]{2,1,0:T(8,128)(2,1)} %copy-done.4), custom_call_target="tpu_custom_call" | custom-call | tf_op jit(solution)/shard_map/group_map/pallas_call | solution.py:381
  133.6 6.3 %all-to-all-start.2 = ((bf16[4,128,128]{2,1,0:T(8,128)(2,1)}), bf16[4,128,128]{2,1,0:T(8,128)(2,1)S(1)}, u32[]{:S(2)}, u32[]{:S(2)}) async-start(bf16[4,128,128]{2,1,0:T(8,128)(2,1)} %get-tuple-element.21), calls=%async_computation.2 | async-start | bytes 262144 | tf_op jit(solution)/shard_map/all_to_all | solution.py:494
  139.9 1.0 slice.8
  140.9 3.3 %collective-permute-start.4 = (bf16[16,2048]{1,0:T(8,128)(2,1)S(1)}, bf16[16,2048]{1,0:T(8,128)(2,1)S(1)}, u32[]{:S(2)}, u32[]{:S(2)}) collective-permute-start(bf16[16,2048]{1,0:T(8,128)(2,1)S(1)} %fusion.8), channel_id=1, source_target_pairs={{0,32},{32,64},{64,96},{96,128},{128,160},{160,192},{192,224},{224... | collective-permute-start | bytes 196616 | tf_op jit(solution)/shard_map/ppermute | solution.py:485
  144.2 0.9 copy.23
  145.1 0.1 reshape.38.init_ref
  145.2 0.3 collective-permute-done.4.halo_ref
  145.5 6.0 %conv_mix.1 = (bf16[1024,128]{1,0:T(8,128)(2,1)}, bf16[1024,128]{1,0:T(8,128)(2,1)}) custom-call(s32[2]{0:T(128)S(1)} %pad_add_fusion.1.place_ref, bf16[4,128,2048]{2,1,0:T(8,128)(2,1)S(1)} %pad_maximum_fusion.same_ref, bf16[4,128,2048]{2,1,0:T(8,128)(2,1)} %collective-permute-done.3.other_ref, bf16[2048,1024]{1,0:T(8,128)(2,1)} %all-gather.2.cloned.1.call-done.w_ref, ...), custom_call_target="tpu_custom_call" | custom-call | tf_op jit(solution)/shard_map/conv_mix/pallas_call | solution.py:286
  151.5 3.7 %local_reads.1 = (f32[1024,128]{1,0:T(8,128)}, bf16[1024,128]{1,0:T(8,128)(2,1)}) custom-call(bf16[1024,128]{1,0:T(8,128)(2,1)} %get-tuple-element.22.q_ref, bf16[1024,128]{1,0:T(8,128)(2,1)} %get-tuple-element.23.gk_ref, bf16[1024,128]{1,0:T(8,128)(2,1)} %get-tuple-element.24.gb_ref, bf16[1024,256]{1,0:T(8,128)(2,1)} %get-tuple-element.25.wu_ref, ...), custom_call_target="tpu_custom_call" | custom-call | tf_op jit(solution)/shard_map/local_reads/pallas_call | solution.py:339
  155.2 0.0 all-to-all-done.2.far_ref
  155.2 3.5 %finish_mix.1 = bf16[1024,256]{1,0:T(8,128)(2,1)} custom-call(s32[2]{0:T(128)S(1)} %copy-done.2, f32[128,128]{1,0:T(8,128)S(1)} %copy-done.1, bf16[4,128,128]{2,1,0:T(8,128)(2,1)S(1)} %all-to-all-done.2.far_ref, f32[64,128]{1,0:T(8,128)S(1)} %reshape.38.init_ref, f32[1024,128]{1,0:T(8,128)} %get-tuple-element.30.o_ref, ...), custom_call_target="tpu_custom_call" | custom-call | tf_op jit(solution)/shard_map/finish_mix/pallas_call | solution.py:421
  158.7 3.5 %all-to-all-start.3 = ((bf16[4,256,256]{2,1,0:T(8,128)(2,1)}), bf16[4,256,256]{2,1,0:T(8,128)(2,1)S(1)}, u32[]{:S(2)}, u32[]{:S(2)}) async-start(bf16[4,256,256]{2,1,0:T(8,128)(2,1)} %bitcast.51), calls=%async_computation.3 | async-start | bytes 1048576 | tf_op jit(solution)/shard_map/all_to_all | solution.py:587
  162.2 0.1 stack.76.pick_ref
  162.3 0.0 collective-permute-done.5.refs_1_
  162.3 0.0 collective-permute-done.6.refs_2_
  162.3 15.5 %collective-permute-done.7.refs_3_ = bf16[256,2048]{1,0:T(8,128)(2,1)} collective-permute-done((bf16[256,2048]{1,0:T(8,128)(2,1)S(1)}, bf16[256,2048]{1,0:T(8,128)(2,1)}, u32[]{:S(2)}, u32[]{:S(2)}) %collective-permute-start.7) | collective-permute-done | bytes 1048608 | tf_op jit(solution)/shard_map/ppermute | solution.py:490
  177.8 1.9 all-to-all-done.3.m_ref
  179.7 2.6 %outward.3 = bf16[128,2048]{1,0:T(8,128)(2,1)S(1)} custom-call(s32[5]{0:T(128)S(1)} %stack.76.pick_ref, bf16[4,256,256]{2,1,0:T(8,128)(2,1)S(1)} %all-to-all-done.3.m_ref, bf16[256,2048]{1,0:T(8,128)(2,1)S(1)} %bitcast.47, bf16[256,2048]{1,0:T(8,128)(2,1)} %collective-permute-done.5.refs_1_, bf16[256,2048]{1,0:T(8,128)(2,1)} %collective-permute-done.6.refs_2_, ...), custom_call_target="tpu_custom_call" | custom-call | tf_op jit(solution)/shard_map/outward/pallas_call | solution.py:455
  182.3 4.7 %collective-permute-start.8 = (bf16[128,2048]{1,0:T(8,128)(2,1)S(1)}, bf16[128,2048]{1,0:T(8,128)(2,1)S(1)}, u32[]{:S(2)}, u32[]{:S(2)}) collective-permute-start(bf16[128,2048]{1,0:T(8,128)(2,1)S(1)} %outward.3), channel_id=1, source_target_pairs={{0,1},{1,0},{2,3},{3,2},{4,5},{5,4},{6,7},{7,6},{8,9},{9,8},{10,11... | collective-permute-start | bytes 1572872 | tf_op jit(solution)/shard_map/ppermute | solution.py:531
  187.0 0.1 stack.64.pick_ref
  187.0 2.6 %outward.2 = bf16[128,2048]{1,0:T(8,128)(2,1)S(1)} custom-call(s32[5]{0:T(128)S(1)} %stack.64.pick_ref, bf16[4,256,256]{2,1,0:T(8,128)(2,1)S(1)} %all-to-all-done.3.m_ref, bf16[256,2048]{1,0:T(8,128)(2,1)S(1)} %bitcast.48, bf16[256,2048]{1,0:T(8,128)(2,1)} %collective-permute-done.5.refs_1_, bf16[256,2048]{1,0:T(8,128)(2,1)} %collective-permute-done.6.refs_2_, ...), custom_call_target="tpu_custom_call" | custom-call | tf_op jit(solution)/shard_map/outward/pallas_call | solution.py:455
  189.6 0.0 collective-permute-done.8
  189.6 0.9 fusion.7
  (16 shorter events, 0.1 us)
Async XLA Ops:
  6.5 24.1 %copy-start.3 = (bf16[1,128,2048]{2,1,0:T(8,128)(2,1)S(1)}, bf16[1,128,2048]{2,1,0:T(8,128)(2,1)}, u32[]{:S(2)}) copy-start(bf16[1,128,2048]{2,1,0:T(8,128)(2,1)} %param.18) | copy-start | bytes 1572868
  6.5 24.1 %copy-start.5 = (f32[2048]{0:T(1024)S(1)}, f32[2048]{0:T(1024)}, u32[]{:S(2)}) copy-start(f32[2048]{0:T(1024)} %param.19) | copy-start | bytes 24580
  6.5 95.5 %all-gather.2.cloned.1.call-start = ((), (), s32[]{:S(2)}) async-start(), calls=%async_computation.6 | async-start | bytes 4456448 | tf_op jit(solution)/shard_map/all_gather | solution.py:549
  21.3 15.5 %collective-permute-start = (bf16[128,2048]{1,0:T(8,128)(2,1)S(1)}, bf16[128,2048]{1,0:T(8,128)(2,1)S(1)}, u32[]{:S(2)}, u32[]{:S(2)}) collective-permute-start(bf16[128,2048]{1,0:T(8,128)(2,1)S(1)} %fusion.4), channel_id=1, source_target_pairs={{0,6},{1,7},{2,0},{3,1},{4,2},{5,3},{6,4},{7,5},{8,14},{9,15},{10,... | collective-permute-start | bytes 1572872 | tf_op jit(solution)/shard_map/ppermute | solution.py:490
  25.7 12.5 %collective-permute-start.1 = (bf16[128,2048]{1,0:T(8,128)(2,1)S(1)}, bf16[128,2048]{1,0:T(8,128)(2,1)S(1)}, u32[]{:S(2)}, u32[]{:S(2)}) collective-permute-start(bf16[128,2048]{1,0:T(8,128)(2,1)S(1)} %fusion.4), channel_id=1, source_target_pairs={{0,4},{1,5},{2,6},{3,7},{4,0},{5,1},{6,2},{7,3},{8,12},{9,13},{10,... | collective-permute-start | bytes 1572872 | tf_op jit(solution)/shard_map/ppermute | solution.py:490
  28.2 25.4 %collective-permute-start.2 = (bf16[128,2048]{1,0:T(8,128)(2,1)S(1)}, bf16[128,2048]{1,0:T(8,128)(2,1)S(1)}, u32[]{:S(2)}, u32[]{:S(2)}) collective-permute-start(bf16[128,2048]{1,0:T(8,128)(2,1)S(1)} %fusion.4), channel_id=1, source_target_pairs={{0,2},{1,3},{2,4},{3,5},{4,6},{5,7},{6,0},{7,1},{8,10},{9,11},{10,... | collective-permute-start | bytes 1572872 | tf_op jit(solution)/shard_map/ppermute | solution.py:490
  53.8 43.7 %collective-permute-start.3 = (bf16[4,128,2048]{2,1,0:T(8,128)(2,1)S(1)}, bf16[4,128,2048]{2,1,0:T(8,128)(2,1)}, u32[]{:S(2)}, u32[]{:S(2)}) collective-permute-start(bf16[4,128,2048]{2,1,0:T(8,128)(2,1)S(1)} %pad_maximum_fusion.same_ref), channel_id=1, source_target_pairs={{0,1},{1,0},{2,3},{3,2},{4,5},{5,4},{6,7},{7,6},{8,9},{9,8},{10,11... | collective-permute-start | bytes 6291464 | tf_op jit(solution)/shard_map/ppermute | solution.py:531
  56.9 40.5 %copy-start.6 = (f32[3,128]{1,0:T(4,128)S(1)}, f32[3,128]{1,0:T(4,128)}, u32[]{:S(2)}) copy-start(f32[3,128]{1,0:T(4,128)} %param.23) | copy-start | bytes 4612
  56.9 40.5 %copy-start.7 = (f32[128]{0:T(128)S(1)}, f32[128]{0:T(128)}, u32[]{:S(2)}) copy-start(f32[128]{0:T(128)} %param.29) | copy-start | bytes 1540
  56.9 40.5 %copy-start.8 = (f32[128]{0:T(128)S(1)}, f32[128]{0:T(128)}, u32[]{:S(2)}) copy-start(f32[128]{0:T(128)} %param.30) | copy-start | bytes 1540
  56.9 40.5 %copy-start.9 = (f32[128]{0:T(128)S(1)}, f32[128]{0:T(128)}, u32[]{:S(2)}) copy-start(f32[128]{0:T(128)} %param.33) | copy-start | bytes 1540
  56.9 45.2 %copy-start = (f32[1,1024,128]{2,1,0:T(8,128)S(1)}, f32[1,1024,128]{2,1,0:T(8,128)}, u32[]{:S(2)}) copy-start(f32[1,1024,128]{2,1,0:T(8,128)} %param.31) | copy-start | bytes 1572868
  93.1 19.8 %all-to-all-start.5 = ((bf16[4,16,32,256]{3,2,1,0:T(8,128)(2,1)}), bf16[4,16,32,256]{3,2,1,0:T(8,128)(2,1)}, u32[]{:S(2)}, u32[]{:S(2)}) async-start(bf16[4,16,32,256]{3,2,1,0:T(8,128)(2,1)} %broadcast_in_dim.27), calls=%async_computation.5 | async-start | bytes 2097152 | tf_op jit(solution)/shard_map/all_to_all | solution.py:494
  112.9 18.0 %all-to-all-start.1 = ((bf16[4,128,128]{2,1,0:T(8,128)(2,1)}), bf16[4,128,128]{2,1,0:T(8,128)(2,1)S(1)}, u32[]{:S(2)}, u32[]{:S(2)}) async-start(bf16[4,128,128]{2,1,0:T(8,128)(2,1)} %get-tuple-element.19), calls=%async_computation.1 | async-start | bytes 262144 | tf_op jit(solution)/shard_map/all_to_all | solution.py:494
  120.9 41.4 %collective-permute-start.5 = (bf16[256,2048]{1,0:T(8,128)(2,1)S(1)}, bf16[256,2048]{1,0:T(8,128)(2,1)}, u32[]{:S(2)}, u32[]{:S(2)}) collective-permute-start(bf16[256,2048]{1,0:T(8,128)(2,1)S(1)} %bitcast.44), channel_id=1, source_target_pairs={{0,6},{1,7},{2,0},{3,1},{4,2},{5,3},{6,4},{7,5},{8,14},{9,15},{10,... | collective-permute-start | bytes 3145736 | tf_op jit(solution)/shard_map/ppermute | solution.py:490
  125.3 37.0 %collective-permute-start.6 = (bf16[256,2048]{1,0:T(8,128)(2,1)S(1)}, bf16[256,2048]{1,0:T(8,128)(2,1)}, u32[]{:S(2)}, u32[]{:S(2)}) collective-permute-start(bf16[256,2048]{1,0:T(8,128)(2,1)S(1)} %bitcast.45), channel_id=1, source_target_pairs={{0,4},{1,5},{2,6},{3,7},{4,0},{5,1},{6,2},{7,3},{8,12},{9,13},{10,... | collective-permute-start | bytes 3145736 | tf_op jit(solution)/shard_map/ppermute | solution.py:490
  127.9 49.9 %collective-permute-start.7 = (bf16[256,2048]{1,0:T(8,128)(2,1)S(1)}, bf16[256,2048]{1,0:T(8,128)(2,1)}, u32[]{:S(2)}, u32[]{:S(2)}) collective-permute-start(bf16[256,2048]{1,0:T(8,128)(2,1)S(1)} %bitcast.46), channel_id=1, source_target_pairs={{0,2},{1,3},{2,4},{3,5},{4,6},{5,7},{6,0},{7,1},{8,10},{9,11},{10,... | collective-permute-start | bytes 3145736 | tf_op jit(solution)/shard_map/ppermute | solution.py:490
  131.0 0.6 copy-start.4
  133.6 21.6 %all-to-all-start.2 = ((bf16[4,128,128]{2,1,0:T(8,128)(2,1)}), bf16[4,128,128]{2,1,0:T(8,128)(2,1)S(1)}, u32[]{:S(2)}, u32[]{:S(2)}) async-start(bf16[4,128,128]{2,1,0:T(8,128)(2,1)} %get-tuple-element.21), calls=%async_computation.2 | async-start | bytes 262144 | tf_op jit(solution)/shard_map/all_to_all | solution.py:494
  140.9 4.7 %collective-permute-start.4 = (bf16[16,2048]{1,0:T(8,128)(2,1)S(1)}, bf16[16,2048]{1,0:T(8,128)(2,1)S(1)}, u32[]{:S(2)}, u32[]{:S(2)}) collective-permute-start(bf16[16,2048]{1,0:T(8,128)(2,1)S(1)} %fusion.8), channel_id=1, source_target_pairs={{0,32},{32,64},{64,96},{96,128},{128,160},{160,192},{192,224},{224... | collective-permute-start | bytes 196616 | tf_op jit(solution)/shard_map/ppermute | solution.py:485
  151.5 3.7 %copy-start.1 = (f32[128,128]{1,0:T(8,128)S(1)}, f32[128,128]{1,0:T(8,128)}, u32[]{:S(2)}) copy-start(f32[128,128]{1,0:T(8,128)} %get-tuple-element.20.before_ref) | copy-start | bytes 196612
  151.5 3.7 %copy-start.2 = (s32[2]{0:T(128)S(1)}, s32[2]{0:T(128)}, u32[]{:S(2)}) copy-start(s32[2]{0:T(128)} %pad_add_fusion.at_ref) | copy-start | bytes 28
  158.7 20.9 %all-to-all-start.3 = ((bf16[4,256,256]{2,1,0:T(8,128)(2,1)}), bf16[4,256,256]{2,1,0:T(8,128)(2,1)S(1)}, u32[]{:S(2)}, u32[]{:S(2)}) async-start(bf16[4,256,256]{2,1,0:T(8,128)(2,1)} %bitcast.51), calls=%async_computation.3 | async-start | bytes 1048576 | tf_op jit(solution)/shard_map/all_to_all | solution.py:587
  182.3 7.4 %collective-permute-start.8 = (bf16[128,2048]{1,0:T(8,128)(2,1)S(1)}, bf16[128,2048]{1,0:T(8,128)(2,1)S(1)}, u32[]{:S(2)}, u32[]{:S(2)}) collective-permute-start(bf16[128,2048]{1,0:T(8,128)(2,1)S(1)} %outward.3), channel_id=1, source_target_pairs={{0,1},{1,0},{2,3},{3,2},{4,5},{5,4},{6,7},{7,6},{8,9},{9,8},{10,11... | collective-permute-start | bytes 1572872 | tf_op jit(solution)/shard_map/ppermute | solution.py:531
Sparse Core Ops, SparseCore 0:
  18.9 83.0 all-gather.1

commit v9 on v8

--- a/solution.py
+++ b/solution.py
@@ -14,6 +14,7 @@
 MAPS_BLOCK = 1024
 READS_BLOCK = 512
 CONV_BLOCK = 1024
+HALO = 16
 norm_eps = 1e-06
 key_eps = 1e-06
 f32, bf16 = jnp.float32, jnp.bfloat16
@@ -90,6 +91,7 @@
     pos_ref,
     full_ref,
     states_ref,
+    last_ref,
     agg_ref,
     st_ref,
 ):
@@ -194,6 +196,7 @@
 
     @pl.when(step == pl.num_programs(0) - 1)
     def _():
+        last_ref[...] = x[MAPS_BLOCK - last_ref.shape[0] :]
         for k in range(agg_ref.shape[0]):
             agg_ref[k] = state.astype(bf16)
 
@@ -228,6 +231,7 @@
                 tile,
                 tile,
                 pl.BlockSpec((pairs, width, width), lambda i, p: (i, 0, 0)),
+                pl.BlockSpec((HALO, depth), lambda i, p: (0, 0)),
                 pl.BlockSpec((copies, width, width), lambda i, p: (0, 0, 0)),
             ],
             scratch_shapes=[pltpu.VMEM((width, width), f32)],
@@ -240,13 +244,14 @@
             like(width, f32),
             like(width, f32),
             array((rows // CHUNK, width, width), bf16),
+            array((HALO, depth), bf16),
             array((copies, width, width), bf16),
         ],
         compiler_params=pltpu.CompilerParams(
             dimension_semantics=("arbitrary",), vmem_limit_bytes=28 * 2**20
         ),
         name="state_maps",
-    )(place, same, other, *in_hbm(w), spike, vec)
+    )(place, same, other, *in_hbm(w, spike), vec)
 
 
 def conv_kernel(place_ref, same_ref, other_ref, w_ref, halo_ref, vec_ref, q_ref, out_ref, tail_ref):
@@ -552,10 +557,12 @@
     outer = jnp.swapaxes(outer, 0, 1).reshape(-1, 2 * channels).T
 
     normed = rms_rows(tokens[0], input_norm_gain)
-    others = [turned(normed, -2), turned(normed, 4), turned(normed, 2)]
-    same = jnp.stack([normed, *others])
+    opposite = turned(normed, 4)
+    ahead, behind = turned(normed, -2), turned(normed, 2)
+    same = jnp.stack([normed, ahead, opposite, behind])
     other = core_swap(same)
-    after, across, before = [turned(outer, k) for k in (-2, 4, 2)]
+    across = turned(outer, 4)
+    after, before = turned(outer, -2), turned(outer, 2)
     vec = jnp.concatenate(
         [
             decay_floor[None],
@@ -567,16 +574,15 @@
         axis=0,
     )
     place = jnp.stack([chip, core])
-    last_rows = jnp.where(core == 0, other[:, -16:], same[:, -16:])
-    last_rows = lax.dynamic_index_in_dim(last_rows, (chips - 1 - chip) & (chips - 1), 0, keepdims=False)
-    halo = passed_along(last_rows, "sp", 1)
     few = 4
     near_blocks = [list(range(k, k + few)) for k in range(0, blocks, few)]
     far_blocks = [list(range(k, blocks, few)) for k in range(few)]
-    *kept, agg = maps_call(place, same, other, weights, decay_spike[0], vec, few)
+    *kept, last_rows, agg = maps_call(place, same, other, weights, decay_spike[0], vec, few)
     near_maps = from_everyone(agg, "sp", near_blocks)
+    halo = passed_along(last_rows, "sp", 1)
     block = lax.axis_index("sp").astype(jnp.int32)
     at = jnp.stack([lax.shift_right_logical(block, 2), block & (few - 1)])
+    at, halo = lax.optimization_barrier((at, halo))
     total, earlier = group_call(at, near_maps, blocks // few)
     far_maps = from_everyone(total, "sp", far_blocks)
     q, conv = conv_call(place, same, other, weights, halo, vec)

time: 199 us -> 202 us (1.015)
  starting transfers between devices: 48 us -> 53.9 us
  local copies, waits for them, and re-layouts: 7.95 us -> 4.67 us
    ppermute x2, starting transfers between devices: 7.76 us -> 13.4 us  [core_swap(): return lax.ppermute(x, 'tp', [(i, i ^ 1) for i in range(devices)])]
    ppermute x6, waiting for transfers between devices: 38.1 us -> 35.5 us  [turned(): lax.ppermute(x, 'tp', [(i, (i + distance) % devices) for i in range(devic...]
    all_to_all x3, waiting for transfers between devices: 0.01 us -> 2.27 us  [from_everyone(): lax.all_to_all(copies, axis, 0, 0, tiled=True, axis_index_groups=groups)]
  transfers between devices with their start and end apart: 14 -> 14, of which waited for: 7 -> 8; matrix products, arithmetic and copies ran while one was open for 6% -> 4% of each run, Pallas kernels for 15% -> 15%
where the time goes in v9:
time: 202 us; the launch traced here: 201 us
  starting transfers between devices  53.9 us (27%)
  waiting for transfers between devices  45.6 us (23%)
  blocking collectives  44.3 us (22%)
  Pallas kernels  34.3 us (17%)
  between operations  13.7 us (7%)
  local copies, waits for them, and re-layouts  4.67 us (2%)
  other arithmetic  4.57 us (2%)
    all_to_all x2, blocking collectives, from_everyone(): lax.all_to_all(copies, axis, 0, 0, tiled=True, axis_index_groups=groups)  44.3 us
    ppermute x6, waiting for transfers between devices, turned(): lax.ppermute(x, 'tp', [(i, (i + distance) % devices) for i in range(devic...  35.5 us
    ppermute x6, starting transfers between devices, turned(): lax.ppermute(x, 'tp', [(i, (i + distance) % devices) for i in range(devic...  18.8 us
    all_to_all x3, starting transfers between devices, from_everyone(): lax.all_to_all(copies, axis, 0, 0, tiled=True, axis_index_groups=groups)  14.9 us
    ppermute x2, starting transfers between devices, core_swap(): return lax.ppermute(x, 'tp', [(i, i ^ 1) for i in range(devices)])  13.4 us
    pallas_call x1, Pallas kernels, maps_call(): pl.pallas_call(maps_kernel, grid_spec=pltpu.PrefetchScalarGridSpec(num_sc...  10.9 us
    all_gather x1, waiting for transfers between devices, mixing(): weights = lax.all_gather(weights, 'sp', axis=0, tiled=True)  5.99 us
    pallas_call x1, Pallas kernels, conv_call(): pl.pallas_call(conv_kernel, grid_spec=pltpu.PrefetchScalarGridSpec(num_sc...  5.97 us
  transfers between devices with their start and end apart: 14, of which 8 were waited for; matrix products, arithmetic and copies ran while one was open for 4% of the time, Pallas kernels for 15%

profile of v9, /device:TPU:1, one launch (start us, length us, event | category | flops | bytes accessed | tf_op | source)
XLA Modules:
  0.0 201.0 jit_solution(6987919446977600026)
XLA Ops:
  6.5 0.0 all-gather.2.cloned.1.call-start
  6.5 1.6 pack_shards.2
  8.2 10.6 %all_to_all.30 = bf16[4,32,1024]{2,1,0:T(8,128)(2,1)} all-to-all(bf16[4,32,1024]{2,1,0:T(8,128)(2,1)} %pack_shards.2), channel_id=1, replica_groups=mesh['sp'=16,'fs'=4,'tp'=8] {'fs'}, dimensions={0} | all-to-all | bytes 524288 | tf_op jit(solution)/shard_map/all_to_all | solution.py:499
  18.8 0.0 all-gather.2.cloned.1.call-update
  18.8 1.2 fusion.2
  20.1 1.2 fusion.4
  21.3 4.4 %collective-permute-start = (bf16[128,2048]{1,0:T(8,128)(2,1)S(1)}, bf16[128,2048]{1,0:T(8,128)(2,1)S(1)}, u32[]{:S(2)}, u32[]{:S(2)}) collective-permute-start(bf16[128,2048]{1,0:T(8,128)(2,1)S(1)} %fusion.4), channel_id=1, source_target_pairs={{0,6},{1,7},{2,0},{3,1},{4,2},{5,3},{6,4},{7,5},{8,14},{9,15},{10,... | collective-permute-start | bytes 1572872 | tf_op jit(solution)/shard_map/ppermute | solution.py:495
  25.7 2.4 %collective-permute-start.1 = (bf16[128,2048]{1,0:T(8,128)(2,1)S(1)}, bf16[128,2048]{1,0:T(8,128)(2,1)S(1)}, u32[]{:S(2)}, u32[]{:S(2)}) collective-permute-start(bf16[128,2048]{1,0:T(8,128)(2,1)S(1)} %fusion.4), channel_id=1, source_target_pairs={{0,4},{1,5},{2,6},{3,7},{4,0},{5,1},{6,2},{7,3},{8,12},{9,13},{10,... | collective-permute-start | bytes 1572872 | tf_op jit(solution)/shard_map/ppermute | solution.py:495
  28.2 2.5 %collective-permute-start.2 = (bf16[128,2048]{1,0:T(8,128)(2,1)S(1)}, bf16[128,2048]{1,0:T(8,128)(2,1)S(1)}, u32[]{:S(2)}, u32[]{:S(2)}) collective-permute-start(bf16[128,2048]{1,0:T(8,128)(2,1)S(1)} %fusion.4), channel_id=1, source_target_pairs={{0,2},{1,3},{2,4},{3,5},{4,6},{5,7},{6,0},{7,1},{8,10},{9,11},{10,... | collective-permute-start | bytes 1572872 | tf_op jit(solution)/shard_map/ppermute | solution.py:495
  30.7 0.0 copy-done.2
  30.7 0.0 copy-done.5
  30.7 0.2 fusion.6
  30.9 5.9 %collective-permute-done = bf16[128,2048]{1,0:T(8,128)(2,1)S(1)} collective-permute-done((bf16[128,2048]{1,0:T(8,128)(2,1)S(1)}, bf16[128,2048]{1,0:T(8,128)(2,1)S(1)}, u32[]{:S(2)}, u32[]{:S(2)}) %collective-permute-start) | collective-permute-done | bytes 524320 | tf_op jit(solution)/shard_map/ppermute | solution.py:495
  36.8 1.4 collective-permute-done.1
  38.2 15.3 %collective-permute-done.2 = bf16[128,2048]{1,0:T(8,128)(2,1)S(1)} collective-permute-done((bf16[128,2048]{1,0:T(8,128)(2,1)S(1)}, bf16[128,2048]{1,0:T(8,128)(2,1)S(1)}, u32[]{:S(2)}, u32[]{:S(2)}) %collective-permute-start.2) | collective-permute-done | bytes 524320 | tf_op jit(solution)/shard_map/ppermute | solution.py:495
  53.5 0.3 pad_maximum_fusion.same_ref
  53.8 3.1 %collective-permute-start.3 = (bf16[4,128,2048]{2,1,0:T(8,128)(2,1)S(1)}, bf16[4,128,2048]{2,1,0:T(8,128)(2,1)}, u32[]{:S(2)}, u32[]{:S(2)}) collective-permute-start(bf16[4,128,2048]{2,1,0:T(8,128)(2,1)S(1)} %pad_maximum_fusion.same_ref), channel_id=1, source_target_pairs={{0,1},{1,0},{2,3},{3,2},{4,5},{5,4},{6,7},{7,6},{8,9},{9,8},{10,11... | collective-permute-start | bytes 6291464 | tf_op jit(solution)/shard_map/ppermute | solution.py:536
  56.9 0.0 copy-start.6
  56.9 0.0 copy-start.7
  56.9 0.0 copy-start.8
  56.9 0.0 copy-start.9
  56.9 1.5 pack_shards.3
  58.4 33.6 %all_to_all.31 = bf16[16,32,256]{2,1,0:T(8,128)(2,1)S(1)} all-to-all(bf16[16,32,256]{2,1,0:T(8,128)(2,1)} %pack_shards.3), channel_id=1, replica_groups=mesh['sp'=16,'fs'=4,'tp'=8] {'sp'}, dimensions={0} | all-to-all | bytes 524288 | tf_op jit(solution)/shard_map/all_to_all | solution.py:499
  92.0 1.1 broadcast_in_dim.27
  93.1 3.5 %all-to-all-start.5 = ((bf16[4,16,32,256]{3,2,1,0:T(8,128)(2,1)}), bf16[4,16,32,256]{3,2,1,0:T(8,128)(2,1)S(1)}, u32[]{:S(2)}, u32[]{:S(2)}) async-start(bf16[4,16,32,256]{3,2,1,0:T(8,128)(2,1)} %broadcast_in_dim.27), calls=%async_computation.5 | async-start | bytes 2097152 | tf_op jit(solution)/shard_map/all_to_all | solution.py:499
  96.7 0.1 pad_add_fusion.1.place_ref
  96.8 0.0 collective-permute-done.3.other_ref
  96.8 6.0 %all-gather.2.cloned.1.call-done.w_ref = bf16[2048,1024]{1,0:T(8,128)(2,1)} async-done(((bf16[128,1024]{1,0:T(8,128)(2,1)}), bf16[2048,1024]{1,0:T(8,128)(2,1)}) %all-gather.2.cloned.1.call-update) | async-done | bytes 4194320 | tf_op jit(solution)/shard_map/all_gather | solution.py:554
  102.8 10.9 %state_maps.1 = (bf16[1024,128]{1,0:T(8,128)(2,1)}, bf16[1024,128]{1,0:T(8,128)(2,1)}, bf16[1024,256]{1,0:T(8,128)(2,1)}, bf16[1024,128]{1,0:T(8,128)(2,1)}, f32...) custom-call(s32[2]{0:T(128)S(1)} %pad_add_fusion.1.place_ref, ...), custom_call_target="tpu_custom_call" | custom-call | tf_op jit(solution)/shard_map/state_maps/pallas_call | solution.py:215
  113.7 0.0 all-to-all-done.5
  113.7 3.3 %all-to-all-start.1 = ((bf16[4,128,128]{2,1,0:T(8,128)(2,1)}), bf16[4,128,128]{2,1,0:T(8,128)(2,1)S(1)}, u32[]{:S(2)}, u32[]{:S(2)}) async-start(bf16[4,128,128]{2,1,0:T(8,128)(2,1)} %get-tuple-element.24), calls=%async_computation.1 | async-start | bytes 262144 | tf_op jit(solution)/shard_map/all_to_all | solution.py:499
  117.0 0.0 copy-start.4
  117.1 1.1 copy.24
  118.1 1.5 copy.25
  119.6 4.5 %collective-permute-start.5 = (bf16[256,2048]{1,0:T(8,128)(2,1)S(1)}, bf16[256,2048]{1,0:T(8,128)(2,1)}, u32[]{:S(2)}, u32[]{:S(2)}) collective-permute-start(bf16[256,2048]{1,0:T(8,128)(2,1)S(1)} %bitcast.42), channel_id=1, source_target_pairs={{0,6},{1,7},{2,0},{3,1},{4,2},{5,3},{6,4},{7,5},{8,14},{9,15},{10,... | collective-permute-start | bytes 3145736 | tf_op jit(solution)/shard_map/ppermute | solution.py:495
  124.1 2.3 %collective-permute-start.6 = (bf16[256,2048]{1,0:T(8,128)(2,1)S(1)}, bf16[256,2048]{1,0:T(8,128)(2,1)}, u32[]{:S(2)}, u32[]{:S(2)}) collective-permute-start(bf16[256,2048]{1,0:T(8,128)(2,1)S(1)} %bitcast.43), channel_id=1, source_target_pairs={{0,4},{1,5},{2,6},{3,7},{4,0},{5,1},{6,2},{7,3},{8,12},{9,13},{10,... | collective-permute-start | bytes 3145736 | tf_op jit(solution)/shard_map/ppermute | solution.py:495
  126.4 2.7 %collective-permute-start.7 = (bf16[256,2048]{1,0:T(8,128)(2,1)S(1)}, bf16[256,2048]{1,0:T(8,128)(2,1)}, u32[]{:S(2)}, u32[]{:S(2)}) collective-permute-start(bf16[256,2048]{1,0:T(8,128)(2,1)S(1)} %bitcast.44), channel_id=1, source_target_pairs={{0,2},{1,3},{2,4},{3,5},{4,6},{5,7},{6,0},{7,1},{8,10},{9,11},{10,... | collective-permute-start | bytes 3145736 | tf_op jit(solution)/shard_map/ppermute | solution.py:495
  129.1 3.3 %collective-permute-start.4 = (bf16[16,2048]{1,0:T(8,128)(2,1)S(1)}, bf16[16,2048]{1,0:T(8,128)(2,1)S(1)}, u32[]{:S(2)}, u32[]{:S(2)}) collective-permute-start(bf16[16,2048]{1,0:T(8,128)(2,1)S(1)} %copy-done.10), channel_id=1, source_target_pairs={{0,32},{32,64},{64,96},{96,128},{128,160},{160,192},{192,224},{224... | collective-permute-start | bytes 196616 | tf_op jit(solution)/shard_map/ppermute | solution.py:490
  132.5 0.6 pad_add_fusion.at_ref
  133.1 0.7 collective-permute-done.4.halo_ref
  133.8 0.0 all-to-all-done.1.pieces_ref
  133.8 0.6 copy-done.3
  134.4 2.0 group_map.1
  136.4 8.1 %all-to-all-start.2 = ((bf16[4,128,128]{2,1,0:T(8,128)(2,1)}), bf16[4,128,128]{2,1,0:T(8,128)(2,1)S(1)}, u32[]{:S(2)}, u32[]{:S(2)}) async-start(bf16[4,128,128]{2,1,0:T(8,128)(2,1)} %get-tuple-element.26), calls=%async_computation.2 | async-start | bytes 262144 | tf_op jit(solution)/shard_map/all_to_all | solution.py:499
  144.5 0.0 copy-done.4
  144.5 0.1 copy.23
  144.5 0.1 reshape.38.init_ref
  144.6 6.0 %conv_mix.1 = (bf16[1024,128]{1,0:T(8,128)(2,1)}, bf16[1024,128]{1,0:T(8,128)(2,1)}) custom-call(s32[2]{0:T(128)S(1)} %pad_add_fusion.1.place_ref, bf16[4,128,2048]{2,1,0:T(8,128)(2,1)S(1)} %pad_maximum_fusion.same_ref, bf16[4,128,2048]{2,1,0:T(8,128)(2,1)} %collective-permute-done.3.other_ref, bf16[2048,1024]{1,0:T(8,128)(2,1)} %all-gather.2.cloned.1.call-done.w_ref, ...), custom_call_target="tpu_custom_call" | custom-call | tf_op jit(solution)/shard_map/conv_mix/pallas_call | solution.py:291
  150.6 3.6 %local_reads.1 = (f32[1024,128]{1,0:T(8,128)}, bf16[1024,128]{1,0:T(8,128)(2,1)}) custom-call(bf16[1024,128]{1,0:T(8,128)(2,1)} %get-tuple-element.28.q_ref, bf16[1024,128]{1,0:T(8,128)(2,1)} %get-tuple-element.29.gk_ref, bf16[1024,128]{1,0:T(8,128)(2,1)} %get-tuple-element.30.gb_ref, bf16[1024,256]{1,0:T(8,128)(2,1)} %get-tuple-element.31.wu_ref, ...), custom_call_target="tpu_custom_call" | custom-call | tf_op jit(solution)/shard_map/local_reads/pallas_call | solution.py:344
  154.3 2.3 %all-to-all-done.2.far_ref = bf16[4,128,128]{2,1,0:T(8,128)(2,1)S(1)} async-done(((bf16[4,128,128]{2,1,0:T(8,128)(2,1)}), bf16[4,128,128]{2,1,0:T(8,128)(2,1)S(1)}, u32[]{:S(2)}, u32[]{:S(2)}) %all-to-all-start.2) | async-done | bytes 131104 | tf_op jit(solution)/shard_map/all_to_all | solution.py:499
  156.5 0.0 copy-done.1
  156.5 3.5 %finish_mix.1 = bf16[1024,256]{1,0:T(8,128)(2,1)} custom-call(s32[2]{0:T(128)S(1)} %copy-done.1, f32[128,128]{1,0:T(8,128)S(1)} %copy-done, bf16[4,128,128]{2,1,0:T(8,128)(2,1)S(1)} %all-to-all-done.2.far_ref, f32[64,128]{1,0:T(8,128)S(1)} %reshape.38.init_ref, f32[1024,128]{1,0:T(8,128)} %get-tuple-element.36.o_ref, ...), custom_call_target="tpu_custom_call" | custom-call | tf_op jit(solution)/shard_map/finish_mix/pallas_call | solution.py:426
  160.1 3.5 %all-to-all-start.3 = ((bf16[4,256,256]{2,1,0:T(8,128)(2,1)}), bf16[4,256,256]{2,1,0:T(8,128)(2,1)S(1)}, u32[]{:S(2)}, u32[]{:S(2)}) async-start(bf16[4,256,256]{2,1,0:T(8,128)(2,1)} %bitcast.48), calls=%async_computation.3 | async-start | bytes 1048576 | tf_op jit(solution)/shard_map/all_to_all | solution.py:593
  163.5 0.1 stack.76.pick_ref
  163.6 0.0 collective-permute-done.5.refs_1_
  163.6 0.0 collective-permute-done.6.refs_2_
  163.6 12.9 %collective-permute-done.7.refs_3_ = bf16[256,2048]{1,0:T(8,128)(2,1)} collective-permute-done((bf16[256,2048]{1,0:T(8,128)(2,1)S(1)}, bf16[256,2048]{1,0:T(8,128)(2,1)}, u32[]{:S(2)}, u32[]{:S(2)}) %collective-permute-start.7) | collective-permute-done | bytes 1048608 | tf_op jit(solution)/shard_map/ppermute | solution.py:495
  176.5 1.1 all-to-all-done.3.m_ref
  177.6 2.6 %outward.3 = bf16[128,2048]{1,0:T(8,128)(2,1)S(1)} custom-call(s32[5]{0:T(128)S(1)} %stack.76.pick_ref, bf16[4,256,256]{2,1,0:T(8,128)(2,1)S(1)} %all-to-all-done.3.m_ref, bf16[256,2048]{1,0:T(8,128)(2,1)S(1)} %bitcast.45, bf16[256,2048]{1,0:T(8,128)(2,1)} %collective-permute-done.5.refs_1_, bf16[256,2048]{1,0:T(8,128)(2,1)} %collective-permute-done.6.refs_2_, ...), custom_call_target="tpu_custom_call" | custom-call | tf_op jit(solution)/shard_map/outward/pallas_call | solution.py:460
  180.2 10.3 %collective-permute-start.8 = (bf16[128,2048]{1,0:T(8,128)(2,1)S(1)}, bf16[128,2048]{1,0:T(8,128)(2,1)S(1)}, u32[]{:S(2)}, u32[]{:S(2)}) collective-permute-start(bf16[128,2048]{1,0:T(8,128)(2,1)S(1)} %outward.3), channel_id=1, source_target_pairs={{0,1},{1,0},{2,3},{3,2},{4,5},{5,4},{6,7},{7,6},{8,9},{9,8},{10,11... | collective-permute-start | bytes 1572872 | tf_op jit(solution)/shard_map/ppermute | solution.py:536
  190.5 0.1 stack.64.pick_ref
  190.6 2.6 %outward.2 = bf16[128,2048]{1,0:T(8,128)(2,1)S(1)} custom-call(s32[5]{0:T(128)S(1)} %stack.64.pick_ref, bf16[4,256,256]{2,1,0:T(8,128)(2,1)S(1)} %all-to-all-done.3.m_ref, bf16[256,2048]{1,0:T(8,128)(2,1)S(1)} %bitcast.46, bf16[256,2048]{1,0:T(8,128)(2,1)} %collective-permute-done.5.refs_1_, bf16[256,2048]{1,0:T(8,128)(2,1)} %collective-permute-done.6.refs_2_, ...), custom_call_target="tpu_custom_call" | custom-call | tf_op jit(solution)/shard_map/outward/pallas_call | solution.py:460
  193.2 0.0 collective-permute-done.8
  193.2 0.9 fusion.7
  (15 shorter events, 0.1 us)
Async XLA Ops:
  6.5 24.1 %copy-start.2 = (bf16[1,128,2048]{2,1,0:T(8,128)(2,1)S(1)}, bf16[1,128,2048]{2,1,0:T(8,128)(2,1)}, u32[]{:S(2)}) copy-start(bf16[1,128,2048]{2,1,0:T(8,128)(2,1)} %param.18) | copy-start | bytes 1572868
  6.5 24.1 %copy-start.5 = (f32[2048]{0:T(1024)S(1)}, f32[2048]{0:T(1024)}, u32[]{:S(2)}) copy-start(f32[2048]{0:T(1024)} %param.19) | copy-start | bytes 24580
  6.5 96.2 %all-gather.2.cloned.1.call-start = ((), (), s32[]{:S(2)}) async-start(), calls=%async_computation.6 | async-start | bytes 4456448 | tf_op jit(solution)/shard_map/all_gather | solution.py:554
  21.3 15.5 %collective-permute-start = (bf16[128,2048]{1,0:T(8,128)(2,1)S(1)}, bf16[128,2048]{1,0:T(8,128)(2,1)S(1)}, u32[]{:S(2)}, u32[]{:S(2)}) collective-permute-start(bf16[128,2048]{1,0:T(8,128)(2,1)S(1)} %fusion.4), channel_id=1, source_target_pairs={{0,6},{1,7},{2,0},{3,1},{4,2},{5,3},{6,4},{7,5},{8,14},{9,15},{10,... | collective-permute-start | bytes 1572872 | tf_op jit(solution)/shard_map/ppermute | solution.py:495
  25.7 12.5 %collective-permute-start.1 = (bf16[128,2048]{1,0:T(8,128)(2,1)S(1)}, bf16[128,2048]{1,0:T(8,128)(2,1)S(1)}, u32[]{:S(2)}, u32[]{:S(2)}) collective-permute-start(bf16[128,2048]{1,0:T(8,128)(2,1)S(1)} %fusion.4), channel_id=1, source_target_pairs={{0,4},{1,5},{2,6},{3,7},{4,0},{5,1},{6,2},{7,3},{8,12},{9,13},{10,... | collective-permute-start | bytes 1572872 | tf_op jit(solution)/shard_map/ppermute | solution.py:495
  28.2 25.4 %collective-permute-start.2 = (bf16[128,2048]{1,0:T(8,128)(2,1)S(1)}, bf16[128,2048]{1,0:T(8,128)(2,1)S(1)}, u32[]{:S(2)}, u32[]{:S(2)}) collective-permute-start(bf16[128,2048]{1,0:T(8,128)(2,1)S(1)} %fusion.4), channel_id=1, source_target_pairs={{0,2},{1,3},{2,4},{3,5},{4,6},{5,7},{6,0},{7,1},{8,10},{9,11},{10,... | collective-permute-start | bytes 1572872 | tf_op jit(solution)/shard_map/ppermute | solution.py:495
  53.8 43.0 %collective-permute-start.3 = (bf16[4,128,2048]{2,1,0:T(8,128)(2,1)S(1)}, bf16[4,128,2048]{2,1,0:T(8,128)(2,1)}, u32[]{:S(2)}, u32[]{:S(2)}) collective-permute-start(bf16[4,128,2048]{2,1,0:T(8,128)(2,1)S(1)} %pad_maximum_fusion.same_ref), channel_id=1, source_target_pairs={{0,1},{1,0},{2,3},{3,2},{4,5},{5,4},{6,7},{7,6},{8,9},{9,8},{10,11... | collective-permute-start | bytes 6291464 | tf_op jit(solution)/shard_map/ppermute | solution.py:536
  56.9 39.8 %copy-start.6 = (f32[3,128]{1,0:T(4,128)S(1)}, f32[3,128]{1,0:T(4,128)}, u32[]{:S(2)}) copy-start(f32[3,128]{1,0:T(4,128)} %param.23) | copy-start | bytes 4612
  56.9 39.8 %copy-start.7 = (f32[128]{0:T(128)S(1)}, f32[128]{0:T(128)}, u32[]{:S(2)}) copy-start(f32[128]{0:T(128)} %param.29) | copy-start | bytes 1540
  56.9 39.8 %copy-start.8 = (f32[128]{0:T(128)S(1)}, f32[128]{0:T(128)}, u32[]{:S(2)}) copy-start(f32[128]{0:T(128)} %param.30) | copy-start | bytes 1540
  56.9 39.8 %copy-start.9 = (f32[128]{0:T(128)S(1)}, f32[128]{0:T(128)}, u32[]{:S(2)}) copy-start(f32[128]{0:T(128)} %param.33) | copy-start | bytes 1540
  93.1 20.6 %all-to-all-start.5 = ((bf16[4,16,32,256]{3,2,1,0:T(8,128)(2,1)}), bf16[4,16,32,256]{3,2,1,0:T(8,128)(2,1)S(1)}, u32[]{:S(2)}, u32[]{:S(2)}) async-start(bf16[4,16,32,256]{3,2,1,0:T(8,128)(2,1)} %broadcast_in_dim.27), calls=%async_computation.5 | async-start | bytes 2097152 | tf_op jit(solution)/shard_map/all_to_all | solution.py:499
  113.7 20.1 %all-to-all-start.1 = ((bf16[4,128,128]{2,1,0:T(8,128)(2,1)}), bf16[4,128,128]{2,1,0:T(8,128)(2,1)S(1)}, u32[]{:S(2)}, u32[]{:S(2)}) async-start(bf16[4,128,128]{2,1,0:T(8,128)(2,1)} %get-tuple-element.24), calls=%async_computation.1 | async-start | bytes 262144 | tf_op jit(solution)/shard_map/all_to_all | solution.py:499
  117.0 12.1 %copy-start.10 = (bf16[16,2048]{1,0:T(8,128)(2,1)S(1)}, bf16[16,2048]{1,0:T(8,128)(2,1)}, u32[]{:S(2)}) copy-start(bf16[16,2048]{1,0:T(8,128)(2,1)} %get-tuple-element.22) | copy-start | bytes 196612
  117.0 27.4 %copy-start.4 = (f32[1,2,64,64]{3,2,1,0:T(8,128)S(1)}, f32[1,2,64,64]{3,2,1,0:T(8,128)}, u32[]{:S(2)}) copy-start(f32[1,2,64,64]{3,2,1,0:T(8,128)} %param.32) | copy-start | bytes 98308
  119.6 44.0 %collective-permute-start.5 = (bf16[256,2048]{1,0:T(8,128)(2,1)S(1)}, bf16[256,2048]{1,0:T(8,128)(2,1)}, u32[]{:S(2)}, u32[]{:S(2)}) collective-permute-start(bf16[256,2048]{1,0:T(8,128)(2,1)S(1)} %bitcast.42), channel_id=1, source_target_pairs={{0,6},{1,7},{2,0},{3,1},{4,2},{5,3},{6,4},{7,5},{8,14},{9,15},{10,... | collective-permute-start | bytes 3145736 | tf_op jit(solution)/shard_map/ppermute | solution.py:495
  124.1 39.6 %collective-permute-start.6 = (bf16[256,2048]{1,0:T(8,128)(2,1)S(1)}, bf16[256,2048]{1,0:T(8,128)(2,1)}, u32[]{:S(2)}, u32[]{:S(2)}) collective-permute-start(bf16[256,2048]{1,0:T(8,128)(2,1)S(1)} %bitcast.43), channel_id=1, source_target_pairs={{0,4},{1,5},{2,6},{3,7},{4,0},{5,1},{6,2},{7,3},{8,12},{9,13},{10,... | collective-permute-start | bytes 3145736 | tf_op jit(solution)/shard_map/ppermute | solution.py:495
  126.4 50.1 %collective-permute-start.7 = (bf16[256,2048]{1,0:T(8,128)(2,1)S(1)}, bf16[256,2048]{1,0:T(8,128)(2,1)}, u32[]{:S(2)}, u32[]{:S(2)}) collective-permute-start(bf16[256,2048]{1,0:T(8,128)(2,1)S(1)} %bitcast.44), channel_id=1, source_target_pairs={{0,2},{1,3},{2,4},{3,5},{4,6},{5,7},{6,0},{7,1},{8,10},{9,11},{10,... | collective-permute-start | bytes 3145736 | tf_op jit(solution)/shard_map/ppermute | solution.py:495
  129.1 4.6 %collective-permute-start.4 = (bf16[16,2048]{1,0:T(8,128)(2,1)S(1)}, bf16[16,2048]{1,0:T(8,128)(2,1)S(1)}, u32[]{:S(2)}, u32[]{:S(2)}) collective-permute-start(bf16[16,2048]{1,0:T(8,128)(2,1)S(1)} %copy-done.10), channel_id=1, source_target_pairs={{0,32},{32,64},{64,96},{96,128},{128,160},{160,192},{192,224},{224... | collective-permute-start | bytes 196616 | tf_op jit(solution)/shard_map/ppermute | solution.py:490
  133.8 0.6 copy-start.3
  136.4 20.1 %all-to-all-start.2 = ((bf16[4,128,128]{2,1,0:T(8,128)(2,1)}), bf16[4,128,128]{2,1,0:T(8,128)(2,1)S(1)}, u32[]{:S(2)}, u32[]{:S(2)}) async-start(bf16[4,128,128]{2,1,0:T(8,128)(2,1)} %get-tuple-element.26), calls=%async_computation.2 | async-start | bytes 262144 | tf_op jit(solution)/shard_map/all_to_all | solution.py:499
  150.6 5.9 %copy-start = (f32[128,128]{1,0:T(8,128)S(1)}, f32[128,128]{1,0:T(8,128)}, u32[]{:S(2)}) copy-start(f32[128,128]{1,0:T(8,128)} %get-tuple-element.25.before_ref) | copy-start | bytes 196612
  150.6 5.9 %copy-start.1 = (s32[2]{0:T(128)S(1)}, s32[2]{0:T(128)}, u32[]{:S(2)}) copy-start(s32[2]{0:T(128)} %pad_add_fusion.at_ref) | copy-start | bytes 28
  160.1 17.6 %all-to-all-start.3 = ((bf16[4,256,256]{2,1,0:T(8,128)(2,1)}), bf16[4,256,256]{2,1,0:T(8,128)(2,1)S(1)}, u32[]{:S(2)}, u32[]{:S(2)}) async-start(bf16[4,256,256]{2,1,0:T(8,128)(2,1)} %bitcast.48), calls=%async_computation.3 | async-start | bytes 1048576 | tf_op jit(solution)/shard_map/all_to_all | solution.py:593
  180.2 13.0 %collective-permute-start.8 = (bf16[128,2048]{1,0:T(8,128)(2,1)S(1)}, bf16[128,2048]{1,0:T(8,128)(2,1)S(1)}, u32[]{:S(2)}, u32[]{:S(2)}) collective-permute-start(bf16[128,2048]{1,0:T(8,128)(2,1)S(1)} %outward.3), channel_id=1, source_target_pairs={{0,1},{1,0},{2,3},{3,2},{4,5},{5,4},{6,7},{7,6},{8,9},{9,8},{10,11... | collective-permute-start | bytes 1572872 | tf_op jit(solution)/shard_map/ppermute | solution.py:536
Sparse Core Ops, SparseCore 0:
  18.9 83.7 all-gather.1

commit v10 on v9

--- a/solution.py
+++ b/solution.py
@@ -91,7 +91,6 @@
     pos_ref,
     full_ref,
     states_ref,
-    last_ref,
     agg_ref,
     st_ref,
 ):
@@ -196,7 +195,6 @@
 
     @pl.when(step == pl.num_programs(0) - 1)
     def _():
-        last_ref[...] = x[MAPS_BLOCK - last_ref.shape[0] :]
         for k in range(agg_ref.shape[0]):
             agg_ref[k] = state.astype(bf16)
 
@@ -231,7 +229,6 @@
                 tile,
                 tile,
                 pl.BlockSpec((pairs, width, width), lambda i, p: (i, 0, 0)),
-                pl.BlockSpec((HALO, depth), lambda i, p: (0, 0)),
                 pl.BlockSpec((copies, width, width), lambda i, p: (0, 0, 0)),
             ],
             scratch_shapes=[pltpu.VMEM((width, width), f32)],
@@ -244,7 +241,6 @@
             like(width, f32),
             like(width, f32),
             array((rows // CHUNK, width, width), bf16),
-            array((HALO, depth), bf16),
             array((copies, width, width), bf16),
         ],
         compiler_params=pltpu.CompilerParams(
@@ -392,7 +388,7 @@
             jax.ShapeDtypeStruct(pieces.shape[1:], f32),
         ],
         name="group_map",
-    )(at, pieces)
+    )(at, pltpu.with_memory_space_constraint(pieces, pltpu.VMEM))
 
 
 def finish_kernel(at_ref, before_ref, far_ref, init_ref, o_ref, y_ref, conv_ref, vec_ref, out_ref, s_ref):
@@ -441,17 +437,18 @@
 
 
 def outward_kernel(pick_ref, m_ref, *refs):
-    *weights, out_ref = refs
-    rows, columns = out_ref.shape
-    at = pl.multiple_of(pick_ref[0], rows)
-    parts = [m_ref[pick_ref[1 + k], pl.ds(at, rows), :] for k in range(len(weights))]
+    *weights, keep_ref, give_ref = refs
+    rows, columns = keep_ref.shape
+    first = pick_ref[0] == 0
     step = 512
-    for first in range(0, columns, step):
+    for at in range(0, columns, step):
         total = None
-        for part, w_ref in zip(parts, weights):
-            got = dot(part, w_ref[:, first : first + step])
+        for k, w_ref in enumerate(weights):
+            got = dot(m_ref[pick_ref[1 + k]], w_ref[:, at : at + step])
             total = got if total is None else total + got
-        out_ref[:, first : first + step] = total.astype(bf16)
+        total = total.astype(bf16)
+        keep_ref[:, at : at + step] = jnp.where(first, total[:rows], total[rows:])
+        give_ref[:, at : at + step] = jnp.where(first, total[rows:], total[:rows])
 
 
 def outward_call(pick, gathered, weights):
@@ -460,8 +457,8 @@
     return pl.pallas_call(
         outward_kernel,
         in_specs=[pl.BlockSpec(memory_space=pltpu.SMEM)] + [here] * (1 + len(weights)),
-        out_specs=here,
-        out_shape=jax.ShapeDtypeStruct((rows, columns), bf16),
+        out_specs=[here, here],
+        out_shape=[jax.ShapeDtypeStruct((rows, columns), bf16)] * 2,
         compiler_params=pltpu.CompilerParams(vmem_limit_bytes=24 * 2**20),
         name="outward",
     )(pick, gathered, *weights)
@@ -573,31 +570,31 @@
         ],
         axis=0,
     )
+    init = jnp.moveaxis(initial_state[0], 0, 1).reshape(HEAD_WIDTH, heads * HEAD_WIDTH)
+    vec, init = lax.optimization_barrier((vec, init))
     place = jnp.stack([chip, core])
+    last_rows = jnp.where(core == 0, other[:, -HALO:], same[:, -HALO:])
+    last_rows = lax.dynamic_index_in_dim(last_rows, (chips - 1 - chip) & (chips - 1), 0, keepdims=False)
+    halo = passed_along(last_rows, "sp", 1)
     few = 4
     near_blocks = [list(range(k, k + few)) for k in range(0, blocks, few)]
     far_blocks = [list(range(k, blocks, few)) for k in range(few)]
-    *kept, last_rows, agg = maps_call(place, same, other, weights, decay_spike[0], vec, few)
+    *kept, agg = maps_call(place, same, other, weights, decay_spike[0], vec, few)
     near_maps = from_everyone(agg, "sp", near_blocks)
-    halo = passed_along(last_rows, "sp", 1)
     block = lax.axis_index("sp").astype(jnp.int32)
     at = jnp.stack([lax.shift_right_logical(block, 2), block & (few - 1)])
-    at, halo = lax.optimization_barrier((at, halo))
     total, earlier = group_call(at, near_maps, blocks // few)
     far_maps = from_everyone(total, "sp", far_blocks)
     q, conv = conv_call(place, same, other, weights, halo, vec)
     o, y = reads_call(q, *kept)
-    init = jnp.moveaxis(initial_state[0], 0, 1).reshape(HEAD_WIDTH, heads * HEAD_WIDTH)
     mixed = finish_call(at, earlier, far_maps, init, o, y, conv, vec)
     groups = [list(range(side, devices, 2)) for side in range(2)]
     gathered = lax.all_to_all(
         mixed.reshape(chips, -1, 2 * channels), "tp", 0, 0, tiled=True, axis_index_groups=groups
     )
     near = [(chip + k) & (chips - 1) for k in (0, 1, 2, chips - 1)]
-    own, ways = normed.shape[0], (outer, after, across, before)
-    given = outward_call(jnp.stack([(1 - core) * own, *near]), gathered, ways)
+    kept, given = outward_call(jnp.stack([core, *near]), gathered, (outer, after, across, before))
     taken = core_swap(given)
-    kept = outward_call(jnp.stack([core * own, *near]), gathered, ways)
     return (kept.astype(f32) + taken.astype(f32)).astype(bf16)[None]
 
 

time: 202 us -> 196 us (0.970)
  starting transfers between devices: 53.9 us -> 49.9 us
  Pallas kernels: 34.3 us -> 32 us
    ppermute x6, waiting for transfers between devices: 35.5 us -> 30.2 us  [turned(): lax.ppermute(x, 'tp', [(i, (i + distance) % devices) for i in range(devic...]
    ppermute x2, starting transfers between devices: 13.4 us -> 9.05 us  [core_swap(): return lax.ppermute(x, 'tp', [(i, i ^ 1) for i in range(devices)])]
    all_gather x1, waiting for transfers between devices: 5.99 us -> 8.72 us  [mixing(): weights = lax.all_gather(weights, 'sp', axis=0, tiled=True)]
    all_to_all x3, waiting for transfers between devices: 2.27 us -> 0.01 us  [from_everyone(): lax.all_to_all(copies, axis, 0, 0, tiled=True, axis_index_groups=groups)]
    pallas_call x2 -> x1, Pallas kernels: 5.17 us -> 3.12 us  [outward_call(): pl.pallas_call(outward_kernel, in_specs=[pl.BlockSpec(memory_space=pltpu....]
  transfers between devices with their start and end apart: 14 -> 14, of which waited for: 8 -> 8; matrix products, arithmetic and copies ran while one was open for 4% -> 4% of each run, Pallas kernels for 15% -> 14%
where the time goes in v10:
time: 196 us; the launch traced here: 195 us
  starting transfers between devices  49.9 us (25%)
  blocking collectives  45.4 us (23%)
  waiting for transfers between devices  44.5 us (23%)
  Pallas kernels  32 us (16%)
  between operations  13.6 us (7%)
  local copies, waits for them, and re-layouts  4.93 us (3%)
  other arithmetic  4.52 us (2%)
    all_to_all x2, blocking collectives, from_everyone(): lax.all_to_all(copies, axis, 0, 0, tiled=True, axis_index_groups=groups)  45.4 us
    ppermute x6, waiting for transfers between devices, turned(): lax.ppermute(x, 'tp', [(i, (i + distance) % devices) for i in range(devic...  30.2 us
    ppermute x6, starting transfers between devices, turned(): lax.ppermute(x, 'tp', [(i, (i + distance) % devices) for i in range(devic...  20.2 us
    all_to_all x3, starting transfers between devices, from_everyone(): lax.all_to_all(copies, axis, 0, 0, tiled=True, axis_index_groups=groups)  13.8 us
    pallas_call x1, Pallas kernels, maps_call(): pl.pallas_call(maps_kernel, grid_spec=pltpu.PrefetchScalarGridSpec(num_sc...  10.9 us
    ppermute x2, starting transfers between devices, core_swap(): return lax.ppermute(x, 'tp', [(i, i ^ 1) for i in range(devices)])  9.05 us
    all_gather x1, waiting for transfers between devices, mixing(): weights = lax.all_gather(weights, 'sp', axis=0, tiled=True)  8.72 us
    pallas_call x1, Pallas kernels, conv_call(): pl.pallas_call(conv_kernel, grid_spec=pltpu.PrefetchScalarGridSpec(num_sc...  5.97 us
  transfers between devices with their start and end apart: 14, of which 8 were waited for; matrix products, arithmetic and copies ran while one was open for 4% of the time, Pallas kernels for 14%

profile of v10, /device:TPU:1, one launch (start us, length us, event | category | flops | bytes accessed | tf_op | source)
XLA Modules:
  0.0 194.9 jit_solution(8451212719403405762)
XLA Ops:
  6.5 0.0 copy-start.2
  6.5 0.0 all-gather.2.cloned.1.call-start
  6.5 1.6 pack_shards.2
  8.2 10.6 %all_to_all.30 = bf16[4,32,1024]{2,1,0:T(8,128)(2,1)} all-to-all(bf16[4,32,1024]{2,1,0:T(8,128)(2,1)} %pack_shards.2), channel_id=1, replica_groups=mesh['sp'=16,'fs'=4,'tp'=8] {'fs'}, dimensions={0} | all-to-all | bytes 524288 | tf_op jit(solution)/shard_map/all_to_all | solution.py:496
  18.8 0.0 all-gather.2.cloned.1.call-update
  18.8 1.2 fusion.2
  20.1 1.2 fusion.4
  21.3 4.7 %collective-permute-start.1 = (bf16[128,2048]{1,0:T(8,128)(2,1)S(1)}, bf16[128,2048]{1,0:T(8,128)(2,1)S(1)}, u32[]{:S(2)}, u32[]{:S(2)}) collective-permute-start(bf16[128,2048]{1,0:T(8,128)(2,1)S(1)} %fusion.4), channel_id=1, source_target_pairs={{0,4},{1,5},{2,6},{3,7},{4,0},{5,1},{6,2},{7,3},{8,12},{9,13},{10,... | collective-permute-start | bytes 1572872 | tf_op jit(solution)/shard_map/ppermute | solution.py:492
  26.0 2.2 %collective-permute-start.2 = (bf16[128,2048]{1,0:T(8,128)(2,1)S(1)}, bf16[128,2048]{1,0:T(8,128)(2,1)S(1)}, u32[]{:S(2)}, u32[]{:S(2)}) collective-permute-start(bf16[128,2048]{1,0:T(8,128)(2,1)S(1)} %fusion.4), channel_id=1, source_target_pairs={{0,2},{1,3},{2,4},{3,5},{4,6},{5,7},{6,0},{7,1},{8,10},{9,11},{10,... | collective-permute-start | bytes 1572872 | tf_op jit(solution)/shard_map/ppermute | solution.py:492
  28.2 4.3 %collective-permute-start = (bf16[128,2048]{1,0:T(8,128)(2,1)S(1)}, bf16[128,2048]{1,0:T(8,128)(2,1)S(1)}, u32[]{:S(2)}, u32[]{:S(2)}) collective-permute-start(bf16[128,2048]{1,0:T(8,128)(2,1)S(1)} %fusion.4), channel_id=1, source_target_pairs={{0,6},{1,7},{2,0},{3,1},{4,2},{5,3},{6,4},{7,5},{8,14},{9,15},{10,... | collective-permute-start | bytes 1572872 | tf_op jit(solution)/shard_map/ppermute | solution.py:492
  32.5 0.0 copy-done.2
  32.5 0.0 copy-done.4
  32.5 0.2 fusion.6
  32.7 0.7 collective-permute-done.1
  33.4 13.8 %collective-permute-done.2 = bf16[128,2048]{1,0:T(8,128)(2,1)S(1)} collective-permute-done((bf16[128,2048]{1,0:T(8,128)(2,1)S(1)}, bf16[128,2048]{1,0:T(8,128)(2,1)S(1)}, u32[]{:S(2)}, u32[]{:S(2)}) %collective-permute-start.2) | collective-permute-done | bytes 524320 | tf_op jit(solution)/shard_map/ppermute | solution.py:492
  47.2 0.4 collective-permute-done
  47.6 0.3 pad_maximum_fusion.same_ref
  47.9 4.7 %collective-permute-start.3 = (bf16[4,128,2048]{2,1,0:T(8,128)(2,1)S(1)}, bf16[4,128,2048]{2,1,0:T(8,128)(2,1)}, u32[]{:S(2)}, u32[]{:S(2)}) collective-permute-start(bf16[4,128,2048]{2,1,0:T(8,128)(2,1)S(1)} %pad_maximum_fusion.same_ref), channel_id=1, source_target_pairs={{0,1},{1,0},{2,3},{3,2},{4,5},{5,4},{6,7},{7,6},{8,9},{9,8},{10,11... | collective-permute-start | bytes 6291464 | tf_op jit(solution)/shard_map/ppermute | solution.py:533
  52.6 0.0 copy-start.3
  52.6 1.5 pack_shards.3
  54.1 34.8 %all_to_all.31 = bf16[16,32,256]{2,1,0:T(8,128)(2,1)S(1)} all-to-all(bf16[16,32,256]{2,1,0:T(8,128)(2,1)} %pack_shards.3), channel_id=1, replica_groups=mesh['sp'=16,'fs'=4,'tp'=8] {'sp'}, dimensions={0} | all-to-all | bytes 524288 | tf_op jit(solution)/shard_map/all_to_all | solution.py:496
  88.9 1.1 broadcast_in_dim.27
  90.0 3.5 %all-to-all-start.5 = ((bf16[4,16,32,256]{3,2,1,0:T(8,128)(2,1)}), bf16[4,16,32,256]{3,2,1,0:T(8,128)(2,1)S(1)}, u32[]{:S(2)}, u32[]{:S(2)}) async-start(bf16[4,16,32,256]{3,2,1,0:T(8,128)(2,1)} %broadcast_in_dim.27), calls=%async_computation.5 | async-start | bytes 2097152 | tf_op jit(solution)/shard_map/all_to_all | solution.py:496
  93.5 0.0 copy-done.3
  93.5 0.1 copy.23
  93.6 0.1 reshape.38.init_ref
  93.7 0.0 copy-done.5
  93.7 0.0 copy-done.6
  93.7 0.0 copy-done.7
  93.7 0.0 copy-done.8
  93.7 0.1 pad_add_fusion.1.place_ref
  93.8 0.0 collective-permute-done.3.other_ref
  93.8 8.7 %all-gather.2.cloned.1.call-done.w_ref = bf16[2048,1024]{1,0:T(8,128)(2,1)} async-done(((bf16[128,1024]{1,0:T(8,128)(2,1)}), bf16[2048,1024]{1,0:T(8,128)(2,1)}) %all-gather.2.cloned.1.call-update) | async-done | bytes 4194320 | tf_op jit(solution)/shard_map/all_gather | solution.py:551
  102.5 10.9 %state_maps.1 = (bf16[1024,128]{1,0:T(8,128)(2,1)}, bf16[1024,128]{1,0:T(8,128)(2,1)}, bf16[1024,256]{1,0:T(8,128)(2,1)}, bf16[1024,128]{1,0:T(8,128)(2,1)}, f32...) custom-call(s32[2]{0:T(128)S(1)} %pad_add_fusion.1.place_ref, ...), custom_call_target="tpu_custom_call" | custom-call | tf_op jit(solution)/shard_map/state_maps/pallas_call | solution.py:213
  113.5 0.0 all-to-all-done.5
  113.5 3.3 %all-to-all-start.1 = ((bf16[4,128,128]{2,1,0:T(8,128)(2,1)}), bf16[4,128,128]{2,1,0:T(8,128)(2,1)S(1)}, u32[]{:S(2)}, u32[]{:S(2)}) async-start(bf16[4,128,128]{2,1,0:T(8,128)(2,1)} %get-tuple-element.24), calls=%async_computation.1 | async-start | bytes 262144 | tf_op jit(solution)/shard_map/all_to_all | solution.py:496
  116.8 1.1 copy.24
  117.9 1.5 copy.25
  119.4 4.1 %collective-permute-start.5 = (bf16[256,2048]{1,0:T(8,128)(2,1)S(1)}, bf16[256,2048]{1,0:T(8,128)(2,1)}, u32[]{:S(2)}, u32[]{:S(2)}) collective-permute-start(bf16[256,2048]{1,0:T(8,128)(2,1)S(1)} %bitcast.42), channel_id=1, source_target_pairs={{0,6},{1,7},{2,0},{3,1},{4,2},{5,3},{6,4},{7,5},{8,14},{9,15},{10,... | collective-permute-start | bytes 3145736 | tf_op jit(solution)/shard_map/ppermute | solution.py:492
  123.5 2.5 %collective-permute-start.6 = (bf16[256,2048]{1,0:T(8,128)(2,1)S(1)}, bf16[256,2048]{1,0:T(8,128)(2,1)}, u32[]{:S(2)}, u32[]{:S(2)}) collective-permute-start(bf16[256,2048]{1,0:T(8,128)(2,1)S(1)} %bitcast.43), channel_id=1, source_target_pairs={{0,4},{1,5},{2,6},{3,7},{4,0},{5,1},{6,2},{7,3},{8,12},{9,13},{10,... | collective-permute-start | bytes 3145736 | tf_op jit(solution)/shard_map/ppermute | solution.py:492
  126.0 2.4 %collective-permute-start.7 = (bf16[256,2048]{1,0:T(8,128)(2,1)S(1)}, bf16[256,2048]{1,0:T(8,128)(2,1)}, u32[]{:S(2)}, u32[]{:S(2)}) collective-permute-start(bf16[256,2048]{1,0:T(8,128)(2,1)S(1)} %bitcast.44), channel_id=1, source_target_pairs={{0,2},{1,3},{2,4},{3,5},{4,6},{5,7},{6,0},{7,1},{8,10},{9,11},{10,... | collective-permute-start | bytes 3145736 | tf_op jit(solution)/shard_map/ppermute | solution.py:492
  128.4 0.6 pad_add_fusion.at_ref
  129.0 0.0 all-to-all-done.1.pieces_ref
  129.0 1.7 group_map.1
  130.8 7.0 %all-to-all-start.2 = ((bf16[4,128,128]{2,1,0:T(8,128)(2,1)}), bf16[4,128,128]{2,1,0:T(8,128)(2,1)S(1)}, u32[]{:S(2)}, u32[]{:S(2)}) async-start(bf16[4,128,128]{2,1,0:T(8,128)(2,1)} %get-tuple-element.26), calls=%async_computation.2 | async-start | bytes 262144 | tf_op jit(solution)/shard_map/all_to_all | solution.py:496
  137.7 1.0 slice.8
  138.8 3.3 %collective-permute-start.4 = (bf16[16,2048]{1,0:T(8,128)(2,1)S(1)}, bf16[16,2048]{1,0:T(8,128)(2,1)S(1)}, u32[]{:S(2)}, u32[]{:S(2)}) collective-permute-start(bf16[16,2048]{1,0:T(8,128)(2,1)S(1)} %fusion.8), channel_id=1, source_target_pairs={{0,32},{32,64},{64,96},{96,128},{128,160},{160,192},{192,224},{224... | collective-permute-start | bytes 196616 | tf_op jit(solution)/shard_map/ppermute | solution.py:487
  142.1 1.3 collective-permute-done.4.halo_ref
  143.4 6.0 %conv_mix.1 = (bf16[1024,128]{1,0:T(8,128)(2,1)}, bf16[1024,128]{1,0:T(8,128)(2,1)}) custom-call(s32[2]{0:T(128)S(1)} %pad_add_fusion.1.place_ref, bf16[4,128,2048]{2,1,0:T(8,128)(2,1)S(1)} %pad_maximum_fusion.same_ref, bf16[4,128,2048]{2,1,0:T(8,128)(2,1)} %collective-permute-done.3.other_ref, bf16[2048,1024]{1,0:T(8,128)(2,1)} %all-gather.2.cloned.1.call-done.w_ref, ...), custom_call_target="tpu_custom_call" | custom-call | tf_op jit(solution)/shard_map/conv_mix/pallas_call | solution.py:287
  149.4 3.6 %local_reads.1 = (f32[1024,128]{1,0:T(8,128)}, bf16[1024,128]{1,0:T(8,128)(2,1)}) custom-call(bf16[1024,128]{1,0:T(8,128)(2,1)} %get-tuple-element.28.q_ref, bf16[1024,128]{1,0:T(8,128)(2,1)} %get-tuple-element.29.gk_ref, bf16[1024,128]{1,0:T(8,128)(2,1)} %get-tuple-element.30.gb_ref, bf16[1024,256]{1,0:T(8,128)(2,1)} %get-tuple-element.31.wu_ref, ...), custom_call_target="tpu_custom_call" | custom-call | tf_op jit(solution)/shard_map/local_reads/pallas_call | solution.py:340
  153.0 0.0 all-to-all-done.2.far_ref
  153.0 0.0 copy-done
  153.0 0.0 copy-done.1
  153.1 3.5 %finish_mix.1 = bf16[1024,256]{1,0:T(8,128)(2,1)} custom-call(s32[2]{0:T(128)S(1)} %copy-done.1, f32[128,128]{1,0:T(8,128)S(1)} %copy-done, bf16[4,128,128]{2,1,0:T(8,128)(2,1)S(1)} %all-to-all-done.2.far_ref, f32[64,128]{1,0:T(8,128)S(1)} %reshape.38.init_ref, f32[1024,128]{1,0:T(8,128)} %get-tuple-element.36.o_ref, ...), custom_call_target="tpu_custom_call" | custom-call | tf_op jit(solution)/shard_map/finish_mix/pallas_call | solution.py:422
  156.6 3.5 %all-to-all-start.3 = ((bf16[4,256,256]{2,1,0:T(8,128)(2,1)}), bf16[4,256,256]{2,1,0:T(8,128)(2,1)S(1)}, u32[]{:S(2)}, u32[]{:S(2)}) async-start(bf16[4,256,256]{2,1,0:T(8,128)(2,1)} %bitcast.47), calls=%async_computation.3 | async-start | bytes 1048576 | tf_op jit(solution)/shard_map/all_to_all | solution.py:592
  160.1 0.1 stack.52.pick_ref
  160.1 0.0 collective-permute-done.5.refs_1_
  160.2 0.0 collective-permute-done.6.refs_2_
  160.2 15.3 %collective-permute-done.7.refs_3_ = bf16[256,2048]{1,0:T(8,128)(2,1)} collective-permute-done((bf16[256,2048]{1,0:T(8,128)(2,1)S(1)}, bf16[256,2048]{1,0:T(8,128)(2,1)}, u32[]{:S(2)}, u32[]{:S(2)}) %collective-permute-start.7) | collective-permute-done | bytes 1048608 | tf_op jit(solution)/shard_map/ppermute | solution.py:492
  175.5 2.7 %all-to-all-done.3.m_ref = bf16[4,256,256]{2,1,0:T(8,128)(2,1)S(1)} async-done(((bf16[4,256,256]{2,1,0:T(8,128)(2,1)}), bf16[4,256,256]{2,1,0:T(8,128)(2,1)S(1)}, u32[]{:S(2)}, u32[]{:S(2)}) %all-to-all-start.3) | async-done | bytes 524320 | tf_op jit(solution)/shard_map/all_to_all | solution.py:592
  178.2 3.1 %outward.1 = (bf16[128,2048]{1,0:T(8,128)(2,1)S(1)}, bf16[128,2048]{1,0:T(8,128)(2,1)S(1)}) custom-call(s32[5]{0:T(128)S(1)} %stack.52.pick_ref, bf16[4,256,256]{2,1,0:T(8,128)(2,1)S(1)} %all-to-all-done.3.m_ref, bf16[256,2048]{1,0:T(8,128)(2,1)S(1)} %bitcast.45, bf16[256,2048]{1,0:T(8,128)(2,1)} %collective-permute-done.5.refs_1_, ...), custom_call_target="tpu_custom_call" | custom-call | tf_op jit(solution)/shard_map/outward/pallas_call | solution.py:457
  181.3 4.3 %collective-permute-start.8 = (bf16[128,2048]{1,0:T(8,128)(2,1)S(1)}, bf16[128,2048]{1,0:T(8,128)(2,1)S(1)}, u32[]{:S(2)}, u32[]{:S(2)}) collective-permute-start(bf16[128,2048]{1,0:T(8,128)(2,1)S(1)} %get-tuple-element.40), channel_id=1, source_target_pairs={{0,1},{1,0},{2,3},{3,2},{4,5},{5,4},{6,7},{7,6},{8,9},{9,8},{10,11... | collective-permute-start | bytes 1572872 | tf_op jit(solution)/shard_map/ppermute | solution.py:533
  185.6 1.5 collective-permute-done.8
  187.1 0.9 fusion.7
  (12 shorter events, 0.1 us)
Async XLA Ops:
  6.5 26.0 %copy-start.2 = (bf16[1,128,2048]{2,1,0:T(8,128)(2,1)S(1)}, bf16[1,128,2048]{2,1,0:T(8,128)(2,1)}, u32[]{:S(2)}) copy-start(bf16[1,128,2048]{2,1,0:T(8,128)(2,1)} %param.18) | copy-start | bytes 1572868
  6.5 26.0 %copy-start.4 = (f32[2048]{0:T(1024)S(1)}, f32[2048]{0:T(1024)}, u32[]{:S(2)}) copy-start(f32[2048]{0:T(1024)} %param.19) | copy-start | bytes 24580
  6.5 96.0 %all-gather.2.cloned.1.call-start = ((), (), s32[]{:S(2)}) async-start(), calls=%async_computation.6 | async-start | bytes 4456448 | tf_op jit(solution)/shard_map/all_gather | solution.py:551
  21.3 12.1 %collective-permute-start.1 = (bf16[128,2048]{1,0:T(8,128)(2,1)S(1)}, bf16[128,2048]{1,0:T(8,128)(2,1)S(1)}, u32[]{:S(2)}, u32[]{:S(2)}) collective-permute-start(bf16[128,2048]{1,0:T(8,128)(2,1)S(1)} %fusion.4), channel_id=1, source_target_pairs={{0,4},{1,5},{2,6},{3,7},{4,0},{5,1},{6,2},{7,3},{8,12},{9,13},{10,... | collective-permute-start | bytes 1572872 | tf_op jit(solution)/shard_map/ppermute | solution.py:492
  26.0 21.2 %collective-permute-start.2 = (bf16[128,2048]{1,0:T(8,128)(2,1)S(1)}, bf16[128,2048]{1,0:T(8,128)(2,1)S(1)}, u32[]{:S(2)}, u32[]{:S(2)}) collective-permute-start(bf16[128,2048]{1,0:T(8,128)(2,1)S(1)} %fusion.4), channel_id=1, source_target_pairs={{0,2},{1,3},{2,4},{3,5},{4,6},{5,7},{6,0},{7,1},{8,10},{9,11},{10,... | collective-permute-start | bytes 1572872 | tf_op jit(solution)/shard_map/ppermute | solution.py:492
  28.2 19.4 %collective-permute-start = (bf16[128,2048]{1,0:T(8,128)(2,1)S(1)}, bf16[128,2048]{1,0:T(8,128)(2,1)S(1)}, u32[]{:S(2)}, u32[]{:S(2)}) collective-permute-start(bf16[128,2048]{1,0:T(8,128)(2,1)S(1)} %fusion.4), channel_id=1, source_target_pairs={{0,6},{1,7},{2,0},{3,1},{4,2},{5,3},{6,4},{7,5},{8,14},{9,15},{10,... | collective-permute-start | bytes 1572872 | tf_op jit(solution)/shard_map/ppermute | solution.py:492
  47.9 46.0 %collective-permute-start.3 = (bf16[4,128,2048]{2,1,0:T(8,128)(2,1)S(1)}, bf16[4,128,2048]{2,1,0:T(8,128)(2,1)}, u32[]{:S(2)}, u32[]{:S(2)}) collective-permute-start(bf16[4,128,2048]{2,1,0:T(8,128)(2,1)S(1)} %pad_maximum_fusion.same_ref), channel_id=1, source_target_pairs={{0,1},{1,0},{2,3},{3,2},{4,5},{5,4},{6,7},{7,6},{8,9},{9,8},{10,11... | collective-permute-start | bytes 6291464 | tf_op jit(solution)/shard_map/ppermute | solution.py:533
  52.6 40.9 %copy-start.3 = (f32[1,2,64,64]{3,2,1,0:T(8,128)S(1)}, f32[1,2,64,64]{3,2,1,0:T(8,128)}, u32[]{:S(2)}) copy-start(f32[1,2,64,64]{3,2,1,0:T(8,128)} %param.32) | copy-start | bytes 98308
  54.1 39.6 %copy-start.5 = (f32[3,128]{1,0:T(4,128)S(1)}, f32[3,128]{1,0:T(4,128)}, u32[]{:S(2)}) copy-start(f32[3,128]{1,0:T(4,128)} %param.23) | copy-start | bytes 4612
  54.1 39.6 %copy-start.6 = (f32[128]{0:T(128)S(1)}, f32[128]{0:T(128)}, u32[]{:S(2)}) copy-start(f32[128]{0:T(128)} %param.29) | copy-start | bytes 1540
  54.1 39.6 %copy-start.7 = (f32[128]{0:T(128)S(1)}, f32[128]{0:T(128)}, u32[]{:S(2)}) copy-start(f32[128]{0:T(128)} %param.30) | copy-start | bytes 1540
  54.1 39.6 %copy-start.8 = (f32[128]{0:T(128)S(1)}, f32[128]{0:T(128)}, u32[]{:S(2)}) copy-start(f32[128]{0:T(128)} %param.33) | copy-start | bytes 1540
  90.0 23.5 %all-to-all-start.5 = ((bf16[4,16,32,256]{3,2,1,0:T(8,128)(2,1)}), bf16[4,16,32,256]{3,2,1,0:T(8,128)(2,1)S(1)}, u32[]{:S(2)}, u32[]{:S(2)}) async-start(bf16[4,16,32,256]{3,2,1,0:T(8,128)(2,1)} %broadcast_in_dim.27), calls=%async_computation.5 | async-start | bytes 2097152 | tf_op jit(solution)/shard_map/all_to_all | solution.py:496
  113.5 15.6 %all-to-all-start.1 = ((bf16[4,128,128]{2,1,0:T(8,128)(2,1)}), bf16[4,128,128]{2,1,0:T(8,128)(2,1)S(1)}, u32[]{:S(2)}, u32[]{:S(2)}) async-start(bf16[4,128,128]{2,1,0:T(8,128)(2,1)} %get-tuple-element.24), calls=%async_computation.1 | async-start | bytes 262144 | tf_op jit(solution)/shard_map/all_to_all | solution.py:496
  119.4 40.8 %collective-permute-start.5 = (bf16[256,2048]{1,0:T(8,128)(2,1)S(1)}, bf16[256,2048]{1,0:T(8,128)(2,1)}, u32[]{:S(2)}, u32[]{:S(2)}) collective-permute-start(bf16[256,2048]{1,0:T(8,128)(2,1)S(1)} %bitcast.42), channel_id=1, source_target_pairs={{0,6},{1,7},{2,0},{3,1},{4,2},{5,3},{6,4},{7,5},{8,14},{9,15},{10,... | collective-permute-start | bytes 3145736 | tf_op jit(solution)/shard_map/ppermute | solution.py:492
  123.5 36.7 %collective-permute-start.6 = (bf16[256,2048]{1,0:T(8,128)(2,1)S(1)}, bf16[256,2048]{1,0:T(8,128)(2,1)}, u32[]{:S(2)}, u32[]{:S(2)}) collective-permute-start(bf16[256,2048]{1,0:T(8,128)(2,1)S(1)} %bitcast.43), channel_id=1, source_target_pairs={{0,4},{1,5},{2,6},{3,7},{4,0},{5,1},{6,2},{7,3},{8,12},{9,13},{10,... | collective-permute-start | bytes 3145736 | tf_op jit(solution)/shard_map/ppermute | solution.py:492
  126.0 49.5 %collective-permute-start.7 = (bf16[256,2048]{1,0:T(8,128)(2,1)S(1)}, bf16[256,2048]{1,0:T(8,128)(2,1)}, u32[]{:S(2)}, u32[]{:S(2)}) collective-permute-start(bf16[256,2048]{1,0:T(8,128)(2,1)S(1)} %bitcast.44), channel_id=1, source_target_pairs={{0,2},{1,3},{2,4},{3,5},{4,6},{5,7},{6,0},{7,1},{8,10},{9,11},{10,... | collective-permute-start | bytes 3145736 | tf_op jit(solution)/shard_map/ppermute | solution.py:492
  130.8 22.3 %all-to-all-start.2 = ((bf16[4,128,128]{2,1,0:T(8,128)(2,1)}), bf16[4,128,128]{2,1,0:T(8,128)(2,1)S(1)}, u32[]{:S(2)}, u32[]{:S(2)}) async-start(bf16[4,128,128]{2,1,0:T(8,128)(2,1)} %get-tuple-element.26), calls=%async_computation.2 | async-start | bytes 262144 | tf_op jit(solution)/shard_map/all_to_all | solution.py:496
  138.8 4.7 %collective-permute-start.4 = (bf16[16,2048]{1,0:T(8,128)(2,1)S(1)}, bf16[16,2048]{1,0:T(8,128)(2,1)S(1)}, u32[]{:S(2)}, u32[]{:S(2)}) collective-permute-start(bf16[16,2048]{1,0:T(8,128)(2,1)S(1)} %fusion.8), channel_id=1, source_target_pairs={{0,32},{32,64},{64,96},{96,128},{128,160},{160,192},{192,224},{224... | collective-permute-start | bytes 196616 | tf_op jit(solution)/shard_map/ppermute | solution.py:487
  149.4 3.7 %copy-start = (f32[128,128]{1,0:T(8,128)S(1)}, f32[128,128]{1,0:T(8,128)}, u32[]{:S(2)}) copy-start(f32[128,128]{1,0:T(8,128)} %get-tuple-element.25.before_ref) | copy-start | bytes 196612
  149.4 3.7 %copy-start.1 = (s32[2]{0:T(128)S(1)}, s32[2]{0:T(128)}, u32[]{:S(2)}) copy-start(s32[2]{0:T(128)} %pad_add_fusion.at_ref) | copy-start | bytes 28
  156.6 21.6 %all-to-all-start.3 = ((bf16[4,256,256]{2,1,0:T(8,128)(2,1)}), bf16[4,256,256]{2,1,0:T(8,128)(2,1)S(1)}, u32[]{:S(2)}, u32[]{:S(2)}) async-start(bf16[4,256,256]{2,1,0:T(8,128)(2,1)} %bitcast.47), calls=%async_computation.3 | async-start | bytes 1048576 | tf_op jit(solution)/shard_map/all_to_all | solution.py:592
  181.3 5.8 %collective-permute-start.8 = (bf16[128,2048]{1,0:T(8,128)(2,1)S(1)}, bf16[128,2048]{1,0:T(8,128)(2,1)S(1)}, u32[]{:S(2)}, u32[]{:S(2)}) collective-permute-start(bf16[128,2048]{1,0:T(8,128)(2,1)S(1)} %get-tuple-element.40), channel_id=1, source_target_pairs={{0,1},{1,0},{2,3},{3,2},{4,5},{5,4},{6,7},{7,6},{8,9},{9,8},{10,11... | collective-permute-start | bytes 1572872 | tf_op jit(solution)/shard_map/ppermute | solution.py:533
Sparse Core Ops, SparseCore 0:
  18.9 83.5 all-gather.1

commit v11 on v10

--- a/solution.py
+++ b/solution.py
@@ -26,6 +26,10 @@
 
 def in_hbm(*arrays):
     return [pltpu.with_memory_space_constraint(a, pltpu.HBM) for a in arrays]
+
+
+def in_vmem(a):
+    return pltpu.with_memory_space_constraint(a, pltpu.VMEM)
 
 
 def dot(a, b, ca=1, cb=0):
@@ -342,7 +346,7 @@
         grid=(rows // READS_BLOCK,),
         in_specs=[tile, tile, tile, wide, tile, tile, tile, starts],
         out_specs=[tile, tile],
-        out_shape=[array((rows, width), f32), array((rows, width), bf16)],
+        out_shape=[pltpu.VMEM((rows, width), f32), pltpu.VMEM((rows, width), bf16)],
         compiler_params=pltpu.CompilerParams(
             dimension_semantics=("arbitrary",), vmem_limit_bytes=20 * 2**20
         ),
@@ -433,7 +437,7 @@
             dimension_semantics=("arbitrary",), vmem_limit_bytes=12 * 2**20
         ),
         name="finish_mix",
-    )(at, before, far, init, *in_hbm(o, y, conv), vec)
+    )(at, before, far, init, in_vmem(o), in_vmem(y), *in_hbm(conv), vec)
 
 
 def outward_kernel(pick_ref, m_ref, *refs):

time: 196 us -> 196 us (level)
  no operation moved by 1% of the time
where the time goes in v11:
time: 196 us; the launch traced here: 195 us
  starting transfers between devices  49.9 us (25%)
  blocking collectives  45.4 us (23%)
  waiting for transfers between devices  45.4 us (23%)
  Pallas kernels  31.1 us (16%)
  between operations  13.7 us (7%)
  local copies, waits for them, and re-layouts  4.93 us (3%)
  other arithmetic  4.52 us (2%)
    all_to_all x2, blocking collectives, from_everyone(): lax.all_to_all(copies, axis, 0, 0, tiled=True, axis_index_groups=groups)  45.4 us
    ppermute x6, waiting for transfers between devices, turned(): lax.ppermute(x, 'tp', [(i, (i + distance) % devices) for i in range(devic...  31.1 us
    ppermute x6, starting transfers between devices, turned(): lax.ppermute(x, 'tp', [(i, (i + distance) % devices) for i in range(devic...  20.2 us
    all_to_all x3, starting transfers between devices, from_everyone(): lax.all_to_all(copies, axis, 0, 0, tiled=True, axis_index_groups=groups)  13.8 us
    pallas_call x1, Pallas kernels, maps_call(): pl.pallas_call(maps_kernel, grid_spec=pltpu.PrefetchScalarGridSpec(num_sc...  10.9 us
    ppermute x2, starting transfers between devices, core_swap(): return lax.ppermute(x, 'tp', [(i, i ^ 1) for i in range(devices)])  9.05 us
    all_gather x1, waiting for transfers between devices, mixing(): weights = lax.all_gather(weights, 'sp', axis=0, tiled=True)  8.72 us
    pallas_call x1, Pallas kernels, conv_call(): pl.pallas_call(conv_kernel, grid_spec=pltpu.PrefetchScalarGridSpec(num_sc...  5.97 us
  transfers between devices with their start and end apart: 14, of which 8 were waited for; matrix products, arithmetic and copies ran while one was open for 4% of the time, Pallas kernels for 14%

profile of v11, /device:TPU:1, one launch (start us, length us, event | category | flops | bytes accessed | tf_op | source)
XLA Modules:
  0.0 194.9 jit_solution(1292018681258595557)
XLA Ops:
  6.5 0.0 copy-start.2
  6.5 0.0 all-gather.2.cloned.1.call-start
  6.5 1.6 pack_shards.2
  8.2 10.6 %all_to_all.30 = bf16[4,32,1024]{2,1,0:T(8,128)(2,1)} all-to-all(bf16[4,32,1024]{2,1,0:T(8,128)(2,1)} %pack_shards.2), channel_id=1, replica_groups=mesh['sp'=16,'fs'=4,'tp'=8] {'fs'}, dimensions={0} | all-to-all | bytes 524288 | tf_op jit(solution)/shard_map/all_to_all | solution.py:500
  18.8 0.0 all-gather.2.cloned.1.call-update
  18.8 1.2 fusion.2
  20.1 1.2 fusion.4
  21.3 4.7 %collective-permute-start.1 = (bf16[128,2048]{1,0:T(8,128)(2,1)S(1)}, bf16[128,2048]{1,0:T(8,128)(2,1)S(1)}, u32[]{:S(2)}, u32[]{:S(2)}) collective-permute-start(bf16[128,2048]{1,0:T(8,128)(2,1)S(1)} %fusion.4), channel_id=1, source_target_pairs={{0,4},{1,5},{2,6},{3,7},{4,0},{5,1},{6,2},{7,3},{8,12},{9,13},{10,... | collective-permute-start | bytes 1572872 | tf_op jit(solution)/shard_map/ppermute | solution.py:496
  26.0 2.2 %collective-permute-start.2 = (bf16[128,2048]{1,0:T(8,128)(2,1)S(1)}, bf16[128,2048]{1,0:T(8,128)(2,1)S(1)}, u32[]{:S(2)}, u32[]{:S(2)}) collective-permute-start(bf16[128,2048]{1,0:T(8,128)(2,1)S(1)} %fusion.4), channel_id=1, source_target_pairs={{0,2},{1,3},{2,4},{3,5},{4,6},{5,7},{6,0},{7,1},{8,10},{9,11},{10,... | collective-permute-start | bytes 1572872 | tf_op jit(solution)/shard_map/ppermute | solution.py:496
  28.2 4.3 %collective-permute-start = (bf16[128,2048]{1,0:T(8,128)(2,1)S(1)}, bf16[128,2048]{1,0:T(8,128)(2,1)S(1)}, u32[]{:S(2)}, u32[]{:S(2)}) collective-permute-start(bf16[128,2048]{1,0:T(8,128)(2,1)S(1)} %fusion.4), channel_id=1, source_target_pairs={{0,6},{1,7},{2,0},{3,1},{4,2},{5,3},{6,4},{7,5},{8,14},{9,15},{10,... | collective-permute-start | bytes 1572872 | tf_op jit(solution)/shard_map/ppermute | solution.py:496
  32.5 0.0 copy-done.2
  32.5 0.0 copy-done.4
  32.5 0.2 fusion.6
  32.7 0.7 collective-permute-done.1
  33.4 13.8 %collective-permute-done.2 = bf16[128,2048]{1,0:T(8,128)(2,1)S(1)} collective-permute-done((bf16[128,2048]{1,0:T(8,128)(2,1)S(1)}, bf16[128,2048]{1,0:T(8,128)(2,1)S(1)}, u32[]{:S(2)}, u32[]{:S(2)}) %collective-permute-start.2) | collective-permute-done | bytes 524320 | tf_op jit(solution)/shard_map/ppermute | solution.py:496
  47.2 0.4 collective-permute-done
  47.6 0.3 pad_maximum_fusion.same_ref
  47.9 4.7 %collective-permute-start.3 = (bf16[4,128,2048]{2,1,0:T(8,128)(2,1)S(1)}, bf16[4,128,2048]{2,1,0:T(8,128)(2,1)}, u32[]{:S(2)}, u32[]{:S(2)}) collective-permute-start(bf16[4,128,2048]{2,1,0:T(8,128)(2,1)S(1)} %pad_maximum_fusion.same_ref), channel_id=1, source_target_pairs={{0,1},{1,0},{2,3},{3,2},{4,5},{5,4},{6,7},{7,6},{8,9},{9,8},{10,11... | collective-permute-start | bytes 6291464 | tf_op jit(solution)/shard_map/ppermute | solution.py:537
  52.6 0.0 copy-start.3
  52.6 1.5 pack_shards.3
  54.1 34.8 %all_to_all.31 = bf16[16,32,256]{2,1,0:T(8,128)(2,1)S(1)} all-to-all(bf16[16,32,256]{2,1,0:T(8,128)(2,1)} %pack_shards.3), channel_id=1, replica_groups=mesh['sp'=16,'fs'=4,'tp'=8] {'sp'}, dimensions={0} | all-to-all | bytes 524288 | tf_op jit(solution)/shard_map/all_to_all | solution.py:500
  88.9 1.1 broadcast_in_dim.27
  90.0 3.5 %all-to-all-start.5 = ((bf16[4,16,32,256]{3,2,1,0:T(8,128)(2,1)}), bf16[4,16,32,256]{3,2,1,0:T(8,128)(2,1)S(1)}, u32[]{:S(2)}, u32[]{:S(2)}) async-start(bf16[4,16,32,256]{3,2,1,0:T(8,128)(2,1)} %broadcast_in_dim.27), calls=%async_computation.5 | async-start | bytes 2097152 | tf_op jit(solution)/shard_map/all_to_all | solution.py:500
  93.5 0.0 copy-done.3
  93.5 0.1 copy.23
  93.6 0.1 reshape.38.init_ref
  93.7 0.0 copy-done.5
  93.7 0.0 copy-done.6
  93.7 0.0 copy-done.7
  93.7 0.0 copy-done.8
  93.7 0.1 pad_add_fusion.1.place_ref
  93.8 0.0 collective-permute-done.3.other_ref
  93.8 8.7 %all-gather.2.cloned.1.call-done.w_ref = bf16[2048,1024]{1,0:T(8,128)(2,1)} async-done(((bf16[128,1024]{1,0:T(8,128)(2,1)}), bf16[2048,1024]{1,0:T(8,128)(2,1)}) %all-gather.2.cloned.1.call-update) | async-done | bytes 4194320 | tf_op jit(solution)/shard_map/all_gather | solution.py:555
  102.5 10.9 %state_maps.1 = (bf16[1024,128]{1,0:T(8,128)(2,1)}, bf16[1024,128]{1,0:T(8,128)(2,1)}, bf16[1024,256]{1,0:T(8,128)(2,1)}, bf16[1024,128]{1,0:T(8,128)(2,1)}, f32...) custom-call(s32[2]{0:T(128)S(1)} %pad_add_fusion.1.place_ref, ...), custom_call_target="tpu_custom_call" | custom-call | tf_op jit(solution)/shard_map/state_maps/pallas_call | solution.py:217
  113.5 0.0 all-to-all-done.5
  113.5 3.3 %all-to-all-start.1 = ((bf16[4,128,128]{2,1,0:T(8,128)(2,1)}), bf16[4,128,128]{2,1,0:T(8,128)(2,1)S(1)}, u32[]{:S(2)}, u32[]{:S(2)}) async-start(bf16[4,128,128]{2,1,0:T(8,128)(2,1)} %get-tuple-element.24), calls=%async_computation.1 | async-start | bytes 262144 | tf_op jit(solution)/shard_map/all_to_all | solution.py:500
  116.8 1.1 copy.24
  117.9 1.5 copy.25
  119.4 4.1 %collective-permute-start.5 = (bf16[256,2048]{1,0:T(8,128)(2,1)S(1)}, bf16[256,2048]{1,0:T(8,128)(2,1)}, u32[]{:S(2)}, u32[]{:S(2)}) collective-permute-start(bf16[256,2048]{1,0:T(8,128)(2,1)S(1)} %bitcast.42), channel_id=1, source_target_pairs={{0,6},{1,7},{2,0},{3,1},{4,2},{5,3},{6,4},{7,5},{8,14},{9,15},{10,... | collective-permute-start | bytes 3145736 | tf_op jit(solution)/shard_map/ppermute | solution.py:496
  123.5 2.5 %collective-permute-start.6 = (bf16[256,2048]{1,0:T(8,128)(2,1)S(1)}, bf16[256,2048]{1,0:T(8,128)(2,1)}, u32[]{:S(2)}, u32[]{:S(2)}) collective-permute-start(bf16[256,2048]{1,0:T(8,128)(2,1)S(1)} %bitcast.43), channel_id=1, source_target_pairs={{0,4},{1,5},{2,6},{3,7},{4,0},{5,1},{6,2},{7,3},{8,12},{9,13},{10,... | collective-permute-start | bytes 3145736 | tf_op jit(solution)/shard_map/ppermute | solution.py:496
  126.0 2.4 %collective-permute-start.7 = (bf16[256,2048]{1,0:T(8,128)(2,1)S(1)}, bf16[256,2048]{1,0:T(8,128)(2,1)}, u32[]{:S(2)}, u32[]{:S(2)}) collective-permute-start(bf16[256,2048]{1,0:T(8,128)(2,1)S(1)} %bitcast.44), channel_id=1, source_target_pairs={{0,2},{1,3},{2,4},{3,5},{4,6},{5,7},{6,0},{7,1},{8,10},{9,11},{10,... | collective-permute-start | bytes 3145736 | tf_op jit(solution)/shard_map/ppermute | solution.py:496
  128.4 0.6 pad_add_fusion.at_ref
  129.0 0.0 all-to-all-done.1.pieces_ref
  129.0 1.7 group_map.1
  130.8 7.0 %all-to-all-start.2 = ((bf16[4,128,128]{2,1,0:T(8,128)(2,1)}), bf16[4,128,128]{2,1,0:T(8,128)(2,1)S(1)}, u32[]{:S(2)}, u32[]{:S(2)}) async-start(bf16[4,128,128]{2,1,0:T(8,128)(2,1)} %get-tuple-element.26), calls=%async_computation.2 | async-start | bytes 262144 | tf_op jit(solution)/shard_map/all_to_all | solution.py:500
  137.7 1.0 slice.8
  138.8 3.3 %collective-permute-start.4 = (bf16[16,2048]{1,0:T(8,128)(2,1)S(1)}, bf16[16,2048]{1,0:T(8,128)(2,1)S(1)}, u32[]{:S(2)}, u32[]{:S(2)}) collective-permute-start(bf16[16,2048]{1,0:T(8,128)(2,1)S(1)} %fusion.8), channel_id=1, source_target_pairs={{0,32},{32,64},{64,96},{96,128},{128,160},{160,192},{192,224},{224... | collective-permute-start | bytes 196616 | tf_op jit(solution)/shard_map/ppermute | solution.py:491
  142.1 1.3 collective-permute-done.4.halo_ref
  143.4 6.0 %conv_mix.1 = (bf16[1024,128]{1,0:T(8,128)(2,1)}, bf16[1024,128]{1,0:T(8,128)(2,1)}) custom-call(s32[2]{0:T(128)S(1)} %pad_add_fusion.1.place_ref, bf16[4,128,2048]{2,1,0:T(8,128)(2,1)S(1)} %pad_maximum_fusion.same_ref, bf16[4,128,2048]{2,1,0:T(8,128)(2,1)} %collective-permute-done.3.other_ref, bf16[2048,1024]{1,0:T(8,128)(2,1)} %all-gather.2.cloned.1.call-done.w_ref, ...), custom_call_target="tpu_custom_call" | custom-call | tf_op jit(solution)/shard_map/conv_mix/pallas_call | solution.py:291
  149.4 2.9 %local_reads.1 = (f32[1024,128]{1,0:T(8,128)S(1)}, bf16[1024,128]{1,0:T(8,128)(2,1)S(1)}) custom-call(bf16[1024,128]{1,0:T(8,128)(2,1)} %get-tuple-element.28.q_ref, bf16[1024,128]{1,0:T(8,128)(2,1)} %get-tuple-element.29.gk_ref, bf16[1024,128]{1,0:T(8,128)(2,1)} %get-tuple-element.30.gb_ref, bf16[1024,256]{1,0:T(8,128)(2,1)} %get-tuple-element.31.wu_ref, ...), custom_call_target="tpu_custom_call" | custom-call | tf_op jit(solution)/shard_map/local_reads/pallas_call | solution.py:344
  152.3 0.0 all-to-all-done.2.far_ref
  152.3 0.0 copy-done
  152.3 0.0 copy-done.1
  152.3 3.4 %finish_mix.1 = bf16[1024,256]{1,0:T(8,128)(2,1)} custom-call(s32[2]{0:T(128)S(1)} %copy-done.1, f32[128,128]{1,0:T(8,128)S(1)} %copy-done, bf16[4,128,128]{2,1,0:T(8,128)(2,1)S(1)} %all-to-all-done.2.far_ref, f32[64,128]{1,0:T(8,128)S(1)} %reshape.38.init_ref, f32[1024,128]{1,0:T(8,128)S(1)} %get-tuple-element.36.o_ref, ...), custom_call_target="tpu_custom_call" | custom-call | tf_op jit(solution)/shard_map/finish_mix/pallas_call | solution.py:426
  155.7 3.5 %all-to-all-start.3 = ((bf16[4,256,256]{2,1,0:T(8,128)(2,1)}), bf16[4,256,256]{2,1,0:T(8,128)(2,1)S(1)}, u32[]{:S(2)}, u32[]{:S(2)}) async-start(bf16[4,256,256]{2,1,0:T(8,128)(2,1)} %bitcast.47), calls=%async_computation.3 | async-start | bytes 1048576 | tf_op jit(solution)/shard_map/all_to_all | solution.py:596
  159.2 0.1 stack.52.pick_ref
  159.3 0.0 collective-permute-done.5.refs_1_
  159.3 0.0 collective-permute-done.6.refs_2_
  159.3 16.2 %collective-permute-done.7.refs_3_ = bf16[256,2048]{1,0:T(8,128)(2,1)} collective-permute-done((bf16[256,2048]{1,0:T(8,128)(2,1)S(1)}, bf16[256,2048]{1,0:T(8,128)(2,1)}, u32[]{:S(2)}, u32[]{:S(2)}) %collective-permute-start.7) | collective-permute-done | bytes 1048608 | tf_op jit(solution)/shard_map/ppermute | solution.py:496
  175.5 2.7 %all-to-all-done.3.m_ref = bf16[4,256,256]{2,1,0:T(8,128)(2,1)S(1)} async-done(((bf16[4,256,256]{2,1,0:T(8,128)(2,1)}), bf16[4,256,256]{2,1,0:T(8,128)(2,1)S(1)}, u32[]{:S(2)}, u32[]{:S(2)}) %all-to-all-start.3) | async-done | bytes 524320 | tf_op jit(solution)/shard_map/all_to_all | solution.py:596
  178.2 3.1 %outward.1 = (bf16[128,2048]{1,0:T(8,128)(2,1)S(1)}, bf16[128,2048]{1,0:T(8,128)(2,1)S(1)}) custom-call(s32[5]{0:T(128)S(1)} %stack.52.pick_ref, bf16[4,256,256]{2,1,0:T(8,128)(2,1)S(1)} %all-to-all-done.3.m_ref, bf16[256,2048]{1,0:T(8,128)(2,1)S(1)} %bitcast.45, bf16[256,2048]{1,0:T(8,128)(2,1)} %collective-permute-done.5.refs_1_, ...), custom_call_target="tpu_custom_call" | custom-call | tf_op jit(solution)/shard_map/outward/pallas_call | solution.py:461
  181.3 4.3 %collective-permute-start.8 = (bf16[128,2048]{1,0:T(8,128)(2,1)S(1)}, bf16[128,2048]{1,0:T(8,128)(2,1)S(1)}, u32[]{:S(2)}, u32[]{:S(2)}) collective-permute-start(bf16[128,2048]{1,0:T(8,128)(2,1)S(1)} %get-tuple-element.40), channel_id=1, source_target_pairs={{0,1},{1,0},{2,3},{3,2},{4,5},{5,4},{6,7},{7,6},{8,9},{9,8},{10,11... | collective-permute-start | bytes 1572872 | tf_op jit(solution)/shard_map/ppermute | solution.py:537
  185.6 1.5 collective-permute-done.8
  187.1 0.9 fusion.7
  (12 shorter events, 0.1 us)
Async XLA Ops:
  6.5 26.0 %copy-start.2 = (bf16[1,128,2048]{2,1,0:T(8,128)(2,1)S(1)}, bf16[1,128,2048]{2,1,0:T(8,128)(2,1)}, u32[]{:S(2)}) copy-start(bf16[1,128,2048]{2,1,0:T(8,128)(2,1)} %param.18) | copy-start | bytes 1572868
  6.5 26.0 %copy-start.4 = (f32[2048]{0:T(1024)S(1)}, f32[2048]{0:T(1024)}, u32[]{:S(2)}) copy-start(f32[2048]{0:T(1024)} %param.19) | copy-start | bytes 24580
  6.5 96.0 %all-gather.2.cloned.1.call-start = ((), (), s32[]{:S(2)}) async-start(), calls=%async_computation.6 | async-start | bytes 4456448 | tf_op jit(solution)/shard_map/all_gather | solution.py:555
  21.3 12.1 %collective-permute-start.1 = (bf16[128,2048]{1,0:T(8,128)(2,1)S(1)}, bf16[128,2048]{1,0:T(8,128)(2,1)S(1)}, u32[]{:S(2)}, u32[]{:S(2)}) collective-permute-start(bf16[128,2048]{1,0:T(8,128)(2,1)S(1)} %fusion.4), channel_id=1, source_target_pairs={{0,4},{1,5},{2,6},{3,7},{4,0},{5,1},{6,2},{7,3},{8,12},{9,13},{10,... | collective-permute-start | bytes 1572872 | tf_op jit(solution)/shard_map/ppermute | solution.py:496
  26.0 21.2 %collective-permute-start.2 = (bf16[128,2048]{1,0:T(8,128)(2,1)S(1)}, bf16[128,2048]{1,0:T(8,128)(2,1)S(1)}, u32[]{:S(2)}, u32[]{:S(2)}) collective-permute-start(bf16[128,2048]{1,0:T(8,128)(2,1)S(1)} %fusion.4), channel_id=1, source_target_pairs={{0,2},{1,3},{2,4},{3,5},{4,6},{5,7},{6,0},{7,1},{8,10},{9,11},{10,... | collective-permute-start | bytes 1572872 | tf_op jit(solution)/shard_map/ppermute | solution.py:496
  28.2 19.4 %collective-permute-start = (bf16[128,2048]{1,0:T(8,128)(2,1)S(1)}, bf16[128,2048]{1,0:T(8,128)(2,1)S(1)}, u32[]{:S(2)}, u32[]{:S(2)}) collective-permute-start(bf16[128,2048]{1,0:T(8,128)(2,1)S(1)} %fusion.4), channel_id=1, source_target_pairs={{0,6},{1,7},{2,0},{3,1},{4,2},{5,3},{6,4},{7,5},{8,14},{9,15},{10,... | collective-permute-start | bytes 1572872 | tf_op jit(solution)/shard_map/ppermute | solution.py:496
  47.9 46.0 %collective-permute-start.3 = (bf16[4,128,2048]{2,1,0:T(8,128)(2,1)S(1)}, bf16[4,128,2048]{2,1,0:T(8,128)(2,1)}, u32[]{:S(2)}, u32[]{:S(2)}) collective-permute-start(bf16[4,128,2048]{2,1,0:T(8,128)(2,1)S(1)} %pad_maximum_fusion.same_ref), channel_id=1, source_target_pairs={{0,1},{1,0},{2,3},{3,2},{4,5},{5,4},{6,7},{7,6},{8,9},{9,8},{10,11... | collective-permute-start | bytes 6291464 | tf_op jit(solution)/shard_map/ppermute | solution.py:537
  52.6 40.9 %copy-start.3 = (f32[1,2,64,64]{3,2,1,0:T(8,128)S(1)}, f32[1,2,64,64]{3,2,1,0:T(8,128)}, u32[]{:S(2)}) copy-start(f32[1,2,64,64]{3,2,1,0:T(8,128)} %param.32) | copy-start | bytes 98308
  54.1 39.6 %copy-start.5 = (f32[3,128]{1,0:T(4,128)S(1)}, f32[3,128]{1,0:T(4,128)}, u32[]{:S(2)}) copy-start(f32[3,128]{1,0:T(4,128)} %param.23) | copy-start | bytes 4612
  54.1 39.6 %copy-start.6 = (f32[128]{0:T(128)S(1)}, f32[128]{0:T(128)}, u32[]{:S(2)}) copy-start(f32[128]{0:T(128)} %param.29) | copy-start | bytes 1540
  54.1 39.6 %copy-start.7 = (f32[128]{0:T(128)S(1)}, f32[128]{0:T(128)}, u32[]{:S(2)}) copy-start(f32[128]{0:T(128)} %param.30) | copy-start | bytes 1540
  54.1 39.6 %copy-start.8 = (f32[128]{0:T(128)S(1)}, f32[128]{0:T(128)}, u32[]{:S(2)}) copy-start(f32[128]{0:T(128)} %param.33) | copy-start | bytes 1540
  90.0 23.5 %all-to-all-start.5 = ((bf16[4,16,32,256]{3,2,1,0:T(8,128)(2,1)}), bf16[4,16,32,256]{3,2,1,0:T(8,128)(2,1)S(1)}, u32[]{:S(2)}, u32[]{:S(2)}) async-start(bf16[4,16,32,256]{3,2,1,0:T(8,128)(2,1)} %broadcast_in_dim.27), calls=%async_computation.5 | async-start | bytes 2097152 | tf_op jit(solution)/shard_map/all_to_all | solution.py:500
  113.5 15.6 %all-to-all-start.1 = ((bf16[4,128,128]{2,1,0:T(8,128)(2,1)}), bf16[4,128,128]{2,1,0:T(8,128)(2,1)S(1)}, u32[]{:S(2)}, u32[]{:S(2)}) async-start(bf16[4,128,128]{2,1,0:T(8,128)(2,1)} %get-tuple-element.24), calls=%async_computation.1 | async-start | bytes 262144 | tf_op jit(solution)/shard_map/all_to_all | solution.py:500
  119.4 39.9 %collective-permute-start.5 = (bf16[256,2048]{1,0:T(8,128)(2,1)S(1)}, bf16[256,2048]{1,0:T(8,128)(2,1)}, u32[]{:S(2)}, u32[]{:S(2)}) collective-permute-start(bf16[256,2048]{1,0:T(8,128)(2,1)S(1)} %bitcast.42), channel_id=1, source_target_pairs={{0,6},{1,7},{2,0},{3,1},{4,2},{5,3},{6,4},{7,5},{8,14},{9,15},{10,... | collective-permute-start | bytes 3145736 | tf_op jit(solution)/shard_map/ppermute | solution.py:496
  123.5 35.8 %collective-permute-start.6 = (bf16[256,2048]{1,0:T(8,128)(2,1)S(1)}, bf16[256,2048]{1,0:T(8,128)(2,1)}, u32[]{:S(2)}, u32[]{:S(2)}) collective-permute-start(bf16[256,2048]{1,0:T(8,128)(2,1)S(1)} %bitcast.43), channel_id=1, source_target_pairs={{0,4},{1,5},{2,6},{3,7},{4,0},{5,1},{6,2},{7,3},{8,12},{9,13},{10,... | collective-permute-start | bytes 3145736 | tf_op jit(solution)/shard_map/ppermute | solution.py:496
  126.0 49.5 %collective-permute-start.7 = (bf16[256,2048]{1,0:T(8,128)(2,1)S(1)}, bf16[256,2048]{1,0:T(8,128)(2,1)}, u32[]{:S(2)}, u32[]{:S(2)}) collective-permute-start(bf16[256,2048]{1,0:T(8,128)(2,1)S(1)} %bitcast.44), channel_id=1, source_target_pairs={{0,2},{1,3},{2,4},{3,5},{4,6},{5,7},{6,0},{7,1},{8,10},{9,11},{10,... | collective-permute-start | bytes 3145736 | tf_op jit(solution)/shard_map/ppermute | solution.py:496
  130.8 21.5 %all-to-all-start.2 = ((bf16[4,128,128]{2,1,0:T(8,128)(2,1)}), bf16[4,128,128]{2,1,0:T(8,128)(2,1)S(1)}, u32[]{:S(2)}, u32[]{:S(2)}) async-start(bf16[4,128,128]{2,1,0:T(8,128)(2,1)} %get-tuple-element.26), calls=%async_computation.2 | async-start | bytes 262144 | tf_op jit(solution)/shard_map/all_to_all | solution.py:500
  138.8 4.7 %collective-permute-start.4 = (bf16[16,2048]{1,0:T(8,128)(2,1)S(1)}, bf16[16,2048]{1,0:T(8,128)(2,1)S(1)}, u32[]{:S(2)}, u32[]{:S(2)}) collective-permute-start(bf16[16,2048]{1,0:T(8,128)(2,1)S(1)} %fusion.8), channel_id=1, source_target_pairs={{0,32},{32,64},{64,96},{96,128},{128,160},{160,192},{192,224},{224... | collective-permute-start | bytes 196616 | tf_op jit(solution)/shard_map/ppermute | solution.py:491
  149.4 2.9 %copy-start = (f32[128,128]{1,0:T(8,128)S(1)}, f32[128,128]{1,0:T(8,128)}, u32[]{:S(2)}) copy-start(f32[128,128]{1,0:T(8,128)} %get-tuple-element.25.before_ref) | copy-start | bytes 196612
  149.4 2.9 %copy-start.1 = (s32[2]{0:T(128)S(1)}, s32[2]{0:T(128)}, u32[]{:S(2)}) copy-start(s32[2]{0:T(128)} %pad_add_fusion.at_ref) | copy-start | bytes 28
  155.7 22.5 %all-to-all-start.3 = ((bf16[4,256,256]{2,1,0:T(8,128)(2,1)}), bf16[4,256,256]{2,1,0:T(8,128)(2,1)S(1)}, u32[]{:S(2)}, u32[]{:S(2)}) async-start(bf16[4,256,256]{2,1,0:T(8,128)(2,1)} %bitcast.47), calls=%async_computation.3 | async-start | bytes 1048576 | tf_op jit(solution)/shard_map/all_to_all | solution.py:596
  181.3 5.8 %collective-permute-start.8 = (bf16[128,2048]{1,0:T(8,128)(2,1)S(1)}, bf16[128,2048]{1,0:T(8,128)(2,1)S(1)}, u32[]{:S(2)}, u32[]{:S(2)}) collective-permute-start(bf16[128,2048]{1,0:T(8,128)(2,1)S(1)} %get-tuple-element.40), channel_id=1, source_target_pairs={{0,1},{1,0},{2,3},{3,2},{4,5},{5,4},{6,7},{7,6},{8,9},{9,8},{10,11... | collective-permute-start | bytes 1572872 | tf_op jit(solution)/shard_map/ppermute | solution.py:537
Sparse Core Ops, SparseCore 0:
  18.9 83.5 all-gather.1
